TPU v7x, 512 devices: a whole 4x4x16 slice. The times are simulated.
512 devices in a mesh: sp: 16 (over z), tp: 4 (over y), dp: 8 (over x, core).
Axes of the slice: x: 4, y: 4, z: 16, core: 2. Of those that a mesh axis runs over, the one named last changes fastest.
Arguments:
- latents: bfloat16 [16384, 2048], P(('dp', 'sp', 'tp')), parts along dimension 0, may hold values from -6 to 6
- sample_vector: float32 [8, 2048], P('dp'), parts along dimension 0, may hold values from -6 to 6
- context: bfloat16 [2048, 2048], P(('dp', 'sp')), parts along dimension 0, may hold values from -6 to 6
- context_vector: float32 [1, 2048], replicated, may hold values from -6 to 6
- norm_gain: float32 [2048], replicated, may hold values from 0.1 to 1.9
- modulator: bfloat16 [2048, 6144], P(None, ('sp', 'tp')), may hold values from -0.25 to 0.25
- query_weight: bfloat16 [2048, 1024], P('sp', 'tp'), may hold values from -0.125 to 0.125
- key_weight: bfloat16 [2048, 1024], P('sp', 'tp'), may hold values from -0.125 to 0.125
- value_weight: bfloat16 [2048, 2048], P('sp', 'tp'), may hold values from -0.125 to 0.125
- decay_down: bfloat16 [2048, 64], replicated, may hold values from -0.125 to 0.125
- decay_up: bfloat16 [2, 32, 1024], P(None, None, 'tp'), may hold values from -1 to 1
- decay_bias: float32 [2, 1024], P(None, 'tp'), as said below
- decay_extra: float32 [2, 16384, 8], P(None, ('dp', 'sp'), 'tp'), parts along dimension 1, may hold values from -2 to 0
- head_gain: float32 [256], replicated, may hold values from 0.1 to 1.9
- out_weight: bfloat16 [2048, 2048], P('tp'), may hold values from -0.125 to 0.125
Outputs:
- updated: bfloat16 [16384, 2048], P(('dp', 'sp', 'tp')), parts along dimension 0
There are 8 independent parts, one for each index of `dp`. A program takes and returns all parts, laid end to end along the dimension named above; an argument that names none is the same for every part. Nothing has to cross between parts.
Inputs may be any that keep to these rules, and one draw needn't show every extreme that they name: `decay_bias`: offsets of the decay gates,.
All inputs are finite; a program needn't handle non-finite values.
Results may differ from a plain program's by a relative error of at most 0.012.
Values may be sent and summed in bfloat16 or wider, within the bound.
No kernel may reach another device: no remote copies, remote signals or barrier semaphores. Data moves between devices by JAX's collectives and lax.ppermute only.
A program may use at most 64 MiB of HBM per device.

v0:
```python
import math

import jax
import jax.numpy as jnp
from jax import lax
from jax.sharding import PartitionSpec as P

DK = 128
DV = 256
RANK = 32
BLOCK = 64
CTX_LIFT = 4


epsilon = 1e-06
exponential_sharpness = 16.0


def joined_along(blocks, dim):
    blocks = jnp.moveaxis(blocks, 0, dim)
    dims = blocks.shape
    return blocks.reshape(*dims[:dim], dims[dim] * dims[dim + 1], *dims[dim + 2 :])


def from_everyone(x, axis):
    size = lax.axis_size(axis)
    return lax.all_to_all(jnp.broadcast_to(x[None], (size, *x.shape)), axis, 0, 0, tiled=True)


def gather_directly(x, axis, dim):
    return joined_along(from_everyone(x, axis), dim)


def in_one_piece(arrays, axis, dim, along):
    widths = [a.shape[along] for a in arrays]
    both = jnp.concatenate(arrays, axis=along)
    whole = lax.all_gather(both, axis, axis=dim, tiled=True)
    return tuple(jnp.split(whole, [sum(widths[:k]) for k in range(1, len(widths))], axis=along))


def sent_together(arrays, axis, dim, along):
    widths = [math.prod(a.shape[along:]) for a in arrays]
    both = jnp.concatenate(
        [a.reshape(*a.shape[:along], w) for a, w in zip(arrays, widths)], axis=along
    )
    whole = lax.all_gather(both, axis, axis=dim, tiled=True)
    blocks = jnp.split(whole, [sum(widths[:k]) for k in range(1, len(widths))], axis=along)
    return tuple(
        (b.reshape(*whole.shape[:along], *a.shape[along:]) for a, b in zip(arrays, blocks))
    )


def cut_along(x, dim, size):
    before, after = (x.shape[:dim], x.shape[dim + 1 :])
    return jnp.moveaxis(x.reshape(*before, size, -1, *after), dim, 0)


def sent_and_summed(x, axis, dim):
    blocks = cut_along(x, dim, lax.axis_size(axis))
    arrived = lax.all_to_all(blocks, axis, split_axis=0, concat_axis=0, tiled=True)
    return arrived.astype(jnp.float32).sum(axis=0)


def rms_rows(values, gains):
    values = values.astype(jnp.float32)
    return values * lax.rsqrt(jnp.mean(values * values, axis=-1, keepdims=True) + epsilon) * gains


def modulated(tokens, gains, modulation, model_width):
    shift_vector = modulation[:model_width]
    scale_vector = modulation[model_width : 2 * model_width]
    return (rms_rows(tokens, gains) * (1.0 + scale_vector) + shift_vector).astype(jnp.bfloat16)


def log_decays(low_rank, decay_up, decay_bias):
    fragment_sequence = []
    for direction in range(2):
        low_piece = lax.optimization_barrier(
            low_rank[:, direction * RANK : (direction + 1) * RANK]
        ).astype(jnp.float32)
        unnormalized_ratings = (
            jnp.dot(low_piece, decay_up[direction].astype(jnp.float32)) + decay_bias[direction]
        )
        fragment_sequence.append(jax.nn.log_sigmoid(unnormalized_ratings) / exponential_sharpness)
    return jnp.stack(fragment_sequence)


def local_sweep(queries, key_rows, value_rows, decays, with_output):
    length = queries.shape[0]
    head_count = queries.shape[1]
    block_count = length // BLOCK

    def to_blocks(values):
        return values.reshape((block_count, BLOCK) + values.shape[1:])

    query_blocks = to_blocks(queries)
    key_blocks = to_blocks(key_rows)
    value_blocks = to_blocks(value_rows)
    within = jnp.cumsum(to_blocks(decays), axis=1)
    block_total = within[:, -1]
    update = jnp.einsum(
        "nshd,nshe->nhde", key_blocks * jnp.exp(block_total[:, None] - within), value_blocks
    )

    def advance(carried, inputs):
        step_decay, step_update = inputs
        return (jnp.exp(step_decay)[:, :, None] * carried + step_update, carried)

    start_state = jnp.zeros((head_count, queries.shape[2], value_rows.shape[2]), jnp.float32)
    summary, previous = lax.scan(advance, start_state, (block_total, update))
    if not with_output:
        return summary
    device_decay = jnp.sum(block_total, axis=0)
    lower_mask = jnp.tril(jnp.ones((BLOCK, BLOCK), dtype=bool))
    query_dec = query_blocks * jnp.exp(within)
    scores = jnp.einsum("nchd,nshd->nhcs", query_dec, key_blocks * jnp.exp(-within))
    scores = jnp.where(lower_mask[None, None], scores, 0.0)
    output = jnp.einsum("nhcs,nshe->nche", scores, value_blocks)
    output = output + jnp.einsum("nchd,nhde->nche", query_dec, previous)
    before = jnp.cumsum(block_total, axis=0) - block_total
    lifted = query_dec * jnp.exp(before)[:, None]
    return (
        output.reshape(length, head_count, -1),
        lifted.reshape(length, head_count, -1),
        device_decay,
        summary,
    )


def per_device(
    latents,
    sample_vector,
    context,
    context_vector,
    norm_gain,
    modulator,
    query_weight,
    key_weight,
    value_weight,
    decay_down,
    decay_up,
    decay_bias,
    decay_extra,
    head_gain,
    out_weight,
):
    model_width = latents.shape[1]
    conditions = jax.nn.silu(jnp.concatenate([sample_vector, context_vector], 0)).astype(
        jnp.bfloat16
    )
    local_mods = jnp.dot(conditions, modulator, preferred_element_type=jnp.float32)
    modulation = gather_directly(local_mods, ("sp", "tp"), 1)
    hidden = modulated(latents, norm_gain, modulation[0], model_width)
    context_hidden = modulated(context, norm_gain, modulation[1], model_width)
    token_rows = gather_directly(hidden, "tp", 0)
    row_count = token_rows.shape[0]
    joined = jnp.concatenate([token_rows, context_hidden], 0)
    head_count = decay_bias.shape[1] // DK
    fragment_sequence = in_one_piece((query_weight, key_weight, value_weight), "sp", 0, 1)
    query_sums = jnp.dot(
        joined[:row_count], fragment_sequence[0], preferred_element_type=jnp.float32
    )
    key_sums = jnp.dot(joined, fragment_sequence[1], preferred_element_type=jnp.float32)
    value_sums = jnp.dot(joined, fragment_sequence[2], preferred_element_type=jnp.float32)
    low_rank = jnp.dot(joined, decay_down, preferred_element_type=jnp.float32).astype(jnp.bfloat16)
    key_all = key_sums.astype(jnp.bfloat16)
    value_all = value_sums.astype(jnp.bfloat16)
    context_keys, context_values, context_low = in_one_piece(
        (key_all[row_count:], value_all[row_count:], low_rank[row_count:]), "sp", 0, 1
    )

    def by_head(values, size):
        return (
            lax.optimization_barrier(values)
            .astype(jnp.float32)
            .reshape(values.shape[0], head_count, size)
        )

    queries = by_head(query_sums.astype(jnp.bfloat16), DK)
    key_rows = by_head(key_all[:row_count], DK)
    value_rows = by_head(value_all[:row_count], DV)
    context_key_rows = by_head(context_keys, DK)
    context_value_rows = by_head(context_values, DV)
    decays = (
        log_decays(low_rank[:row_count], decay_up, decay_bias).reshape(2, row_count, head_count, DK)
        + decay_extra[:, :, :, None]
    )
    context_decays = log_decays(context_low, decay_up, decay_bias).reshape(
        2, context_low.shape[0], head_count, DK
    )
    forward_out, forward_lift, forward_decay, forward_state = local_sweep(
        queries, key_rows, value_rows, decays[0], True
    )
    backward_out, backward_lift, backward_decay, backward_state = local_sweep(
        queries[::-1], key_rows[::-1], value_rows[::-1], decays[1][::-1], True
    )
    context_forward = CTX_LIFT * local_sweep(
        context_key_rows, context_key_rows, context_value_rows, context_decays[0], False
    )
    context_backward = CTX_LIFT * local_sweep(
        context_key_rows[::-1],
        context_key_rows[::-1],
        context_value_rows[::-1],
        context_decays[1][::-1],
        False,
    )
    decays_all, states_all = tuple(
        (
            part.astype(jnp.float32)
            for part in sent_together(
                (
                    jnp.stack([forward_decay, backward_decay])[None].astype(jnp.bfloat16),
                    jnp.stack([forward_state, backward_state])[None].astype(jnp.bfloat16),
                ),
                "sp",
                0,
                4,
            )
        )
    )
    my_index = lax.axis_index("sp")
    device_count = lax.axis_size("sp")

    def fold_step(turn_index, carries):
        forward_in, backward_in = carries
        back_index = device_count - 1 - turn_index
        moved_forward = (
            jnp.exp(decays_all[turn_index, 0])[:, :, None] * forward_in + states_all[turn_index, 0]
        )
        moved_backward = (
            jnp.exp(decays_all[back_index, 1])[:, :, None] * backward_in + states_all[back_index, 1]
        )
        forward_in = jnp.where(turn_index < my_index, moved_forward, forward_in)
        backward_in = jnp.where(back_index > my_index, moved_backward, backward_in)
        return (forward_in, backward_in)

    forward_in, backward_in = lax.fori_loop(
        0, device_count, fold_step, (context_forward, context_backward)
    )
    forward = forward_out + jnp.einsum("lhd,hde->lhe", forward_lift, forward_in)
    backward = backward_out + jnp.einsum("lhd,hde->lhe", backward_lift, backward_in)
    mixed = forward + backward[::-1]
    normed = rms_rows(mixed, head_gain).astype(jnp.bfloat16).reshape(row_count, head_count * DV)
    summed = sent_and_summed(
        jnp.dot(normed, out_weight, preferred_element_type=jnp.float32).astype(jnp.bfloat16),
        "tp",
        0,
    )
    projected = lax.optimization_barrier(summed.astype(jnp.bfloat16)).astype(jnp.float32)
    gate_vector = modulation[0, 2 * model_width :]
    return (latents.astype(jnp.float32) + gate_vector * projected).astype(jnp.bfloat16)


def solution(mesh):
    placed = (
        P(("dp", "sp", "tp"), None),
        P("dp", None),
        P(("dp", "sp"), None),
        P(),
        P(),
        P(None, ("sp", "tp")),
        P("sp", "tp"),
        P("sp", "tp"),
        P("sp", "tp"),
        P(),
        P(None, None, "tp"),
        P(None, "tp"),
        P(None, ("dp", "sp"), "tp"),
        P(),
        P("tp", None),
    )
    return jax.shard_map(
        per_device,
        mesh=mesh,
        in_specs=placed,
        out_specs=P(("dp", "sp", "tp"), None),
        check_vma=False,
    )
```

profile of v0, /device:TPU:6, one launch (start us, length us, event | category | flops | bytes accessed | tf_op | source)
XLA Modules:
  0.0 255.6 jit_solution(7290991516524991231)
XLA Ops:
  6.6 1.8 pad_maximum_fusion.1
  8.4 1.2 fusion.81
  10.3 18.7 %all-to-all-start = ((f32[64,2,96]{2,1,0:T(2,128)}), f32[64,2,96]{2,1,0:T(2,128)S(1)}, u32[]{:S(2)}, u32[]{:S(2)}) async-start(f32[64,2,96]{2,1,0:T(2,128)} %broadcast_in_dim.39), calls=%async_computation | async-start | bytes 131072 | tf_op jit(solution)/shard_map/all_to_all | solution.py:27
  33.3 11.0 %all-to-all-done = f32[64,2,96]{2,1,0:T(2,128)S(1)} async-done(((f32[64,2,96]{2,1,0:T(2,128)}), f32[64,2,96]{2,1,0:T(2,128)S(1)}, u32[]{:S(2)}, u32[]{:S(2)}) %all-to-all-start) | async-done | bytes 49184 | tf_op jit(solution)/shard_map/all_to_all | solution.py:27
  46.3 3.5 %all-to-all-start.1 = ((bf16[4,32,2048]{2,1,0:T(8,128)(2,1)}), bf16[4,32,2048]{2,1,0:T(8,128)(2,1)S(1)}, u32[]{:S(2)}, u32[]{:S(2)}) async-start(bf16[4,32,2048]{2,1,0:T(8,128)(2,1)} %broadcast_in_dim.41), calls=%async_computation.1 | async-start | bytes 1048576 | tf_op jit(solution)/shard_map/all_to_all | solution.py:27
  51.3 6.7 %all-to-all-done.1 = bf16[4,32,2048]{2,1,0:T(8,128)(2,1)S(1)} async-done(((bf16[4,32,2048]{2,1,0:T(8,128)(2,1)}), bf16[4,32,2048]{2,1,0:T(8,128)(2,1)S(1)}, u32[]{:S(2)}, u32[]{:S(2)}) %all-to-all-start.1) | async-done | bytes 524320 | tf_op jit(solution)/shard_map/all_to_all | solution.py:27
  58.0 1.4 convolution_convert_fusion.3
  60.0 1.6 fusion.51
  62.7 1.6 fusion.49
  66.7 26.3 %all-gather.3.cloned.1.call-done = bf16[2048,1024]{1,0:T(8,128)(2,1)} async-done(((bf16[128,1024]{1,0:T(8,128)(2,1)}), bf16[2048,1024]{1,0:T(8,128)(2,1)}) %all-gather.3.cloned.1.call-update) | async-done | bytes 4194320 | tf_op jit(solution)/shard_map/all_gather | solution.py:37
  93.1 1.7 convolution_convert_fusion.1
  96.2 1.7 convolution_convert_fusion.2
  98.7 2.2 fusion.11
  101.7 1.3 rev.29
  106.1 1.7 while.69
  107.7 1.8 exponential_multiply_fusion.5
  110.6 1.7 while.66
  116.0 33.2 %all_gather.10 = bf16[256,832]{1,0:T(8,128)(2,1)S(1)} all-gather(bf16[16,832]{1,0:T(8,128)(2,1)S(1)} %pad_maximum_fusion.5), channel_id=1, replica_groups=mesh['sp'=16,'tp'=4,'dp'=8] {'sp'}, dimensions={0}, use_global_device_ids=true | all-gather | bytes 452608 | tf_op jit(solution)/shard_map/all_gather | solution.py:37
  151.0 1.9 fusion.14
  154.9 1.8 copy.149
  156.7 1.9 fusion.15
  158.5 1.2 fusion.8
  160.5 1.8 copy.138
  166.2 1.8 rev.24
  169.5 4.4 %rev.26 = bf16[256,2,256]{2,0,1:T(8,128)(2,1)} reverse(bf16[256,2,256]{2,0,1:T(8,128)(2,1)} %bitcast.175), dimensions={0} | reverse | bytes 524288 | tf_op jit(solution)/shard_map/rev | solution.py:203
  178.4 1.3 fusion.24
  179.7 1.3 fusion.37
  181.0 4.4 %while.68 = (s32[]{:T(128)}, f32[2,128,256]{2,1,0:T(8,128)S(1)}, f32[4,2,128]{2,1,0:T(2,128)S(1)}, f32[4,2,128,256]{3,2,1,0:T(8,128)}, s32[]{:T(128)}, /*index=5*/s32[]{:T(128)}) while((s32[]{:T(128)}, f32[2,128,256]{2,1,0:T(8,128)S(1)}, f32[4,2,128]{2,1,0:T(2,128)S(1)}, f32[4,2,128,256]{3,2,1,0:T(8,128)}, s32[]{:T(128)}, ...), condition=%wide.region_10.11_spmd.clone, body=%wide.region_9.10_spmd.clone.sunk | while | flops 196611 | bytes 789599 | solution.py:110
  185.5 4.4 %while.67 = (s32[]{:T(128)}, f32[2,128,256]{2,1,0:T(8,128)S(1)}, f32[4,2,128]{2,1,0:T(2,128)S(1)}, f32[4,2,128,256]{3,2,1,0:T(8,128)}, s32[]{:T(128)}, /*index=5*/s32[]{:T(128)}) while((s32[]{:T(128)}, f32[2,128,256]{2,1,0:T(8,128)S(1)}, f32[4,2,128]{2,1,0:T(2,128)S(1)}, f32[4,2,128,256]{3,2,1,0:T(8,128)}, s32[]{:T(128)}, ...), condition=%wide.region_7.8_spmd.clone, body=%wide.region_6.7_spmd.clone.sunk | while | flops 196611 | bytes 789599 | solution.py:110
  190.8 8.9 %slice_convert_fusion = f32[16,2,2,128,256]{3,2,4,1,0:T(2,128)} fusion(bf16[16,2,2,128,257]{3,2,4,1,0:T(2,128)(2,1)} %all-gather.5.cloned.1.call-done), kind=kLoop, calls=%fused_computation.18 | loop fusion | flops 2097152 | bytes 12582912 | tf_op jit(solution)/shard_map/convert_element_type | solution.py:209
  199.7 13.2 %copy.133 = f32[16,2,2,128,256]{4,3,2,1,0:T(8,128)} copy(f32[16,2,2,128,256]{3,2,4,1,0:T(2,128)} %slice_convert_fusion) | data formatting | bytes 16777216 | tf_op jit(solution)/shard_map/while | solution.py:237
  212.9 20.4 %while.65 = (s32[]{:T(128)}, f32[2,128,256]{2,1,0:T(8,128)S(1)}, f32[2,128,256]{2,1,0:T(8,128)S(1)}, s32[]{:T(128)}, f32[16,2,2,128]{3,2,1,0:T(2,128)S(1)}, /*in...) while((s32[]{:T(128)}, f32[2,128,256]{2,1,0:T(8,128)S(1)}, ...), condition=%wide.region_17.18_spmd, body=%wide.region_16.17_spmd.sunk | while | flops 393224 | bytes 1579199 | solution.py:237
  212.9 1.3 fusion.121
  214.2 1.2 fusion.121
  215.5 1.2 fusion.121
  216.8 1.2 fusion.121
  218.0 1.2 fusion.121
  219.3 1.2 fusion.121
  221.9 1.2 fusion.121
  224.4 1.2 fusion.121
  227.0 1.2 fusion.121
  228.2 1.2 fusion.121
  229.5 1.2 fusion.121
  230.8 1.2 fusion.121
  232.1 1.2 fusion.121
  234.4 1.3 convolution_convert_fusion
  235.6 4.3 %all-to-all-start.2 = ((bf16[4,32,2048]{2,1,0:T(8,128)(2,1)}), bf16[4,32,2048]{2,1,0:T(8,128)(2,1)S(1)}, u32[]{:S(2)}, u32[]{:S(2)}) async-start(bf16[4,32,2048]{2,1,0:T(8,128)(2,1)} %bitcast.42), calls=%async_computation.2 | async-start | bytes 1048576 | tf_op jit(solution)/shard_map/all_to_all | solution.py:60
  240.1 7.9 %all-to-all-done.2 = bf16[4,32,2048]{2,1,0:T(8,128)(2,1)S(1)} async-done(((bf16[4,32,2048]{2,1,0:T(8,128)(2,1)}), bf16[4,32,2048]{2,1,0:T(8,128)(2,1)S(1)}, u32[]{:S(2)}, u32[]{:S(2)}) %all-to-all-start.2) | async-done | bytes 524320 | tf_op jit(solution)/shard_map/all_to_all | solution.py:60
  (217 shorter events, 55.5 us)
Async XLA Ops:
  6.5 227.8 %copy-start = (bf16[512,2048]{1,0:T(8,128)(2,1)S(1)}, bf16[512,2048]{1,0:T(8,128)(2,1)}, u32[]{:S(2)}) copy-start(bf16[512,2048]{1,0:T(8,128)(2,1)} %param.39) | copy-start | bytes 6291460
  6.5 44.0 %copy-start.20 = (bf16[16,2048]{1,0:T(8,128)(2,1)S(1)}, bf16[16,2048]{1,0:T(8,128)(2,1)}, u32[]{:S(2)}) copy-start(bf16[16,2048]{1,0:T(8,128)(2,1)} %param.27) | copy-start | bytes 196612
  6.5 38.7 %copy-start.1 = (bf16[32,2048]{1,0:T(8,128)(2,1)S(1)}, bf16[32,2048]{1,0:T(8,128)(2,1)}, u32[]{:S(2)}) copy-start(bf16[32,2048]{1,0:T(8,128)(2,1)} %param.25) | copy-start | bytes 393220
  6.5 38.7 %copy-start.26 = (f32[2048]{0:T(1024)S(1)}, f32[2048]{0:T(1024)}, u32[]{:S(2)}) copy-start(f32[2048]{0:T(1024)} %param.29) | copy-start | bytes 24580
  6.5 86.5 %all-gather.3.cloned.1.call-start = ((), (), s32[]{:S(2)}) async-start(), calls=%async_computation.3 | async-start | bytes 4456448 | tf_op jit(solution)/shard_map/all_gather | solution.py:37
  10.3 34.0 %all-to-all-start = ((f32[64,2,96]{2,1,0:T(2,128)}), f32[64,2,96]{2,1,0:T(2,128)S(1)}, u32[]{:S(2)}, u32[]{:S(2)}) async-start(f32[64,2,96]{2,1,0:T(2,128)} %broadcast_in_dim.39), calls=%async_computation | async-start | bytes 131072 | tf_op jit(solution)/shard_map/all_to_all | solution.py:27
  33.3 28.4 %copy-start.28 = (f32[1,256]{1,0:T(1,128)}, f32[1,256]{1,0:T(1,128)S(1)}, u32[]{:S(2)}) copy-start(f32[1,256]{1,0:T(1,128)S(1)} %get-tuple-element.427) | copy-start | bytes 3076
  33.3 29.4 %copy-start.29 = (f32[1,256]{1,0:T(1,128)}, f32[1,256]{1,0:T(1,128)S(1)}, u32[]{:S(2)}) copy-start(f32[1,256]{1,0:T(1,128)S(1)} %get-tuple-element.426) | copy-start | bytes 3076
  44.3 17.3 %copy-start.16 = (f32[64,2,96]{2,1,0:T(2,128)}, f32[64,2,96]{2,1,0:T(2,128)S(1)}, u32[]{:S(2)}) copy-start(f32[64,2,96]{2,1,0:T(2,128)S(1)} %all-to-all-done) | copy-start | bytes 147460
  46.3 11.7 %all-to-all-start.1 = ((bf16[4,32,2048]{2,1,0:T(8,128)(2,1)}), bf16[4,32,2048]{2,1,0:T(8,128)(2,1)S(1)}, u32[]{:S(2)}, u32[]{:S(2)}) async-start(bf16[4,32,2048]{2,1,0:T(8,128)(2,1)} %broadcast_in_dim.41), calls=%async_computation.1 | async-start | bytes 1048576 | tf_op jit(solution)/shard_map/all_to_all | solution.py:27
  49.7 140.3 %all-gather.5.cloned.1.call-start = ((), (), s32[]{:S(2)}) async-start(), calls=%async_computation.4 | async-start | bytes 4473856 | tf_op jit(solution)/shard_map/all_gather | solution.py:46
  51.3 8.8 %copy-start.24 = (bf16[16,2048]{1,0:T(8,128)(2,1)}, bf16[16,2048]{1,0:T(8,128)(2,1)S(1)}, u32[]{:S(2)}) copy-start(bf16[16,2048]{1,0:T(8,128)(2,1)S(1)} %fusion.47) | copy-start | bytes 196612
  58.0 4.7 %copy-start.19 = (bf16[4,32,2048]{2,1,0:T(8,128)(2,1)}, bf16[4,32,2048]{2,1,0:T(8,128)(2,1)S(1)}, u32[]{:S(2)}) copy-start(bf16[4,32,2048]{2,1,0:T(8,128)(2,1)S(1)} %all-to-all-done.1) | copy-start | bytes 1572868
  59.4 0.6 copy-start.22
  61.6 31.4 %copy-start.25 = (bf16[16,2048]{1,0:T(8,128)(2,1)S(1)}, bf16[16,2048]{1,0:T(8,128)(2,1)}, u32[]{:S(2)}) copy-start(bf16[16,2048]{1,0:T(8,128)(2,1)} %copy-done.24) | copy-start | bytes 196612
  94.8 0.6 copy-start.23
  97.9 0.8 copy-start.15
  101.0 0.7 copy-start.21
  101.7 7.9 %copy-start.5 = (bf16[2,64,2,256]{3,2,1,0:T(2,128)(2,1)}, bf16[2,64,2,256]{3,2,1,0:T(2,128)(2,1)S(1)}, u32[]{:S(2)}) copy-start(bf16[2,64,2,256]{3,2,1,0:T(2,128)(2,1)S(1)} %reshape_reshape.17) | copy-start | bytes 393220
  103.2 1.0 copy-start.3
  112.3 3.7 %slice-start = ((bf16[144,512]{1,0:T(8,128)(2,1)}), bf16[16,512]{1,0:T(8,128)(2,1)S(1)}, s32[]{:S(2)}) async-start(bf16[144,512]{1,0:T(8,128)(2,1)} %copy-done.21), calls=%async_computation.5 | async-start | bytes 32768 | tf_op jit(solution)/shard_map/slice | solution.py:169
  112.3 3.7 %slice-start.1 = ((bf16[144,64]{1,0:T(8,128)(2,1)}), bf16[16,64]{1,0:T(8,128)(2,1)S(1)}, s32[]{:S(2)}) async-start(bf16[144,64]{1,0:T(8,128)(2,1)} %copy-done.22), calls=%async_computation.6 | async-start | bytes 8192 | tf_op jit(solution)/shard_map/slice | solution.py:169
  112.3 3.7 %slice-start.2 = ((bf16[144,256]{1,0:T(8,128)(2,1)}), bf16[16,256]{1,0:T(8,128)(2,1)S(1)}, s32[]{:S(2)}) async-start(bf16[144,256]{1,0:T(8,128)(2,1)} %copy-done.23), calls=%async_computation.7 | async-start | bytes 16384 | tf_op jit(solution)/shard_map/slice | solution.py:169
  112.4 38.6 %copy-start.18 = (bf16[2,64,2,128]{3,2,1,0:T(2,128)(2,1)S(1)}, bf16[2,64,2,128]{3,2,1,0:T(2,128)(2,1)}, u32[]{:S(2)}) copy-start(bf16[2,64,2,128]{3,2,1,0:T(2,128)(2,1)} %get-tuple-element.419) | copy-start | bytes 196612
  151.0 5.7 %copy-start.6 = (bf16[2,64,2,256]{3,2,1,0:T(2,128)(2,1)S(1)}, bf16[2,64,2,256]{3,2,1,0:T(2,128)(2,1)}, u32[]{:S(2)}) copy-start(bf16[2,64,2,256]{3,2,1,0:T(2,128)(2,1)} %copy-done.5) | copy-start | bytes 393220
  154.1 8.9 %copy-start.30 = (f32[1,256]{1,0:T(1,128)S(1)}, f32[1,256]{1,0:T(1,128)}, u32[]{:S(2)}) copy-start(f32[1,256]{1,0:T(1,128)} %copy-done.29) | copy-start | bytes 3076
  154.1 8.9 %copy-start.31 = (bf16[2,32,256]{2,1,0:T(8,128)(2,1)S(1)}, bf16[2,32,256]{2,1,0:T(8,128)(2,1)}, u32[]{:S(2)}) copy-start(bf16[2,32,256]{2,1,0:T(8,128)(2,1)} %param.35) | copy-start | bytes 98308
  163.3 10.6 %copy-start.10 = (f32[256,2,128]{2,1,0:T(2,128)S(1)}, f32[256,2,128]{2,1,0:T(2,128)}, u32[]{:S(2)}) copy-start(f32[256,2,128]{2,1,0:T(2,128)} %reshape.255) | copy-start | bytes 786436
  164.2 11.6 %copy-start.4 = (f32[128,2,128]{2,0,1:T(8,128)S(1)}, f32[128,2,128]{2,0,1:T(8,128)}, u32[]{:S(2)}) copy-start(f32[128,2,128]{2,0,1:T(8,128)} %copy-done.3) | copy-start | bytes 393220
  166.2 11.7 %copy-start.9 = (f32[4,64,2,128]{3,2,1,0:T(2,128)S(1)}, f32[4,64,2,128]{3,2,1,0:T(2,128)}, u32[]{:S(2)}) copy-start(f32[4,64,2,128]{3,2,1,0:T(2,128)} %reshape_reshape.20) | copy-start | bytes 786436
  169.5 8.3 %copy-start.11 = (f32[256,2,128]{2,1,0:T(2,128)S(1)}, f32[256,2,128]{2,1,0:T(2,128)}, u32[]{:S(2)}) copy-start(f32[256,2,128]{2,1,0:T(2,128)} %rev.24) | copy-start | bytes 786436
  174.8 3.4 %copy-start.12 = (f32[256,2,128]{2,1,0:T(2,128)S(1)}, f32[256,2,128]{2,1,0:T(2,128)}, u32[]{:S(2)}) copy-start(f32[256,2,128]{2,1,0:T(2,128)} %rev.25) | copy-start | bytes 786436
  174.8 3.6 %copy-start.14 = (bf16[256,2,256]{2,0,1:T(8,128)(2,1)S(1)}, bf16[256,2,256]{2,0,1:T(8,128)(2,1)}, u32[]{:S(2)}) copy-start(bf16[256,2,256]{2,0,1:T(8,128)(2,1)} %rev.26) | copy-start | bytes 786436
  175.8 3.9 %copy-start.13 = (bf16[4,64,2,256]{3,2,1,0:T(2,128)(2,1)S(1)}, bf16[4,64,2,256]{3,2,1,0:T(2,128)(2,1)}, u32[]{:S(2)}) copy-start(bf16[4,64,2,256]{3,2,1,0:T(2,128)(2,1)} %reshape_reshape.21) | copy-start | bytes 786436
  212.9 20.4 %copy-start.8 = (f32[128,2,256]{0,2,1:T(8,128)S(1)}, f32[128,2,256]{0,2,1:T(8,128)}, u32[]{:S(2)}) copy-start(f32[128,2,256]{0,2,1:T(8,128)} %copy.149) | copy-start | bytes 786436
  212.9 21.1 %copy-start.7 = (f32[128,2,256]{0,2,1:T(8,128)S(1)}, f32[128,2,256]{0,2,1:T(8,128)}, u32[]{:S(2)}) copy-start(f32[128,2,256]{0,2,1:T(8,128)} %copy.138) | copy-start | bytes 786436
  233.3 0.9 copy-start.27
  234.2 5.7 %copy-start.17 = (f32[64,2,96]{2,1,0:T(2,128)S(1)}, f32[64,2,96]{2,1,0:T(2,128)}, u32[]{:S(2)}) copy-start(f32[64,2,96]{2,1,0:T(2,128)} %copy-done.16) | copy-start | bytes 147460
  234.3 13.7 %copy-start.2 = (bf16[32,2048]{1,0:T(8,128)(2,1)S(1)}, bf16[32,2048]{1,0:T(8,128)(2,1)}, u32[]{:S(2)}) copy-start(bf16[32,2048]{1,0:T(8,128)(2,1)} %param.25) | copy-start | bytes 393220
  235.6 12.3 %all-to-all-start.2 = ((bf16[4,32,2048]{2,1,0:T(8,128)(2,1)}), bf16[4,32,2048]{2,1,0:T(8,128)(2,1)S(1)}, u32[]{:S(2)}, u32[]{:S(2)}) async-start(bf16[4,32,2048]{2,1,0:T(8,128)(2,1)} %bitcast.42), calls=%async_computation.2 | async-start | bytes 1048576 | tf_op jit(solution)/shard_map/all_to_all | solution.py:60
Sparse Core Ops, SparseCore 0:
  9.4 83.5 all-gather.2
  114.6 74.6 all-gather.4
where the time goes:
time: 258 us; the launch traced here: 256 us
  other arithmetic  55.2 us (21%)
  waiting for transfers between devices  52 us (20%)
  local copies, waits for them, and re-layouts  48.4 us (19%)
  blocking collectives  33.2 us (13%)
  starting transfers between devices  26.5 us (10%)
  matrix products  25.1 us (10%)
  between operations  14.2 us (6%)
    all_gather x1, blocking collectives, in_one_piece(): whole = lax.all_gather(both, axis, axis=dim, tiled=True)  33.2 us
    all_gather x1, waiting for transfers between devices, in_one_piece(): whole = lax.all_gather(both, axis, axis=dim, tiled=True)  26.3 us
    all_to_all x2, starting transfers between devices, from_everyone(): lax.all_to_all(jnp.broadcast_to(x[None], (size, *x.shape)), axis, 0, 0, t...  22.2 us
    select_n x16, other arithmetic, fold_step(): backward_in = jnp.where(back_index > my_index, moved_backward, backward_in)  19.6 us
    all_to_all x2, waiting for transfers between devices, from_everyone(): lax.all_to_all(jnp.broadcast_to(x[None], (size, *x.shape)), axis, 0, 0, t...  17.7 us
    while x2, local copies, waits for them, and re-layouts, per_device(): lax.fori_loop(0, device_count, fold_step, (context_forward, context_backw...  13.2 us
    add x12, other arithmetic, advance(): return (jnp.exp(step_decay)[:, :, None] * carried + step_update, carried)  9.05 us
    convert_element_type x2, other arithmetic, per_device(): part.astype(jnp.float32)  8.92 us
  transfers between devices with their start and end apart: 5, of which 4 were waited for; matrix products, arithmetic and copies ran while one was open for 23% of the time, Pallas kernels for 0%

commit v1 on v0

v1 whole, which is shorter than its diff:
```python
import jax
import jax.numpy as jnp
from jax import lax
from jax.experimental import pallas as pl
from jax.experimental.pallas import tpu as pltpu
from jax.sharding import Mesh, PartitionSpec as P

D = 2048
DK = 128
RANK = 32
BLOCK = 64
CTX_LIFT = 4.0
EPS = 1e-06
SHARP = 16.0
SEG = 512
CTX_SEG = 64
ROWS = SEG + CTX_SEG
PAYLOAD = 336
bf16 = jnp.bfloat16
f32 = jnp.float32
VM = pl.BlockSpec(memory_space=pltpu.VMEM)
SM = pl.BlockSpec(memory_space=pltpu.SMEM)


def to_everyone(x, axis):
    size = lax.axis_size(axis)
    return lax.all_to_all(jnp.broadcast_to(x[None], (size, *x.shape)), axis, 0, 0, tiled=True)


def three_parts(x):
    hi = x.astype(bf16)
    rest = x - hi.astype(f32)
    mid = rest.astype(bf16)
    lo = (rest - mid.astype(f32)).astype(bf16)
    return hi, mid, lo


def tri(rows, cols, upper):
    r = lax.broadcasted_iota(jnp.int32, (rows, cols), 0)
    c = lax.broadcasted_iota(jnp.int32, (rows, cols), 1)
    return (c >= r) if upper else (c <= r)


def summed_by(mask, a):
    m = mask.astype(f32).astype(bf16)
    stacked = jnp.concatenate(three_parts(a), axis=0)
    return jnp.dot(jnp.concatenate([m, m, m], axis=1), stacked, preferred_element_type=f32)


def nt(a, b):
    return lax.dot_general(a, b, (((1,), (1,)), ((), ())), preferred_element_type=f32)


def tn(a, b):
    return lax.dot_general(a, b, (((0,), (0,)), ((), ())), preferred_element_type=f32)


def project_kernel(
    place, x_ref, mod_ref, gain_ref, own_ref, other_ref, down_ref, up_ref, bias_ref, extra_ref,
    pay_ref, q_ref, k_ref, v_ref, cum_ref, h_ref, w_ref,
):
    seg, core = place[0], place[1]
    for xi in range(4):
        for z in range(16):
            at = z * 128 + xi * 32
            w_ref[pl.ds(pl.multiple_of(at + core * 16, 16), 16), 0:384] = own_ref[xi, z]
            w_ref[pl.ds(pl.multiple_of(at + 16 - core * 16, 16), 16), 0:384] = other_ref[xi, z]
    w_ref[:, 384:448] = down_ref[...]
    w_ref[:, 448:512] = jnp.zeros((D, 64), bf16)

    def normed_rows(rows, which):
        v = rows.astype(f32)
        r = lax.rsqrt(jnp.mean(v * v, axis=-1, keepdims=True) + EPS)
        scale = gain_ref[...] * (1.0 + mod_ref[which : which + 1, D : 2 * D])
        return (v * r * scale + mod_ref[which : which + 1, 0:D]).astype(bf16)

    def chunk(n, carry):
        y, zb = n // 4, n % 4
        rows = x_ref[y, pl.ds(pl.multiple_of(zb * 32, 32), 32), :]
        h_ref[pl.ds(pl.multiple_of(zb * 128 + y * 32, 32), 32), :] = normed_rows(rows, 0)
        return carry

    lax.fori_loop(0, 16, chunk, 0)
    for y in range(4):
        h_ref[SEG + y * 16 : SEG + y * 16 + 16, :] = normed_rows(x_ref[y, 128:144, :], 1)

    out = jnp.dot(h_ref[...], w_ref[...], preferred_element_type=f32).astype(bf16)
    q_ref[...] = out[:SEG, 0:128]
    k_ref[...] = out[:SEG, 128:256]
    v_ref[...] = out[:SEG, 256:384]
    low = out[:, 384:448]
    raw = jnp.dot(low, up_ref[...], preferred_element_type=f32) + bias_ref[...]
    logs = (jnp.minimum(raw, 0.0) - jnp.log1p(jnp.exp(-jnp.abs(raw)))) * (1.0 / SHARP)
    ef = extra_ref[:, 0:1]
    eb = extra_ref[:, 1:2]
    af = logs[:SEG, 0:128] + ef
    ab = logs[:SEG, 128:256] + eb
    low_mask = tri(BLOCK, BLOCK, False)
    up_mask = tri(BLOCK, BLOCK, True)
    wf, wb = [], []
    for n in range(SEG // BLOCK):
        sl = slice(n * BLOCK, (n + 1) * BLOCK)
        wf.append(summed_by(low_mask, af[sl]))
        wb.append(summed_by(up_mask, ab[sl]))
        cum_ref[0, sl, :] = wf[-1]
        cum_ref[1, sl, :] = wb[-1]
    tot_f = [w[BLOCK - 1 : BLOCK] for w in wf]
    tot_b = [w[0:1] for w in wb]
    dev_f = sum(tot_f)
    dev_b = sum(tot_b)
    kk = out[:SEG, 128:256].astype(f32)
    before = jnp.zeros((1, DK), f32)
    kf = []
    for n in range(SEG // BLOCK):
        kf.append(kk[n * BLOCK : (n + 1) * BLOCK] * jnp.exp(dev_f - before - wf[n]))
        before = before + tot_f[n]
    after = jnp.zeros((1, DK), f32)
    kb = [None] * (SEG // BLOCK)
    for n in reversed(range(SEG // BLOCK)):
        kb[n] = kk[n * BLOCK : (n + 1) * BLOCK] * jnp.exp(dev_b - after - wb[n])
        after = after + tot_b[n]
    both = jnp.concatenate(
        [jnp.concatenate(kf, 0).astype(bf16), jnp.concatenate(kb, 0).astype(bf16)], axis=1
    )
    states = tn(out[:SEG, 256:384], both).astype(bf16)

    def order(i):
        return ((i % 16) // 4) * 16 + (i // 16) * 4 + i % 4

    r = order(lax.broadcasted_iota(jnp.int32, (CTX_SEG, CTX_SEG), 0))
    c = order(lax.broadcasted_iota(jnp.int32, (CTX_SEG, CTX_SEG), 1))
    later = summed_by(c > r, logs[SEG:, 0:128])
    earlier = summed_by(c < r, logs[SEG:, 128:256])
    ctx_f = jnp.sum(logs[SEG:, 0:128], axis=0, keepdims=True)
    ctx_b = jnp.sum(logs[SEG:, 128:256], axis=0, keepdims=True)
    ck = out[SEG:, 128:256].astype(f32)
    ckf = (ck * jnp.exp(later)).astype(bf16)
    ckb = (ck * jnp.exp(earlier)).astype(bf16)
    cv = out[SEG:, 256:384]
    zero = jnp.zeros((7, DK), bf16)
    for peer in range(4):
        ahead = peer > seg
        pay_ref[peer, 0:128, :] = jnp.where(ahead, states[:, 0:128], states[:, 128:256])
        pay_ref[peer, 128:192, :] = ckf
        pay_ref[peer, 192:256, :] = ckb
        pay_ref[peer, 256:320, :] = cv
        dev = jnp.where(ahead, dev_f, dev_b)
        pay_ref[peer, 320:336, :] = jnp.concatenate(
            [*three_parts(dev), *three_parts(ctx_f), *three_parts(ctx_b), zero], axis=0
        )


def local_kernel(q_ref, k_ref, v_ref, cum_ref, o_ref, lift_f_ref, lift_b_ref):
    blocks = SEG // BLOCK
    low_mask = tri(BLOCK, BLOCK, False)
    up_mask = tri(BLOCK, BLOCK, True)
    tot_f = [cum_ref[0, (n + 1) * BLOCK - 1 : (n + 1) * BLOCK, :] for n in range(blocks)]
    tot_b = [cum_ref[1, n * BLOCK : n * BLOCK + 1, :] for n in range(blocks)]
    state = jnp.zeros((DK, DK), f32)
    before = jnp.zeros((1, DK), f32)
    for n in range(blocks):
        sl = slice(n * BLOCK, (n + 1) * BLOCK)
        q = q_ref[sl, :].astype(f32)
        k = k_ref[sl, :].astype(f32)
        v = v_ref[sl, :]
        wf = cum_ref[0, sl, :]
        wb = cum_ref[1, sl, :]
        mf = 0.5 * tot_f[n]
        mb = 0.5 * tot_b[n]
        sf = nt((q * jnp.exp(wf - mf)).astype(bf16), (k * jnp.exp(mf - wf)).astype(bf16))
        sb = nt((q * jnp.exp(wb - mb)).astype(bf16), (k * jnp.exp(mb - wb)).astype(bf16))
        scores = jnp.where(low_mask, sf, 0.0) + jnp.where(up_mask, sb, 0.0)
        out = jnp.dot(scores.astype(bf16), v, preferred_element_type=f32)
        qd = q * jnp.exp(wf)
        lift_f_ref[sl, :] = (qd * jnp.exp(before)).astype(bf16)
        if n > 0:
            out = out + nt(qd.astype(bf16), state.astype(bf16))
        o_ref[sl, :] = out
        if n < blocks - 1:
            state = jnp.exp(tot_f[n]) * state + tn(v, (k * jnp.exp(tot_f[n] - wf)).astype(bf16))
        before = before + tot_f[n]
    state = jnp.zeros((DK, DK), f32)
    after = jnp.zeros((1, DK), f32)
    for n in reversed(range(blocks)):
        sl = slice(n * BLOCK, (n + 1) * BLOCK)
        q = q_ref[sl, :].astype(f32)
        k = k_ref[sl, :].astype(f32)
        v = v_ref[sl, :]
        wb = cum_ref[1, sl, :]
        qd = q * jnp.exp(wb)
        lift_b_ref[sl, :] = (qd * jnp.exp(after)).astype(bf16)
        if n < blocks - 1:
            o_ref[sl, :] = o_ref[sl, :] + nt(qd.astype(bf16), state.astype(bf16))
        if n > 0:
            state = jnp.exp(tot_b[n]) * state + tn(v, (k * jnp.exp(tot_b[n] - wb)).astype(bf16))
        after = after + tot_b[n]


def combine_kernel(place, in_ref, o_ref, lift_f_ref, lift_b_ref, out_ref):
    seg = place[0]

    def vec(peer, at):
        rows = in_ref[peer, 320:336, :].astype(f32)
        return rows[at : at + 1] + rows[at + 1 : at + 2] + rows[at + 2 : at + 3]

    ctx_f = jnp.zeros((DK, DK), f32)
    ctx_b = jnp.zeros((DK, DK), f32)
    for q in range(4):
        ctx_f = jnp.exp(vec(q, 3)) * ctx_f + tn(in_ref[q, 256:320, :], in_ref[q, 128:192, :])
    for q in reversed(range(4)):
        ctx_b = jnp.exp(vec(q, 6)) * ctx_b + tn(in_ref[q, 256:320, :], in_ref[q, 192:256, :])
    fwd = CTX_LIFT * ctx_f
    for a in range(3):
        moved = jnp.exp(vec(a, 0)) * fwd + in_ref[a, 0:128, :].astype(f32)
        fwd = jnp.where(a < seg, moved, fwd)
    bwd = CTX_LIFT * ctx_b
    for a in (3, 2, 1):
        moved = jnp.exp(vec(a, 0)) * bwd + in_ref[a, 0:128, :].astype(f32)
        bwd = jnp.where(a > seg, moved, bwd)
    out = o_ref[...] + nt(lift_f_ref[...], fwd.astype(bf16)) + nt(lift_b_ref[...], bwd.astype(bf16))
    out_ref[...] = out.astype(bf16)


def output_kernel(mix_ref, gain_ref, w_ref, out_ref):
    total = None
    for h in range(2):
        v = jnp.concatenate([mix_ref[2 * h], mix_ref[2 * h + 1]], axis=1).astype(f32)
        r = lax.rsqrt(jnp.mean(v * v, axis=-1, keepdims=True) + EPS)
        n = (v * r * gain_ref[...]).astype(bf16)
        part = jnp.dot(n, w_ref[h * 256 : (h + 1) * 256, :], preferred_element_type=f32)
        total = part if total is None else total + part
    out_ref[...] = total.astype(bf16)


def final_kernel(parts_ref, lat_ref, gate_ref, out_ref):
    total = parts_ref[0].astype(f32)
    for g in range(1, 4):
        total = total + parts_ref[g].astype(f32)
    projected = total.astype(bf16).astype(f32)
    out_ref[...] = (lat_ref[...].astype(f32) + gate_ref[...] * projected).astype(bf16)


def per_device(
    latents,
    sample_vector,
    context,
    context_vector,
    norm_gain,
    modulator,
    query_weight,
    key_weight,
    value_weight,
    decay_down,
    decay_up,
    decay_bias,
    decay_extra,
    head_gain,
    out_weight,
):
    seg = lax.axis_index("A")
    sub = lax.axis_index("B")
    y = lax.axis_index("tp")
    core = lax.axis_index("core")
    dp = lax.axis_index("x") * 2 + core
    head = sub // 2
    place = jnp.stack([seg, core]).astype(jnp.int32)

    wq = lax.dynamic_slice_in_dim(query_weight, dp * 16, 16, 0)
    wk = lax.dynamic_slice_in_dim(key_weight, dp * 16, 16, 0)
    wv = lax.dynamic_slice_in_dim(value_weight, dp * 16, 16, 0)
    cut = jnp.stack(
        [
            jnp.concatenate(
                [
                    wq[:, (b // 2) * 128 : (b // 2 + 1) * 128],
                    wk[:, (b // 2) * 128 : (b // 2 + 1) * 128],
                    wv[:, b * 128 : (b + 1) * 128],
                ],
                axis=1,
            )
            for b in range(4)
        ]
    )
    cut = jnp.broadcast_to(cut[None], (4, 4, 16, 384)).reshape(16, 16, 384)
    with jax.named_scope("weights_z"):
        rows_z = lax.all_to_all(cut, ("A", "B"), 0, 0, tiled=True)

    conditions = jax.nn.silu(jnp.concatenate([sample_vector, context_vector], 0)).astype(bf16)
    local_mods = jnp.dot(conditions, modulator, preferred_element_type=f32)
    with jax.named_scope("modulation"):
        mods = to_everyone(local_mods, ("A", "B", "tp"))
    modulation = jnp.moveaxis(mods, 0, 1).reshape(2, 3 * D)

    ctx_rows = lax.dynamic_slice_in_dim(context, y * 4, 4, 0)
    extra = jnp.moveaxis(decay_extra, 1, 2).reshape(4, 128)
    extra_row = jnp.concatenate([p.reshape(1, 512) for p in three_parts(extra)], axis=1)
    extra_row = jnp.pad(extra_row, ((0, 3), (0, 512)))
    with jax.named_scope("rows_z"):
        near = to_everyone(jnp.concatenate([latents, ctx_rows, extra_row], 0), "B")
    extras = near[:, 36, :1536].astype(f32).reshape(4, 3, 2, 2, 128).sum(1)
    extras = lax.dynamic_index_in_dim(extras, head, 2, keepdims=False)
    extras = jnp.transpose(extras, (0, 2, 1)).reshape(SEG, 2)
    near_rows = jnp.concatenate(
        [near[:, :32].reshape(128, D), near[:, 32:36].reshape(16, D)], axis=0
    )
    with jax.named_scope("rows_y"):
        all_rows = to_everyone(near_rows, "tp")

    with jax.named_scope("weights_x"):
        own = to_everyone(rows_z, "x")
    with jax.named_scope("weights_core"):
        other = lax.ppermute(own, "core", [(0, 1), (1, 0)])

    up = lax.dynamic_slice_in_dim(decay_up, head * 128, 128, 2)
    up_both = jnp.concatenate(
        [jnp.pad(up[0], ((0, 0), (0, 128))), jnp.pad(up[1], ((0, 0), (128, 0)))], axis=0
    )
    bias = lax.dynamic_slice_in_dim(decay_bias, head * 128, 128, 1).reshape(1, 256)

    sds = jax.ShapeDtypeStruct
    payload, q, k, v, cum = pl.pallas_call(
        project_kernel,
        out_shape=(
            sds((4, PAYLOAD, DK), bf16),
            sds((SEG, DK), bf16),
            sds((SEG, DK), bf16),
            sds((SEG, DK), bf16),
            sds((2, SEG, DK), f32),
        ),
        in_specs=[SM] + [VM] * 9,
        out_specs=(VM,) * 5,
        scratch_shapes=[pltpu.VMEM((ROWS, D), bf16), pltpu.VMEM((D, 512), bf16)],
        name="project",
    )(
        place, all_rows, modulation, norm_gain.reshape(1, D), own, other, decay_down,
        up_both, bias, extras,
    )
    with jax.named_scope("states"):
        got = lax.all_to_all(payload, "A", 0, 0, tiled=True)
    local, lift_f, lift_b = pl.pallas_call(
        local_kernel,
        out_shape=(sds((SEG, DK), f32), sds((SEG, DK), bf16), sds((SEG, DK), bf16)),
        in_specs=[VM] * 4,
        out_specs=(VM,) * 3,
        name="local",
    )(q, k, v, cum)
    mixed = pl.pallas_call(
        combine_kernel,
        out_shape=sds((SEG, DK), bf16),
        in_specs=[SM] + [VM] * 4,
        out_specs=VM,
        name="combine",
    )(place, got, local, lift_f, lift_b)
    with jax.named_scope("mixed_z"):
        mine = lax.all_to_all(mixed.reshape(4, 128, DK), "B", 0, 0, tiled=True)
    partial = pl.pallas_call(
        output_kernel,
        out_shape=sds((128, D), bf16),
        in_specs=[VM] * 3,
        out_specs=VM,
        name="output",
    )(mine, head_gain.reshape(1, 256), out_weight)
    with jax.named_scope("summed_y"):
        parts = lax.all_to_all(partial.reshape(4, 32, D), "tp", 0, 0, tiled=True)
    return pl.pallas_call(
        final_kernel,
        out_shape=sds((32, D), bf16),
        in_specs=[VM] * 3,
        out_specs=VM,
        name="final",
    )(parts, latents, modulation[0:1, 2 * D :])


def solution(mesh):
    mesh = Mesh(mesh.devices.reshape(4, 4, 4, 4, 2), ("A", "B", "tp", "x", "core"))
    dp = ("x", "core")
    sp = ("A", "B")
    placed = (
        P((*dp, *sp, "tp"), None),
        P(dp, None),
        P((*dp, *sp), None),
        P(),
        P(),
        P(None, (*sp, "tp")),
        P(sp, "tp"),
        P(sp, "tp"),
        P(sp, "tp"),
        P(),
        P(None, None, "tp"),
        P(None, "tp"),
        P(None, (*dp, *sp), "tp"),
        P(),
        P("tp", None),
    )
    return jax.shard_map(
        per_device,
        mesh=mesh,
        in_specs=placed,
        out_specs=P((*dp, *sp, "tp"), None),
        check_vma=False,
    )
```

time: 258 us -> 188 us (0.73)
  other arithmetic: 55.2 us -> 6.69 us
  local copies, waits for them, and re-layouts: 48.4 us -> 18.2 us
  matrix products: 25.1 us -> 0.92 us
  Pallas kernels: 0 us -> 18.5 us
  waiting for transfers between devices: 52 us -> 70.1 us
  starting transfers between devices: 26.5 us -> 43.3 us
  between operations: 14.2 us -> 0.16 us
  blocking collectives: 33.2 us -> 28.2 us
    all_to_all x3 -> x6, waiting for transfers between devices: 25.6 us -> 70.1 us  [the longest x3 35.3 us: to_everyone(): lax.all_to_all(jnp.broadcast_to(x[None], (size, *x.shape)), axis, 0, 0, t...]
    all_gather x1 -> x0, blocking collectives: 33.2 us -> none  [in_one_piece(): whole = lax.all_gather(both, axis, axis=dim, tiled=True)]
    all_to_all x0 -> x2, blocking collectives: none -> 28.2 us  [the longest x1 18.3 us: to_everyone(): lax.all_to_all(jnp.broadcast_to(x[None], (size, *x.shape)), axis, 0, 0, t...]
    all_gather x2 -> x0, waiting for transfers between devices: 26.4 us -> none  [the longest x1 26.3 us: in_one_piece(): whole = lax.all_gather(both, axis, axis=dim, tiled=True)]
    dot_general x20 -> x1, matrix products: 25.1 us -> 0.92 us  [per_device(): local_mods = jnp.dot(conditions, modulator, preferred_element_type=f32)]
    select_n x16 -> x0, other arithmetic: 19.6 us -> none  [fold_step(): backward_in = jnp.where(back_index > my_index, moved_backward, backward_in)]
    pallas_call x0 -> x5, Pallas kernels: none -> 18.5 us  [the longest x1 8.28 us: per_device(): pl.pallas_call(project_kernel, out_shape=(sds((4, PAYLOAD, DK), bf16), sd...]
    all_to_all x3 -> x6, starting transfers between devices: 26.5 us -> 41.4 us  [the longest x3 27.3 us: to_everyone(): lax.all_to_all(jnp.broadcast_to(x[None], (size, *x.shape)), axis, 0, 0, t...]
  transfers between devices with their start and end apart: 5 -> 7, of which waited for: 4 -> 6; matrix products, arithmetic and copies ran while one was open for 23% -> 9% of each run, Pallas kernels for 0% -> 2%
where the time goes in v1:
time: 188 us; the launch traced here: 186 us
  waiting for transfers between devices  70.1 us (37%)
  starting transfers between devices  43.3 us (23%)
  blocking collectives  28.2 us (15%)
  Pallas kernels  18.5 us (10%)
  local copies, waits for them, and re-layouts  18.2 us (10%)
  other arithmetic  6.69 us (4%)
    all_to_all x3, waiting for transfers between devices, to_everyone(): lax.all_to_all(jnp.broadcast_to(x[None], (size, *x.shape)), axis, 0, 0, t...  35.3 us
    all_to_all x3, starting transfers between devices, to_everyone(): lax.all_to_all(jnp.broadcast_to(x[None], (size, *x.shape)), axis, 0, 0, t...  27.3 us
    all_to_all x1, blocking collectives, to_everyone(): lax.all_to_all(jnp.broadcast_to(x[None], (size, *x.shape)), axis, 0, 0, t...  18.3 us
    all_to_all x1, waiting for transfers between devices, per_device(): got = lax.all_to_all(payload, 'A', 0, 0, tiled=True)  15.5 us
    all_to_all x1, waiting for transfers between devices, per_device(): rows_z = lax.all_to_all(cut, ('A', 'B'), 0, 0, tiled=True)  12.5 us
    all_to_all x1, blocking collectives, per_device(): mine = lax.all_to_all(mixed.reshape(4, 128, DK), 'B', 0, 0, tiled=True)  9.93 us
    pallas_call x1, Pallas kernels, per_device(): pl.pallas_call(project_kernel, out_shape=(sds((4, PAYLOAD, DK), bf16), sd...  8.28 us
    all_to_all x1, waiting for transfers between devices, per_device(): parts = lax.all_to_all(partial.reshape(4, 32, D), 'tp', 0, 0, tiled=True)  6.77 us
  transfers between devices with their start and end apart: 7, of which 6 were waited for; matrix products, arithmetic and copies ran while one was open for 9% of the time, Pallas kernels for 2%

profile of v1, /device:TPU:6, one launch (start us, length us, event | category | flops | bytes accessed | tf_op | source)
XLA Modules:
  0.0 186.0 jit_solution(15234521546554119792)
XLA Ops:
  0.0 1.0 copy-done
  1.0 0.9 fusion.13
  1.9 0.7 broadcast_in_dim.12
  2.6 18.7 %all-to-all-start.2 = ((f32[64,2,96]{2,1,0:T(2,128)}), f32[64,2,96]{2,1,0:T(2,128)S(1)}, u32[]{:S(2)}, u32[]{:S(2)}) async-start(f32[64,2,96]{2,1,0:T(2,128)} %broadcast_in_dim.12), calls=%async_computation.2 | async-start | bytes 131072 | tf_op jit(solution)/shard_map/modulation/all_to_all | solution.py:27
  21.3 0.7 constant_dynamic-slice_fusion.2
  22.0 0.8 constant_dynamic-slice_fusion
  22.9 13.7 %all-to-all-done.2 = f32[64,2,96]{2,1,0:T(2,128)S(1)} async-done(((f32[64,2,96]{2,1,0:T(2,128)}), f32[64,2,96]{2,1,0:T(2,128)S(1)}, u32[]{:S(2)}, u32[]{:S(2)}) %all-to-all-start.2) | async-done | bytes 49184 | tf_op jit(solution)/shard_map/modulation/all_to_all | solution.py:27
  36.5 0.7 broadcast_in_dim.13
  37.2 3.5 %all-to-all-start.3 = ((bf16[16,16,384]{2,1,0:T(8,128)(2,1)}), bf16[16,16,384]{2,1,0:T(8,128)(2,1)S(1)}, u32[]{:S(2)}, u32[]{:S(2)}) async-start(bf16[16,16,384]{2,1,0:T(8,128)(2,1)} %bitcast.12), calls=%async_computation.3 | async-start | bytes 393216 | tf_op jit(solution)/shard_map/weights_z/all_to_all | solution.py:286
  40.8 0.7 convert_element_type.86
  41.5 0.8 fusion.16
  42.2 0.8 fusion.9
  43.0 0.9 pad_maximum_fusion.1
  43.9 12.5 %all-to-all-done.3 = bf16[16,16,384]{2,1,0:T(8,128)(2,1)S(1)} async-done(((bf16[16,16,384]{2,1,0:T(8,128)(2,1)}), bf16[16,16,384]{2,1,0:T(8,128)(2,1)S(1)}, u32[]{:S(2)}, u32[]{:S(2)}) %all-to-all-start.3) | async-done | bytes 196640 | tf_op jit(solution)/shard_map/weights_z/all_to_all | solution.py:286
  56.5 0.1 broadcast_in_dim.10
  56.5 18.3 %all_to_all.40 = bf16[4,40,2048]{2,1,0:T(8,128)(2,1)S(1)} all-to-all(bf16[4,40,2048]{2,1,0:T(8,128)(2,1)S(1)} %broadcast_in_dim.10), channel_id=1, replica_groups=mesh['A'=4,'B'=4,'tp'=4,'x'=4,'core'=2] {'B'}, dimensions={0} | all-to-all | bytes 1310720 | tf_op jit(solution)/shard_map/rows_z/all_to_all | solution.py:27
  74.8 1.0 broadcast_in_dim.14
  75.8 4.8 %all-to-all-start.4 = ((bf16[4,16,16,384]{3,2,1,0:T(8,128)(2,1)}), bf16[4,16,16,384]{3,2,1,0:T(8,128)(2,1)S(1)}, u32[]{:S(2)}, u32[]{:S(2)}) async-start(bf16[4,16,16,384]{3,2,1,0:T(8,128)(2,1)} %broadcast_in_dim.14), calls=%async_computation.4 | async-start | bytes 1572864 | tf_op jit(solution)/shard_map/weights_x/all_to_all | solution.py:27
  80.7 8.1 %all-to-all-done.4.own_ref = bf16[4,16,16,384]{3,2,1,0:T(8,128)(2,1)S(1)} async-done(((bf16[4,16,16,384]{3,2,1,0:T(8,128)(2,1)}), bf16[4,16,16,384]{3,2,1,0:T(8,128)(2,1)S(1)}, u32[]{:S(2)}, u32[]{:S(2)}) %all-to-all-start.4) | async-done | bytes 786464 | tf_op jit(solution)/shard_map/weights_x/all_to_all | solution.py:27
  88.9 1.7 broadcast_in_dim.11
  90.6 3.8 %all-to-all-start.1 = ((bf16[4,144,2048]{2,1,0:T(8,128)(2,1)}), bf16[4,144,2048]{2,1,0:T(8,128)(2,1)S(1)}, u32[]{:S(2)}, u32[]{:S(2)}) async-start(bf16[4,144,2048]{2,1,0:T(8,128)(2,1)} %broadcast_in_dim.11), calls=%async_computation.1 | async-start | bytes 4718592 | tf_op jit(solution)/shard_map/rows_y/all_to_all | solution.py:27
  94.4 2.0 %copy.28.down_ref = bf16[2048,64]{1,0:T(8,128)(2,1)} copy(bf16[2048,64]{0,1:T(8,128)(2,1)} %param.24) | data formatting | bytes 524288 | tf_op args[9]
  96.4 0.6 constant_dynamic-slice_fusion.4
  97.0 0.7 dynamic-slice_bitcast_fusion.1
  97.7 1.9 %collective-permute-start = (bf16[4,16,16,384]{3,2,1,0:T(8,128)(2,1)S(1)}, bf16[4,16,16,384]{3,2,1,0:T(8,128)(2,1)}, u32[]{:S(2)}, u32[]{:S(2)}) collective-permute-start(bf16[4,16,16,384]{3,2,1,0:T(8,128)(2,1)S(1)} %all-to-all-done.4.own_ref), channel_id=1, source_target_pairs={{0,1},{1,0},{2,3},{3,2},{4,5},{5,4},{6,7},{7,6},{8,9},{9,8},{10,11... | collective-permute-start | bytes 2359304 | tf_op jit(solution)/shard_map/weights_core/ppermute | solution.py:312
  99.6 0.6 pad_add_fusion.place
  100.2 0.6 fusion.2.up_ref
  100.8 1.5 copy.26
  102.3 1.6 reshape.93.mod_ref
  103.9 1.5 slice_convert_fusion
  105.4 0.8 reduce_sum.9
  106.2 0.9 copy.27
  107.0 0.0 collective-permute-done.other_ref
  107.0 13.4 %all-to-all-done.1.x_ref = bf16[4,144,2048]{2,1,0:T(8,128)(2,1)S(1)} async-done(((bf16[4,144,2048]{2,1,0:T(8,128)(2,1)}), bf16[4,144,2048]{2,1,0:T(8,128)(2,1)S(1)}, u32[]{:S(2)}, u32[]{:S(2)}) %all-to-all-start.1) | async-done | bytes 2359328 | tf_op jit(solution)/shard_map/rows_y/all_to_all | solution.py:27
  120.4 1.4 copy-done.1
  121.9 8.3 %project.1 = (bf16[4,336,128]{2,1,0:T(8,128)(2,1)}, bf16[512,128]{1,0:T(8,128)(2,1)}, bf16[512,128]{1,0:T(8,128)(2,1)}, bf16[512,128]{1,0:T(8,128)(2,1)}, f32[2,512,128]{2,1,0:T(8,128)}) custom-call(s32[2]{0:T(128)} %pad_add_fusion.place, bf16[4,144,2048]{2,1,0:T(8,128)(2,1)} %copy-done.1, f32[2,6144]{1,0:T(2,128)} %reshape.93.mod_ref, f32[1,2048]{1,0:T(1,128)} %bitcast.38, ...), custom_call_target="tpu_custom_call" | custom-call | tf_op jit(solution)/shard_map/project/pallas_call | solution.py:321
  130.2 6.6 %all-to-all-start.5 = ((bf16[4,336,128]{2,1,0:T(8,128)(2,1)}), bf16[4,336,128]{2,1,0:T(8,128)(2,1)S(1)}, u32[]{:S(2)}, u32[]{:S(2)}) async-start(bf16[4,336,128]{2,1,0:T(8,128)(2,1)} %get-tuple-element.13), calls=%async_computation.5 | async-start | bytes 688128 | tf_op jit(solution)/shard_map/states/all_to_all | solution.py:339
  136.8 3.0 %local.1 = (f32[512,128]{1,0:T(8,128)}, bf16[512,128]{1,0:T(8,128)(2,1)}, bf16[512,128]{1,0:T(8,128)(2,1)}) custom-call(bf16[512,128]{1,0:T(8,128)(2,1)} %get-tuple-element.14.q_ref, bf16[512,128]{1,0:T(8,128)(2,1)} %get-tuple-element.15.k_ref, bf16[512,128]{1,0:T(8,128)(2,1)} %get-tuple-element.16.v_ref, f32[2,512,128]{2,1,0:T(8,128)} %get-tuple-element.17.cum_ref), custom_call_target="tpu_custom_call" | custom-call | tf_op jit(solution)/shard_map/local/pallas_call | solution.py:340
  139.8 15.5 %all-to-all-done.5.in_ref = bf16[4,336,128]{2,1,0:T(8,128)(2,1)S(1)} async-done(((bf16[4,336,128]{2,1,0:T(8,128)(2,1)}), bf16[4,336,128]{2,1,0:T(8,128)(2,1)S(1)}, u32[]{:S(2)}, u32[]{:S(2)}) %all-to-all-start.5) | async-done | bytes 344096 | tf_op jit(solution)/shard_map/states/all_to_all | solution.py:339
  155.4 0.7 copy-done.5
  156.1 2.3 %combine.1 = bf16[512,128]{1,0:T(8,128)(2,1)} custom-call(s32[2]{0:T(128)} %pad_add_fusion.place, bf16[4,336,128]{2,1,0:T(8,128)(2,1)} %copy-done.5, f32[512,128]{1,0:T(8,128)} %get-tuple-element.18.o_ref, bf16[512,128]{1,0:T(8,128)(2,1)} %get-tuple-element.19.lift_f_ref, bf16[512,128]{1,0:T(8,128)(2,1)} %get-tuple-element.20.lift_b_ref), custom_call_target="tpu_custom_call" | custom-call | tf_op jit(solution)/shard_map/combine/pallas_call | solution.py:347
  158.4 9.9 %all_to_all.41.mix_ref = bf16[4,128,128]{2,1,0:T(8,128)(2,1)} all-to-all(bf16[4,128,128]{2,1,0:T(8,128)(2,1)} %bitcast.34), channel_id=1, replica_groups=mesh['A'=4,'B'=4,'tp'=4,'x'=4,'core'=2] {'B'}, dimensions={0} | all-to-all | bytes 262144 | tf_op jit(solution)/shard_map/mixed_z/all_to_all | solution.py:355
  168.3 3.0 %output.1 = bf16[128,2048]{1,0:T(8,128)(2,1)} custom-call(bf16[4,128,128]{2,1,0:T(8,128)(2,1)} %all_to_all.41.mix_ref, f32[1,256]{1,0:T(1,128)} %bitcast.42, bf16[512,2048]{1,0:T(8,128)(2,1)} %w_ref.1), custom_call_target="tpu_custom_call" | custom-call | tf_op jit(solution)/shard_map/output/pallas_call | solution.py:356
  171.3 3.9 %all-to-all-start.7 = ((bf16[4,32,2048]{2,1,0:T(8,128)(2,1)}), bf16[4,32,2048]{2,1,0:T(8,128)(2,1)S(1)}, u32[]{:S(2)}, u32[]{:S(2)}) async-start(bf16[4,32,2048]{2,1,0:T(8,128)(2,1)} %bitcast.31), calls=%async_computation.7 | async-start | bytes 1048576 | tf_op jit(solution)/shard_map/summed_y/all_to_all | solution.py:364
  175.2 1.3 slice.63.gate_ref
  176.6 6.8 %all-to-all-done.7.parts_ref = bf16[4,32,2048]{2,1,0:T(8,128)(2,1)S(1)} async-done(((bf16[4,32,2048]{2,1,0:T(8,128)(2,1)}), bf16[4,32,2048]{2,1,0:T(8,128)(2,1)S(1)}, u32[]{:S(2)}, u32[]{:S(2)}) %all-to-all-start.7) | async-done | bytes 524320 | tf_op jit(solution)/shard_map/summed_y/all_to_all | solution.py:364
  183.3 0.8 copy-done.4
  184.1 1.9 %final.1 = bf16[32,2048]{1,0:T(8,128)(2,1)} custom-call(bf16[4,32,2048]{2,1,0:T(8,128)(2,1)} %copy-done.4, bf16[32,2048]{1,0:T(8,128)(2,1)} %lat_ref.1, f32[1,2048]{1,0:T(1,128)} %slice.63.gate_ref), custom_call_target="tpu_custom_call" | custom-call | tf_op jit(solution)/shard_map/final/pallas_call | solution.py:365
  (20 shorter events, 0.2 us)
Async XLA Ops:
  0.0 1.0 copy-start
  2.6 34.0 %all-to-all-start.2 = ((f32[64,2,96]{2,1,0:T(2,128)}), f32[64,2,96]{2,1,0:T(2,128)S(1)}, u32[]{:S(2)}, u32[]{:S(2)}) async-start(f32[64,2,96]{2,1,0:T(2,128)} %broadcast_in_dim.12), calls=%async_computation.2 | async-start | bytes 131072 | tf_op jit(solution)/shard_map/modulation/all_to_all | solution.py:27
  36.5 0.7 copy-start.6
  37.2 19.2 %all-to-all-start.3 = ((bf16[16,16,384]{2,1,0:T(8,128)(2,1)}), bf16[16,16,384]{2,1,0:T(8,128)(2,1)S(1)}, u32[]{:S(2)}, u32[]{:S(2)}) async-start(bf16[16,16,384]{2,1,0:T(8,128)(2,1)} %bitcast.12), calls=%async_computation.3 | async-start | bytes 393216 | tf_op jit(solution)/shard_map/weights_z/all_to_all | solution.py:286
  74.8 5.9 %copy-start.3 = (bf16[4,40,2048]{2,1,0:T(8,128)(2,1)}, bf16[4,40,2048]{2,1,0:T(8,128)(2,1)S(1)}, u32[]{:S(2)}) copy-start(bf16[4,40,2048]{2,1,0:T(8,128)(2,1)S(1)} %all_to_all.40) | copy-start | bytes 1966084
  75.8 13.1 %all-to-all-start.4 = ((bf16[4,16,16,384]{3,2,1,0:T(8,128)(2,1)}), bf16[4,16,16,384]{3,2,1,0:T(8,128)(2,1)S(1)}, u32[]{:S(2)}, u32[]{:S(2)}) async-start(bf16[4,16,16,384]{3,2,1,0:T(8,128)(2,1)} %broadcast_in_dim.14), calls=%async_computation.4 | async-start | bytes 1572864 | tf_op jit(solution)/shard_map/weights_x/all_to_all | solution.py:27
  88.9 8.8 %copy-start.2 = (bf16[4,16,16,384]{3,2,1,0:T(8,128)(2,1)}, bf16[4,16,16,384]{3,2,1,0:T(8,128)(2,1)S(1)}, u32[]{:S(2)}) copy-start(bf16[4,16,16,384]{3,2,1,0:T(8,128)(2,1)S(1)} %all-to-all-done.4.own_ref) | copy-start | bytes 2359300
  90.6 5.8 %copy-start.7 = (f32[2,256]{1,0:T(2,128)S(1)}, f32[2,256]{1,0:T(2,128)}, u32[]{:S(2)}) copy-start(f32[2,256]{1,0:T(2,128)} %param.26) | copy-start | bytes 6148
  90.6 29.8 %all-to-all-start.1 = ((bf16[4,144,2048]{2,1,0:T(8,128)(2,1)}), bf16[4,144,2048]{2,1,0:T(8,128)(2,1)S(1)}, u32[]{:S(2)}, u32[]{:S(2)}) async-start(bf16[4,144,2048]{2,1,0:T(8,128)(2,1)} %broadcast_in_dim.11), calls=%async_computation.1 | async-start | bytes 4718592 | tf_op jit(solution)/shard_map/rows_y/all_to_all | solution.py:27
  97.7 9.3 %collective-permute-start = (bf16[4,16,16,384]{3,2,1,0:T(8,128)(2,1)S(1)}, bf16[4,16,16,384]{3,2,1,0:T(8,128)(2,1)}, u32[]{:S(2)}, u32[]{:S(2)}) collective-permute-start(bf16[4,16,16,384]{3,2,1,0:T(8,128)(2,1)S(1)} %all-to-all-done.4.own_ref), channel_id=1, source_target_pairs={{0,1},{1,0},{2,3},{3,2},{4,5},{5,4},{6,7},{7,6},{8,9},{9,8},{10,11... | collective-permute-start | bytes 2359304 | tf_op jit(solution)/shard_map/weights_core/ppermute | solution.py:312
  120.4 1.4 copy-start.1
  130.2 25.2 %all-to-all-start.5 = ((bf16[4,336,128]{2,1,0:T(8,128)(2,1)}), bf16[4,336,128]{2,1,0:T(8,128)(2,1)S(1)}, u32[]{:S(2)}, u32[]{:S(2)}) async-start(bf16[4,336,128]{2,1,0:T(8,128)(2,1)} %get-tuple-element.13), calls=%async_computation.5 | async-start | bytes 688128 | tf_op jit(solution)/shard_map/states/all_to_all | solution.py:339
  155.4 0.7 copy-start.5
  171.3 12.0 %all-to-all-start.7 = ((bf16[4,32,2048]{2,1,0:T(8,128)(2,1)}), bf16[4,32,2048]{2,1,0:T(8,128)(2,1)S(1)}, u32[]{:S(2)}, u32[]{:S(2)}) async-start(bf16[4,32,2048]{2,1,0:T(8,128)(2,1)} %bitcast.31), calls=%async_computation.7 | async-start | bytes 1048576 | tf_op jit(solution)/shard_map/summed_y/all_to_all | solution.py:364
  183.3 0.8 copy-start.4

commit v2 on v1

--- a/solution.py
+++ b/solution.py
@@ -35,6 +35,12 @@
     return hi, mid, lo
 
 
+def three_pieces(x):
+    hi = lax.reduce_precision(x, 8, 7)
+    mid = lax.reduce_precision(x - hi, 8, 7)
+    return hi.astype(bf16), mid.astype(bf16), (x - hi - mid).astype(bf16)
+
+
 def tri(rows, cols, upper):
     r = lax.broadcasted_iota(jnp.int32, (rows, cols), 0)
     c = lax.broadcasted_iota(jnp.int32, (rows, cols), 1)
@@ -56,15 +62,18 @@
 
 
 def project_kernel(
-    place, x_ref, mod_ref, gain_ref, own_ref, other_ref, down_ref, up_ref, bias_ref, extra_ref,
+    place, own_ref, minus_ref, plus_ref, low_ref, high_ref, mod_ref, gain_ref, mine_ref, other_ref,
+    down_ref, up_ref, bias_ref, extra_ref,
     pay_ref, q_ref, k_ref, v_ref, cum_ref, h_ref, w_ref,
 ):
-    seg, core = place[0], place[1]
+    seg, core, sub, y = place[0], place[1], place[2], place[3]
     for xi in range(4):
         for z in range(16):
             at = z * 128 + xi * 32
-            w_ref[pl.ds(pl.multiple_of(at + core * 16, 16), 16), 0:384] = own_ref[xi, z]
-            w_ref[pl.ds(pl.multiple_of(at + 16 - core * 16, 16), 16), 0:384] = other_ref[xi, z]
+            here = pl.ds(pl.multiple_of(at + core * 16, 16), 16)
+            there = pl.ds(pl.multiple_of(at + 16 - core * 16, 16), 16)
+            w_ref[here, 0:384] = mine_ref[xi, z, :, 0:384]
+            w_ref[there, 0:384] = other_ref[xi, z, :, 0:384]
     w_ref[:, 384:448] = down_ref[...]
     w_ref[:, 448:512] = jnp.zeros((D, 64), bf16)
 
@@ -74,15 +83,19 @@
         scale = gain_ref[...] * (1.0 + mod_ref[which : which + 1, D : 2 * D])
         return (v * r * scale + mod_ref[which : which + 1, 0:D]).astype(bf16)
 
-    def chunk(n, carry):
-        y, zb = n // 4, n % 4
-        rows = x_ref[y, pl.ds(pl.multiple_of(zb * 32, 32), 32), :]
-        h_ref[pl.ds(pl.multiple_of(zb * 128 + y * 32, 32), 32), :] = normed_rows(rows, 0)
-        return carry
-
-    lax.fori_loop(0, 16, chunk, 0)
-    for y in range(4):
-        h_ref[SEG + y * 16 : SEG + y * 16 + 16, :] = normed_rows(x_ref[y, 128:144, :], 1)
+    y_of = [y, (y + 3) % 4, (y + 1) % 4, (y + 2) % 4]
+    for slot in range(4):
+        for j in range(4):
+            if slot < 3:
+                rows = (own_ref, minus_ref, plus_ref)[slot][j * 32 : j * 32 + 32, :]
+            elif j < 2:
+                rows = low_ref[j * 32 : j * 32 + 32, :]
+            else:
+                rows = high_ref[(j - 2) * 32 : (j - 2) * 32 + 32, :]
+            at = pl.multiple_of((sub ^ j) * 128 + y_of[slot] * 32, 32)
+            h_ref[pl.ds(at, 32), :] = normed_rows(rows, 0)
+        rows = (own_ref, minus_ref, plus_ref)[slot][128:144, :] if slot < 3 else high_ref[64:80, :]
+        h_ref[SEG + slot * 16 : SEG + slot * 16 + 16, :] = normed_rows(rows, 1)
 
     out = jnp.dot(h_ref[...], w_ref[...], preferred_element_type=f32).astype(bf16)
     q_ref[...] = out[:SEG, 0:128]
@@ -91,8 +104,9 @@
     low = out[:, 384:448]
     raw = jnp.dot(low, up_ref[...], preferred_element_type=f32) + bias_ref[...]
     logs = (jnp.minimum(raw, 0.0) - jnp.log1p(jnp.exp(-jnp.abs(raw)))) * (1.0 / SHARP)
-    ef = extra_ref[:, 0:1]
-    eb = extra_ref[:, 1:2]
+    extra = jnp.concatenate([extra_ref[sub ^ zb] for zb in range(4)], axis=0)
+    ef = extra[:, 0:1]
+    eb = extra[:, 1:2]
     af = logs[:SEG, 0:128] + ef
     ab = logs[:SEG, 128:256] + eb
     low_mask = tri(BLOCK, BLOCK, False)
@@ -125,7 +139,9 @@
     states = tn(out[:SEG, 256:384], both).astype(bf16)
 
     def order(i):
-        return ((i % 16) // 4) * 16 + (i // 16) * 4 + i % 4
+        slot = i // 16
+        step = jnp.where(slot == 0, 0, jnp.where(slot == 1, 3, slot - 1))
+        return (((i % 16) // 4) ^ sub) * 16 + ((step + y) % 4) * 4 + i % 4
 
     r = order(lax.broadcasted_iota(jnp.int32, (CTX_SEG, CTX_SEG), 0))
     c = order(lax.broadcasted_iota(jnp.int32, (CTX_SEG, CTX_SEG), 1))
@@ -263,11 +279,27 @@
     core = lax.axis_index("core")
     dp = lax.axis_index("x") * 2 + core
     head = sub // 2
-    place = jnp.stack([seg, core]).astype(jnp.int32)
+    place = jnp.stack([seg, core, sub, y]).astype(jnp.int32)
+
+    ctx_rows = lax.dynamic_slice_in_dim(context, y * 4, 4, 0)
+    extra = jnp.moveaxis(decay_extra, 1, 2).reshape(4, 128)
+    extra_row = jnp.concatenate([p.reshape(1, 512) for p in three_pieces(extra)], axis=1)
+    extra_row = jnp.pad(extra_row, ((0, 3), (0, 512)))
+    rows = jnp.concatenate([latents, ctx_rows, extra_row], 0)
+    near = [rows]
+    for j in range(1, 4):
+        with jax.named_scope(f"rows_z{j}"):
+            near.append(lax.ppermute(rows, "B", [(b, b ^ j) for b in range(4)]))
+    extras = jnp.stack([n[36, :1536] for n in near]).astype(f32).reshape(4, 3, 2, 2, 128).sum(1)
+    extras = lax.dynamic_index_in_dim(extras, head, 2, keepdims=False)
+    extras = jnp.transpose(extras, (0, 2, 1))
 
     wq = lax.dynamic_slice_in_dim(query_weight, dp * 16, 16, 0)
     wk = lax.dynamic_slice_in_dim(key_weight, dp * 16, 16, 0)
     wv = lax.dynamic_slice_in_dim(value_weight, dp * 16, 16, 0)
+    conditions = jax.nn.silu(jnp.concatenate([sample_vector, context_vector], 0)).astype(bf16)
+    local_mods = jnp.dot(conditions, modulator, preferred_element_type=f32)
+    riding = jnp.pad(jnp.concatenate(three_pieces(local_mods), axis=0), ((0, 10), (0, 32)))
     cut = jnp.stack(
         [
             jnp.concatenate(
@@ -275,41 +307,42 @@
                     wq[:, (b // 2) * 128 : (b // 2 + 1) * 128],
                     wk[:, (b // 2) * 128 : (b // 2 + 1) * 128],
                     wv[:, b * 128 : (b + 1) * 128],
+                    riding,
                 ],
                 axis=1,
             )
             for b in range(4)
         ]
     )
-    cut = jnp.broadcast_to(cut[None], (4, 4, 16, 384)).reshape(16, 16, 384)
+    cut = jnp.broadcast_to(cut[None], (4, 4, 16, 512)).reshape(16, 16, 512)
     with jax.named_scope("weights_z"):
         rows_z = lax.all_to_all(cut, ("A", "B"), 0, 0, tiled=True)
-
-    conditions = jax.nn.silu(jnp.concatenate([sample_vector, context_vector], 0)).astype(bf16)
-    local_mods = jnp.dot(conditions, modulator, preferred_element_type=f32)
-    with jax.named_scope("modulation"):
-        mods = to_everyone(local_mods, ("A", "B", "tp"))
-    modulation = jnp.moveaxis(mods, 0, 1).reshape(2, 3 * D)
-
-    ctx_rows = lax.dynamic_slice_in_dim(context, y * 4, 4, 0)
-    extra = jnp.moveaxis(decay_extra, 1, 2).reshape(4, 128)
-    extra_row = jnp.concatenate([p.reshape(1, 512) for p in three_parts(extra)], axis=1)
-    extra_row = jnp.pad(extra_row, ((0, 3), (0, 512)))
-    with jax.named_scope("rows_z"):
-        near = to_everyone(jnp.concatenate([latents, ctx_rows, extra_row], 0), "B")
-    extras = near[:, 36, :1536].astype(f32).reshape(4, 3, 2, 2, 128).sum(1)
-    extras = lax.dynamic_index_in_dim(extras, head, 2, keepdims=False)
-    extras = jnp.transpose(extras, (0, 2, 1)).reshape(SEG, 2)
-    near_rows = jnp.concatenate(
-        [near[:, :32].reshape(128, D), near[:, 32:36].reshape(16, D)], axis=0
-    )
-    with jax.named_scope("rows_y"):
-        all_rows = to_everyone(near_rows, "tp")
-
+    mods = rows_z[:, 0:8, 384:512]
+    around = [mods]
+    for j in range(1, 4):
+        with jax.named_scope(f"mods_y{j}"):
+            around.append(lax.ppermute(mods, "tp", [(i, i ^ j) for i in range(4)]))
     with jax.named_scope("weights_x"):
-        own = to_everyone(rows_z, "x")
+        mine = to_everyone(rows_z, "x")
     with jax.named_scope("weights_core"):
-        other = lax.ppermute(own, "core", [(0, 1), (1, 0)])
+        other = lax.ppermute(mine, "core", [(0, 1), (1, 0)])
+    around = jnp.stack(around)
+    around = jnp.stack([lax.dynamic_index_in_dim(around, y ^ t, 0, keepdims=False) for t in range(4)])
+    parts = around[:, :, 0:6, 0:96].astype(f32)
+    parts = parts[:, :, 0:2] + parts[:, :, 2:4] + parts[:, :, 4:6]
+    modulation = jnp.transpose(parts, (2, 1, 0, 3)).reshape(2, 3 * D)
+
+    own = jnp.concatenate([n[:32] for n in near] + [n[32:36] for n in near], axis=0)
+    up_shift = [(i, (i + 1) % 4) for i in range(4)]
+    down_shift = [(i, (i + 3) % 4) for i in range(4)]
+    with jax.named_scope("rows_up"):
+        minus = lax.ppermute(own, "tp", up_shift)
+    with jax.named_scope("rows_down"):
+        plus = lax.ppermute(own, "tp", down_shift)
+    with jax.named_scope("rows_up2"):
+        low = lax.ppermute(minus[:64], "tp", up_shift)
+    with jax.named_scope("rows_down2"):
+        high = lax.ppermute(plus[64:], "tp", down_shift)
 
     up = lax.dynamic_slice_in_dim(decay_up, head * 128, 128, 2)
     up_both = jnp.concatenate(
@@ -327,13 +360,13 @@
             sds((SEG, DK), bf16),
             sds((2, SEG, DK), f32),
         ),
-        in_specs=[SM] + [VM] * 9,
+        in_specs=[SM] + [VM] * 13,
         out_specs=(VM,) * 5,
         scratch_shapes=[pltpu.VMEM((ROWS, D), bf16), pltpu.VMEM((D, 512), bf16)],
         name="project",
     )(
-        place, all_rows, modulation, norm_gain.reshape(1, D), own, other, decay_down,
-        up_both, bias, extras,
+        place, own, minus, plus, low, high, modulation, norm_gain.reshape(1, D), mine, other,
+        decay_down, up_both, bias, extras,
     )
     with jax.named_scope("states"):
         got = lax.all_to_all(payload, "A", 0, 0, tiled=True)
@@ -352,23 +385,23 @@
         name="combine",
     )(place, got, local, lift_f, lift_b)
     with jax.named_scope("mixed_z"):
-        mine = lax.all_to_all(mixed.reshape(4, 128, DK), "B", 0, 0, tiled=True)
+        heads = lax.all_to_all(mixed.reshape(4, 128, DK), "B", 0, 0, tiled=True)
     partial = pl.pallas_call(
         output_kernel,
         out_shape=sds((128, D), bf16),
         in_specs=[VM] * 3,
         out_specs=VM,
         name="output",
-    )(mine, head_gain.reshape(1, 256), out_weight)
+    )(heads, head_gain.reshape(1, 256), out_weight)
     with jax.named_scope("summed_y"):
-        parts = lax.all_to_all(partial.reshape(4, 32, D), "tp", 0, 0, tiled=True)
+        shares = lax.all_to_all(partial.reshape(4, 32, D), "tp", 0, 0, tiled=True)
     return pl.pallas_call(
         final_kernel,
         out_shape=sds((32, D), bf16),
         in_specs=[VM] * 3,
         out_specs=VM,
         name="final",
-    )(parts, latents, modulation[0:1, 2 * D :])
+    )(shares, latents, modulation[0:1, 2 * D :])
 
 
 def solution(mesh):

time: 188 us -> 172 us (0.915)
  starting transfers between devices: 43.3 us -> 65.1 us
  waiting for transfers between devices: 70.1 us -> 54.2 us
  blocking collectives: 28.2 us -> 13.5 us
  other arithmetic: 6.69 us -> 3.66 us
  local copies, waits for them, and re-layouts: 18.2 us -> 15.8 us
    all_to_all x3 -> x1, waiting for transfers between devices: 35.3 us -> 0.01 us  [to_everyone(): lax.all_to_all(jnp.broadcast_to(x[None], (size, *x.shape)), axis, 0, 0, t...]
    ppermute x1 -> x11, starting transfers between devices: 1.91 us -> 35.1 us  [the longest x3 10.4 us: per_device(): around.append(lax.ppermute(mods, 'tp', [(i, i ^ j) for i in range(4)]))]
    all_to_all x3 -> x1, starting transfers between devices: 27.3 us -> 4.9 us  [to_everyone(): lax.all_to_all(jnp.broadcast_to(x[None], (size, *x.shape)), axis, 0, 0, t...]
    ppermute x1 -> x11, waiting for transfers between devices: 0.01 us -> 15.3 us  [the longest x3 7.09 us: per_device(): near.append(lax.ppermute(rows, 'B', [(b, b ^ j) for b in range(4)]))]
    all_to_all x2 -> x1, blocking collectives: 28.2 us -> 13.5 us  [per_device(): heads = lax.all_to_all(mixed.reshape(4, 128, DK), 'B', 0, 0, tiled=True)]
    all_to_all x1, starting transfers between devices: 3.52 us -> 15.3 us  [per_device(): rows_z = lax.all_to_all(cut, ('A', 'B'), 0, 0, tiled=True)]
    all_to_all x1, waiting for transfers between devices: 12.5 us -> 16.9 us  [per_device(): rows_z = lax.all_to_all(cut, ('A', 'B'), 0, 0, tiled=True)]
    slice x3 -> x11, local copies, waits for them, and re-layouts: 0.77 us -> 3.84 us  [the longest x3 2.3 us: per_device(): n[36, :1536]]
  transfers between devices with their start and end apart: 7 -> 15, of which waited for: 6 -> 6; matrix products, arithmetic and copies ran while one was open for 9% -> 7% of each run, Pallas kernels for 2% -> 2%
where the time goes in v2:
time: 172 us; the launch traced here: 171 us
  starting transfers between devices  65.1 us (38%)
  waiting for transfers between devices  54.2 us (32%)
  Pallas kernels  17.3 us (10%)
  local copies, waits for them, and re-layouts  15.8 us (9%)
  blocking collectives  13.5 us (8%)
  other arithmetic  3.66 us (2%)
    all_to_all x1, waiting for transfers between devices, per_device(): rows_z = lax.all_to_all(cut, ('A', 'B'), 0, 0, tiled=True)  16.9 us
    all_to_all x1, starting transfers between devices, per_device(): rows_z = lax.all_to_all(cut, ('A', 'B'), 0, 0, tiled=True)  15.3 us
    all_to_all x1, waiting for transfers between devices, per_device(): got = lax.all_to_all(payload, 'A', 0, 0, tiled=True)  14.9 us
    all_to_all x1, blocking collectives, per_device(): heads = lax.all_to_all(mixed.reshape(4, 128, DK), 'B', 0, 0, tiled=True)  13.5 us
    ppermute x3, starting transfers between devices, per_device(): around.append(lax.ppermute(mods, 'tp', [(i, i ^ j) for i in range(4)]))  10.4 us
    ppermute x3, starting transfers between devices, per_device(): near.append(lax.ppermute(rows, 'B', [(b, b ^ j) for b in range(4)]))  10.1 us
    pallas_call x1, Pallas kernels, per_device(): pl.pallas_call(project_kernel, out_shape=(sds((4, PAYLOAD, DK), bf16), sd...  7.13 us
    ppermute x3, waiting for transfers between devices, per_device(): near.append(lax.ppermute(rows, 'B', [(b, b ^ j) for b in range(4)]))  7.09 us
  transfers between devices with their start and end apart: 15, of which 6 were waited for; matrix products, arithmetic and copies ran while one was open for 7% of the time, Pallas kernels for 2%

profile of v2, /device:TPU:6, one launch (start us, length us, event | category | flops | bytes accessed | tf_op | source)
XLA Modules:
  0.0 170.9 jit_solution(11166800833645700118)
XLA Ops:
  0.0 1.0 copy-done
  1.0 0.9 reduce-precision_convert_fusion.5
  1.9 0.7 constant_dynamic-slice_fusion.2
  2.6 0.8 constant_dynamic-slice_fusion
  3.5 0.7 broadcast_in_dim.4
  4.2 15.3 %all-to-all-start = ((bf16[16,16,512]{2,1,0:T(8,128)(2,1)}), bf16[16,16,512]{2,1,0:T(8,128)(2,1)S(1)}, u32[]{:S(2)}, u32[]{:S(2)}) async-start(bf16[16,16,512]{2,1,0:T(8,128)(2,1)} %bitcast.11), calls=%async_computation | async-start | bytes 524288 | tf_op jit(solution)/shard_map/weights_z/all_to_all | solution.py:319
  19.5 0.7 reduce-precision_convert_fusion.3
  20.2 0.8 constant_dynamic-slice_fusion.9
  21.0 16.9 %all-to-all-done = bf16[16,16,512]{2,1,0:T(8,128)(2,1)S(1)} async-done(((bf16[16,16,512]{2,1,0:T(8,128)(2,1)}), bf16[16,16,512]{2,1,0:T(8,128)(2,1)S(1)}, u32[]{:S(2)}, u32[]{:S(2)}) %all-to-all-start) | async-done | bytes 262176 | tf_op jit(solution)/shard_map/weights_z/all_to_all | solution.py:319
  37.9 1.1 broadcast_in_dim.5
  39.0 4.9 %all-to-all-start.1 = ((bf16[4,16,16,512]{3,2,1,0:T(8,128)(2,1)}), bf16[4,16,16,512]{3,2,1,0:T(8,128)(2,1)S(1)}, u32[]{:S(2)}, u32[]{:S(2)}) async-start(bf16[4,16,16,512]{3,2,1,0:T(8,128)(2,1)} %broadcast_in_dim.5), calls=%async_computation.1 | async-start | bytes 2097152 | tf_op jit(solution)/shard_map/weights_x/all_to_all | solution.py:27
  44.0 3.4 %collective-permute-start = (bf16[40,2048]{1,0:T(8,128)(2,1)S(1)}, bf16[40,2048]{1,0:T(8,128)(2,1)S(1)}, u32[]{:S(2)}, u32[]{:S(2)}) collective-permute-start(bf16[40,2048]{1,0:T(8,128)(2,1)S(1)} %pad_maximum_fusion), channel_id=1, source_target_pairs={{0,32},{32,0},{64,96},{96,64},{1,33},{33,1},{65,97},{97,65},{2,34}... | collective-permute-start | bytes 491528 | tf_op jit(solution)/shard_map/rows_z1/ppermute | solution.py:292
  47.3 4.2 %collective-permute-start.1 = (bf16[40,2048]{1,0:T(8,128)(2,1)S(1)}, bf16[40,2048]{1,0:T(8,128)(2,1)S(1)}, u32[]{:S(2)}, u32[]{:S(2)}) collective-permute-start(bf16[40,2048]{1,0:T(8,128)(2,1)S(1)} %pad_maximum_fusion), channel_id=1, source_target_pairs={{0,64},{32,96},{64,0},{96,32},{1,65},{33,97},{65,1},{97,33},{2,66}... | collective-permute-start | bytes 491528 | tf_op jit(solution)/shard_map/rows_z2/ppermute | solution.py:292
  51.5 2.6 %collective-permute-start.2 = (bf16[40,2048]{1,0:T(8,128)(2,1)S(1)}, bf16[40,2048]{1,0:T(8,128)(2,1)S(1)}, u32[]{:S(2)}, u32[]{:S(2)}) collective-permute-start(bf16[40,2048]{1,0:T(8,128)(2,1)S(1)} %pad_maximum_fusion), channel_id=1, source_target_pairs={{0,96},{32,64},{64,32},{96,0},{1,97},{33,65},{65,33},{97,1},{2,98}... | collective-permute-start | bytes 491528 | tf_op jit(solution)/shard_map/rows_z3/ppermute | solution.py:292
  55.4 7.1 %collective-permute-done.1 = bf16[40,2048]{1,0:T(8,128)(2,1)S(1)} collective-permute-done((bf16[40,2048]{1,0:T(8,128)(2,1)S(1)}, bf16[40,2048]{1,0:T(8,128)(2,1)S(1)}, u32[]{:S(2)}, u32[]{:S(2)}) %collective-permute-start.1) | collective-permute-done | bytes 163872 | tf_op jit(solution)/shard_map/rows_z2/ppermute | solution.py:292
  63.3 4.9 %collective-permute-start.4 = (bf16[144,2048]{1,0:T(8,128)(2,1)S(1)}, bf16[144,2048]{1,0:T(8,128)(2,1)S(1)}, u32[]{:S(2)}, u32[]{:S(2)}) collective-permute-start(bf16[144,2048]{1,0:T(8,128)(2,1)S(1)} %concatenate.36.own_ref), channel_id=1, source_target_pairs={{0,24},{8,0},{16,8},{24,16},{1,25},{9,1},{17,9},{25,17},{2,26},{10... | collective-permute-start | bytes 1769480 | tf_op jit(solution)/shard_map/rows_down/ppermute | solution.py:341
  68.3 1.9 %collective-permute-start.10 = (bf16[4,16,16,512]{3,2,1,0:T(8,128)(2,1)S(1)}, bf16[4,16,16,512]{3,2,1,0:T(8,128)(2,1)}, u32[]{:S(2)}, u32[]{:S(2)}) collective-permute-start(bf16[4,16,16,512]{3,2,1,0:T(8,128)(2,1)S(1)} %all-to-all-done.1.mine_ref), channel_id=1, source_target_pairs={{0,1},{1,0},{2,3},{3,2},{4,5},{5,4},{6,7},{7,6},{8,9},{9,8},{10,11... | collective-permute-start | bytes 3145736 | tf_op jit(solution)/shard_map/weights_core/ppermute | solution.py:328
  70.2 0.6 pad_add_fusion.place
  70.9 1.0 copy.26.down_ref
  71.9 1.9 %collective-permute-start.3 = (bf16[144,2048]{1,0:T(8,128)(2,1)S(1)}, bf16[144,2048]{1,0:T(8,128)(2,1)S(1)}, u32[]{:S(2)}, u32[]{:S(2)}) collective-permute-start(bf16[144,2048]{1,0:T(8,128)(2,1)S(1)} %concatenate.36.own_ref), channel_id=1, source_target_pairs={{0,8},{8,16},{16,24},{24,0},{1,9},{9,17},{17,25},{25,1},{2,10},{10... | collective-permute-start | bytes 1769480 | tf_op jit(solution)/shard_map/rows_up/ppermute | solution.py:339
  73.8 0.8 slice_reduce_fusion.2
  74.6 0.8 slice_reduce_fusion.1
  75.4 0.8 slice_reduce_fusion
  76.2 2.5 %collective-permute-start.7 = (bf16[16,8,128]{2,1,0:T(8,128)(2,1)S(1)}, bf16[16,8,128]{2,1,0:T(8,128)(2,1)}, u32[]{:S(2)}, u32[]{:S(2)}) collective-permute-start(bf16[16,8,128]{2,1,0:T(8,128)(2,1)S(1)} %get-tuple-element.22), channel_id=1, source_target_pairs={{0,8},{8,0},{16,24},{24,16},{1,9},{9,1},{17,25},{25,17},{2,10},{10... | collective-permute-start | bytes 98312 | tf_op jit(solution)/shard_map/mods_y1/ppermute | solution.py:324
  78.7 6.0 %collective-permute-start.8 = (bf16[16,8,128]{2,1,0:T(8,128)(2,1)S(1)}, bf16[16,8,128]{2,1,0:T(8,128)(2,1)}, u32[]{:S(2)}, u32[]{:S(2)}) collective-permute-start(bf16[16,8,128]{2,1,0:T(8,128)(2,1)S(1)} %get-tuple-element.22), channel_id=1, source_target_pairs={{0,16},{8,24},{16,0},{24,8},{1,17},{9,25},{17,1},{25,9},{2,18},{10... | collective-permute-start | bytes 98312 | tf_op jit(solution)/shard_map/mods_y2/ppermute | solution.py:324
  84.8 1.9 %collective-permute-start.9 = (bf16[16,8,128]{2,1,0:T(8,128)(2,1)S(1)}, bf16[16,8,128]{2,1,0:T(8,128)(2,1)}, u32[]{:S(2)}, u32[]{:S(2)}) collective-permute-start(bf16[16,8,128]{2,1,0:T(8,128)(2,1)S(1)} %get-tuple-element.22), channel_id=1, source_target_pairs={{0,24},{8,16},{16,8},{24,0},{1,25},{9,17},{17,9},{25,1},{2,26},{10... | collective-permute-start | bytes 98312 | tf_op jit(solution)/shard_map/mods_y3/ppermute | solution.py:324
  86.7 0.8 copy.25
  87.5 0.8 slice.120
  88.3 3.5 %collective-permute-done.3.minus_ref = bf16[144,2048]{1,0:T(8,128)(2,1)S(1)} collective-permute-done((bf16[144,2048]{1,0:T(8,128)(2,1)S(1)}, bf16[144,2048]{1,0:T(8,128)(2,1)S(1)}, u32[]{:S(2)}, u32[]{:S(2)}) %collective-permute-start.3) | collective-permute-done | bytes 589856 | tf_op jit(solution)/shard_map/rows_up/ppermute | solution.py:339
  91.8 1.9 %collective-permute-start.6 = (bf16[80,2048]{1,0:T(8,128)(2,1)}, bf16[80,2048]{1,0:T(8,128)(2,1)}, u32[]{:S(2)}, u32[]{:S(2)}) collective-permute-start(bf16[80,2048]{1,0:T(8,128)(2,1)} %slice.120), channel_id=1, source_target_pairs={{0,24},{8,0},{16,8},{24,16},{1,25},{9,1},{17,9},{25,17},{2,26},{10... | collective-permute-start | bytes 983048 | tf_op jit(solution)/shard_map/rows_down2/ppermute | solution.py:345
  93.7 0.7 slice.119
  94.4 3.9 %collective-permute-start.5 = (bf16[64,2048]{1,0:T(8,128)(2,1)}, bf16[64,2048]{1,0:T(8,128)(2,1)S(1)}, u32[]{:S(2)}, u32[]{:S(2)}) collective-permute-start(bf16[64,2048]{1,0:T(8,128)(2,1)} %slice.119), channel_id=1, source_target_pairs={{0,8},{8,16},{16,24},{24,0},{1,9},{9,17},{17,25},{25,1},{2,10},{10... | collective-permute-start | bytes 786440 | tf_op jit(solution)/shard_map/rows_up2/ppermute | solution.py:343
  98.4 0.8 pad_maximum_fusion.1
  99.3 0.7 reshape.96.mod_ref
  100.1 4.8 %collective-permute-done.5.low_ref = bf16[64,2048]{1,0:T(8,128)(2,1)S(1)} collective-permute-done((bf16[64,2048]{1,0:T(8,128)(2,1)}, bf16[64,2048]{1,0:T(8,128)(2,1)S(1)}, u32[]{:S(2)}, u32[]{:S(2)}) %collective-permute-start.5) | collective-permute-done | bytes 262176 | tf_op jit(solution)/shard_map/rows_up2/ppermute | solution.py:343
  105.5 7.1 %project.1 = (bf16[4,336,128]{2,1,0:T(8,128)(2,1)}, bf16[512,128]{1,0:T(8,128)(2,1)}, bf16[512,128]{1,0:T(8,128)(2,1)}, bf16[512,128]{1,0:T(8,128)(2,1)}, f32[2,512,128]{2,1,0:T(8,128)}) custom-call(s32[4]{0:T(128)} %pad_add_fusion.place, bf16[144,2048]{1,0:T(8,128)(2,1)} %copy-done.2, bf16[144,2048]{1,0:T(8,128)(2,1)} %copy-done.6, ...), custom_call_target="tpu_custom_call" | custom-call | tf_op jit(solution)/shard_map/project/pallas_call | solution.py:354
  112.7 6.3 %all-to-all-start.2 = ((bf16[4,336,128]{2,1,0:T(8,128)(2,1)}), bf16[4,336,128]{2,1,0:T(8,128)(2,1)S(1)}, u32[]{:S(2)}, u32[]{:S(2)}) async-start(bf16[4,336,128]{2,1,0:T(8,128)(2,1)} %get-tuple-element.13), calls=%async_computation.2 | async-start | bytes 688128 | tf_op jit(solution)/shard_map/states/all_to_all | solution.py:372
  118.9 3.0 %local.1 = (f32[512,128]{1,0:T(8,128)}, bf16[512,128]{1,0:T(8,128)(2,1)}, bf16[512,128]{1,0:T(8,128)(2,1)}) custom-call(bf16[512,128]{1,0:T(8,128)(2,1)} %get-tuple-element.14.q_ref, bf16[512,128]{1,0:T(8,128)(2,1)} %get-tuple-element.15.k_ref, bf16[512,128]{1,0:T(8,128)(2,1)} %get-tuple-element.16.v_ref, f32[2,512,128]{2,1,0:T(8,128)} %get-tuple-element.17.cum_ref), custom_call_target="tpu_custom_call" | custom-call | tf_op jit(solution)/shard_map/local/pallas_call | solution.py:373
  122.0 14.9 %all-to-all-done.2.in_ref = bf16[4,336,128]{2,1,0:T(8,128)(2,1)S(1)} async-done(((bf16[4,336,128]{2,1,0:T(8,128)(2,1)}), bf16[4,336,128]{2,1,0:T(8,128)(2,1)S(1)}, u32[]{:S(2)}, u32[]{:S(2)}) %all-to-all-start.2) | async-done | bytes 344096 | tf_op jit(solution)/shard_map/states/all_to_all | solution.py:372
  136.9 0.7 copy-done.5
  137.6 2.3 %combine.1 = bf16[512,128]{1,0:T(8,128)(2,1)} custom-call(s32[4]{0:T(128)} %pad_add_fusion.place, bf16[4,336,128]{2,1,0:T(8,128)(2,1)} %copy-done.5, f32[512,128]{1,0:T(8,128)} %get-tuple-element.18.o_ref, bf16[512,128]{1,0:T(8,128)(2,1)} %get-tuple-element.19.lift_f_ref, bf16[512,128]{1,0:T(8,128)(2,1)} %get-tuple-element.20.lift_b_ref), custom_call_target="tpu_custom_call" | custom-call | tf_op jit(solution)/shard_map/combine/pallas_call | solution.py:380
  139.9 13.5 %all_to_all.25.mix_ref = bf16[4,128,128]{2,1,0:T(8,128)(2,1)} all-to-all(bf16[4,128,128]{2,1,0:T(8,128)(2,1)} %bitcast.56), channel_id=1, replica_groups=mesh['A'=4,'B'=4,'tp'=4,'x'=4,'core'=2] {'B'}, dimensions={0} | all-to-all | bytes 262144 | tf_op jit(solution)/shard_map/mixed_z/all_to_all | solution.py:388
  153.4 3.0 %output.1 = bf16[128,2048]{1,0:T(8,128)(2,1)} custom-call(bf16[4,128,128]{2,1,0:T(8,128)(2,1)} %all_to_all.25.mix_ref, f32[1,256]{1,0:T(1,128)} %bitcast.60, bf16[512,2048]{1,0:T(8,128)(2,1)} %w_ref.1), custom_call_target="tpu_custom_call" | custom-call | tf_op jit(solution)/shard_map/output/pallas_call | solution.py:389
  156.4 3.5 %all-to-all-start.4 = ((bf16[4,32,2048]{2,1,0:T(8,128)(2,1)}), bf16[4,32,2048]{2,1,0:T(8,128)(2,1)S(1)}, u32[]{:S(2)}, u32[]{:S(2)}) async-start(bf16[4,32,2048]{2,1,0:T(8,128)(2,1)} %bitcast.54), calls=%async_computation.4 | async-start | bytes 1048576 | tf_op jit(solution)/shard_map/summed_y/all_to_all | solution.py:397
  159.9 1.3 slice.125.gate_ref
  161.2 7.1 %all-to-all-done.4.parts_ref = bf16[4,32,2048]{2,1,0:T(8,128)(2,1)S(1)} async-done(((bf16[4,32,2048]{2,1,0:T(8,128)(2,1)}), bf16[4,32,2048]{2,1,0:T(8,128)(2,1)S(1)}, u32[]{:S(2)}, u32[]{:S(2)}) %all-to-all-start.4) | async-done | bytes 524320 | tf_op jit(solution)/shard_map/summed_y/all_to_all | solution.py:397
  168.3 0.8 copy-done.3
  169.1 1.9 %final.1 = bf16[32,2048]{1,0:T(8,128)(2,1)} custom-call(bf16[4,32,2048]{2,1,0:T(8,128)(2,1)} %copy-done.3, bf16[32,2048]{1,0:T(8,128)(2,1)} %lat_ref.1, f32[1,2048]{1,0:T(1,128)} %slice.125.gate_ref), custom_call_target="tpu_custom_call" | custom-call | tf_op jit(solution)/shard_map/final/pallas_call | solution.py:398
  (62 shorter events, 3.0 us)
Async XLA Ops:
  0.0 1.0 copy-start
  3.5 40.5 %copy-start.7 = (bf16[32,2048]{1,0:T(8,128)(2,1)S(1)}, bf16[32,2048]{1,0:T(8,128)(2,1)}, u32[]{:S(2)}) copy-start(bf16[32,2048]{1,0:T(8,128)(2,1)} %lat_ref.1) | copy-start | bytes 393220
  4.2 49.9 %copy-start.13 = (bf16[2,32,256]{2,1,0:T(8,128)(2,1)S(1)}, bf16[2,32,256]{2,1,0:T(8,128)(2,1)}, u32[]{:S(2)}) copy-start(bf16[2,32,256]{2,1,0:T(8,128)(2,1)} %param.25) | copy-start | bytes 98308
  4.2 50.0 %copy-start.14 = (f32[2,128,2]{1,2,0:T(2,128)S(1)}, f32[2,128,2]{1,2,0:T(2,128)}, u32[]{:S(2)}) copy-start(f32[2,128,2]{1,2,0:T(2,128)} %param.27) | copy-start | bytes 6148
  4.2 50.0 %copy-start.15 = (f32[2,256]{1,0:T(2,128)S(1)}, f32[2,256]{1,0:T(2,128)}, u32[]{:S(2)}) copy-start(f32[2,256]{1,0:T(2,128)} %param.26) | copy-start | bytes 6148
  4.2 33.7 %all-to-all-start = ((bf16[16,16,512]{2,1,0:T(8,128)(2,1)}), bf16[16,16,512]{2,1,0:T(8,128)(2,1)S(1)}, u32[]{:S(2)}, u32[]{:S(2)}) async-start(bf16[16,16,512]{2,1,0:T(8,128)(2,1)} %bitcast.11), calls=%async_computation | async-start | bytes 524288 | tf_op jit(solution)/shard_map/weights_z/all_to_all | solution.py:319
  39.0 31.8 %copy-start.8 = (bf16[2048,64]{0,1:T(8,128)(2,1)S(1)}, bf16[2048,64]{0,1:T(8,128)(2,1)}, u32[]{:S(2)}) copy-start(bf16[2048,64]{0,1:T(8,128)(2,1)} %param.24) | copy-start | bytes 786436
  39.0 29.2 %all-to-all-start.1 = ((bf16[4,16,16,512]{3,2,1,0:T(8,128)(2,1)}), bf16[4,16,16,512]{3,2,1,0:T(8,128)(2,1)S(1)}, u32[]{:S(2)}, u32[]{:S(2)}) async-start(bf16[4,16,16,512]{3,2,1,0:T(8,128)(2,1)} %broadcast_in_dim.5), calls=%async_computation.1 | async-start | bytes 2097152 | tf_op jit(solution)/shard_map/weights_x/all_to_all | solution.py:27
  44.0 11.4 %collective-permute-start = (bf16[40,2048]{1,0:T(8,128)(2,1)S(1)}, bf16[40,2048]{1,0:T(8,128)(2,1)S(1)}, u32[]{:S(2)}, u32[]{:S(2)}) collective-permute-start(bf16[40,2048]{1,0:T(8,128)(2,1)S(1)} %pad_maximum_fusion), channel_id=1, source_target_pairs={{0,32},{32,0},{64,96},{96,64},{1,33},{33,1},{65,97},{97,65},{2,34}... | collective-permute-start | bytes 491528 | tf_op jit(solution)/shard_map/rows_z1/ppermute | solution.py:292
  47.3 15.1 %collective-permute-start.1 = (bf16[40,2048]{1,0:T(8,128)(2,1)S(1)}, bf16[40,2048]{1,0:T(8,128)(2,1)S(1)}, u32[]{:S(2)}, u32[]{:S(2)}) collective-permute-start(bf16[40,2048]{1,0:T(8,128)(2,1)S(1)} %pad_maximum_fusion), channel_id=1, source_target_pairs={{0,64},{32,96},{64,0},{96,32},{1,65},{33,97},{65,1},{97,33},{2,66}... | collective-permute-start | bytes 491528 | tf_op jit(solution)/shard_map/rows_z2/ppermute | solution.py:292
  51.5 11.0 %collective-permute-start.2 = (bf16[40,2048]{1,0:T(8,128)(2,1)S(1)}, bf16[40,2048]{1,0:T(8,128)(2,1)S(1)}, u32[]{:S(2)}, u32[]{:S(2)}) collective-permute-start(bf16[40,2048]{1,0:T(8,128)(2,1)S(1)} %pad_maximum_fusion), channel_id=1, source_target_pairs={{0,96},{32,64},{64,32},{96,0},{1,97},{33,65},{65,33},{97,1},{2,98}... | collective-permute-start | bytes 491528 | tf_op jit(solution)/shard_map/rows_z3/ppermute | solution.py:292
  55.4 7.2 %copy-start.10 = (bf16[40,2048]{1,0:T(8,128)(2,1)}, bf16[40,2048]{1,0:T(8,128)(2,1)S(1)}, u32[]{:S(2)}) copy-start(bf16[40,2048]{1,0:T(8,128)(2,1)S(1)} %collective-permute-done) | copy-start | bytes 491524
  62.5 0.7 copy-start.11
  62.5 0.7 copy-start.12
  63.3 41.5 %copy-start.2 = (bf16[144,2048]{1,0:T(8,128)(2,1)}, bf16[144,2048]{1,0:T(8,128)(2,1)S(1)}, u32[]{:S(2)}) copy-start(bf16[144,2048]{1,0:T(8,128)(2,1)S(1)} %concatenate.36.own_ref) | copy-start | bytes 1769476
  63.3 21.4 %collective-permute-start.4 = (bf16[144,2048]{1,0:T(8,128)(2,1)S(1)}, bf16[144,2048]{1,0:T(8,128)(2,1)S(1)}, u32[]{:S(2)}, u32[]{:S(2)}) collective-permute-start(bf16[144,2048]{1,0:T(8,128)(2,1)S(1)} %concatenate.36.own_ref), channel_id=1, source_target_pairs={{0,24},{8,0},{16,8},{24,16},{1,25},{9,1},{17,9},{25,17},{2,26},{10... | collective-permute-start | bytes 1769480 | tf_op jit(solution)/shard_map/rows_down/ppermute | solution.py:341
  68.3 36.6 %copy-start.1 = (bf16[4,16,16,512]{3,2,1,0:T(8,128)(2,1)}, bf16[4,16,16,512]{3,2,1,0:T(8,128)(2,1)S(1)}, u32[]{:S(2)}) copy-start(bf16[4,16,16,512]{3,2,1,0:T(8,128)(2,1)S(1)} %all-to-all-done.1.mine_ref) | copy-start | bytes 3145732
  68.3 36.5 %collective-permute-start.10 = (bf16[4,16,16,512]{3,2,1,0:T(8,128)(2,1)S(1)}, bf16[4,16,16,512]{3,2,1,0:T(8,128)(2,1)}, u32[]{:S(2)}, u32[]{:S(2)}) collective-permute-start(bf16[4,16,16,512]{3,2,1,0:T(8,128)(2,1)S(1)} %all-to-all-done.1.mine_ref), channel_id=1, source_target_pairs={{0,1},{1,0},{2,3},{3,2},{4,5},{5,4},{6,7},{7,6},{8,9},{9,8},{10,11... | collective-permute-start | bytes 3145736 | tf_op jit(solution)/shard_map/weights_core/ppermute | solution.py:328
  71.9 19.9 %collective-permute-start.3 = (bf16[144,2048]{1,0:T(8,128)(2,1)S(1)}, bf16[144,2048]{1,0:T(8,128)(2,1)S(1)}, u32[]{:S(2)}, u32[]{:S(2)}) collective-permute-start(bf16[144,2048]{1,0:T(8,128)(2,1)S(1)} %concatenate.36.own_ref), channel_id=1, source_target_pairs={{0,8},{8,16},{16,24},{24,0},{1,9},{9,17},{17,25},{25,1},{2,10},{10... | collective-permute-start | bytes 1769480 | tf_op jit(solution)/shard_map/rows_up/ppermute | solution.py:339
  76.2 18.2 %collective-permute-start.7 = (bf16[16,8,128]{2,1,0:T(8,128)(2,1)S(1)}, bf16[16,8,128]{2,1,0:T(8,128)(2,1)}, u32[]{:S(2)}, u32[]{:S(2)}) collective-permute-start(bf16[16,8,128]{2,1,0:T(8,128)(2,1)S(1)} %get-tuple-element.22), channel_id=1, source_target_pairs={{0,8},{8,0},{16,24},{24,16},{1,9},{9,1},{17,25},{25,17},{2,10},{10... | collective-permute-start | bytes 98312 | tf_op jit(solution)/shard_map/mods_y1/ppermute | solution.py:324
  78.7 19.6 %collective-permute-start.8 = (bf16[16,8,128]{2,1,0:T(8,128)(2,1)S(1)}, bf16[16,8,128]{2,1,0:T(8,128)(2,1)}, u32[]{:S(2)}, u32[]{:S(2)}) collective-permute-start(bf16[16,8,128]{2,1,0:T(8,128)(2,1)S(1)} %get-tuple-element.22), channel_id=1, source_target_pairs={{0,16},{8,24},{16,0},{24,8},{1,17},{9,25},{17,1},{25,9},{2,18},{10... | collective-permute-start | bytes 98312 | tf_op jit(solution)/shard_map/mods_y2/ppermute | solution.py:324
  84.7 20.1 %copy-start.4 = (bf16[144,2048]{1,0:T(8,128)(2,1)}, bf16[144,2048]{1,0:T(8,128)(2,1)S(1)}, u32[]{:S(2)}) copy-start(bf16[144,2048]{1,0:T(8,128)(2,1)S(1)} %collective-permute-done.4.plus_ref) | copy-start | bytes 1769476
  84.8 13.6 %collective-permute-start.9 = (bf16[16,8,128]{2,1,0:T(8,128)(2,1)S(1)}, bf16[16,8,128]{2,1,0:T(8,128)(2,1)}, u32[]{:S(2)}, u32[]{:S(2)}) collective-permute-start(bf16[16,8,128]{2,1,0:T(8,128)(2,1)S(1)} %get-tuple-element.22), channel_id=1, source_target_pairs={{0,24},{8,16},{16,8},{24,0},{1,25},{9,17},{17,9},{25,1},{2,26},{10... | collective-permute-start | bytes 98312 | tf_op jit(solution)/shard_map/mods_y3/ppermute | solution.py:324
  91.8 13.1 %copy-start.6 = (bf16[144,2048]{1,0:T(8,128)(2,1)}, bf16[144,2048]{1,0:T(8,128)(2,1)S(1)}, u32[]{:S(2)}) copy-start(bf16[144,2048]{1,0:T(8,128)(2,1)S(1)} %collective-permute-done.3.minus_ref) | copy-start | bytes 1769476
  91.8 13.1 %collective-permute-start.6 = (bf16[80,2048]{1,0:T(8,128)(2,1)}, bf16[80,2048]{1,0:T(8,128)(2,1)}, u32[]{:S(2)}, u32[]{:S(2)}) collective-permute-start(bf16[80,2048]{1,0:T(8,128)(2,1)} %slice.120), channel_id=1, source_target_pairs={{0,24},{8,0},{16,8},{24,16},{1,25},{9,1},{17,9},{25,17},{2,26},{10... | collective-permute-start | bytes 983048 | tf_op jit(solution)/shard_map/rows_down2/ppermute | solution.py:345
  94.4 10.4 %collective-permute-start.5 = (bf16[64,2048]{1,0:T(8,128)(2,1)}, bf16[64,2048]{1,0:T(8,128)(2,1)S(1)}, u32[]{:S(2)}, u32[]{:S(2)}) collective-permute-start(bf16[64,2048]{1,0:T(8,128)(2,1)} %slice.119), channel_id=1, source_target_pairs={{0,8},{8,16},{16,24},{24,0},{1,9},{9,17},{17,25},{25,1},{2,10},{10... | collective-permute-start | bytes 786440 | tf_op jit(solution)/shard_map/rows_up2/ppermute | solution.py:343
  104.8 0.7 copy-start.9
  112.7 24.2 %all-to-all-start.2 = ((bf16[4,336,128]{2,1,0:T(8,128)(2,1)}), bf16[4,336,128]{2,1,0:T(8,128)(2,1)S(1)}, u32[]{:S(2)}, u32[]{:S(2)}) async-start(bf16[4,336,128]{2,1,0:T(8,128)(2,1)} %get-tuple-element.13), calls=%async_computation.2 | async-start | bytes 688128 | tf_op jit(solution)/shard_map/states/all_to_all | solution.py:372
  136.9 0.7 copy-start.5
  156.4 11.9 %all-to-all-start.4 = ((bf16[4,32,2048]{2,1,0:T(8,128)(2,1)}), bf16[4,32,2048]{2,1,0:T(8,128)(2,1)S(1)}, u32[]{:S(2)}, u32[]{:S(2)}) async-start(bf16[4,32,2048]{2,1,0:T(8,128)(2,1)} %bitcast.54), calls=%async_computation.4 | async-start | bytes 1048576 | tf_op jit(solution)/shard_map/summed_y/all_to_all | solution.py:397
  168.3 0.8 copy-start.3

commit v3 on v2

--- a/solution.py
+++ b/solution.py
@@ -5,9 +5,9 @@
 from jax.experimental.pallas import tpu as pltpu
 from jax.sharding import Mesh, PartitionSpec as P
 
+
 D = 2048
 DK = 128
-RANK = 32
 BLOCK = 64
 CTX_LIFT = 4.0
 EPS = 1e-06
@@ -104,7 +104,7 @@
     low = out[:, 384:448]
     raw = jnp.dot(low, up_ref[...], preferred_element_type=f32) + bias_ref[...]
     logs = (jnp.minimum(raw, 0.0) - jnp.log1p(jnp.exp(-jnp.abs(raw)))) * (1.0 / SHARP)
-    extra = jnp.concatenate([extra_ref[sub ^ zb] for zb in range(4)], axis=0)
+    extra = jnp.concatenate([extra_ref[zb] for zb in range(4)], axis=0)
     ef = extra[:, 0:1]
     eb = extra[:, 1:2]
     af = logs[:SEG, 0:128] + ef
@@ -256,7 +256,7 @@
     out_ref[...] = (lat_ref[...].astype(f32) + gate_ref[...] * projected).astype(bf16)
 
 
-def per_device(
+def device_body(
     latents,
     sample_vector,
     context,
@@ -282,24 +282,19 @@
     place = jnp.stack([seg, core, sub, y]).astype(jnp.int32)
 
     ctx_rows = lax.dynamic_slice_in_dim(context, y * 4, 4, 0)
-    extra = jnp.moveaxis(decay_extra, 1, 2).reshape(4, 128)
-    extra_row = jnp.concatenate([p.reshape(1, 512) for p in three_pieces(extra)], axis=1)
-    extra_row = jnp.pad(extra_row, ((0, 3), (0, 512)))
-    rows = jnp.concatenate([latents, ctx_rows, extra_row], 0)
+    rows = jnp.concatenate([latents, ctx_rows], 0)
     near = [rows]
     for j in range(1, 4):
-        with jax.named_scope(f"rows_z{j}"):
-            near.append(lax.ppermute(rows, "B", [(b, b ^ j) for b in range(4)]))
-    extras = jnp.stack([n[36, :1536] for n in near]).astype(f32).reshape(4, 3, 2, 2, 128).sum(1)
-    extras = lax.dynamic_index_in_dim(extras, head, 2, keepdims=False)
-    extras = jnp.transpose(extras, (0, 2, 1))
+        near.append(lax.ppermute(rows, "B", [(b, b ^ j) for b in range(4)]))
 
     wq = lax.dynamic_slice_in_dim(query_weight, dp * 16, 16, 0)
     wk = lax.dynamic_slice_in_dim(key_weight, dp * 16, 16, 0)
     wv = lax.dynamic_slice_in_dim(value_weight, dp * 16, 16, 0)
     conditions = jax.nn.silu(jnp.concatenate([sample_vector, context_vector], 0)).astype(bf16)
     local_mods = jnp.dot(conditions, modulator, preferred_element_type=f32)
-    riding = jnp.pad(jnp.concatenate(three_pieces(local_mods), axis=0), ((0, 10), (0, 32)))
+    extra = jnp.moveaxis(decay_extra, 1, 2).reshape(4, 128)
+    riding = jnp.pad(jnp.concatenate(three_pieces(local_mods), axis=0), ((0, 0), (0, 32)))
+    riding = jnp.concatenate([riding, *three_pieces(extra)[:2], jnp.zeros((2, 128), bf16)], axis=0)
     cut = jnp.stack(
         [
             jnp.concatenate(
@@ -315,17 +310,17 @@
         ]
     )
     cut = jnp.broadcast_to(cut[None], (4, 4, 16, 512)).reshape(16, 16, 512)
-    with jax.named_scope("weights_z"):
-        rows_z = lax.all_to_all(cut, ("A", "B"), 0, 0, tiled=True)
+    rows_z = lax.all_to_all(cut, ("A", "B"), 0, 0, tiled=True)
     mods = rows_z[:, 0:8, 384:512]
+    extras = lax.dynamic_slice_in_dim(rows_z, seg * 4, 4, 0)[:, 6:14, 384:512].astype(f32)
+    extras = (extras[:, 0:4] + extras[:, 4:8]).reshape(4, 2, 2, 128)
+    extras = lax.dynamic_index_in_dim(extras, head, 2, keepdims=False)
+    extras = jnp.transpose(extras, (0, 2, 1))
     around = [mods]
     for j in range(1, 4):
-        with jax.named_scope(f"mods_y{j}"):
-            around.append(lax.ppermute(mods, "tp", [(i, i ^ j) for i in range(4)]))
-    with jax.named_scope("weights_x"):
-        mine = to_everyone(rows_z, "x")
-    with jax.named_scope("weights_core"):
-        other = lax.ppermute(mine, "core", [(0, 1), (1, 0)])
+        around.append(lax.ppermute(mods, "tp", [(i, i ^ j) for i in range(4)]))
+    mine = to_everyone(rows_z, "x")
+    other = lax.ppermute(mine, "core", [(0, 1), (1, 0)])
     around = jnp.stack(around)
     around = jnp.stack([lax.dynamic_index_in_dim(around, y ^ t, 0, keepdims=False) for t in range(4)])
     parts = around[:, :, 0:6, 0:96].astype(f32)
@@ -335,14 +330,10 @@
     own = jnp.concatenate([n[:32] for n in near] + [n[32:36] for n in near], axis=0)
     up_shift = [(i, (i + 1) % 4) for i in range(4)]
     down_shift = [(i, (i + 3) % 4) for i in range(4)]
-    with jax.named_scope("rows_up"):
-        minus = lax.ppermute(own, "tp", up_shift)
-    with jax.named_scope("rows_down"):
-        plus = lax.ppermute(own, "tp", down_shift)
-    with jax.named_scope("rows_up2"):
-        low = lax.ppermute(minus[:64], "tp", up_shift)
-    with jax.named_scope("rows_down2"):
-        high = lax.ppermute(plus[64:], "tp", down_shift)
+    minus = lax.ppermute(own, "tp", up_shift)
+    plus = lax.ppermute(own, "tp", down_shift)
+    low = lax.ppermute(minus[:64], "tp", up_shift)
+    high = lax.ppermute(plus[64:], "tp", down_shift)
 
     up = lax.dynamic_slice_in_dim(decay_up, head * 128, 128, 2)
     up_both = jnp.concatenate(
@@ -368,8 +359,7 @@
         place, own, minus, plus, low, high, modulation, norm_gain.reshape(1, D), mine, other,
         decay_down, up_both, bias, extras,
     )
-    with jax.named_scope("states"):
-        got = lax.all_to_all(payload, "A", 0, 0, tiled=True)
+    got = lax.all_to_all(payload, "A", 0, 0, tiled=True)
     local, lift_f, lift_b = pl.pallas_call(
         local_kernel,
         out_shape=(sds((SEG, DK), f32), sds((SEG, DK), bf16), sds((SEG, DK), bf16)),
@@ -384,8 +374,7 @@
         out_specs=VM,
         name="combine",
     )(place, got, local, lift_f, lift_b)
-    with jax.named_scope("mixed_z"):
-        heads = lax.all_to_all(mixed.reshape(4, 128, DK), "B", 0, 0, tiled=True)
+    heads = lax.all_to_all(mixed.reshape(4, 128, DK), "B", 0, 0, tiled=True)
     partial = pl.pallas_call(
         output_kernel,
         out_shape=sds((128, D), bf16),
@@ -393,8 +382,7 @@
         out_specs=VM,
         name="output",
     )(heads, head_gain.reshape(1, 256), out_weight)
-    with jax.named_scope("summed_y"):
-        shares = lax.all_to_all(partial.reshape(4, 32, D), "tp", 0, 0, tiled=True)
+    shares = lax.all_to_all(partial.reshape(4, 32, D), "tp", 0, 0, tiled=True)
     return pl.pallas_call(
         final_kernel,
         out_shape=sds((32, D), bf16),
@@ -426,7 +414,7 @@
         P("tp", None),
     )
     return jax.shard_map(
-        per_device,
+        device_body,
         mesh=mesh,
         in_specs=placed,
         out_specs=P((*dp, *sp, "tp"), None),

time: 172 us -> 171 us (level)
  local copies, waits for them, and re-layouts: 15.8 us -> 13 us
  blocking collectives: 13.5 us -> 15.5 us
  waiting for transfers between devices: 54.2 us -> 52.3 us
  starting transfers between devices: 65.1 us -> 66.9 us
    all_to_all x1, blocking collectives: 13.5 us -> 15.5 us  [device_body(): heads = lax.all_to_all(mixed.reshape(4, 128, DK), 'B', 0, 0, tiled=True)]
    all_to_all x3, waiting for transfers between devices: 38.9 us -> 37 us  [the longest x1 17.6 us: device_body(): rows_z = lax.all_to_all(cut, ('A', 'B'), 0, 0, tiled=True)]
    slice x13 -> x11, local copies, waits for them, and re-layouts: 5.95 us -> 4.44 us  [the longest x1 1.31 us: device_body(): modulation[0:1, 2 * D:]]
    unnamed x33 -> x22, local copies, waits for them, and re-layouts: 4.88 us -> 4.37 us
  transfers between devices with their start and end apart: 15 -> 15, of which waited for: 6 -> 6; matrix products, arithmetic and copies ran while one was open for 7% -> 6% of each run, Pallas kernels for 2% -> 2%
where the time goes in v3:
time: 171 us; the launch traced here: 169 us
  starting transfers between devices  66.9 us (39%)
  waiting for transfers between devices  52.3 us (31%)
  Pallas kernels  17.3 us (10%)
  blocking collectives  15.5 us (9%)
  local copies, waits for them, and re-layouts  13 us (8%)
  other arithmetic  3.07 us (2%)
    all_to_all x1, waiting for transfers between devices, device_body(): rows_z = lax.all_to_all(cut, ('A', 'B'), 0, 0, tiled=True)  17.6 us
    all_to_all x1, blocking collectives, device_body(): heads = lax.all_to_all(mixed.reshape(4, 128, DK), 'B', 0, 0, tiled=True)  15.5 us
    all_to_all x1, starting transfers between devices, device_body(): rows_z = lax.all_to_all(cut, ('A', 'B'), 0, 0, tiled=True)  15.2 us
    all_to_all x1, waiting for transfers between devices, device_body(): got = lax.all_to_all(payload, 'A', 0, 0, tiled=True)  12.7 us
    ppermute x3, starting transfers between devices, device_body(): around.append(lax.ppermute(mods, 'tp', [(i, i ^ j) for i in range(4)]))  10.4 us
    ppermute x3, starting transfers between devices, device_body(): near.append(lax.ppermute(rows, 'B', [(b, b ^ j) for b in range(4)]))  10.1 us
    ppermute x3, waiting for transfers between devices, device_body(): near.append(lax.ppermute(rows, 'B', [(b, b ^ j) for b in range(4)]))  8.33 us
    pallas_call x1, Pallas kernels, device_body(): pl.pallas_call(project_kernel, out_shape=(sds((4, PAYLOAD, DK), bf16), sd...  7.12 us
  transfers between devices with their start and end apart: 15, of which 6 were waited for; matrix products, arithmetic and copies ran while one was open for 6% of the time, Pallas kernels for 2%

profile of v3, /device:TPU:6, one launch (start us, length us, event | category | flops | bytes accessed | tf_op | source)
XLA Modules:
  0.0 169.3 jit_solution(13964948917122204525)
XLA Ops:
  0.0 0.7 reduce-precision_convert_fusion
  0.7 0.7 constant_dynamic-slice_fusion.2
  1.4 0.9 reduce-precision_convert_fusion.2
  2.4 0.8 constant_dynamic-slice_fusion
  3.3 0.7 broadcast_in_dim.7
  4.0 15.2 %all-to-all-start = ((bf16[16,16,512]{2,1,0:T(8,128)(2,1)}), bf16[16,16,512]{2,1,0:T(8,128)(2,1)S(1)}, u32[]{:S(2)}, u32[]{:S(2)}) async-start(bf16[16,16,512]{2,1,0:T(8,128)(2,1)} %bitcast.11), calls=%async_computation | async-start | bytes 524288 | tf_op jit(solution)/shard_map/all_to_all | solution.py:313
  19.2 0.8 constant_dynamic-slice_fusion.9
  20.0 17.6 %all-to-all-done = bf16[16,16,512]{2,1,0:T(8,128)(2,1)S(1)} async-done(((bf16[16,16,512]{2,1,0:T(8,128)(2,1)}), bf16[16,16,512]{2,1,0:T(8,128)(2,1)S(1)}, u32[]{:S(2)}, u32[]{:S(2)}) %all-to-all-start) | async-done | bytes 262176 | tf_op jit(solution)/shard_map/all_to_all | solution.py:313
  37.6 1.1 broadcast_in_dim.8
  38.7 4.9 %all-to-all-start.1 = ((bf16[4,16,16,512]{3,2,1,0:T(8,128)(2,1)}), bf16[4,16,16,512]{3,2,1,0:T(8,128)(2,1)S(1)}, u32[]{:S(2)}, u32[]{:S(2)}) async-start(bf16[4,16,16,512]{3,2,1,0:T(8,128)(2,1)} %broadcast_in_dim.8), calls=%async_computation.1 | async-start | bytes 2097152 | tf_op jit(solution)/shard_map/all_to_all | solution.py:27
  43.6 3.4 %collective-permute-start = (bf16[36,2048]{1,0:T(8,128)(2,1)S(1)}, bf16[36,2048]{1,0:T(8,128)(2,1)S(1)}, u32[]{:S(2)}, u32[]{:S(2)}) collective-permute-start(bf16[36,2048]{1,0:T(8,128)(2,1)S(1)} %pad_maximum_fusion), channel_id=1, source_target_pairs={{0,32},{32,0},{64,96},{96,64},{1,33},{33,1},{65,97},{97,65},{2,34}... | collective-permute-start | bytes 442376 | tf_op jit(solution)/shard_map/ppermute | solution.py:288
  47.0 4.2 %collective-permute-start.1 = (bf16[36,2048]{1,0:T(8,128)(2,1)S(1)}, bf16[36,2048]{1,0:T(8,128)(2,1)S(1)}, u32[]{:S(2)}, u32[]{:S(2)}) collective-permute-start(bf16[36,2048]{1,0:T(8,128)(2,1)S(1)} %pad_maximum_fusion), channel_id=1, source_target_pairs={{0,64},{32,96},{64,0},{96,32},{1,65},{33,97},{65,1},{97,33},{2,66}... | collective-permute-start | bytes 442376 | tf_op jit(solution)/shard_map/ppermute | solution.py:288
  51.2 2.6 %collective-permute-start.2 = (bf16[36,2048]{1,0:T(8,128)(2,1)S(1)}, bf16[36,2048]{1,0:T(8,128)(2,1)S(1)}, u32[]{:S(2)}, u32[]{:S(2)}) collective-permute-start(bf16[36,2048]{1,0:T(8,128)(2,1)S(1)} %pad_maximum_fusion), channel_id=1, source_target_pairs={{0,96},{32,64},{64,32},{96,0},{1,97},{33,65},{65,33},{97,1},{2,98}... | collective-permute-start | bytes 442376 | tf_op jit(solution)/shard_map/ppermute | solution.py:288
  53.8 8.3 %collective-permute-done.1 = bf16[36,2048]{1,0:T(8,128)(2,1)S(1)} collective-permute-done((bf16[36,2048]{1,0:T(8,128)(2,1)S(1)}, bf16[36,2048]{1,0:T(8,128)(2,1)S(1)}, u32[]{:S(2)}, u32[]{:S(2)}) %collective-permute-start.1) | collective-permute-done | bytes 147488 | tf_op jit(solution)/shard_map/ppermute | solution.py:288
  62.2 0.1 concatenate.31.own_ref
  62.3 4.9 %collective-permute-start.4 = (bf16[144,2048]{1,0:T(8,128)(2,1)S(1)}, bf16[144,2048]{1,0:T(8,128)(2,1)S(1)}, u32[]{:S(2)}, u32[]{:S(2)}) collective-permute-start(bf16[144,2048]{1,0:T(8,128)(2,1)S(1)} %concatenate.31.own_ref), channel_id=1, source_target_pairs={{0,24},{8,0},{16,8},{24,16},{1,25},{9,1},{17,9},{25,17},{2,26},{10... | collective-permute-start | bytes 1769480 | tf_op jit(solution)/shard_map/ppermute | solution.py:334
  67.2 1.9 %collective-permute-start.3 = (bf16[144,2048]{1,0:T(8,128)(2,1)S(1)}, bf16[144,2048]{1,0:T(8,128)(2,1)S(1)}, u32[]{:S(2)}, u32[]{:S(2)}) collective-permute-start(bf16[144,2048]{1,0:T(8,128)(2,1)S(1)} %concatenate.31.own_ref), channel_id=1, source_target_pairs={{0,8},{8,16},{16,24},{24,0},{1,9},{9,17},{17,25},{25,1},{2,10},{10... | collective-permute-start | bytes 1769480 | tf_op jit(solution)/shard_map/ppermute | solution.py:333
  69.2 0.6 constant_dynamic-slice_fusion.4
  69.8 0.6 fusion.4.up_ref
  70.4 1.9 %collective-permute-start.10 = (bf16[4,16,16,512]{3,2,1,0:T(8,128)(2,1)S(1)}, bf16[4,16,16,512]{3,2,1,0:T(8,128)(2,1)}, u32[]{:S(2)}, u32[]{:S(2)}) collective-permute-start(bf16[4,16,16,512]{3,2,1,0:T(8,128)(2,1)S(1)} %all-to-all-done.1.mine_ref), channel_id=1, source_target_pairs={{0,1},{1,0},{2,3},{3,2},{4,5},{5,4},{6,7},{7,6},{8,9},{9,8},{10,11... | collective-permute-start | bytes 3145736 | tf_op jit(solution)/shard_map/ppermute | solution.py:323
  72.3 0.7 pad_add_fusion.place
  73.0 1.9 %copy.25.down_ref = bf16[2048,64]{1,0:T(8,128)(2,1)} copy(bf16[2048,64]{0,1:T(8,128)(2,1)} %param.24) | data formatting | bytes 524288 | tf_op args[9]
  74.9 0.8 collective-permute-done.4.plus_ref
  75.7 0.8 slice.119
  76.6 5.6 %collective-permute-start.6 = (bf16[80,2048]{1,0:T(8,128)(2,1)}, bf16[80,2048]{1,0:T(8,128)(2,1)}, u32[]{:S(2)}, u32[]{:S(2)}) collective-permute-start(bf16[80,2048]{1,0:T(8,128)(2,1)} %slice.119), channel_id=1, source_target_pairs={{0,24},{8,0},{16,8},{24,16},{1,25},{9,1},{17,9},{25,17},{2,26},{10... | collective-permute-start | bytes 983048 | tf_op jit(solution)/shard_map/ppermute | solution.py:336
  82.2 0.8 slice.118
  83.0 1.9 %collective-permute-start.7 = (bf16[16,8,128]{2,1,0:T(8,128)(2,1)S(1)}, bf16[16,8,128]{2,1,0:T(8,128)(2,1)}, u32[]{:S(2)}, u32[]{:S(2)}) collective-permute-start(bf16[16,8,128]{2,1,0:T(8,128)(2,1)S(1)} %get-tuple-element.22), channel_id=1, source_target_pairs={{0,8},{8,0},{16,24},{24,16},{1,9},{9,1},{17,25},{25,17},{2,10},{10... | collective-permute-start | bytes 98312 | tf_op jit(solution)/shard_map/ppermute | solution.py:321
  84.9 3.4 %collective-permute-start.8 = (bf16[16,8,128]{2,1,0:T(8,128)(2,1)S(1)}, bf16[16,8,128]{2,1,0:T(8,128)(2,1)}, u32[]{:S(2)}, u32[]{:S(2)}) collective-permute-start(bf16[16,8,128]{2,1,0:T(8,128)(2,1)S(1)} %get-tuple-element.22), channel_id=1, source_target_pairs={{0,16},{8,24},{16,0},{24,8},{1,17},{9,25},{17,1},{25,9},{2,18},{10... | collective-permute-start | bytes 98312 | tf_op jit(solution)/shard_map/ppermute | solution.py:321
  88.3 5.1 %collective-permute-start.9 = (bf16[16,8,128]{2,1,0:T(8,128)(2,1)S(1)}, bf16[16,8,128]{2,1,0:T(8,128)(2,1)}, u32[]{:S(2)}, u32[]{:S(2)}) collective-permute-start(bf16[16,8,128]{2,1,0:T(8,128)(2,1)S(1)} %get-tuple-element.22), channel_id=1, source_target_pairs={{0,24},{8,16},{16,8},{24,0},{1,25},{9,17},{17,9},{25,1},{2,26},{10... | collective-permute-start | bytes 98312 | tf_op jit(solution)/shard_map/ppermute | solution.py:321
  93.4 0.1 dynamic-slice_convert_fusion
  93.5 0.9 copy.26
  94.4 1.9 %collective-permute-start.5 = (bf16[64,2048]{1,0:T(8,128)(2,1)}, bf16[64,2048]{1,0:T(8,128)(2,1)}, u32[]{:S(2)}, u32[]{:S(2)}) collective-permute-start(bf16[64,2048]{1,0:T(8,128)(2,1)} %slice.118), channel_id=1, source_target_pairs={{0,8},{8,16},{16,24},{24,0},{1,9},{9,17},{17,25},{25,1},{2,10},{10... | collective-permute-start | bytes 786440 | tf_op jit(solution)/shard_map/ppermute | solution.py:335
  96.3 0.8 pad_maximum_fusion.1
  97.3 0.7 reshape.31.mod_ref
  98.0 6.1 %collective-permute-done.5.low_ref = bf16[64,2048]{1,0:T(8,128)(2,1)} collective-permute-done((bf16[64,2048]{1,0:T(8,128)(2,1)}, bf16[64,2048]{1,0:T(8,128)(2,1)}, u32[]{:S(2)}, u32[]{:S(2)}) %collective-permute-start.5) | collective-permute-done | bytes 262176 | tf_op jit(solution)/shard_map/ppermute | solution.py:335
  104.2 7.1 %project.1 = (bf16[4,336,128]{2,1,0:T(8,128)(2,1)}, bf16[512,128]{1,0:T(8,128)(2,1)}, bf16[512,128]{1,0:T(8,128)(2,1)}, bf16[512,128]{1,0:T(8,128)(2,1)}, f32[2,512,128]{2,1,0:T(8,128)}) custom-call(s32[4]{0:T(128)} %pad_add_fusion.place, bf16[144,2048]{1,0:T(8,128)(2,1)} %copy-done.2, bf16[144,2048]{1,0:T(8,128)(2,1)} %copy-done.6, ...), custom_call_target="tpu_custom_call" | custom-call | tf_op jit(solution)/shard_map/project/pallas_call | solution.py:345
  111.3 6.5 %all-to-all-start.2 = ((bf16[4,336,128]{2,1,0:T(8,128)(2,1)}), bf16[4,336,128]{2,1,0:T(8,128)(2,1)S(1)}, u32[]{:S(2)}, u32[]{:S(2)}) async-start(bf16[4,336,128]{2,1,0:T(8,128)(2,1)} %get-tuple-element.13), calls=%async_computation.2 | async-start | bytes 688128 | tf_op jit(solution)/shard_map/all_to_all | solution.py:362
  117.9 3.1 %local.1 = (f32[512,128]{1,0:T(8,128)}, bf16[512,128]{1,0:T(8,128)(2,1)}, bf16[512,128]{1,0:T(8,128)(2,1)}) custom-call(bf16[512,128]{1,0:T(8,128)(2,1)} %get-tuple-element.14.q_ref, bf16[512,128]{1,0:T(8,128)(2,1)} %get-tuple-element.15.k_ref, bf16[512,128]{1,0:T(8,128)(2,1)} %get-tuple-element.16.v_ref, f32[2,512,128]{2,1,0:T(8,128)} %get-tuple-element.17.cum_ref), custom_call_target="tpu_custom_call" | custom-call | tf_op jit(solution)/shard_map/local/pallas_call | solution.py:363
  120.9 12.7 %all-to-all-done.2.in_ref = bf16[4,336,128]{2,1,0:T(8,128)(2,1)S(1)} async-done(((bf16[4,336,128]{2,1,0:T(8,128)(2,1)}), bf16[4,336,128]{2,1,0:T(8,128)(2,1)S(1)}, u32[]{:S(2)}, u32[]{:S(2)}) %all-to-all-start.2) | async-done | bytes 344096 | tf_op jit(solution)/shard_map/all_to_all | solution.py:362
  133.6 0.7 copy-done.5
  134.3 2.3 %combine.1 = bf16[512,128]{1,0:T(8,128)(2,1)} custom-call(s32[4]{0:T(128)} %pad_add_fusion.place, bf16[4,336,128]{2,1,0:T(8,128)(2,1)} %copy-done.5, f32[512,128]{1,0:T(8,128)} %get-tuple-element.18.o_ref, bf16[512,128]{1,0:T(8,128)(2,1)} %get-tuple-element.19.lift_f_ref, bf16[512,128]{1,0:T(8,128)(2,1)} %get-tuple-element.20.lift_b_ref), custom_call_target="tpu_custom_call" | custom-call | tf_op jit(solution)/shard_map/combine/pallas_call | solution.py:370
  136.6 15.5 %all_to_all.25.mix_ref = bf16[4,128,128]{2,1,0:T(8,128)(2,1)} all-to-all(bf16[4,128,128]{2,1,0:T(8,128)(2,1)} %bitcast.39), channel_id=1, replica_groups=mesh['A'=4,'B'=4,'tp'=4,'x'=4,'core'=2] {'B'}, dimensions={0} | all-to-all | bytes 262144 | tf_op jit(solution)/shard_map/all_to_all | solution.py:377
  152.1 3.0 %output.1 = bf16[128,2048]{1,0:T(8,128)(2,1)} custom-call(bf16[4,128,128]{2,1,0:T(8,128)(2,1)} %all_to_all.25.mix_ref, f32[1,256]{1,0:T(1,128)} %bitcast.44, bf16[512,2048]{1,0:T(8,128)(2,1)} %w_ref.1), custom_call_target="tpu_custom_call" | custom-call | tf_op jit(solution)/shard_map/output/pallas_call | solution.py:378
  155.1 3.5 %all-to-all-start.4 = ((bf16[4,32,2048]{2,1,0:T(8,128)(2,1)}), bf16[4,32,2048]{2,1,0:T(8,128)(2,1)S(1)}, u32[]{:S(2)}, u32[]{:S(2)}) async-start(bf16[4,32,2048]{2,1,0:T(8,128)(2,1)} %bitcast.37), calls=%async_computation.4 | async-start | bytes 1048576 | tf_op jit(solution)/shard_map/all_to_all | solution.py:385
  158.6 1.3 slice.123.gate_ref
  159.9 6.8 %all-to-all-done.4.parts_ref = bf16[4,32,2048]{2,1,0:T(8,128)(2,1)S(1)} async-done(((bf16[4,32,2048]{2,1,0:T(8,128)(2,1)}), bf16[4,32,2048]{2,1,0:T(8,128)(2,1)S(1)}, u32[]{:S(2)}, u32[]{:S(2)}) %all-to-all-start.4) | async-done | bytes 524320 | tf_op jit(solution)/shard_map/all_to_all | solution.py:385
  166.7 0.8 copy-done.3
  167.5 1.9 %final.1 = bf16[32,2048]{1,0:T(8,128)(2,1)} custom-call(bf16[4,32,2048]{2,1,0:T(8,128)(2,1)} %copy-done.3, bf16[32,2048]{1,0:T(8,128)(2,1)} %lat_ref.1, f32[1,2048]{1,0:T(1,128)} %slice.123.gate_ref), custom_call_target="tpu_custom_call" | custom-call | tf_op jit(solution)/shard_map/final/pallas_call | solution.py:386
  (46 shorter events, 0.4 us)
Async XLA Ops:
  0.0 1.4 copy-start
  3.2 40.3 %copy-start.7 = (bf16[32,2048]{1,0:T(8,128)(2,1)S(1)}, bf16[32,2048]{1,0:T(8,128)(2,1)}, u32[]{:S(2)}) copy-start(bf16[32,2048]{1,0:T(8,128)(2,1)} %lat_ref.1) | copy-start | bytes 393220
  4.0 33.6 %all-to-all-start = ((bf16[16,16,512]{2,1,0:T(8,128)(2,1)}), bf16[16,16,512]{2,1,0:T(8,128)(2,1)S(1)}, u32[]{:S(2)}, u32[]{:S(2)}) async-start(bf16[16,16,512]{2,1,0:T(8,128)(2,1)} %bitcast.11), calls=%async_computation | async-start | bytes 524288 | tf_op jit(solution)/shard_map/all_to_all | solution.py:313
  38.7 30.5 %copy-start.9 = (f32[2,256]{1,0:T(2,128)S(1)}, f32[2,256]{1,0:T(2,128)}, u32[]{:S(2)}) copy-start(f32[2,256]{1,0:T(2,128)} %param.26) | copy-start | bytes 6148
  38.7 31.1 %copy-start.8 = (bf16[2,32,256]{2,1,0:T(8,128)(2,1)S(1)}, bf16[2,32,256]{2,1,0:T(8,128)(2,1)}, u32[]{:S(2)}) copy-start(bf16[2,32,256]{2,1,0:T(8,128)(2,1)} %param.25) | copy-start | bytes 98308
  38.7 31.7 %all-to-all-start.1 = ((bf16[4,16,16,512]{3,2,1,0:T(8,128)(2,1)}), bf16[4,16,16,512]{3,2,1,0:T(8,128)(2,1)S(1)}, u32[]{:S(2)}, u32[]{:S(2)}) async-start(bf16[4,16,16,512]{3,2,1,0:T(8,128)(2,1)} %broadcast_in_dim.8), calls=%async_computation.1 | async-start | bytes 2097152 | tf_op jit(solution)/shard_map/all_to_all | solution.py:27
  43.6 10.1 %collective-permute-start = (bf16[36,2048]{1,0:T(8,128)(2,1)S(1)}, bf16[36,2048]{1,0:T(8,128)(2,1)S(1)}, u32[]{:S(2)}, u32[]{:S(2)}) collective-permute-start(bf16[36,2048]{1,0:T(8,128)(2,1)S(1)} %pad_maximum_fusion), channel_id=1, source_target_pairs={{0,32},{32,0},{64,96},{96,64},{1,33},{33,1},{65,97},{97,65},{2,34}... | collective-permute-start | bytes 442376 | tf_op jit(solution)/shard_map/ppermute | solution.py:288
  47.0 15.1 %collective-permute-start.1 = (bf16[36,2048]{1,0:T(8,128)(2,1)S(1)}, bf16[36,2048]{1,0:T(8,128)(2,1)S(1)}, u32[]{:S(2)}, u32[]{:S(2)}) collective-permute-start(bf16[36,2048]{1,0:T(8,128)(2,1)S(1)} %pad_maximum_fusion), channel_id=1, source_target_pairs={{0,64},{32,96},{64,0},{96,32},{1,65},{33,97},{65,1},{97,33},{2,66}... | collective-permute-start | bytes 442376 | tf_op jit(solution)/shard_map/ppermute | solution.py:288
  51.2 11.0 %collective-permute-start.2 = (bf16[36,2048]{1,0:T(8,128)(2,1)S(1)}, bf16[36,2048]{1,0:T(8,128)(2,1)S(1)}, u32[]{:S(2)}, u32[]{:S(2)}) collective-permute-start(bf16[36,2048]{1,0:T(8,128)(2,1)S(1)} %pad_maximum_fusion), channel_id=1, source_target_pairs={{0,96},{32,64},{64,32},{96,0},{1,97},{33,65},{65,33},{97,1},{2,98}... | collective-permute-start | bytes 442376 | tf_op jit(solution)/shard_map/ppermute | solution.py:288
  62.3 41.9 %copy-start.2 = (bf16[144,2048]{1,0:T(8,128)(2,1)}, bf16[144,2048]{1,0:T(8,128)(2,1)S(1)}, u32[]{:S(2)}) copy-start(bf16[144,2048]{1,0:T(8,128)(2,1)S(1)} %concatenate.31.own_ref) | copy-start | bytes 1769476
  62.3 13.4 %collective-permute-start.4 = (bf16[144,2048]{1,0:T(8,128)(2,1)S(1)}, bf16[144,2048]{1,0:T(8,128)(2,1)S(1)}, u32[]{:S(2)}, u32[]{:S(2)}) collective-permute-start(bf16[144,2048]{1,0:T(8,128)(2,1)S(1)} %concatenate.31.own_ref), channel_id=1, source_target_pairs={{0,24},{8,0},{16,8},{24,16},{1,25},{9,1},{17,9},{25,17},{2,26},{10... | collective-permute-start | bytes 1769480 | tf_op jit(solution)/shard_map/ppermute | solution.py:334
  67.2 14.9 %collective-permute-start.3 = (bf16[144,2048]{1,0:T(8,128)(2,1)S(1)}, bf16[144,2048]{1,0:T(8,128)(2,1)S(1)}, u32[]{:S(2)}, u32[]{:S(2)}) collective-permute-start(bf16[144,2048]{1,0:T(8,128)(2,1)S(1)} %concatenate.31.own_ref), channel_id=1, source_target_pairs={{0,8},{8,16},{16,24},{24,0},{1,9},{9,17},{17,25},{25,1},{2,10},{10... | collective-permute-start | bytes 1769480 | tf_op jit(solution)/shard_map/ppermute | solution.py:333
  70.4 33.8 %copy-start.1 = (bf16[4,16,16,512]{3,2,1,0:T(8,128)(2,1)}, bf16[4,16,16,512]{3,2,1,0:T(8,128)(2,1)S(1)}, u32[]{:S(2)}) copy-start(bf16[4,16,16,512]{3,2,1,0:T(8,128)(2,1)S(1)} %all-to-all-done.1.mine_ref) | copy-start | bytes 3145732
  70.4 33.8 %collective-permute-start.10 = (bf16[4,16,16,512]{3,2,1,0:T(8,128)(2,1)S(1)}, bf16[4,16,16,512]{3,2,1,0:T(8,128)(2,1)}, u32[]{:S(2)}, u32[]{:S(2)}) collective-permute-start(bf16[4,16,16,512]{3,2,1,0:T(8,128)(2,1)S(1)} %all-to-all-done.1.mine_ref), channel_id=1, source_target_pairs={{0,1},{1,0},{2,3},{3,2},{4,5},{5,4},{6,7},{7,6},{8,9},{9,8},{10,11... | collective-permute-start | bytes 3145736 | tf_op jit(solution)/shard_map/ppermute | solution.py:323
  75.7 28.5 %copy-start.4 = (bf16[144,2048]{1,0:T(8,128)(2,1)}, bf16[144,2048]{1,0:T(8,128)(2,1)S(1)}, u32[]{:S(2)}) copy-start(bf16[144,2048]{1,0:T(8,128)(2,1)S(1)} %collective-permute-done.4.plus_ref) | copy-start | bytes 1769476
  76.6 27.6 %collective-permute-start.6 = (bf16[80,2048]{1,0:T(8,128)(2,1)}, bf16[80,2048]{1,0:T(8,128)(2,1)}, u32[]{:S(2)}, u32[]{:S(2)}) collective-permute-start(bf16[80,2048]{1,0:T(8,128)(2,1)} %slice.119), channel_id=1, source_target_pairs={{0,24},{8,0},{16,8},{24,16},{1,25},{9,1},{17,9},{25,17},{2,26},{10... | collective-permute-start | bytes 983048 | tf_op jit(solution)/shard_map/ppermute | solution.py:336
  82.2 22.0 %copy-start.6 = (bf16[144,2048]{1,0:T(8,128)(2,1)}, bf16[144,2048]{1,0:T(8,128)(2,1)S(1)}, u32[]{:S(2)}) copy-start(bf16[144,2048]{1,0:T(8,128)(2,1)S(1)} %collective-permute-done.3.minus_ref) | copy-start | bytes 1769476
  83.0 11.4 %collective-permute-start.7 = (bf16[16,8,128]{2,1,0:T(8,128)(2,1)S(1)}, bf16[16,8,128]{2,1,0:T(8,128)(2,1)}, u32[]{:S(2)}, u32[]{:S(2)}) collective-permute-start(bf16[16,8,128]{2,1,0:T(8,128)(2,1)S(1)} %get-tuple-element.22), channel_id=1, source_target_pairs={{0,8},{8,0},{16,24},{24,16},{1,9},{9,1},{17,25},{25,17},{2,10},{10... | collective-permute-start | bytes 98312 | tf_op jit(solution)/shard_map/ppermute | solution.py:321
  84.9 11.4 %collective-permute-start.8 = (bf16[16,8,128]{2,1,0:T(8,128)(2,1)S(1)}, bf16[16,8,128]{2,1,0:T(8,128)(2,1)}, u32[]{:S(2)}, u32[]{:S(2)}) collective-permute-start(bf16[16,8,128]{2,1,0:T(8,128)(2,1)S(1)} %get-tuple-element.22), channel_id=1, source_target_pairs={{0,16},{8,24},{16,0},{24,8},{1,17},{9,25},{17,1},{25,9},{2,18},{10... | collective-permute-start | bytes 98312 | tf_op jit(solution)/shard_map/ppermute | solution.py:321
  88.3 8.1 %collective-permute-start.9 = (bf16[16,8,128]{2,1,0:T(8,128)(2,1)S(1)}, bf16[16,8,128]{2,1,0:T(8,128)(2,1)}, u32[]{:S(2)}, u32[]{:S(2)}) collective-permute-start(bf16[16,8,128]{2,1,0:T(8,128)(2,1)S(1)} %get-tuple-element.22), channel_id=1, source_target_pairs={{0,24},{8,16},{16,8},{24,0},{1,25},{9,17},{17,9},{25,1},{2,26},{10... | collective-permute-start | bytes 98312 | tf_op jit(solution)/shard_map/ppermute | solution.py:321
  94.4 9.8 %collective-permute-start.5 = (bf16[64,2048]{1,0:T(8,128)(2,1)}, bf16[64,2048]{1,0:T(8,128)(2,1)}, u32[]{:S(2)}, u32[]{:S(2)}) collective-permute-start(bf16[64,2048]{1,0:T(8,128)(2,1)} %slice.118), channel_id=1, source_target_pairs={{0,8},{8,16},{16,24},{24,0},{1,9},{9,17},{17,25},{25,1},{2,10},{10... | collective-permute-start | bytes 786440 | tf_op jit(solution)/shard_map/ppermute | solution.py:335
  111.3 22.2 %all-to-all-start.2 = ((bf16[4,336,128]{2,1,0:T(8,128)(2,1)}), bf16[4,336,128]{2,1,0:T(8,128)(2,1)S(1)}, u32[]{:S(2)}, u32[]{:S(2)}) async-start(bf16[4,336,128]{2,1,0:T(8,128)(2,1)} %get-tuple-element.13), calls=%async_computation.2 | async-start | bytes 688128 | tf_op jit(solution)/shard_map/all_to_all | solution.py:362
  133.6 0.7 copy-start.5
  155.1 11.6 %all-to-all-start.4 = ((bf16[4,32,2048]{2,1,0:T(8,128)(2,1)}), bf16[4,32,2048]{2,1,0:T(8,128)(2,1)S(1)}, u32[]{:S(2)}, u32[]{:S(2)}) async-start(bf16[4,32,2048]{2,1,0:T(8,128)(2,1)} %bitcast.37), calls=%async_computation.4 | async-start | bytes 1048576 | tf_op jit(solution)/shard_map/all_to_all | solution.py:385
  166.7 0.8 copy-start.3

commit v4 on v3

--- a/solution.py
+++ b/solution.py
@@ -8,6 +8,7 @@
 
 D = 2048
 DK = 128
+RANK = 32
 BLOCK = 64
 CTX_LIFT = 4.0
 EPS = 1e-06
@@ -35,12 +36,6 @@
     return hi, mid, lo
 
 
-def three_pieces(x):
-    hi = lax.reduce_precision(x, 8, 7)
-    mid = lax.reduce_precision(x - hi, 8, 7)
-    return hi.astype(bf16), mid.astype(bf16), (x - hi - mid).astype(bf16)
-
-
 def tri(rows, cols, upper):
     r = lax.broadcasted_iota(jnp.int32, (rows, cols), 0)
     c = lax.broadcasted_iota(jnp.int32, (rows, cols), 1)
@@ -61,21 +56,49 @@
     return lax.dot_general(a, b, (((0,), (0,)), ((), ())), preferred_element_type=f32)
 
 
+def pack_kernel(
+    lat_ref, ctx_ref, sv_ref, cv_ref, mod_ref, wq_ref, wk_ref, wv_ref, extra_ref, rows_ref, cut_ref
+):
+    y = lax.axis_index("tp")
+    dp = lax.axis_index("x") * 2 + lax.axis_index("core")
+    rows_ref[0:32, :] = lat_ref[...]
+    ctx = ctx_ref[...].astype(f32)
+    picked = ctx[12:16]
+    for i in range(3):
+        picked = jnp.where(y == i, ctx[4 * i : 4 * i + 4], picked)
+    rows_ref[32:36, :] = picked.astype(bf16)
+
+    both = jnp.concatenate([sv_ref[...], cv_ref[...]], axis=0)
+    conditions = (both / (1.0 + jnp.exp(-both))).astype(bf16)
+    local_mods = nt(conditions, mod_ref[...])
+    mods = jnp.concatenate([p.astype(f32) for p in three_parts(local_mods)], axis=0)
+    mods = jnp.concatenate([mods, jnp.zeros((6, 32), f32)], axis=1)
+    extra = jnp.concatenate([p.astype(f32) for p in three_parts(extra_ref[...])[:2]], axis=0)
+    riding = jnp.concatenate([mods, extra, jnp.zeros((2, 128), f32)], axis=0).astype(bf16)
+    mine = pl.ds(pl.multiple_of(dp * 16, 16), 16)
+    for d in range(16):
+        b = d % 4
+        cut_ref[d, :, 0:128] = wq_ref[mine, (b // 2) * 128 : (b // 2 + 1) * 128]
+        cut_ref[d, :, 128:256] = wk_ref[mine, (b // 2) * 128 : (b // 2 + 1) * 128]
+        cut_ref[d, :, 256:384] = wv_ref[mine, b * 128 : (b + 1) * 128]
+        cut_ref[d, :, 384:512] = riding
+
+
 def project_kernel(
-    place, own_ref, minus_ref, plus_ref, low_ref, high_ref, mod_ref, gain_ref, mine_ref, other_ref,
-    down_ref, up_ref, bias_ref, extra_ref,
+    own_ref, minus_ref, plus_ref, low_ref, high_ref, mod_ref, gain_ref, mine_ref, other_ref,
+    down_ref, up_ref, bias_ref, ride_ref,
     pay_ref, q_ref, k_ref, v_ref, cum_ref, h_ref, w_ref,
 ):
-    seg, core, sub, y = place[0], place[1], place[2], place[3]
+    seg, sub = lax.axis_index("A"), lax.axis_index("B")
+    y, core = lax.axis_index("tp"), lax.axis_index("core")
+    second = sub >= 2
     for xi in range(4):
         for z in range(16):
             at = z * 128 + xi * 32
             here = pl.ds(pl.multiple_of(at + core * 16, 16), 16)
             there = pl.ds(pl.multiple_of(at + 16 - core * 16, 16), 16)
-            w_ref[here, 0:384] = mine_ref[xi, z, :, 0:384]
-            w_ref[there, 0:384] = other_ref[xi, z, :, 0:384]
-    w_ref[:, 384:448] = down_ref[...]
-    w_ref[:, 448:512] = jnp.zeros((D, 64), bf16)
+            w_ref[here, :] = mine_ref[xi, z]
+            w_ref[there, :] = other_ref[xi, z]
 
     def normed_rows(rows, which):
         v = rows.astype(f32)
@@ -101,12 +124,25 @@
     q_ref[...] = out[:SEG, 0:128]
     k_ref[...] = out[:SEG, 128:256]
     v_ref[...] = out[:SEG, 256:384]
-    low = out[:, 384:448]
-    raw = jnp.dot(low, up_ref[...], preferred_element_type=f32) + bias_ref[...]
+    low = nt(h_ref[...], down_ref[...]).astype(bf16)
+
+    def of_head(a):
+        return jnp.where(second, a[:, 128:256].astype(f32), a[:, 0:128].astype(f32))
+
+    raw = []
+    for z in range(2):
+        up = of_head(up_ref[z]).astype(bf16)
+        part = jnp.dot(low[:, z * RANK : (z + 1) * RANK], up, preferred_element_type=f32)
+        raw.append(part + of_head(bias_ref[z : z + 1, :]))
+    raw = jnp.concatenate(raw, axis=1)
     logs = (jnp.minimum(raw, 0.0) - jnp.log1p(jnp.exp(-jnp.abs(raw)))) * (1.0 / SHARP)
-    extra = jnp.concatenate([extra_ref[zb] for zb in range(4)], axis=0)
-    ef = extra[:, 0:1]
-    eb = extra[:, 1:2]
+    ef, eb = [], []
+    for zb in range(4):
+        t = jnp.transpose(ride_ref[seg * 4 + zb].astype(f32))
+        ef.append(jnp.where(second, t[:, 7:8] + t[:, 11:12], t[:, 6:7] + t[:, 10:11]))
+        eb.append(jnp.where(second, t[:, 9:10] + t[:, 13:14], t[:, 8:9] + t[:, 12:13]))
+    ef = jnp.concatenate(ef, axis=0)
+    eb = jnp.concatenate(eb, axis=0)
     af = logs[:SEG, 0:128] + ef
     ab = logs[:SEG, 128:256] + eb
     low_mask = tri(BLOCK, BLOCK, False)
@@ -212,8 +248,8 @@
         after = after + tot_b[n]
 
 
-def combine_kernel(place, in_ref, o_ref, lift_f_ref, lift_b_ref, out_ref):
-    seg = place[0]
+def combine_kernel(in_ref, o_ref, lift_f_ref, lift_b_ref, out_ref):
+    seg = lax.axis_index("A")
 
     def vec(peer, at):
         rows = in_ref[peer, 320:336, :].astype(f32)
@@ -246,14 +282,6 @@
         part = jnp.dot(n, w_ref[h * 256 : (h + 1) * 256, :], preferred_element_type=f32)
         total = part if total is None else total + part
     out_ref[...] = total.astype(bf16)
-
-
-def final_kernel(parts_ref, lat_ref, gate_ref, out_ref):
-    total = parts_ref[0].astype(f32)
-    for g in range(1, 4):
-        total = total + parts_ref[g].astype(f32)
-    projected = total.astype(bf16).astype(f32)
-    out_ref[...] = (lat_ref[...].astype(f32) + gate_ref[...] * projected).astype(bf16)
 
 
 def device_body(
@@ -273,59 +301,40 @@
     head_gain,
     out_weight,
 ):
-    seg = lax.axis_index("A")
-    sub = lax.axis_index("B")
     y = lax.axis_index("tp")
-    core = lax.axis_index("core")
-    dp = lax.axis_index("x") * 2 + core
-    head = sub // 2
-    place = jnp.stack([seg, core, sub, y]).astype(jnp.int32)
-
-    ctx_rows = lax.dynamic_slice_in_dim(context, y * 4, 4, 0)
-    rows = jnp.concatenate([latents, ctx_rows], 0)
+    sds = jax.ShapeDtypeStruct
+    rows, cut = pl.pallas_call(
+        pack_kernel,
+        out_shape=(sds((36, D), bf16), sds((16, 16, 512), bf16)),
+        in_specs=[VM] * 9,
+        out_specs=(VM, VM),
+        name="pack",
+    )(
+        latents, context, sample_vector, context_vector, modulator.T,
+        query_weight, key_weight, value_weight, jnp.moveaxis(decay_extra, 1, 2).reshape(4, 128),
+    )
     near = [rows]
     for j in range(1, 4):
         near.append(lax.ppermute(rows, "B", [(b, b ^ j) for b in range(4)]))
-
-    wq = lax.dynamic_slice_in_dim(query_weight, dp * 16, 16, 0)
-    wk = lax.dynamic_slice_in_dim(key_weight, dp * 16, 16, 0)
-    wv = lax.dynamic_slice_in_dim(value_weight, dp * 16, 16, 0)
-    conditions = jax.nn.silu(jnp.concatenate([sample_vector, context_vector], 0)).astype(bf16)
-    local_mods = jnp.dot(conditions, modulator, preferred_element_type=f32)
-    extra = jnp.moveaxis(decay_extra, 1, 2).reshape(4, 128)
-    riding = jnp.pad(jnp.concatenate(three_pieces(local_mods), axis=0), ((0, 0), (0, 32)))
-    riding = jnp.concatenate([riding, *three_pieces(extra)[:2], jnp.zeros((2, 128), bf16)], axis=0)
-    cut = jnp.stack(
-        [
-            jnp.concatenate(
-                [
-                    wq[:, (b // 2) * 128 : (b // 2 + 1) * 128],
-                    wk[:, (b // 2) * 128 : (b // 2 + 1) * 128],
-                    wv[:, b * 128 : (b + 1) * 128],
-                    riding,
-                ],
-                axis=1,
-            )
-            for b in range(4)
-        ]
-    )
-    cut = jnp.broadcast_to(cut[None], (4, 4, 16, 512)).reshape(16, 16, 512)
     rows_z = lax.all_to_all(cut, ("A", "B"), 0, 0, tiled=True)
-    mods = rows_z[:, 0:8, 384:512]
-    extras = lax.dynamic_slice_in_dim(rows_z, seg * 4, 4, 0)[:, 6:14, 384:512].astype(f32)
-    extras = (extras[:, 0:4] + extras[:, 4:8]).reshape(4, 2, 2, 128)
-    extras = lax.dynamic_index_in_dim(extras, head, 2, keepdims=False)
-    extras = jnp.transpose(extras, (0, 2, 1))
-    around = [mods]
-    for j in range(1, 4):
-        around.append(lax.ppermute(mods, "tp", [(i, i ^ j) for i in range(4)]))
-    mine = to_everyone(rows_z, "x")
+    mine = to_everyone(rows_z[:, :, 0:384], "x")
     other = lax.ppermute(mine, "core", [(0, 1), (1, 0)])
-    around = jnp.stack(around)
-    around = jnp.stack([lax.dynamic_index_in_dim(around, y ^ t, 0, keepdims=False) for t in range(4)])
-    parts = around[:, :, 0:6, 0:96].astype(f32)
-    parts = parts[:, :, 0:2] + parts[:, :, 2:4] + parts[:, :, 4:6]
-    modulation = jnp.transpose(parts, (2, 1, 0, 3)).reshape(2, 3 * D)
+    ride = rows_z[:, :, 384:512]
+    beside = lax.ppermute(ride, "tp", [(i, i ^ 1) for i in range(4)])
+    pair = jnp.stack([ride, beside])
+    across = lax.ppermute(pair, "tp", [(i, i ^ 3) for i in range(4)])
+    parts = [p[:, 0:6, 0:96].astype(f32) for p in (ride, beside, across[0], across[1])]
+    parts = [p[:, 0:2] + p[:, 2:4] + p[:, 4:6] for p in parts]
+    odd, high_half = (y % 2) == 1, y >= 2
+    near0, near1 = jnp.where(odd, parts[1], parts[0]), jnp.where(odd, parts[0], parts[1])
+    far0, far1 = jnp.where(odd, parts[2], parts[3]), jnp.where(odd, parts[3], parts[2])
+    ordered = [
+        jnp.where(high_half, far0, near0),
+        jnp.where(high_half, far1, near1),
+        jnp.where(high_half, near0, far0),
+        jnp.where(high_half, near1, far1),
+    ]
+    modulation = jnp.transpose(jnp.stack(ordered, axis=1), (2, 0, 1, 3)).reshape(2, 3 * D)
 
     own = jnp.concatenate([n[:32] for n in near] + [n[32:36] for n in near], axis=0)
     up_shift = [(i, (i + 1) % 4) for i in range(4)]
@@ -335,13 +344,6 @@
     low = lax.ppermute(minus[:64], "tp", up_shift)
     high = lax.ppermute(plus[64:], "tp", down_shift)
 
-    up = lax.dynamic_slice_in_dim(decay_up, head * 128, 128, 2)
-    up_both = jnp.concatenate(
-        [jnp.pad(up[0], ((0, 0), (0, 128))), jnp.pad(up[1], ((0, 0), (128, 0)))], axis=0
-    )
-    bias = lax.dynamic_slice_in_dim(decay_bias, head * 128, 128, 1).reshape(1, 256)
-
-    sds = jax.ShapeDtypeStruct
     payload, q, k, v, cum = pl.pallas_call(
         project_kernel,
         out_shape=(
@@ -351,13 +353,13 @@
             sds((SEG, DK), bf16),
             sds((2, SEG, DK), f32),
         ),
-        in_specs=[SM] + [VM] * 13,
+        in_specs=[VM] * 13,
         out_specs=(VM,) * 5,
-        scratch_shapes=[pltpu.VMEM((ROWS, D), bf16), pltpu.VMEM((D, 512), bf16)],
+        scratch_shapes=[pltpu.VMEM((ROWS, D), bf16), pltpu.VMEM((D, 384), bf16)],
         name="project",
     )(
-        place, own, minus, plus, low, high, modulation, norm_gain.reshape(1, D), mine, other,
-        decay_down, up_both, bias, extras,
+        own, minus, plus, low, high, modulation, norm_gain.reshape(1, D), mine, other,
+        decay_down.T, decay_up, decay_bias, ride,
     )
     got = lax.all_to_all(payload, "A", 0, 0, tiled=True)
     local, lift_f, lift_b = pl.pallas_call(
@@ -370,10 +372,10 @@
     mixed = pl.pallas_call(
         combine_kernel,
         out_shape=sds((SEG, DK), bf16),
-        in_specs=[SM] + [VM] * 4,
+        in_specs=[VM] * 4,
         out_specs=VM,
         name="combine",
-    )(place, got, local, lift_f, lift_b)
+    )(got, local, lift_f, lift_b)
     heads = lax.all_to_all(mixed.reshape(4, 128, DK), "B", 0, 0, tiled=True)
     partial = pl.pallas_call(
         output_kernel,
@@ -383,13 +385,9 @@
         name="output",
     )(heads, head_gain.reshape(1, 256), out_weight)
     shares = lax.all_to_all(partial.reshape(4, 32, D), "tp", 0, 0, tiled=True)
-    return pl.pallas_call(
-        final_kernel,
-        out_shape=sds((32, D), bf16),
-        in_specs=[VM] * 3,
-        out_specs=VM,
-        name="final",
-    )(shares, latents, modulation[0:1, 2 * D :])
+    projected = shares.astype(f32).sum(axis=0)
+    projected = lax.optimization_barrier(projected.astype(bf16)).astype(f32)
+    return (latents.astype(f32) + modulation[0:1, 2 * D :] * projected).astype(bf16)
 
 
 def solution(mesh):

time: 171 us -> 166 us (0.971)
  local copies, waits for them, and re-layouts: 13 us -> 7.51 us
    all_to_all x1, waiting for transfers between devices: 17.6 us -> 0.01 us  [device_body(): rows_z = lax.all_to_all(cut, ('A', 'B'), 0, 0, tiled=True)]
    ppermute x1, waiting for transfers between devices: 0.79 us -> 10 us  [device_body(): plus = lax.ppermute(own, 'tp', down_shift)]
    ppermute x1, waiting for transfers between devices: 6.13 us -> 0.01 us  [device_body(): low = lax.ppermute(minus[:64], 'tp', up_shift)]
    ppermute x3, waiting for transfers between devices: 8.33 us -> 14.2 us  [device_body(): near.append(lax.ppermute(rows, 'B', [(b, b ^ j) for b in range(4)]))]
    all_to_all x1, waiting for transfers between devices: 12.7 us -> 16.3 us  [device_body(): got = lax.all_to_all(payload, 'A', 0, 0, tiled=True)]
    ppermute x3 -> x2, starting transfers between devices: 10.4 us -> 7.04 us  [the longest x1 5.13 us: device_body(): across = lax.ppermute(pair, 'tp', [(i, i ^ 3) for i in range(4)])]
    unnamed x22 -> x18, local copies, waits for them, and re-layouts: 4.37 us -> 1.68 us
    all_to_all x1, starting transfers between devices: 6.52 us -> 8.94 us  [device_body(): got = lax.all_to_all(payload, 'A', 0, 0, tiled=True)]
  transfers between devices with their start and end apart: 15 -> 14, of which waited for: 6 -> 7; matrix products, arithmetic and copies ran while one was open for 6% -> 5% of each run, Pallas kernels for 2% -> 2%
where the time goes in v4:
time: 166 us; the launch traced here: 164 us
  starting transfers between devices  67.7 us (41%)
  waiting for transfers between devices  51.7 us (31%)
  Pallas kernels  18.7 us (11%)
  blocking collectives  15.6 us (9%)
  local copies, waits for them, and re-layouts  7.51 us (5%)
  other arithmetic  2.58 us (2%)
    all_to_all x1, waiting for transfers between devices, device_body(): got = lax.all_to_all(payload, 'A', 0, 0, tiled=True)  16.3 us
    all_to_all x1, blocking collectives, device_body(): heads = lax.all_to_all(mixed.reshape(4, 128, DK), 'B', 0, 0, tiled=True)  15.6 us
    all_to_all x1, starting transfers between devices, device_body(): rows_z = lax.all_to_all(cut, ('A', 'B'), 0, 0, tiled=True)  15.2 us
    ppermute x3, waiting for transfers between devices, device_body(): near.append(lax.ppermute(rows, 'B', [(b, b ^ j) for b in range(4)]))  14.2 us
    ppermute x3, starting transfers between devices, device_body(): near.append(lax.ppermute(rows, 'B', [(b, b ^ j) for b in range(4)]))  10.1 us
    ppermute x1, waiting for transfers between devices, device_body(): plus = lax.ppermute(own, 'tp', down_shift)  10 us
    all_to_all x1, starting transfers between devices, device_body(): got = lax.all_to_all(payload, 'A', 0, 0, tiled=True)  8.94 us
    pallas_call x1, Pallas kernels, device_body(): pl.pallas_call(project_kernel, out_shape=(sds((4, PAYLOAD, DK), bf16), sd...  8.21 us
  transfers between devices with their start and end apart: 14, of which 7 were waited for; matrix products, arithmetic and copies ran while one was open for 5% of the time, Pallas kernels for 2%

profile of v4, /device:TPU:6, one launch (start us, length us, event | category | flops | bytes accessed | tf_op | source)
XLA Modules:
  0.0 164.2 jit_solution(4055057867278019402)
XLA Ops:
  0.0 2.2 %pack.1 = (bf16[36,2048]{1,0:T(8,128)(2,1)}, bf16[16,16,512]{2,1,0:T(8,128)(2,1)}) custom-call(bf16[32,2048]{1,0:T(8,128)(2,1)} %lat_ref.1, bf16[16,2048]{1,0:T(8,128)(2,1)} %ctx_ref.1, f32[1,2048]{1,0:T(1,128)} %sv_ref.1, f32[1,2048]{1,0:T(1,128)} %cv_ref.1, bf16[96,2048]{1,0:T(8,128)(2,1)} %bitcast.29, bf16[128,256]{1,0:T(8,128)(2,1)} %wq_ref.1, ...), custom_call_target="tpu_custom_call" | custom-call | tf_op jit(solution)/shard_map/pack/pallas_call | solution.py:306
  2.2 15.2 %all-to-all-start = ((bf16[16,16,512]{2,1,0:T(8,128)(2,1)}), bf16[16,16,512]{2,1,0:T(8,128)(2,1)S(1)}, u32[]{:S(2)}, u32[]{:S(2)}) async-start(bf16[16,16,512]{2,1,0:T(8,128)(2,1)} %get-tuple-element.15), calls=%async_computation | async-start | bytes 524288 | tf_op jit(solution)/shard_map/all_to_all | solution.py:319
  17.4 3.8 %collective-permute-start.2 = (bf16[36,2048]{1,0:T(8,128)(2,1)}, bf16[36,2048]{1,0:T(8,128)(2,1)S(1)}, u32[]{:S(2)}, u32[]{:S(2)}) collective-permute-start(bf16[36,2048]{1,0:T(8,128)(2,1)} %get-tuple-element.16), channel_id=1, source_target_pairs={{0,32},{32,0},{64,96},{96,64},{1,33},{33,1},{65,97},{97,65},{2,34}... | collective-permute-start | bytes 442376 | tf_op jit(solution)/shard_map/ppermute | solution.py:318
  21.2 4.3 %collective-permute-start.3 = (bf16[36,2048]{1,0:T(8,128)(2,1)}, bf16[36,2048]{1,0:T(8,128)(2,1)S(1)}, u32[]{:S(2)}, u32[]{:S(2)}) collective-permute-start(bf16[36,2048]{1,0:T(8,128)(2,1)} %get-tuple-element.16), channel_id=1, source_target_pairs={{0,64},{32,96},{64,0},{96,32},{1,65},{33,97},{65,1},{97,33},{2,66}... | collective-permute-start | bytes 442376 | tf_op jit(solution)/shard_map/ppermute | solution.py:318
  25.5 2.0 %collective-permute-start.4 = (bf16[36,2048]{1,0:T(8,128)(2,1)}, bf16[36,2048]{1,0:T(8,128)(2,1)S(1)}, u32[]{:S(2)}, u32[]{:S(2)}) collective-permute-start(bf16[36,2048]{1,0:T(8,128)(2,1)} %get-tuple-element.16), channel_id=1, source_target_pairs={{0,96},{32,64},{64,32},{96,0},{1,97},{33,65},{65,33},{97,1},{2,98}... | collective-permute-start | bytes 442376 | tf_op jit(solution)/shard_map/ppermute | solution.py:318
  27.5 0.9 slice.114
  28.4 0.8 slice.118
  29.2 8.7 %collective-permute-done.2 = bf16[36,2048]{1,0:T(8,128)(2,1)S(1)} collective-permute-done((bf16[36,2048]{1,0:T(8,128)(2,1)}, bf16[36,2048]{1,0:T(8,128)(2,1)S(1)}, u32[]{:S(2)}, u32[]{:S(2)}) %collective-permute-start.2) | collective-permute-done | bytes 147488 | tf_op jit(solution)/shard_map/ppermute | solution.py:318
  37.9 5.5 %collective-permute-done.3 = bf16[36,2048]{1,0:T(8,128)(2,1)S(1)} collective-permute-done((bf16[36,2048]{1,0:T(8,128)(2,1)}, bf16[36,2048]{1,0:T(8,128)(2,1)S(1)}, u32[]{:S(2)}, u32[]{:S(2)}) %collective-permute-start.3) | collective-permute-done | bytes 147488 | tf_op jit(solution)/shard_map/ppermute | solution.py:318
  43.4 0.0 collective-permute-done.4
  43.5 0.1 concatenate.3.own_ref
  43.6 4.9 %collective-permute-start.6 = (bf16[144,2048]{1,0:T(8,128)(2,1)S(1)}, bf16[144,2048]{1,0:T(8,128)(2,1)S(1)}, u32[]{:S(2)}, u32[]{:S(2)}) collective-permute-start(bf16[144,2048]{1,0:T(8,128)(2,1)S(1)} %concatenate.3.own_ref), channel_id=1, source_target_pairs={{0,24},{8,0},{16,8},{24,16},{1,25},{9,1},{17,9},{25,17},{2,26},{10... | collective-permute-start | bytes 1769480 | tf_op jit(solution)/shard_map/ppermute | solution.py:343
  48.5 1.9 %collective-permute-start.5 = (bf16[144,2048]{1,0:T(8,128)(2,1)S(1)}, bf16[144,2048]{1,0:T(8,128)(2,1)S(1)}, u32[]{:S(2)}, u32[]{:S(2)}) collective-permute-start(bf16[144,2048]{1,0:T(8,128)(2,1)S(1)} %concatenate.3.own_ref), channel_id=1, source_target_pairs={{0,8},{8,16},{16,24},{24,0},{1,9},{9,17},{17,25},{25,1},{2,10},{10... | collective-permute-start | bytes 1769480 | tf_op jit(solution)/shard_map/ppermute | solution.py:342
  50.5 10.0 %collective-permute-done.6.plus_ref = bf16[144,2048]{1,0:T(8,128)(2,1)S(1)} collective-permute-done((bf16[144,2048]{1,0:T(8,128)(2,1)S(1)}, bf16[144,2048]{1,0:T(8,128)(2,1)S(1)}, u32[]{:S(2)}, u32[]{:S(2)}) %collective-permute-start.6) | collective-permute-done | bytes 589856 | tf_op jit(solution)/shard_map/ppermute | solution.py:343
  60.5 5.6 %collective-permute-start.8 = (bf16[80,2048]{1,0:T(8,128)(2,1)S(1)}, bf16[80,2048]{1,0:T(8,128)(2,1)S(1)}, u32[]{:S(2)}, u32[]{:S(2)}) collective-permute-start(bf16[80,2048]{1,0:T(8,128)(2,1)S(1)} %slice.152), channel_id=1, source_target_pairs={{0,24},{8,0},{16,8},{24,16},{1,25},{9,1},{17,9},{25,17},{2,26},{10... | collective-permute-start | bytes 983048 | tf_op jit(solution)/shard_map/ppermute | solution.py:345
  66.1 0.0 collective-permute-done.5.minus_ref
  66.1 0.8 slice.151
  66.9 1.9 %collective-permute-start.7 = (bf16[64,2048]{1,0:T(8,128)(2,1)}, bf16[64,2048]{1,0:T(8,128)(2,1)}, u32[]{:S(2)}, u32[]{:S(2)}) collective-permute-start(bf16[64,2048]{1,0:T(8,128)(2,1)} %slice.151), channel_id=1, source_target_pairs={{0,8},{8,16},{16,24},{24,0},{1,9},{9,17},{17,25},{25,1},{2,10},{10... | collective-permute-start | bytes 786440 | tf_op jit(solution)/shard_map/ppermute | solution.py:344
  68.8 0.0 all-to-all-done
  68.9 0.6 slice_bitcast_fusion.2
  69.5 1.9 %collective-permute-start = (bf16[16,16,128]{2,1,0:T(8,128)(2,1)S(1)}, bf16[16,16,128]{2,1,0:T(8,128)(2,1)}, u32[]{:S(2)}, u32[]{:S(2)}) collective-permute-start(bf16[16,16,128]{2,1,0:T(8,128)(2,1)S(1)} %get-tuple-element.31.ride_ref), channel_id=1, source_target_pairs={{0,8},{8,0},{16,24},{24,16},{1,9},{9,1},{17,25},{25,17},{2,10},{10... | collective-permute-start | bytes 196616 | tf_op jit(solution)/shard_map/ppermute | solution.py:323
  71.4 1.0 broadcast_in_dim.2
  72.4 4.8 %all-to-all-start.1 = ((bf16[4,16,16,384]{3,2,1,0:T(8,128)(2,1)}), bf16[4,16,16,384]{3,2,1,0:T(8,128)(2,1)S(1)}, u32[]{:S(2)}, u32[]{:S(2)}) async-start(bf16[4,16,16,384]{3,2,1,0:T(8,128)(2,1)} %broadcast_in_dim.2), calls=%async_computation.1 | async-start | bytes 1572864 | tf_op jit(solution)/shard_map/all_to_all | solution.py:28
  77.2 0.0 collective-permute-done
  77.2 0.9 pad_maximum_fusion
  78.1 5.1 %collective-permute-start.1 = (bf16[2,16,16,128]{3,2,1,0:T(8,128)(2,1)S(1)}, bf16[2,16,16,128]{3,2,1,0:T(8,128)(2,1)S(1)}, u32[]{:S(2)}, u32[]{:S(2)}) collective-permute-start(bf16[2,16,16,128]{3,2,1,0:T(8,128)(2,1)S(1)} %pad_maximum_fusion), channel_id=1, source_target_pairs={{0,24},{8,16},{16,8},{24,0},{1,25},{9,17},{17,9},{25,1},{2,26},{10... | collective-permute-start | bytes 393224 | tf_op jit(solution)/shard_map/ppermute | solution.py:325
  83.2 0.8 slice_convert_fusion.1
  84.0 2.2 %collective-permute-done.1 = bf16[2,16,16,128]{3,2,1,0:T(8,128)(2,1)S(1)} collective-permute-done((bf16[2,16,16,128]{3,2,1,0:T(8,128)(2,1)S(1)}, bf16[2,16,16,128]{3,2,1,0:T(8,128)(2,1)S(1)}, u32[]{:S(2)}, u32[]{:S(2)}) %collective-permute-start.1) | collective-permute-done | bytes 131104 | tf_op jit(solution)/shard_map/ppermute | solution.py:325
  86.2 1.9 %collective-permute-start.9 = (bf16[4,16,16,384]{3,2,1,0:T(8,128)(2,1)S(1)}, bf16[4,16,16,384]{3,2,1,0:T(8,128)(2,1)S(1)}, u32[]{:S(2)}, u32[]{:S(2)}) collective-permute-start(bf16[4,16,16,384]{3,2,1,0:T(8,128)(2,1)S(1)} %all-to-all-done.1.mine_ref), channel_id=1, source_target_pairs={{0,1},{1,0},{2,3},{3,2},{4,5},{5,4},{6,7},{7,6},{8,9},{9,8},{10,11... | collective-permute-start | bytes 2359304 | tf_op jit(solution)/shard_map/ppermute | solution.py:321
  88.2 0.1 select_bitcast_fusion.3
  88.4 0.8 reshape.20.mod_ref
  89.1 0.0 collective-permute-done.7.low_ref
  89.1 0.0 collective-permute-done.8.high_ref
  89.2 1.3 collective-permute-done.9.other_ref
  90.4 0.9 copy-done.5
  91.3 8.2 %project.1 = (bf16[4,336,128]{2,1,0:T(8,128)(2,1)}, bf16[512,128]{1,0:T(8,128)(2,1)}, bf16[512,128]{1,0:T(8,128)(2,1)}, bf16[512,128]{1,0:T(8,128)(2,1)}, f32[2,512,128]{2,1,0:T(8,128)}) custom-call(bf16[144,2048]{1,0:T(8,128)(2,1)} %copy-done.1, bf16[144,2048]{1,0:T(8,128)(2,1)} %copy-done.4, bf16[144,2048]{1,0:T(8,128)(2,1)} %copy-done.2, ...), custom_call_target="tpu_custom_call" | custom-call | tf_op jit(solution)/shard_map/project/pallas_call | solution.py:347
  99.5 8.9 %all-to-all-start.2 = ((bf16[4,336,128]{2,1,0:T(8,128)(2,1)}), bf16[4,336,128]{2,1,0:T(8,128)(2,1)S(1)}, u32[]{:S(2)}, u32[]{:S(2)}) async-start(bf16[4,336,128]{2,1,0:T(8,128)(2,1)} %get-tuple-element.17), calls=%async_computation.2 | async-start | bytes 688128 | tf_op jit(solution)/shard_map/all_to_all | solution.py:364
  108.5 3.0 %local.1 = (f32[512,128]{1,0:T(8,128)}, bf16[512,128]{1,0:T(8,128)(2,1)}, bf16[512,128]{1,0:T(8,128)(2,1)}) custom-call(bf16[512,128]{1,0:T(8,128)(2,1)} %get-tuple-element.18.q_ref, bf16[512,128]{1,0:T(8,128)(2,1)} %get-tuple-element.19.k_ref, bf16[512,128]{1,0:T(8,128)(2,1)} %get-tuple-element.20.v_ref, f32[2,512,128]{2,1,0:T(8,128)} %get-tuple-element.21.cum_ref), custom_call_target="tpu_custom_call" | custom-call | tf_op jit(solution)/shard_map/local/pallas_call | solution.py:365
  111.5 16.3 %all-to-all-done.2.in_ref = bf16[4,336,128]{2,1,0:T(8,128)(2,1)S(1)} async-done(((bf16[4,336,128]{2,1,0:T(8,128)(2,1)}), bf16[4,336,128]{2,1,0:T(8,128)(2,1)S(1)}, u32[]{:S(2)}, u32[]{:S(2)}) %all-to-all-start.2) | async-done | bytes 344096 | tf_op jit(solution)/shard_map/all_to_all | solution.py:364
  127.8 0.7 copy-done.3
  128.5 2.3 %combine.1 = bf16[512,128]{1,0:T(8,128)(2,1)} custom-call(bf16[4,336,128]{2,1,0:T(8,128)(2,1)} %copy-done.3, f32[512,128]{1,0:T(8,128)} %get-tuple-element.22.o_ref, bf16[512,128]{1,0:T(8,128)(2,1)} %get-tuple-element.23.lift_f_ref, bf16[512,128]{1,0:T(8,128)(2,1)} %get-tuple-element.24.lift_b_ref), custom_call_target="tpu_custom_call" | custom-call | tf_op jit(solution)/shard_map/combine/pallas_call | solution.py:372
  130.8 15.6 %all_to_all.25.mix_ref = bf16[4,128,128]{2,1,0:T(8,128)(2,1)} all-to-all(bf16[4,128,128]{2,1,0:T(8,128)(2,1)} %bitcast.28), channel_id=1, replica_groups=mesh['A'=4,'B'=4,'tp'=4,'x'=4,'core'=2] {'B'}, dimensions={0} | all-to-all | bytes 262144 | tf_op jit(solution)/shard_map/all_to_all | solution.py:379
  146.4 3.0 %output.1 = bf16[128,2048]{1,0:T(8,128)(2,1)} custom-call(bf16[4,128,128]{2,1,0:T(8,128)(2,1)} %all_to_all.25.mix_ref, f32[1,256]{1,0:T(1,128)} %bitcast.34, bf16[512,2048]{1,0:T(8,128)(2,1)} %w_ref.1), custom_call_target="tpu_custom_call" | custom-call | tf_op jit(solution)/shard_map/output/pallas_call | solution.py:380
  149.4 5.4 %all-to-all-start.4 = ((bf16[4,32,2048]{2,1,0:T(8,128)(2,1)}), bf16[4,32,2048]{2,1,0:T(8,128)(2,1)S(1)}, u32[]{:S(2)}, u32[]{:S(2)}) async-start(bf16[4,32,2048]{2,1,0:T(8,128)(2,1)} %bitcast.27), calls=%async_computation.4 | async-start | bytes 1048576 | tf_op jit(solution)/shard_map/all_to_all | solution.py:387
  154.8 0.7 slice.144
  155.5 7.8 %all-to-all-done.4 = bf16[4,32,2048]{2,1,0:T(8,128)(2,1)S(1)} async-done(((bf16[4,32,2048]{2,1,0:T(8,128)(2,1)}), bf16[4,32,2048]{2,1,0:T(8,128)(2,1)S(1)}, u32[]{:S(2)}, u32[]{:S(2)}) %all-to-all-start.4) | async-done | bytes 524320 | tf_op jit(solution)/shard_map/all_to_all | solution.py:387
  163.4 0.1 reduce_sum.12
  163.5 0.7 add_convert_fusion
  (31 shorter events, 0.3 us)
Async XLA Ops:
  2.2 66.7 %all-to-all-start = ((bf16[16,16,512]{2,1,0:T(8,128)(2,1)}), bf16[16,16,512]{2,1,0:T(8,128)(2,1)S(1)}, u32[]{:S(2)}, u32[]{:S(2)}) async-start(bf16[16,16,512]{2,1,0:T(8,128)(2,1)} %get-tuple-element.15), calls=%async_computation | async-start | bytes 524288 | tf_op jit(solution)/shard_map/all_to_all | solution.py:319
  17.4 20.5 %collective-permute-start.2 = (bf16[36,2048]{1,0:T(8,128)(2,1)}, bf16[36,2048]{1,0:T(8,128)(2,1)S(1)}, u32[]{:S(2)}, u32[]{:S(2)}) collective-permute-start(bf16[36,2048]{1,0:T(8,128)(2,1)} %get-tuple-element.16), channel_id=1, source_target_pairs={{0,32},{32,0},{64,96},{96,64},{1,33},{33,1},{65,97},{97,65},{2,34}... | collective-permute-start | bytes 442376 | tf_op jit(solution)/shard_map/ppermute | solution.py:318
  21.2 22.2 %collective-permute-start.3 = (bf16[36,2048]{1,0:T(8,128)(2,1)}, bf16[36,2048]{1,0:T(8,128)(2,1)S(1)}, u32[]{:S(2)}, u32[]{:S(2)}) collective-permute-start(bf16[36,2048]{1,0:T(8,128)(2,1)} %get-tuple-element.16), channel_id=1, source_target_pairs={{0,64},{32,96},{64,0},{96,32},{1,65},{33,97},{65,1},{97,33},{2,66}... | collective-permute-start | bytes 442376 | tf_op jit(solution)/shard_map/ppermute | solution.py:318
  25.5 17.9 %collective-permute-start.4 = (bf16[36,2048]{1,0:T(8,128)(2,1)}, bf16[36,2048]{1,0:T(8,128)(2,1)S(1)}, u32[]{:S(2)}, u32[]{:S(2)}) collective-permute-start(bf16[36,2048]{1,0:T(8,128)(2,1)} %get-tuple-element.16), channel_id=1, source_target_pairs={{0,96},{32,64},{64,32},{96,0},{1,97},{33,65},{65,33},{97,1},{2,98}... | collective-permute-start | bytes 442376 | tf_op jit(solution)/shard_map/ppermute | solution.py:318
  43.6 28.8 %copy-start.1 = (bf16[144,2048]{1,0:T(8,128)(2,1)}, bf16[144,2048]{1,0:T(8,128)(2,1)S(1)}, u32[]{:S(2)}) copy-start(bf16[144,2048]{1,0:T(8,128)(2,1)S(1)} %concatenate.3.own_ref) | copy-start | bytes 1769476
  43.6 16.9 %collective-permute-start.6 = (bf16[144,2048]{1,0:T(8,128)(2,1)S(1)}, bf16[144,2048]{1,0:T(8,128)(2,1)S(1)}, u32[]{:S(2)}, u32[]{:S(2)}) collective-permute-start(bf16[144,2048]{1,0:T(8,128)(2,1)S(1)} %concatenate.3.own_ref), channel_id=1, source_target_pairs={{0,24},{8,0},{16,8},{24,16},{1,25},{9,1},{17,9},{25,17},{2,26},{10... | collective-permute-start | bytes 1769480 | tf_op jit(solution)/shard_map/ppermute | solution.py:343
  48.5 17.6 %collective-permute-start.5 = (bf16[144,2048]{1,0:T(8,128)(2,1)S(1)}, bf16[144,2048]{1,0:T(8,128)(2,1)S(1)}, u32[]{:S(2)}, u32[]{:S(2)}) collective-permute-start(bf16[144,2048]{1,0:T(8,128)(2,1)S(1)} %concatenate.3.own_ref), channel_id=1, source_target_pairs={{0,8},{8,16},{16,24},{24,0},{1,9},{9,17},{17,25},{25,1},{2,10},{10... | collective-permute-start | bytes 1769480 | tf_op jit(solution)/shard_map/ppermute | solution.py:342
  60.5 11.9 %copy-start.2 = (bf16[144,2048]{1,0:T(8,128)(2,1)}, bf16[144,2048]{1,0:T(8,128)(2,1)S(1)}, u32[]{:S(2)}) copy-start(bf16[144,2048]{1,0:T(8,128)(2,1)S(1)} %collective-permute-done.6.plus_ref) | copy-start | bytes 1769476
  60.5 28.6 %collective-permute-start.8 = (bf16[80,2048]{1,0:T(8,128)(2,1)S(1)}, bf16[80,2048]{1,0:T(8,128)(2,1)S(1)}, u32[]{:S(2)}, u32[]{:S(2)}) collective-permute-start(bf16[80,2048]{1,0:T(8,128)(2,1)S(1)} %slice.152), channel_id=1, source_target_pairs={{0,24},{8,0},{16,8},{24,16},{1,25},{9,1},{17,9},{25,17},{2,26},{10... | collective-permute-start | bytes 983048 | tf_op jit(solution)/shard_map/ppermute | solution.py:345
  66.1 20.1 %copy-start.4 = (bf16[144,2048]{1,0:T(8,128)(2,1)}, bf16[144,2048]{1,0:T(8,128)(2,1)S(1)}, u32[]{:S(2)}) copy-start(bf16[144,2048]{1,0:T(8,128)(2,1)S(1)} %collective-permute-done.5.minus_ref) | copy-start | bytes 1769476
  66.9 22.2 %collective-permute-start.7 = (bf16[64,2048]{1,0:T(8,128)(2,1)}, bf16[64,2048]{1,0:T(8,128)(2,1)}, u32[]{:S(2)}, u32[]{:S(2)}) collective-permute-start(bf16[64,2048]{1,0:T(8,128)(2,1)} %slice.151), channel_id=1, source_target_pairs={{0,8},{8,16},{16,24},{24,0},{1,9},{9,17},{17,25},{25,1},{2,10},{10... | collective-permute-start | bytes 786440 | tf_op jit(solution)/shard_map/ppermute | solution.py:344
  69.5 18.8 %copy-start.8 = (bf16[16,16,128]{2,1,0:T(8,128)(2,1)}, bf16[16,16,128]{2,1,0:T(8,128)(2,1)S(1)}, u32[]{:S(2)}) copy-start(bf16[16,16,128]{2,1,0:T(8,128)(2,1)S(1)} %get-tuple-element.31.ride_ref) | copy-start | bytes 196612
  69.5 7.7 %collective-permute-start = (bf16[16,16,128]{2,1,0:T(8,128)(2,1)S(1)}, bf16[16,16,128]{2,1,0:T(8,128)(2,1)}, u32[]{:S(2)}, u32[]{:S(2)}) collective-permute-start(bf16[16,16,128]{2,1,0:T(8,128)(2,1)S(1)} %get-tuple-element.31.ride_ref), channel_id=1, source_target_pairs={{0,8},{8,0},{16,24},{24,16},{1,9},{9,1},{17,25},{25,17},{2,10},{10... | collective-permute-start | bytes 196616 | tf_op jit(solution)/shard_map/ppermute | solution.py:323
  72.4 13.8 %all-to-all-start.1 = ((bf16[4,16,16,384]{3,2,1,0:T(8,128)(2,1)}), bf16[4,16,16,384]{3,2,1,0:T(8,128)(2,1)S(1)}, u32[]{:S(2)}, u32[]{:S(2)}) async-start(bf16[4,16,16,384]{3,2,1,0:T(8,128)(2,1)} %broadcast_in_dim.2), calls=%async_computation.1 | async-start | bytes 1572864 | tf_op jit(solution)/shard_map/all_to_all | solution.py:28
  78.1 8.1 %collective-permute-start.1 = (bf16[2,16,16,128]{3,2,1,0:T(8,128)(2,1)S(1)}, bf16[2,16,16,128]{3,2,1,0:T(8,128)(2,1)S(1)}, u32[]{:S(2)}, u32[]{:S(2)}) collective-permute-start(bf16[2,16,16,128]{3,2,1,0:T(8,128)(2,1)S(1)} %pad_maximum_fusion), channel_id=1, source_target_pairs={{0,24},{8,16},{16,8},{24,0},{1,25},{9,17},{17,9},{25,1},{2,26},{10... | collective-permute-start | bytes 393224 | tf_op jit(solution)/shard_map/ppermute | solution.py:325
  86.2 4.2 %copy-start = (bf16[4,16,16,384]{3,2,1,0:T(8,128)(2,1)}, bf16[4,16,16,384]{3,2,1,0:T(8,128)(2,1)S(1)}, u32[]{:S(2)}) copy-start(bf16[4,16,16,384]{3,2,1,0:T(8,128)(2,1)S(1)} %all-to-all-done.1.mine_ref) | copy-start | bytes 2359300
  86.2 4.2 %collective-permute-start.9 = (bf16[4,16,16,384]{3,2,1,0:T(8,128)(2,1)S(1)}, bf16[4,16,16,384]{3,2,1,0:T(8,128)(2,1)S(1)}, u32[]{:S(2)}, u32[]{:S(2)}) collective-permute-start(bf16[4,16,16,384]{3,2,1,0:T(8,128)(2,1)S(1)} %all-to-all-done.1.mine_ref), channel_id=1, source_target_pairs={{0,1},{1,0},{2,3},{3,2},{4,5},{5,4},{6,7},{7,6},{8,9},{9,8},{10,11... | collective-permute-start | bytes 2359304 | tf_op jit(solution)/shard_map/ppermute | solution.py:321
  89.1 1.3 copy-start.7
  90.4 0.9 copy-start.5
  99.5 28.3 %all-to-all-start.2 = ((bf16[4,336,128]{2,1,0:T(8,128)(2,1)}), bf16[4,336,128]{2,1,0:T(8,128)(2,1)S(1)}, u32[]{:S(2)}, u32[]{:S(2)}) async-start(bf16[4,336,128]{2,1,0:T(8,128)(2,1)} %get-tuple-element.17), calls=%async_computation.2 | async-start | bytes 688128 | tf_op jit(solution)/shard_map/all_to_all | solution.py:364
  127.8 0.7 copy-start.3
  146.4 17.1 %copy-start.6 = (bf16[32,2048]{1,0:T(8,128)(2,1)S(1)}, bf16[32,2048]{1,0:T(8,128)(2,1)}, u32[]{:S(2)}) copy-start(bf16[32,2048]{1,0:T(8,128)(2,1)} %lat_ref.1) | copy-start | bytes 393220
  149.4 14.0 %all-to-all-start.4 = ((bf16[4,32,2048]{2,1,0:T(8,128)(2,1)}), bf16[4,32,2048]{2,1,0:T(8,128)(2,1)S(1)}, u32[]{:S(2)}, u32[]{:S(2)}) async-start(bf16[4,32,2048]{2,1,0:T(8,128)(2,1)} %bitcast.27), calls=%async_computation.4 | async-start | bytes 1048576 | tf_op jit(solution)/shard_map/all_to_all | solution.py:387

commit v5 on v4

--- a/solution.py
+++ b/solution.py
@@ -320,10 +320,11 @@
     mine = to_everyone(rows_z[:, :, 0:384], "x")
     other = lax.ppermute(mine, "core", [(0, 1), (1, 0)])
     ride = rows_z[:, :, 384:512]
-    beside = lax.ppermute(ride, "tp", [(i, i ^ 1) for i in range(4)])
-    pair = jnp.stack([ride, beside])
+    mods = rows_z[:, 0:8, 384:512]
+    beside = lax.ppermute(mods, "tp", [(i, i ^ 1) for i in range(4)])
+    pair = jnp.stack([mods, beside])
     across = lax.ppermute(pair, "tp", [(i, i ^ 3) for i in range(4)])
-    parts = [p[:, 0:6, 0:96].astype(f32) for p in (ride, beside, across[0], across[1])]
+    parts = [p[:, 0:6, 0:96].astype(f32) for p in (mods, beside, across[0], across[1])]
     parts = [p[:, 0:2] + p[:, 2:4] + p[:, 4:6] for p in parts]
     odd, high_half = (y % 2) == 1, y >= 2
     near0, near1 = jnp.where(odd, parts[1], parts[0]), jnp.where(odd, parts[0], parts[1])

time: 166 us -> 166 us (level)
  transfers between devices with their start and end apart: 14 -> 14, of which waited for: 7 -> 8; matrix products, arithmetic and copies ran while one was open for 5% -> 4% of each run, Pallas kernels for 2% -> 2%
where the time goes in v5:
time: 166 us; the launch traced here: 164 us
  starting transfers between devices  68 us (41%)
  waiting for transfers between devices  52.3 us (32%)
  Pallas kernels  18.7 us (11%)
  blocking collectives  15.8 us (10%)
  local copies, waits for them, and re-layouts  8.12 us (5%)
    all_to_all x1, waiting for transfers between devices, device_body(): got = lax.all_to_all(payload, 'A', 0, 0, tiled=True)  16.3 us
    all_to_all x1, blocking collectives, device_body(): heads = lax.all_to_all(mixed.reshape(4, 128, DK), 'B', 0, 0, tiled=True)  15.8 us
    all_to_all x1, starting transfers between devices, device_body(): rows_z = lax.all_to_all(cut, ('A', 'B'), 0, 0, tiled=True)  15.2 us
    ppermute x3, waiting for transfers between devices, device_body(): near.append(lax.ppermute(rows, 'B', [(b, b ^ j) for b in range(4)]))  14.2 us
    ppermute x3, starting transfers between devices, device_body(): near.append(lax.ppermute(rows, 'B', [(b, b ^ j) for b in range(4)]))  10.1 us
    ppermute x1, waiting for transfers between devices, device_body(): plus = lax.ppermute(own, 'tp', down_shift)  10 us
    all_to_all x1, starting transfers between devices, device_body(): got = lax.all_to_all(payload, 'A', 0, 0, tiled=True)  9.17 us
    pallas_call x1, Pallas kernels, device_body(): pl.pallas_call(project_kernel, out_shape=(sds((4, PAYLOAD, DK), bf16), sd...  8.21 us
  transfers between devices with their start and end apart: 14, of which 8 were waited for; matrix products, arithmetic and copies ran while one was open for 4% of the time, Pallas kernels for 2%

profile of v5, /device:TPU:6, one launch (start us, length us, event | category | flops | bytes accessed | tf_op | source)
XLA Modules:
  0.0 164.1 jit_solution(5712550407243619523)
XLA Ops:
  0.0 2.2 %pack.1 = (bf16[36,2048]{1,0:T(8,128)(2,1)}, bf16[16,16,512]{2,1,0:T(8,128)(2,1)}) custom-call(bf16[32,2048]{1,0:T(8,128)(2,1)} %lat_ref.1, bf16[16,2048]{1,0:T(8,128)(2,1)} %ctx_ref.1, f32[1,2048]{1,0:T(1,128)} %sv_ref.1, f32[1,2048]{1,0:T(1,128)} %cv_ref.1, bf16[96,2048]{1,0:T(8,128)(2,1)} %bitcast.29, bf16[128,256]{1,0:T(8,128)(2,1)} %wq_ref.1, ...), custom_call_target="tpu_custom_call" | custom-call | tf_op jit(solution)/shard_map/pack/pallas_call | solution.py:306
  2.2 15.2 %all-to-all-start = ((bf16[16,16,512]{2,1,0:T(8,128)(2,1)}), bf16[16,16,512]{2,1,0:T(8,128)(2,1)S(1)}, u32[]{:S(2)}, u32[]{:S(2)}) async-start(bf16[16,16,512]{2,1,0:T(8,128)(2,1)} %get-tuple-element.15), calls=%async_computation | async-start | bytes 524288 | tf_op jit(solution)/shard_map/all_to_all | solution.py:319
  17.4 3.8 %collective-permute-start.2 = (bf16[36,2048]{1,0:T(8,128)(2,1)}, bf16[36,2048]{1,0:T(8,128)(2,1)S(1)}, u32[]{:S(2)}, u32[]{:S(2)}) collective-permute-start(bf16[36,2048]{1,0:T(8,128)(2,1)} %get-tuple-element.16), channel_id=1, source_target_pairs={{0,32},{32,0},{64,96},{96,64},{1,33},{33,1},{65,97},{97,65},{2,34}... | collective-permute-start | bytes 442376 | tf_op jit(solution)/shard_map/ppermute | solution.py:318
  21.2 4.3 %collective-permute-start.3 = (bf16[36,2048]{1,0:T(8,128)(2,1)}, bf16[36,2048]{1,0:T(8,128)(2,1)S(1)}, u32[]{:S(2)}, u32[]{:S(2)}) collective-permute-start(bf16[36,2048]{1,0:T(8,128)(2,1)} %get-tuple-element.16), channel_id=1, source_target_pairs={{0,64},{32,96},{64,0},{96,32},{1,65},{33,97},{65,1},{97,33},{2,66}... | collective-permute-start | bytes 442376 | tf_op jit(solution)/shard_map/ppermute | solution.py:318
  25.5 2.0 %collective-permute-start.4 = (bf16[36,2048]{1,0:T(8,128)(2,1)}, bf16[36,2048]{1,0:T(8,128)(2,1)S(1)}, u32[]{:S(2)}, u32[]{:S(2)}) collective-permute-start(bf16[36,2048]{1,0:T(8,128)(2,1)} %get-tuple-element.16), channel_id=1, source_target_pairs={{0,96},{32,64},{64,32},{96,0},{1,97},{33,65},{65,33},{97,1},{2,98}... | collective-permute-start | bytes 442376 | tf_op jit(solution)/shard_map/ppermute | solution.py:318
  27.5 0.9 slice.117
  28.4 0.8 slice.121
  29.2 8.7 %collective-permute-done.2 = bf16[36,2048]{1,0:T(8,128)(2,1)S(1)} collective-permute-done((bf16[36,2048]{1,0:T(8,128)(2,1)}, bf16[36,2048]{1,0:T(8,128)(2,1)S(1)}, u32[]{:S(2)}, u32[]{:S(2)}) %collective-permute-start.2) | collective-permute-done | bytes 147488 | tf_op jit(solution)/shard_map/ppermute | solution.py:318
  37.9 5.5 %collective-permute-done.3 = bf16[36,2048]{1,0:T(8,128)(2,1)S(1)} collective-permute-done((bf16[36,2048]{1,0:T(8,128)(2,1)}, bf16[36,2048]{1,0:T(8,128)(2,1)S(1)}, u32[]{:S(2)}, u32[]{:S(2)}) %collective-permute-start.3) | collective-permute-done | bytes 147488 | tf_op jit(solution)/shard_map/ppermute | solution.py:318
  43.4 0.0 collective-permute-done.4
  43.5 0.1 concatenate.3.own_ref
  43.6 4.9 %collective-permute-start.6 = (bf16[144,2048]{1,0:T(8,128)(2,1)S(1)}, bf16[144,2048]{1,0:T(8,128)(2,1)S(1)}, u32[]{:S(2)}, u32[]{:S(2)}) collective-permute-start(bf16[144,2048]{1,0:T(8,128)(2,1)S(1)} %concatenate.3.own_ref), channel_id=1, source_target_pairs={{0,24},{8,0},{16,8},{24,16},{1,25},{9,1},{17,9},{25,17},{2,26},{10... | collective-permute-start | bytes 1769480 | tf_op jit(solution)/shard_map/ppermute | solution.py:344
  48.5 1.9 %collective-permute-start.5 = (bf16[144,2048]{1,0:T(8,128)(2,1)S(1)}, bf16[144,2048]{1,0:T(8,128)(2,1)S(1)}, u32[]{:S(2)}, u32[]{:S(2)}) collective-permute-start(bf16[144,2048]{1,0:T(8,128)(2,1)S(1)} %concatenate.3.own_ref), channel_id=1, source_target_pairs={{0,8},{8,16},{16,24},{24,0},{1,9},{9,17},{17,25},{25,1},{2,10},{10... | collective-permute-start | bytes 1769480 | tf_op jit(solution)/shard_map/ppermute | solution.py:343
  50.5 10.0 %collective-permute-done.6.plus_ref = bf16[144,2048]{1,0:T(8,128)(2,1)S(1)} collective-permute-done((bf16[144,2048]{1,0:T(8,128)(2,1)S(1)}, bf16[144,2048]{1,0:T(8,128)(2,1)S(1)}, u32[]{:S(2)}, u32[]{:S(2)}) %collective-permute-start.6) | collective-permute-done | bytes 589856 | tf_op jit(solution)/shard_map/ppermute | solution.py:344
  60.5 5.6 %collective-permute-start.8 = (bf16[80,2048]{1,0:T(8,128)(2,1)S(1)}, bf16[80,2048]{1,0:T(8,128)(2,1)S(1)}, u32[]{:S(2)}, u32[]{:S(2)}) collective-permute-start(bf16[80,2048]{1,0:T(8,128)(2,1)S(1)} %slice.156), channel_id=1, source_target_pairs={{0,24},{8,0},{16,8},{24,16},{1,25},{9,1},{17,9},{25,17},{2,26},{10... | collective-permute-start | bytes 983048 | tf_op jit(solution)/shard_map/ppermute | solution.py:346
  66.1 0.0 collective-permute-done.5.minus_ref
  66.1 0.8 slice.155
  66.9 1.9 %collective-permute-start.7 = (bf16[64,2048]{1,0:T(8,128)(2,1)}, bf16[64,2048]{1,0:T(8,128)(2,1)}, u32[]{:S(2)}, u32[]{:S(2)}) collective-permute-start(bf16[64,2048]{1,0:T(8,128)(2,1)} %slice.155), channel_id=1, source_target_pairs={{0,8},{8,16},{16,24},{24,0},{1,9},{9,17},{17,25},{25,1},{2,10},{10... | collective-permute-start | bytes 786440 | tf_op jit(solution)/shard_map/ppermute | solution.py:345
  68.8 0.0 all-to-all-done
  68.8 0.6 slice_bitcast_fusion.2
  69.5 1.9 %collective-permute-start = (bf16[16,8,128]{2,1,0:T(8,128)(2,1)}, bf16[16,8,128]{2,1,0:T(8,128)(2,1)S(1)}, u32[]{:S(2)}, u32[]{:S(2)}) collective-permute-start(bf16[16,8,128]{2,1,0:T(8,128)(2,1)} %get-tuple-element.31), channel_id=1, source_target_pairs={{0,8},{8,0},{16,24},{24,16},{1,9},{9,1},{17,25},{25,17},{2,10},{10... | collective-permute-start | bytes 98312 | tf_op jit(solution)/shard_map/ppermute | solution.py:324
  71.4 1.0 broadcast_in_dim.2
  72.4 4.8 %all-to-all-start.1 = ((bf16[4,16,16,384]{3,2,1,0:T(8,128)(2,1)}), bf16[4,16,16,384]{3,2,1,0:T(8,128)(2,1)S(1)}, u32[]{:S(2)}, u32[]{:S(2)}) async-start(bf16[4,16,16,384]{3,2,1,0:T(8,128)(2,1)} %broadcast_in_dim.2), calls=%async_computation.1 | async-start | bytes 1572864 | tf_op jit(solution)/shard_map/all_to_all | solution.py:28
  77.2 0.7 slice.158.ride_ref
  77.8 0.0 collective-permute-done
  77.8 5.1 %collective-permute-start.1 = (bf16[2,16,8,128]{3,2,1,0:T(8,128)(2,1)S(1)}, bf16[2,16,8,128]{3,2,1,0:T(8,128)(2,1)S(1)}, u32[]{:S(2)}, u32[]{:S(2)}) collective-permute-start(bf16[2,16,8,128]{3,2,1,0:T(8,128)(2,1)S(1)} %pad_maximum_fusion), channel_id=1, source_target_pairs={{0,24},{8,16},{16,8},{24,0},{1,25},{9,17},{17,9},{25,1},{2,26},{10... | collective-permute-start | bytes 196616 | tf_op jit(solution)/shard_map/ppermute | solution.py:326
  83.0 2.2 %collective-permute-done.1 = bf16[2,16,8,128]{3,2,1,0:T(8,128)(2,1)S(1)} collective-permute-done((bf16[2,16,8,128]{3,2,1,0:T(8,128)(2,1)S(1)}, bf16[2,16,8,128]{3,2,1,0:T(8,128)(2,1)S(1)}, u32[]{:S(2)}, u32[]{:S(2)}) %collective-permute-start.1) | collective-permute-done | bytes 65568 | tf_op jit(solution)/shard_map/ppermute | solution.py:326
  85.2 0.5 all-to-all-done.1.mine_ref
  85.7 1.9 %collective-permute-start.9 = (bf16[4,16,16,384]{3,2,1,0:T(8,128)(2,1)S(1)}, bf16[4,16,16,384]{3,2,1,0:T(8,128)(2,1)S(1)}, u32[]{:S(2)}, u32[]{:S(2)}) collective-permute-start(bf16[4,16,16,384]{3,2,1,0:T(8,128)(2,1)S(1)} %all-to-all-done.1.mine_ref), channel_id=1, source_target_pairs={{0,1},{1,0},{2,3},{3,2},{4,5},{5,4},{6,7},{7,6},{8,9},{9,8},{10,11... | collective-permute-start | bytes 2359304 | tf_op jit(solution)/shard_map/ppermute | solution.py:321
  87.6 0.1 select_bitcast_fusion.3
  87.8 0.7 reshape.20.mod_ref
  88.6 0.0 collective-permute-done.7.low_ref
  88.6 0.0 collective-permute-done.8.high_ref
  88.6 1.3 collective-permute-done.9.other_ref
  89.9 0.9 copy-done.5
  90.8 8.2 %project.1 = (bf16[4,336,128]{2,1,0:T(8,128)(2,1)}, bf16[512,128]{1,0:T(8,128)(2,1)}, bf16[512,128]{1,0:T(8,128)(2,1)}, bf16[512,128]{1,0:T(8,128)(2,1)}, f32[2,512,128]{2,1,0:T(8,128)}) custom-call(bf16[144,2048]{1,0:T(8,128)(2,1)} %copy-done.1, bf16[144,2048]{1,0:T(8,128)(2,1)} %copy-done.4, bf16[144,2048]{1,0:T(8,128)(2,1)} %copy-done.2, ...), custom_call_target="tpu_custom_call" | custom-call | tf_op jit(solution)/shard_map/project/pallas_call | solution.py:348
  99.0 9.2 %all-to-all-start.2 = ((bf16[4,336,128]{2,1,0:T(8,128)(2,1)}), bf16[4,336,128]{2,1,0:T(8,128)(2,1)S(1)}, u32[]{:S(2)}, u32[]{:S(2)}) async-start(bf16[4,336,128]{2,1,0:T(8,128)(2,1)} %get-tuple-element.17), calls=%async_computation.2 | async-start | bytes 688128 | tf_op jit(solution)/shard_map/all_to_all | solution.py:365
  108.2 3.0 %local.1 = (f32[512,128]{1,0:T(8,128)}, bf16[512,128]{1,0:T(8,128)(2,1)}, bf16[512,128]{1,0:T(8,128)(2,1)}) custom-call(bf16[512,128]{1,0:T(8,128)(2,1)} %get-tuple-element.18.q_ref, bf16[512,128]{1,0:T(8,128)(2,1)} %get-tuple-element.19.k_ref, bf16[512,128]{1,0:T(8,128)(2,1)} %get-tuple-element.20.v_ref, f32[2,512,128]{2,1,0:T(8,128)} %get-tuple-element.21.cum_ref), custom_call_target="tpu_custom_call" | custom-call | tf_op jit(solution)/shard_map/local/pallas_call | solution.py:366
  111.2 16.3 %all-to-all-done.2.in_ref = bf16[4,336,128]{2,1,0:T(8,128)(2,1)S(1)} async-done(((bf16[4,336,128]{2,1,0:T(8,128)(2,1)}), bf16[4,336,128]{2,1,0:T(8,128)(2,1)S(1)}, u32[]{:S(2)}, u32[]{:S(2)}) %all-to-all-start.2) | async-done | bytes 344096 | tf_op jit(solution)/shard_map/all_to_all | solution.py:365
  127.6 0.7 copy-done.3
  128.3 2.3 %combine.1 = bf16[512,128]{1,0:T(8,128)(2,1)} custom-call(bf16[4,336,128]{2,1,0:T(8,128)(2,1)} %copy-done.3, f32[512,128]{1,0:T(8,128)} %get-tuple-element.22.o_ref, bf16[512,128]{1,0:T(8,128)(2,1)} %get-tuple-element.23.lift_f_ref, bf16[512,128]{1,0:T(8,128)(2,1)} %get-tuple-element.24.lift_b_ref), custom_call_target="tpu_custom_call" | custom-call | tf_op jit(solution)/shard_map/combine/pallas_call | solution.py:373
  130.5 15.8 %all_to_all.25.mix_ref = bf16[4,128,128]{2,1,0:T(8,128)(2,1)} all-to-all(bf16[4,128,128]{2,1,0:T(8,128)(2,1)} %bitcast.28), channel_id=1, replica_groups=mesh['A'=4,'B'=4,'tp'=4,'x'=4,'core'=2] {'B'}, dimensions={0} | all-to-all | bytes 262144 | tf_op jit(solution)/shard_map/all_to_all | solution.py:380
  146.3 3.0 %output.1 = bf16[128,2048]{1,0:T(8,128)(2,1)} custom-call(bf16[4,128,128]{2,1,0:T(8,128)(2,1)} %all_to_all.25.mix_ref, f32[1,256]{1,0:T(1,128)} %bitcast.35, bf16[512,2048]{1,0:T(8,128)(2,1)} %w_ref.1), custom_call_target="tpu_custom_call" | custom-call | tf_op jit(solution)/shard_map/output/pallas_call | solution.py:381
  149.3 5.4 %all-to-all-start.4 = ((bf16[4,32,2048]{2,1,0:T(8,128)(2,1)}), bf16[4,32,2048]{2,1,0:T(8,128)(2,1)S(1)}, u32[]{:S(2)}, u32[]{:S(2)}) async-start(bf16[4,32,2048]{2,1,0:T(8,128)(2,1)} %bitcast.27), calls=%async_computation.4 | async-start | bytes 1048576 | tf_op jit(solution)/shard_map/all_to_all | solution.py:388
  154.8 0.7 slice.148
  155.5 7.8 %all-to-all-done.4 = bf16[4,32,2048]{2,1,0:T(8,128)(2,1)S(1)} async-done(((bf16[4,32,2048]{2,1,0:T(8,128)(2,1)}), bf16[4,32,2048]{2,1,0:T(8,128)(2,1)S(1)}, u32[]{:S(2)}, u32[]{:S(2)}) %all-to-all-start.4) | async-done | bytes 524320 | tf_op jit(solution)/shard_map/all_to_all | solution.py:388
  163.3 0.1 reduce_sum.12
  163.4 0.7 add_convert_fusion
  (30 shorter events, 0.3 us)
Async XLA Ops:
  2.2 66.6 %all-to-all-start = ((bf16[16,16,512]{2,1,0:T(8,128)(2,1)}), bf16[16,16,512]{2,1,0:T(8,128)(2,1)S(1)}, u32[]{:S(2)}, u32[]{:S(2)}) async-start(bf16[16,16,512]{2,1,0:T(8,128)(2,1)} %get-tuple-element.15), calls=%async_computation | async-start | bytes 524288 | tf_op jit(solution)/shard_map/all_to_all | solution.py:319
  17.4 20.5 %collective-permute-start.2 = (bf16[36,2048]{1,0:T(8,128)(2,1)}, bf16[36,2048]{1,0:T(8,128)(2,1)S(1)}, u32[]{:S(2)}, u32[]{:S(2)}) collective-permute-start(bf16[36,2048]{1,0:T(8,128)(2,1)} %get-tuple-element.16), channel_id=1, source_target_pairs={{0,32},{32,0},{64,96},{96,64},{1,33},{33,1},{65,97},{97,65},{2,34}... | collective-permute-start | bytes 442376 | tf_op jit(solution)/shard_map/ppermute | solution.py:318
  21.2 22.2 %collective-permute-start.3 = (bf16[36,2048]{1,0:T(8,128)(2,1)}, bf16[36,2048]{1,0:T(8,128)(2,1)S(1)}, u32[]{:S(2)}, u32[]{:S(2)}) collective-permute-start(bf16[36,2048]{1,0:T(8,128)(2,1)} %get-tuple-element.16), channel_id=1, source_target_pairs={{0,64},{32,96},{64,0},{96,32},{1,65},{33,97},{65,1},{97,33},{2,66}... | collective-permute-start | bytes 442376 | tf_op jit(solution)/shard_map/ppermute | solution.py:318
  25.5 17.9 %collective-permute-start.4 = (bf16[36,2048]{1,0:T(8,128)(2,1)}, bf16[36,2048]{1,0:T(8,128)(2,1)S(1)}, u32[]{:S(2)}, u32[]{:S(2)}) collective-permute-start(bf16[36,2048]{1,0:T(8,128)(2,1)} %get-tuple-element.16), channel_id=1, source_target_pairs={{0,96},{32,64},{64,32},{96,0},{1,97},{33,65},{65,33},{97,1},{2,98}... | collective-permute-start | bytes 442376 | tf_op jit(solution)/shard_map/ppermute | solution.py:318
  43.6 28.8 %copy-start.1 = (bf16[144,2048]{1,0:T(8,128)(2,1)}, bf16[144,2048]{1,0:T(8,128)(2,1)S(1)}, u32[]{:S(2)}) copy-start(bf16[144,2048]{1,0:T(8,128)(2,1)S(1)} %concatenate.3.own_ref) | copy-start | bytes 1769476
  43.6 16.9 %collective-permute-start.6 = (bf16[144,2048]{1,0:T(8,128)(2,1)S(1)}, bf16[144,2048]{1,0:T(8,128)(2,1)S(1)}, u32[]{:S(2)}, u32[]{:S(2)}) collective-permute-start(bf16[144,2048]{1,0:T(8,128)(2,1)S(1)} %concatenate.3.own_ref), channel_id=1, source_target_pairs={{0,24},{8,0},{16,8},{24,16},{1,25},{9,1},{17,9},{25,17},{2,26},{10... | collective-permute-start | bytes 1769480 | tf_op jit(solution)/shard_map/ppermute | solution.py:344
  48.5 17.6 %collective-permute-start.5 = (bf16[144,2048]{1,0:T(8,128)(2,1)S(1)}, bf16[144,2048]{1,0:T(8,128)(2,1)S(1)}, u32[]{:S(2)}, u32[]{:S(2)}) collective-permute-start(bf16[144,2048]{1,0:T(8,128)(2,1)S(1)} %concatenate.3.own_ref), channel_id=1, source_target_pairs={{0,8},{8,16},{16,24},{24,0},{1,9},{9,17},{17,25},{25,1},{2,10},{10... | collective-permute-start | bytes 1769480 | tf_op jit(solution)/shard_map/ppermute | solution.py:343
  60.5 11.9 %copy-start.2 = (bf16[144,2048]{1,0:T(8,128)(2,1)}, bf16[144,2048]{1,0:T(8,128)(2,1)S(1)}, u32[]{:S(2)}) copy-start(bf16[144,2048]{1,0:T(8,128)(2,1)S(1)} %collective-permute-done.6.plus_ref) | copy-start | bytes 1769476
  60.5 28.1 %collective-permute-start.8 = (bf16[80,2048]{1,0:T(8,128)(2,1)S(1)}, bf16[80,2048]{1,0:T(8,128)(2,1)S(1)}, u32[]{:S(2)}, u32[]{:S(2)}) collective-permute-start(bf16[80,2048]{1,0:T(8,128)(2,1)S(1)} %slice.156), channel_id=1, source_target_pairs={{0,24},{8,0},{16,8},{24,16},{1,25},{9,1},{17,9},{25,17},{2,26},{10... | collective-permute-start | bytes 983048 | tf_op jit(solution)/shard_map/ppermute | solution.py:346
  66.1 21.5 %copy-start.4 = (bf16[144,2048]{1,0:T(8,128)(2,1)}, bf16[144,2048]{1,0:T(8,128)(2,1)S(1)}, u32[]{:S(2)}) copy-start(bf16[144,2048]{1,0:T(8,128)(2,1)S(1)} %collective-permute-done.5.minus_ref) | copy-start | bytes 1769476
  66.9 21.7 %collective-permute-start.7 = (bf16[64,2048]{1,0:T(8,128)(2,1)}, bf16[64,2048]{1,0:T(8,128)(2,1)}, u32[]{:S(2)}, u32[]{:S(2)}) collective-permute-start(bf16[64,2048]{1,0:T(8,128)(2,1)} %slice.155), channel_id=1, source_target_pairs={{0,8},{8,16},{16,24},{24,0},{1,9},{9,17},{17,25},{25,1},{2,10},{10... | collective-permute-start | bytes 786440 | tf_op jit(solution)/shard_map/ppermute | solution.py:345
  69.5 8.4 %collective-permute-start = (bf16[16,8,128]{2,1,0:T(8,128)(2,1)}, bf16[16,8,128]{2,1,0:T(8,128)(2,1)S(1)}, u32[]{:S(2)}, u32[]{:S(2)}) collective-permute-start(bf16[16,8,128]{2,1,0:T(8,128)(2,1)} %get-tuple-element.31), channel_id=1, source_target_pairs={{0,8},{8,0},{16,24},{24,16},{1,9},{9,1},{17,25},{25,17},{2,10},{10... | collective-permute-start | bytes 98312 | tf_op jit(solution)/shard_map/ppermute | solution.py:324
  72.4 13.3 %all-to-all-start.1 = ((bf16[4,16,16,384]{3,2,1,0:T(8,128)(2,1)}), bf16[4,16,16,384]{3,2,1,0:T(8,128)(2,1)S(1)}, u32[]{:S(2)}, u32[]{:S(2)}) async-start(bf16[4,16,16,384]{3,2,1,0:T(8,128)(2,1)} %broadcast_in_dim.2), calls=%async_computation.1 | async-start | bytes 1572864 | tf_op jit(solution)/shard_map/all_to_all | solution.py:28
  77.8 7.4 %collective-permute-start.1 = (bf16[2,16,8,128]{3,2,1,0:T(8,128)(2,1)S(1)}, bf16[2,16,8,128]{3,2,1,0:T(8,128)(2,1)S(1)}, u32[]{:S(2)}, u32[]{:S(2)}) collective-permute-start(bf16[2,16,8,128]{3,2,1,0:T(8,128)(2,1)S(1)} %pad_maximum_fusion), channel_id=1, source_target_pairs={{0,24},{8,16},{16,8},{24,0},{1,25},{9,17},{17,9},{25,1},{2,26},{10... | collective-permute-start | bytes 196616 | tf_op jit(solution)/shard_map/ppermute | solution.py:326
  85.7 4.2 %copy-start = (bf16[4,16,16,384]{3,2,1,0:T(8,128)(2,1)}, bf16[4,16,16,384]{3,2,1,0:T(8,128)(2,1)S(1)}, u32[]{:S(2)}) copy-start(bf16[4,16,16,384]{3,2,1,0:T(8,128)(2,1)S(1)} %all-to-all-done.1.mine_ref) | copy-start | bytes 2359300
  85.7 4.2 %collective-permute-start.9 = (bf16[4,16,16,384]{3,2,1,0:T(8,128)(2,1)S(1)}, bf16[4,16,16,384]{3,2,1,0:T(8,128)(2,1)S(1)}, u32[]{:S(2)}, u32[]{:S(2)}) collective-permute-start(bf16[4,16,16,384]{3,2,1,0:T(8,128)(2,1)S(1)} %all-to-all-done.1.mine_ref), channel_id=1, source_target_pairs={{0,1},{1,0},{2,3},{3,2},{4,5},{5,4},{6,7},{7,6},{8,9},{9,8},{10,11... | collective-permute-start | bytes 2359304 | tf_op jit(solution)/shard_map/ppermute | solution.py:321
  88.6 1.3 copy-start.7
  89.8 0.9 copy-start.5
  99.0 28.6 %all-to-all-start.2 = ((bf16[4,336,128]{2,1,0:T(8,128)(2,1)}), bf16[4,336,128]{2,1,0:T(8,128)(2,1)S(1)}, u32[]{:S(2)}, u32[]{:S(2)}) async-start(bf16[4,336,128]{2,1,0:T(8,128)(2,1)} %get-tuple-element.17), calls=%async_computation.2 | async-start | bytes 688128 | tf_op jit(solution)/shard_map/all_to_all | solution.py:365
  127.6 0.7 copy-start.3
  146.3 17.1 %copy-start.6 = (bf16[32,2048]{1,0:T(8,128)(2,1)S(1)}, bf16[32,2048]{1,0:T(8,128)(2,1)}, u32[]{:S(2)}) copy-start(bf16[32,2048]{1,0:T(8,128)(2,1)} %lat_ref.1) | copy-start | bytes 393220
  149.3 14.0 %all-to-all-start.4 = ((bf16[4,32,2048]{2,1,0:T(8,128)(2,1)}), bf16[4,32,2048]{2,1,0:T(8,128)(2,1)S(1)}, u32[]{:S(2)}, u32[]{:S(2)}) async-start(bf16[4,32,2048]{2,1,0:T(8,128)(2,1)} %bitcast.27), calls=%async_computation.4 | async-start | bytes 1048576 | tf_op jit(solution)/shard_map/all_to_all | solution.py:388

commit v6 on v4

--- a/solution.py
+++ b/solution.py
@@ -56,38 +56,67 @@
     return lax.dot_general(a, b, (((0,), (0,)), ((), ())), preferred_element_type=f32)
 
 
-def pack_kernel(
-    lat_ref, ctx_ref, sv_ref, cv_ref, mod_ref, wq_ref, wk_ref, wv_ref, extra_ref, rows_ref, cut_ref
-):
+def rows_kernel(lat_ref, ctx_ref, sv_ref, cv_ref, mod_ref, rows_ref, mods_ref):
     y = lax.axis_index("tp")
-    dp = lax.axis_index("x") * 2 + lax.axis_index("core")
     rows_ref[0:32, :] = lat_ref[...]
     ctx = ctx_ref[...].astype(f32)
     picked = ctx[12:16]
     for i in range(3):
         picked = jnp.where(y == i, ctx[4 * i : 4 * i + 4], picked)
     rows_ref[32:36, :] = picked.astype(bf16)
-
     both = jnp.concatenate([sv_ref[...], cv_ref[...]], axis=0)
     conditions = (both / (1.0 + jnp.exp(-both))).astype(bf16)
     local_mods = nt(conditions, mod_ref[...])
-    mods = jnp.concatenate([p.astype(f32) for p in three_parts(local_mods)], axis=0)
-    mods = jnp.concatenate([mods, jnp.zeros((6, 32), f32)], axis=1)
-    extra = jnp.concatenate([p.astype(f32) for p in three_parts(extra_ref[...])[:2]], axis=0)
-    riding = jnp.concatenate([mods, extra, jnp.zeros((2, 128), f32)], axis=0).astype(bf16)
+    for i in range(4):
+        mods_ref[i] = local_mods
+
+
+def pack_kernel(mods_ref, wq_ref, wk_ref, wv_ref, extra_ref, cut_ref):
+    dp = lax.axis_index("x") * 2 + lax.axis_index("core")
+    mods = jnp.concatenate([mods_ref[i] for i in range(4)], axis=1)
+    hi, mid, _ = three_parts(mods)
+    pieces = [p[:, 128 * j : 128 * (j + 1)].astype(f32) for p in (hi, mid) for j in range(3)]
+    e_hi, e_mid, _ = three_parts(extra_ref[...])
+    e_hi, e_mid = e_hi.astype(f32), e_mid.astype(f32)
+    riding = []
+    for h in range(2):
+        added = [e_hi[h : h + 1], e_mid[h : h + 1], e_hi[2 + h : 3 + h], e_mid[2 + h : 3 + h]]
+        riding.append(jnp.concatenate([*pieces, *added], axis=0).astype(bf16))
     mine = pl.ds(pl.multiple_of(dp * 16, 16), 16)
     for d in range(16):
         b = d % 4
-        cut_ref[d, :, 0:128] = wq_ref[mine, (b // 2) * 128 : (b // 2 + 1) * 128]
-        cut_ref[d, :, 128:256] = wk_ref[mine, (b // 2) * 128 : (b // 2 + 1) * 128]
+        h = b // 2
+        cut_ref[d, :, 0:128] = wq_ref[mine, h * 128 : (h + 1) * 128]
+        cut_ref[d, :, 128:256] = wk_ref[mine, h * 128 : (h + 1) * 128]
         cut_ref[d, :, 256:384] = wv_ref[mine, b * 128 : (b + 1) * 128]
-        cut_ref[d, :, 384:512] = riding
+        cut_ref[d, :, 384:512] = riding[h]
+
+
+def normed_rows(rows, which, mod_ref, gain_ref):
+    v = rows.astype(f32)
+    r = lax.rsqrt(jnp.mean(v * v, axis=-1, keepdims=True) + EPS)
+    scale = gain_ref[...] * (1.0 + mod_ref[which : which + 1, D : 2 * D])
+    return (v * r * scale + mod_ref[which : which + 1, 0:D]).astype(bf16)
+
+
+def hidden_kernel(own_ref, minus_ref, plus_ref, ride_ref, gain_ref, h_ref, mod_ref):
+    for z in range(16):
+        r = ride_ref[z].astype(f32)
+        for j in range(3):
+            both = r[2 * j : 2 * j + 2] + r[6 + 2 * j : 8 + 2 * j]
+            mod_ref[:, (z * 3 + j) * 128 : (z * 3 + j + 1) * 128] = both
+    for slot, ref in enumerate((own_ref, minus_ref, plus_ref)):
+        for j in range(4):
+            at = slot * 144 + j * 32
+            h_ref[at : at + 32, :] = normed_rows(ref[j * 32 : j * 32 + 32, :], 0, mod_ref, gain_ref)
+        at = slot * 144 + 128
+        h_ref[at : at + 16, :] = normed_rows(ref[128:144, :], 1, mod_ref, gain_ref)
 
 
 def project_kernel(
-    own_ref, minus_ref, plus_ref, low_ref, high_ref, mod_ref, gain_ref, mine_ref, other_ref,
+    h_ref, low_ref, high_ref, mod_ref, gain_ref, mine_ref, other_ref,
     down_ref, up_ref, bias_ref, ride_ref,
-    pay_ref, q_ref, k_ref, v_ref, cum_ref, h_ref, w_ref,
+    pay_ref, q_ref, k_ref, v_ref, cum_ref, far_ref, w_ref, out_ref,
 ):
     seg, sub = lax.axis_index("A"), lax.axis_index("B")
     y, core = lax.axis_index("tp"), lax.axis_index("core")
@@ -99,32 +128,25 @@
             there = pl.ds(pl.multiple_of(at + 16 - core * 16, 16), 16)
             w_ref[here, :] = mine_ref[xi, z]
             w_ref[there, :] = other_ref[xi, z]
-
-    def normed_rows(rows, which):
-        v = rows.astype(f32)
-        r = lax.rsqrt(jnp.mean(v * v, axis=-1, keepdims=True) + EPS)
-        scale = gain_ref[...] * (1.0 + mod_ref[which : which + 1, D : 2 * D])
-        return (v * r * scale + mod_ref[which : which + 1, 0:D]).astype(bf16)
-
+    for j in range(4):
+        rows = (low_ref, high_ref)[j // 2][(j % 2) * 32 : (j % 2) * 32 + 32, :]
+        far_ref[j * 32 : j * 32 + 32, :] = normed_rows(rows, 0, mod_ref, gain_ref)
+    far_ref[128:144, :] = normed_rows(high_ref[64:80, :], 1, mod_ref, gain_ref)
     y_of = [y, (y + 3) % 4, (y + 1) % 4, (y + 2) % 4]
-    for slot in range(4):
-        for j in range(4):
-            if slot < 3:
-                rows = (own_ref, minus_ref, plus_ref)[slot][j * 32 : j * 32 + 32, :]
-            elif j < 2:
-                rows = low_ref[j * 32 : j * 32 + 32, :]
-            else:
-                rows = high_ref[(j - 2) * 32 : (j - 2) * 32 + 32, :]
-            at = pl.multiple_of((sub ^ j) * 128 + y_of[slot] * 32, 32)
-            h_ref[pl.ds(at, 32), :] = normed_rows(rows, 0)
-        rows = (own_ref, minus_ref, plus_ref)[slot][128:144, :] if slot < 3 else high_ref[64:80, :]
-        h_ref[SEG + slot * 16 : SEG + slot * 16 + 16, :] = normed_rows(rows, 1)
-
-    out = jnp.dot(h_ref[...], w_ref[...], preferred_element_type=f32).astype(bf16)
+    for first, rows in ((0, h_ref[...]), (3, far_ref[...])):
+        res = jnp.dot(rows, w_ref[...], preferred_element_type=f32).astype(bf16)
+        res = jnp.concatenate([res, nt(rows, down_ref[...]).astype(bf16)], axis=1)
+        for n in range(rows.shape[0] // 144):
+            for j in range(4):
+                at = pl.multiple_of((sub ^ j) * 128 + y_of[first + n] * 32, 32)
+                out_ref[pl.ds(at, 32), 0:448] = res[n * 144 + j * 32 : n * 144 + j * 32 + 32]
+            at = SEG + (first + n) * 16
+            out_ref[at : at + 16, 0:448] = res[n * 144 + 128 : n * 144 + 144]
+    out = out_ref[:, 0:448]
     q_ref[...] = out[:SEG, 0:128]
     k_ref[...] = out[:SEG, 128:256]
     v_ref[...] = out[:SEG, 256:384]
-    low = nt(h_ref[...], down_ref[...]).astype(bf16)
+    low = out[:, 384:448]
 
     def of_head(a):
         return jnp.where(second, a[:, 128:256].astype(f32), a[:, 0:128].astype(f32))
@@ -139,8 +161,8 @@
     ef, eb = [], []
     for zb in range(4):
         t = jnp.transpose(ride_ref[seg * 4 + zb].astype(f32))
-        ef.append(jnp.where(second, t[:, 7:8] + t[:, 11:12], t[:, 6:7] + t[:, 10:11]))
-        eb.append(jnp.where(second, t[:, 9:10] + t[:, 13:14], t[:, 8:9] + t[:, 12:13]))
+        ef.append(t[:, 12:13] + t[:, 13:14])
+        eb.append(t[:, 14:15] + t[:, 15:16])
     ef = jnp.concatenate(ef, axis=0)
     eb = jnp.concatenate(eb, axis=0)
     af = logs[:SEG, 0:128] + ef
@@ -301,40 +323,32 @@
     head_gain,
     out_weight,
 ):
-    y = lax.axis_index("tp")
     sds = jax.ShapeDtypeStruct
-    rows, cut = pl.pallas_call(
-        pack_kernel,
-        out_shape=(sds((36, D), bf16), sds((16, 16, 512), bf16)),
-        in_specs=[VM] * 9,
+    rows, mods = pl.pallas_call(
+        rows_kernel,
+        out_shape=(sds((36, D), bf16), sds((4, 2, 96), f32)),
+        in_specs=[VM] * 5,
         out_specs=(VM, VM),
-        name="pack",
-    )(
-        latents, context, sample_vector, context_vector, modulator.T,
-        query_weight, key_weight, value_weight, jnp.moveaxis(decay_extra, 1, 2).reshape(4, 128),
-    )
+        name="rows",
+    )(latents, context, sample_vector, context_vector, modulator.T)
+    mods = lax.all_to_all(mods, "tp", 0, 0, tiled=True)
     near = [rows]
     for j in range(1, 4):
         near.append(lax.ppermute(rows, "B", [(b, b ^ j) for b in range(4)]))
+    cut = pl.pallas_call(
+        pack_kernel,
+        out_shape=sds((16, 16, 512), bf16),
+        in_specs=[VM] * 5,
+        out_specs=VM,
+        name="pack",
+    )(
+        mods, query_weight, key_weight, value_weight,
+        jnp.moveaxis(decay_extra, 1, 2).reshape(4, 128),
+    )
     rows_z = lax.all_to_all(cut, ("A", "B"), 0, 0, tiled=True)
     mine = to_everyone(rows_z[:, :, 0:384], "x")
     other = lax.ppermute(mine, "core", [(0, 1), (1, 0)])
     ride = rows_z[:, :, 384:512]
-    beside = lax.ppermute(ride, "tp", [(i, i ^ 1) for i in range(4)])
-    pair = jnp.stack([ride, beside])
-    across = lax.ppermute(pair, "tp", [(i, i ^ 3) for i in range(4)])
-    parts = [p[:, 0:6, 0:96].astype(f32) for p in (ride, beside, across[0], across[1])]
-    parts = [p[:, 0:2] + p[:, 2:4] + p[:, 4:6] for p in parts]
-    odd, high_half = (y % 2) == 1, y >= 2
-    near0, near1 = jnp.where(odd, parts[1], parts[0]), jnp.where(odd, parts[0], parts[1])
-    far0, far1 = jnp.where(odd, parts[2], parts[3]), jnp.where(odd, parts[3], parts[2])
-    ordered = [
-        jnp.where(high_half, far0, near0),
-        jnp.where(high_half, far1, near1),
-        jnp.where(high_half, near0, far0),
-        jnp.where(high_half, near1, far1),
-    ]
-    modulation = jnp.transpose(jnp.stack(ordered, axis=1), (2, 0, 1, 3)).reshape(2, 3 * D)
 
     own = jnp.concatenate([n[:32] for n in near] + [n[32:36] for n in near], axis=0)
     up_shift = [(i, (i + 1) % 4) for i in range(4)]
@@ -344,6 +358,13 @@
     low = lax.ppermute(minus[:64], "tp", up_shift)
     high = lax.ppermute(plus[64:], "tp", down_shift)
 
+    near_hidden, modulation = pl.pallas_call(
+        hidden_kernel,
+        out_shape=(sds((432, D), bf16), sds((2, 3 * D), f32)),
+        in_specs=[VM] * 5,
+        out_specs=(VM, VM),
+        name="hidden",
+    )(own, minus, plus, ride, norm_gain.reshape(1, D))
     payload, q, k, v, cum = pl.pallas_call(
         project_kernel,
         out_shape=(
@@ -353,12 +374,16 @@
             sds((SEG, DK), bf16),
             sds((2, SEG, DK), f32),
         ),
-        in_specs=[VM] * 13,
+        in_specs=[VM] * 11,
         out_specs=(VM,) * 5,
-        scratch_shapes=[pltpu.VMEM((ROWS, D), bf16), pltpu.VMEM((D, 384), bf16)],
+        scratch_shapes=[
+            pltpu.VMEM((144, D), bf16),
+            pltpu.VMEM((D, 384), bf16),
+            pltpu.VMEM((ROWS, 512), bf16),
+        ],
         name="project",
     )(
-        own, minus, plus, low, high, modulation, norm_gain.reshape(1, D), mine, other,
+        near_hidden, low, high, modulation, norm_gain.reshape(1, D), mine, other,
         decay_down.T, decay_up, decay_bias, ride,
     )
     got = lax.all_to_all(payload, "A", 0, 0, tiled=True)

time: 166 us -> 157 us (0.946)
  blocking collectives: 15.6 us -> 52.9 us
  starting transfers between devices: 67.7 us -> 38.6 us
  waiting for transfers between devices: 51.7 us -> 36.6 us
  Pallas kernels: 18.7 us -> 22.1 us
  local copies, waits for them, and re-layouts: 7.51 us -> 4.77 us
  other arithmetic: 2.58 us -> 0.78 us
    all_to_all x0 -> x2, blocking collectives: none -> 42.5 us  [the longest x1 32.5 us: device_body(): rows_z = lax.all_to_all(cut, ('A', 'B'), 0, 0, tiled=True)]
    all_to_all x1 -> x0, starting transfers between devices: 15.2 us -> none  [device_body(): rows_z = lax.all_to_all(cut, ('A', 'B'), 0, 0, tiled=True)]
    ppermute x3, waiting for transfers between devices: 14.2 us -> 6.22 us  [device_body(): near.append(lax.ppermute(rows, 'B', [(b, b ^ j) for b in range(4)]))]
    ppermute x2 -> x0, starting transfers between devices: 7.04 us -> none  [the longest x1 5.13 us: device_body(): across = lax.ppermute(pair, 'tp', [(i, i ^ 3) for i in range(4)])]
    pallas_call x1 -> x3, Pallas kernels: 2.18 us -> 7.37 us  [the longest x1 3.69 us: device_body(): pl.pallas_call(hidden_kernel, out_shape=(sds((432, D), bf16), sds((2, 3 *...]
    all_to_all x1, blocking collectives: 15.6 us -> 10.5 us  [device_body(): heads = lax.all_to_all(mixed.reshape(4, 128, DK), 'B', 0, 0, tiled=True)]
    ppermute x1, waiting for transfers between devices: 10 us -> 5.06 us  [device_body(): plus = lax.ppermute(own, 'tp', down_shift)]
    ppermute x1, waiting for transfers between devices: 0.01 us -> 3.53 us  [device_body(): low = lax.ppermute(minus[:64], 'tp', up_shift)]
  transfers between devices with their start and end apart: 14 -> 11, of which waited for: 7 -> 6; matrix products, arithmetic and copies ran while one was open for 5% -> 1% of each run, Pallas kernels for 2% -> 4%
where the time goes in v6:
time: 157 us; the launch traced here: 156 us
  blocking collectives  52.9 us (34%)
  starting transfers between devices  38.6 us (25%)
  waiting for transfers between devices  36.6 us (23%)
  Pallas kernels  22.1 us (14%)
  local copies, waits for them, and re-layouts  4.77 us (3%)
    all_to_all x1, blocking collectives, device_body(): rows_z = lax.all_to_all(cut, ('A', 'B'), 0, 0, tiled=True)  32.5 us
    all_to_all x1, waiting for transfers between devices, device_body(): got = lax.all_to_all(payload, 'A', 0, 0, tiled=True)  14.5 us
    all_to_all x1, blocking collectives, device_body(): heads = lax.all_to_all(mixed.reshape(4, 128, DK), 'B', 0, 0, tiled=True)  10.5 us
    ppermute x3, starting transfers between devices, device_body(): near.append(lax.ppermute(rows, 'B', [(b, b ^ j) for b in range(4)]))  10.4 us
    all_to_all x1, blocking collectives, device_body(): mods = lax.all_to_all(mods, 'tp', 0, 0, tiled=True)  10 us
    all_to_all x1, waiting for transfers between devices, device_body(): shares = lax.all_to_all(partial.reshape(4, 32, D), 'tp', 0, 0, tiled=True)  7.32 us
    pallas_call x1, Pallas kernels, device_body(): pl.pallas_call(project_kernel, out_shape=(sds((4, PAYLOAD, DK), bf16), sd...  6.41 us
    ppermute x3, waiting for transfers between devices, device_body(): near.append(lax.ppermute(rows, 'B', [(b, b ^ j) for b in range(4)]))  6.22 us
  transfers between devices with their start and end apart: 11, of which 6 were waited for; matrix products, arithmetic and copies ran while one was open for 1% of the time, Pallas kernels for 4%

profile of v6, /device:TPU:6, one launch (start us, length us, event | category | flops | bytes accessed | tf_op | source)
XLA Modules:
  0.0 156.0 jit_solution(6266830382318654064)
XLA Ops:
  0.0 1.9 %rows.1 = (bf16[36,2048]{1,0:T(8,128)(2,1)}, f32[4,2,96]{2,1,0:T(2,128)}) custom-call(bf16[32,2048]{1,0:T(8,128)(2,1)} %lat_ref.1, bf16[16,2048]{1,0:T(8,128)(2,1)} %ctx_ref.1, f32[1,2048]{1,0:T(1,128)} %sv_ref.1, f32[1,2048]{1,0:T(1,128)} %cv_ref.1, bf16[96,2048]{1,0:T(8,128)(2,1)} %bitcast.12), custom_call_target="tpu_custom_call" | custom-call | tf_op jit(solution)/shard_map/rows/pallas_call | solution.py:327
  1.9 10.0 %all_to_all.30.mods_ref = f32[4,2,96]{2,1,0:T(2,128)} all-to-all(f32[4,2,96]{2,1,0:T(2,128)} %get-tuple-element.18), channel_id=1, replica_groups=mesh['A'=4,'B'=4,'tp'=4,'x'=4,'core'=2] {'tp'}, dimensions={0} | all-to-all | bytes 6144 | tf_op jit(solution)/shard_map/all_to_all | solution.py:334
  11.9 1.7 %pack.1 = bf16[16,16,512]{2,1,0:T(8,128)(2,1)} custom-call(f32[4,2,96]{2,1,0:T(2,128)} %all_to_all.30.mods_ref, bf16[128,256]{1,0:T(8,128)(2,1)} %wq_ref.1, bf16[128,256]{1,0:T(8,128)(2,1)} %wk_ref.1, bf16[128,512]{1,0:T(8,128)(2,1)} %wv_ref.1, f32[4,128]{1,0:T(4,128)} %bitcast.17), custom_call_target="tpu_custom_call" | custom-call | tf_op jit(solution)/shard_map/pack/pallas_call | solution.py:338
  13.7 32.5 %all_to_all.31 = bf16[16,16,512]{2,1,0:T(8,128)(2,1)S(1)} all-to-all(bf16[16,16,512]{2,1,0:T(8,128)(2,1)} %pack.1), channel_id=1, replica_groups=mesh['A'=4,'B'=4,'tp'=4,'x'=4,'core'=2] {'A','B'}, dimensions={0} | all-to-all | bytes 524288 | tf_op jit(solution)/shard_map/all_to_all | solution.py:348
  46.2 1.0 broadcast_in_dim.2
  47.1 4.8 %all-to-all-start.2 = ((bf16[4,16,16,384]{3,2,1,0:T(8,128)(2,1)}), bf16[4,16,16,384]{3,2,1,0:T(8,128)(2,1)S(1)}, u32[]{:S(2)}, u32[]{:S(2)}) async-start(bf16[4,16,16,384]{3,2,1,0:T(8,128)(2,1)} %broadcast_in_dim.2), calls=%async_computation.2 | async-start | bytes 1572864 | tf_op jit(solution)/shard_map/all_to_all | solution.py:28
  51.9 0.0 copy-done.7
  51.9 4.2 %collective-permute-start = (bf16[36,2048]{1,0:T(8,128)(2,1)S(1)}, bf16[36,2048]{1,0:T(8,128)(2,1)S(1)}, u32[]{:S(2)}, u32[]{:S(2)}) collective-permute-start(bf16[36,2048]{1,0:T(8,128)(2,1)S(1)} %copy-done.7), channel_id=1, source_target_pairs={{0,32},{32,0},{64,96},{96,64},{1,33},{33,1},{65,97},{97,65},{2,34}... | collective-permute-start | bytes 442376 | tf_op jit(solution)/shard_map/ppermute | solution.py:337
  56.1 3.4 %collective-permute-start.1 = (bf16[36,2048]{1,0:T(8,128)(2,1)S(1)}, bf16[36,2048]{1,0:T(8,128)(2,1)S(1)}, u32[]{:S(2)}, u32[]{:S(2)}) collective-permute-start(bf16[36,2048]{1,0:T(8,128)(2,1)S(1)} %copy-done.7), channel_id=1, source_target_pairs={{0,64},{32,96},{64,0},{96,32},{1,65},{33,97},{65,1},{97,33},{2,66}... | collective-permute-start | bytes 442376 | tf_op jit(solution)/shard_map/ppermute | solution.py:337
  59.5 2.8 %collective-permute-start.2 = (bf16[36,2048]{1,0:T(8,128)(2,1)S(1)}, bf16[36,2048]{1,0:T(8,128)(2,1)S(1)}, u32[]{:S(2)}, u32[]{:S(2)}) collective-permute-start(bf16[36,2048]{1,0:T(8,128)(2,1)S(1)} %copy-done.7), channel_id=1, source_target_pairs={{0,96},{32,64},{64,32},{96,0},{1,97},{33,65},{65,33},{97,1},{2,98}... | collective-permute-start | bytes 442376 | tf_op jit(solution)/shard_map/ppermute | solution.py:337
  62.4 0.0 collective-permute-done
  62.4 4.3 %collective-permute-done.1 = bf16[36,2048]{1,0:T(8,128)(2,1)S(1)} collective-permute-done((bf16[36,2048]{1,0:T(8,128)(2,1)S(1)}, bf16[36,2048]{1,0:T(8,128)(2,1)S(1)}, u32[]{:S(2)}, u32[]{:S(2)}) %collective-permute-start.1) | collective-permute-done | bytes 147488 | tf_op jit(solution)/shard_map/ppermute | solution.py:337
  66.7 1.9 %collective-permute-done.2 = bf16[36,2048]{1,0:T(8,128)(2,1)S(1)} collective-permute-done((bf16[36,2048]{1,0:T(8,128)(2,1)S(1)}, bf16[36,2048]{1,0:T(8,128)(2,1)S(1)}, u32[]{:S(2)}, u32[]{:S(2)}) %collective-permute-start.2) | collective-permute-done | bytes 147488 | tf_op jit(solution)/shard_map/ppermute | solution.py:337
  68.7 0.1 concatenate.3.own_ref
  68.8 0.0 copy-start.1
  68.8 3.1 %collective-permute-start.4 = (bf16[144,2048]{1,0:T(8,128)(2,1)S(1)}, bf16[144,2048]{1,0:T(8,128)(2,1)S(1)}, u32[]{:S(2)}, u32[]{:S(2)}) collective-permute-start(bf16[144,2048]{1,0:T(8,128)(2,1)S(1)} %concatenate.3.own_ref), channel_id=1, source_target_pairs={{0,24},{8,0},{16,8},{24,16},{1,25},{9,1},{17,9},{25,17},{2,26},{10... | collective-permute-start | bytes 1769480 | tf_op jit(solution)/shard_map/ppermute | solution.py:357
  71.9 2.8 %collective-permute-start.3 = (bf16[144,2048]{1,0:T(8,128)(2,1)S(1)}, bf16[144,2048]{1,0:T(8,128)(2,1)S(1)}, u32[]{:S(2)}, u32[]{:S(2)}) collective-permute-start(bf16[144,2048]{1,0:T(8,128)(2,1)S(1)} %concatenate.3.own_ref), channel_id=1, source_target_pairs={{0,8},{8,16},{16,24},{24,0},{1,9},{9,17},{17,25},{25,1},{2,10},{10... | collective-permute-start | bytes 1769480 | tf_op jit(solution)/shard_map/ppermute | solution.py:356
  74.6 0.0 all-to-all-done.2.mine_ref
  74.7 0.0 copy-start
  74.7 1.9 %collective-permute-start.7 = (bf16[4,16,16,384]{3,2,1,0:T(8,128)(2,1)S(1)}, bf16[4,16,16,384]{3,2,1,0:T(8,128)(2,1)}, u32[]{:S(2)}, u32[]{:S(2)}) collective-permute-start(bf16[4,16,16,384]{3,2,1,0:T(8,128)(2,1)S(1)} %all-to-all-done.2.mine_ref), channel_id=1, source_target_pairs={{0,1},{1,0},{2,3},{3,2},{4,5},{5,4},{6,7},{7,6},{8,9},{9,8},{10,11... | collective-permute-start | bytes 2359304 | tf_op jit(solution)/shard_map/ppermute | solution.py:350
  76.6 5.1 %collective-permute-done.4.plus_ref = bf16[144,2048]{1,0:T(8,128)(2,1)S(1)} collective-permute-done((bf16[144,2048]{1,0:T(8,128)(2,1)S(1)}, bf16[144,2048]{1,0:T(8,128)(2,1)S(1)}, u32[]{:S(2)}, u32[]{:S(2)}) %collective-permute-start.4) | collective-permute-done | bytes 589856 | tf_op jit(solution)/shard_map/ppermute | solution.py:357
  81.7 4.3 %collective-permute-start.6 = (bf16[80,2048]{1,0:T(8,128)(2,1)S(1)}, bf16[80,2048]{1,0:T(8,128)(2,1)S(1)}, u32[]{:S(2)}, u32[]{:S(2)}) collective-permute-start(bf16[80,2048]{1,0:T(8,128)(2,1)S(1)} %slice.60), channel_id=1, source_target_pairs={{0,24},{8,0},{16,8},{24,16},{1,25},{9,1},{17,9},{25,17},{2,26},{10... | collective-permute-start | bytes 983048 | tf_op jit(solution)/shard_map/ppermute | solution.py:359
  86.0 0.0 collective-permute-done.3.minus_ref
  86.0 0.0 copy-start.4
  86.0 0.8 slice.59
  86.8 1.9 %collective-permute-start.5 = (bf16[64,2048]{1,0:T(8,128)(2,1)}, bf16[64,2048]{1,0:T(8,128)(2,1)}, u32[]{:S(2)}, u32[]{:S(2)}) collective-permute-start(bf16[64,2048]{1,0:T(8,128)(2,1)} %slice.59), channel_id=1, source_target_pairs={{0,8},{8,16},{16,24},{24,0},{1,9},{9,17},{17,25},{25,1},{2,10},{10... | collective-permute-start | bytes 786440 | tf_op jit(solution)/shard_map/ppermute | solution.py:358
  88.7 0.6 slice.58.ride_ref
  89.3 0.0 copy-done.1
  89.3 0.0 copy-done.2
  89.3 0.0 copy-done.4
  89.3 3.7 %hidden.1 = (bf16[432,2048]{1,0:T(8,128)(2,1)}, f32[2,6144]{1,0:T(2,128)}) custom-call(bf16[144,2048]{1,0:T(8,128)(2,1)} %copy-done.1, bf16[144,2048]{1,0:T(8,128)(2,1)} %copy-done.4, bf16[144,2048]{1,0:T(8,128)(2,1)} %copy-done.2, bf16[16,16,128]{2,1,0:T(8,128)(2,1)} %slice.58.ride_ref, f32[1,2048]{1,0:T(1,128)} %bitcast.14), custom_call_target="tpu_custom_call" | custom-call | tf_op jit(solution)/shard_map/hidden/pallas_call | solution.py:361
  93.0 3.5 %collective-permute-done.5.low_ref = bf16[64,2048]{1,0:T(8,128)(2,1)} collective-permute-done((bf16[64,2048]{1,0:T(8,128)(2,1)}, bf16[64,2048]{1,0:T(8,128)(2,1)}, u32[]{:S(2)}, u32[]{:S(2)}) %collective-permute-start.5) | collective-permute-done | bytes 262176 | tf_op jit(solution)/shard_map/ppermute | solution.py:358
  96.5 0.0 collective-permute-done.6.high_ref
  96.6 0.0 collective-permute-done.7.other_ref
  96.6 0.7 copy-done.6
  97.3 6.4 %project.1 = (bf16[4,336,128]{2,1,0:T(8,128)(2,1)}, bf16[512,128]{1,0:T(8,128)(2,1)}, bf16[512,128]{1,0:T(8,128)(2,1)}, bf16[512,128]{1,0:T(8,128)(2,1)}, f32[2,512,128]{2,1,0:T(8,128)}) custom-call(bf16[432,2048]{1,0:T(8,128)(2,1)} %get-tuple-element.20.h_ref, bf16[64,2048]{1,0:T(8,128)(2,1)} %collective-permute-done.5.low_ref, bf16[80,2048]{1,0:T(8,128)(2,1)} %copy-done.6, ...), custom_call_target="tpu_custom_call" | custom-call | tf_op jit(solution)/shard_map/project/pallas_call | solution.py:368
  103.7 6.0 %all-to-all-start.3 = ((bf16[4,336,128]{2,1,0:T(8,128)(2,1)}), bf16[4,336,128]{2,1,0:T(8,128)(2,1)S(1)}, u32[]{:S(2)}, u32[]{:S(2)}) async-start(bf16[4,336,128]{2,1,0:T(8,128)(2,1)} %get-tuple-element.21), calls=%async_computation.3 | async-start | bytes 688128 | tf_op jit(solution)/shard_map/all_to_all | solution.py:389
  109.7 3.0 %local.1 = (f32[512,128]{1,0:T(8,128)}, bf16[512,128]{1,0:T(8,128)(2,1)}, bf16[512,128]{1,0:T(8,128)(2,1)}) custom-call(bf16[512,128]{1,0:T(8,128)(2,1)} %get-tuple-element.22.q_ref, bf16[512,128]{1,0:T(8,128)(2,1)} %get-tuple-element.23.k_ref, bf16[512,128]{1,0:T(8,128)(2,1)} %get-tuple-element.24.v_ref, f32[2,512,128]{2,1,0:T(8,128)} %get-tuple-element.25.cum_ref), custom_call_target="tpu_custom_call" | custom-call | tf_op jit(solution)/shard_map/local/pallas_call | solution.py:390
  112.7 14.5 %all-to-all-done.3.in_ref = bf16[4,336,128]{2,1,0:T(8,128)(2,1)S(1)} async-done(((bf16[4,336,128]{2,1,0:T(8,128)(2,1)}), bf16[4,336,128]{2,1,0:T(8,128)(2,1)S(1)}, u32[]{:S(2)}, u32[]{:S(2)}) %all-to-all-start.3) | async-done | bytes 344096 | tf_op jit(solution)/shard_map/all_to_all | solution.py:389
  127.2 0.7 copy-done.3
  127.9 2.3 %combine.1 = bf16[512,128]{1,0:T(8,128)(2,1)} custom-call(bf16[4,336,128]{2,1,0:T(8,128)(2,1)} %copy-done.3, f32[512,128]{1,0:T(8,128)} %get-tuple-element.26.o_ref, bf16[512,128]{1,0:T(8,128)(2,1)} %get-tuple-element.27.lift_f_ref, bf16[512,128]{1,0:T(8,128)(2,1)} %get-tuple-element.28.lift_b_ref), custom_call_target="tpu_custom_call" | custom-call | tf_op jit(solution)/shard_map/combine/pallas_call | solution.py:397
  130.2 10.5 %all_to_all.32.mix_ref = bf16[4,128,128]{2,1,0:T(8,128)(2,1)} all-to-all(bf16[4,128,128]{2,1,0:T(8,128)(2,1)} %bitcast.11), channel_id=1, replica_groups=mesh['A'=4,'B'=4,'tp'=4,'x'=4,'core'=2] {'B'}, dimensions={0} | all-to-all | bytes 262144 | tf_op jit(solution)/shard_map/all_to_all | solution.py:404
  140.7 3.0 %output.1 = bf16[128,2048]{1,0:T(8,128)(2,1)} custom-call(bf16[4,128,128]{2,1,0:T(8,128)(2,1)} %all_to_all.32.mix_ref, f32[1,256]{1,0:T(1,128)} %bitcast.18, bf16[512,2048]{1,0:T(8,128)(2,1)} %w_ref.1), custom_call_target="tpu_custom_call" | custom-call | tf_op jit(solution)/shard_map/output/pallas_call | solution.py:405
  143.7 3.5 %all-to-all-start.5 = ((bf16[4,32,2048]{2,1,0:T(8,128)(2,1)}), bf16[4,32,2048]{2,1,0:T(8,128)(2,1)S(1)}, u32[]{:S(2)}, u32[]{:S(2)}) async-start(bf16[4,32,2048]{2,1,0:T(8,128)(2,1)} %bitcast.10), calls=%async_computation.5 | async-start | bytes 1048576 | tf_op jit(solution)/shard_map/all_to_all | solution.py:412
  147.2 0.7 slice.48
  147.9 7.3 %all-to-all-done.5 = bf16[4,32,2048]{2,1,0:T(8,128)(2,1)S(1)} async-done(((bf16[4,32,2048]{2,1,0:T(8,128)(2,1)}), bf16[4,32,2048]{2,1,0:T(8,128)(2,1)S(1)}, u32[]{:S(2)}, u32[]{:S(2)}) %all-to-all-start.5) | async-done | bytes 524320 | tf_op jit(solution)/shard_map/all_to_all | solution.py:412
  155.2 0.1 reduce_sum.12
  155.3 0.7 add_convert_fusion
  (17 shorter events, 0.1 us)
Async XLA Ops:
  1.9 49.9 %copy-start.7 = (bf16[36,2048]{1,0:T(8,128)(2,1)S(1)}, bf16[36,2048]{1,0:T(8,128)(2,1)}, u32[]{:S(2)}) copy-start(bf16[36,2048]{1,0:T(8,128)(2,1)} %get-tuple-element.17) | copy-start | bytes 442372
  47.1 27.5 %all-to-all-start.2 = ((bf16[4,16,16,384]{3,2,1,0:T(8,128)(2,1)}), bf16[4,16,16,384]{3,2,1,0:T(8,128)(2,1)S(1)}, u32[]{:S(2)}, u32[]{:S(2)}) async-start(bf16[4,16,16,384]{3,2,1,0:T(8,128)(2,1)} %broadcast_in_dim.2), calls=%async_computation.2 | async-start | bytes 1572864 | tf_op jit(solution)/shard_map/all_to_all | solution.py:28
  51.9 10.5 %collective-permute-start = (bf16[36,2048]{1,0:T(8,128)(2,1)S(1)}, bf16[36,2048]{1,0:T(8,128)(2,1)S(1)}, u32[]{:S(2)}, u32[]{:S(2)}) collective-permute-start(bf16[36,2048]{1,0:T(8,128)(2,1)S(1)} %copy-done.7), channel_id=1, source_target_pairs={{0,32},{32,0},{64,96},{96,64},{1,33},{33,1},{65,97},{97,65},{2,34}... | collective-permute-start | bytes 442376 | tf_op jit(solution)/shard_map/ppermute | solution.py:337
  56.1 10.6 %collective-permute-start.1 = (bf16[36,2048]{1,0:T(8,128)(2,1)S(1)}, bf16[36,2048]{1,0:T(8,128)(2,1)S(1)}, u32[]{:S(2)}, u32[]{:S(2)}) collective-permute-start(bf16[36,2048]{1,0:T(8,128)(2,1)S(1)} %copy-done.7), channel_id=1, source_target_pairs={{0,64},{32,96},{64,0},{96,32},{1,65},{33,97},{65,1},{97,33},{2,66}... | collective-permute-start | bytes 442376 | tf_op jit(solution)/shard_map/ppermute | solution.py:337
  59.5 9.1 %collective-permute-start.2 = (bf16[36,2048]{1,0:T(8,128)(2,1)S(1)}, bf16[36,2048]{1,0:T(8,128)(2,1)S(1)}, u32[]{:S(2)}, u32[]{:S(2)}) collective-permute-start(bf16[36,2048]{1,0:T(8,128)(2,1)S(1)} %copy-done.7), channel_id=1, source_target_pairs={{0,96},{32,64},{64,32},{96,0},{1,97},{33,65},{65,33},{97,1},{2,98}... | collective-permute-start | bytes 442376 | tf_op jit(solution)/shard_map/ppermute | solution.py:337
  68.8 20.5 %copy-start.1 = (bf16[144,2048]{1,0:T(8,128)(2,1)}, bf16[144,2048]{1,0:T(8,128)(2,1)S(1)}, u32[]{:S(2)}) copy-start(bf16[144,2048]{1,0:T(8,128)(2,1)S(1)} %concatenate.3.own_ref) | copy-start | bytes 1769476
  68.8 12.9 %collective-permute-start.4 = (bf16[144,2048]{1,0:T(8,128)(2,1)S(1)}, bf16[144,2048]{1,0:T(8,128)(2,1)S(1)}, u32[]{:S(2)}, u32[]{:S(2)}) collective-permute-start(bf16[144,2048]{1,0:T(8,128)(2,1)S(1)} %concatenate.3.own_ref), channel_id=1, source_target_pairs={{0,24},{8,0},{16,8},{24,16},{1,25},{9,1},{17,9},{25,17},{2,26},{10... | collective-permute-start | bytes 1769480 | tf_op jit(solution)/shard_map/ppermute | solution.py:357
  71.9 14.1 %collective-permute-start.3 = (bf16[144,2048]{1,0:T(8,128)(2,1)S(1)}, bf16[144,2048]{1,0:T(8,128)(2,1)S(1)}, u32[]{:S(2)}, u32[]{:S(2)}) collective-permute-start(bf16[144,2048]{1,0:T(8,128)(2,1)S(1)} %concatenate.3.own_ref), channel_id=1, source_target_pairs={{0,8},{8,16},{16,24},{24,0},{1,9},{9,17},{17,25},{25,1},{2,10},{10... | collective-permute-start | bytes 1769480 | tf_op jit(solution)/shard_map/ppermute | solution.py:356
  74.7 21.9 %copy-start = (bf16[4,16,16,384]{3,2,1,0:T(8,128)(2,1)}, bf16[4,16,16,384]{3,2,1,0:T(8,128)(2,1)S(1)}, u32[]{:S(2)}) copy-start(bf16[4,16,16,384]{3,2,1,0:T(8,128)(2,1)S(1)} %all-to-all-done.2.mine_ref) | copy-start | bytes 2359300
  74.7 21.9 %collective-permute-start.7 = (bf16[4,16,16,384]{3,2,1,0:T(8,128)(2,1)S(1)}, bf16[4,16,16,384]{3,2,1,0:T(8,128)(2,1)}, u32[]{:S(2)}, u32[]{:S(2)}) collective-permute-start(bf16[4,16,16,384]{3,2,1,0:T(8,128)(2,1)S(1)} %all-to-all-done.2.mine_ref), channel_id=1, source_target_pairs={{0,1},{1,0},{2,3},{3,2},{4,5},{5,4},{6,7},{7,6},{8,9},{9,8},{10,11... | collective-permute-start | bytes 2359304 | tf_op jit(solution)/shard_map/ppermute | solution.py:350
  81.7 7.7 %copy-start.2 = (bf16[144,2048]{1,0:T(8,128)(2,1)}, bf16[144,2048]{1,0:T(8,128)(2,1)S(1)}, u32[]{:S(2)}) copy-start(bf16[144,2048]{1,0:T(8,128)(2,1)S(1)} %collective-permute-done.4.plus_ref) | copy-start | bytes 1769476
  81.7 14.9 %collective-permute-start.6 = (bf16[80,2048]{1,0:T(8,128)(2,1)S(1)}, bf16[80,2048]{1,0:T(8,128)(2,1)S(1)}, u32[]{:S(2)}, u32[]{:S(2)}) collective-permute-start(bf16[80,2048]{1,0:T(8,128)(2,1)S(1)} %slice.60), channel_id=1, source_target_pairs={{0,24},{8,0},{16,8},{24,16},{1,25},{9,1},{17,9},{25,17},{2,26},{10... | collective-permute-start | bytes 983048 | tf_op jit(solution)/shard_map/ppermute | solution.py:359
  86.0 3.3 %copy-start.4 = (bf16[144,2048]{1,0:T(8,128)(2,1)}, bf16[144,2048]{1,0:T(8,128)(2,1)S(1)}, u32[]{:S(2)}) copy-start(bf16[144,2048]{1,0:T(8,128)(2,1)S(1)} %collective-permute-done.3.minus_ref) | copy-start | bytes 1769476
  86.8 9.8 %collective-permute-start.5 = (bf16[64,2048]{1,0:T(8,128)(2,1)}, bf16[64,2048]{1,0:T(8,128)(2,1)}, u32[]{:S(2)}, u32[]{:S(2)}) collective-permute-start(bf16[64,2048]{1,0:T(8,128)(2,1)} %slice.59), channel_id=1, source_target_pairs={{0,8},{8,16},{16,24},{24,0},{1,9},{9,17},{17,25},{25,1},{2,10},{10... | collective-permute-start | bytes 786440 | tf_op jit(solution)/shard_map/ppermute | solution.py:358
  96.5 0.7 copy-start.6
  103.7 23.5 %all-to-all-start.3 = ((bf16[4,336,128]{2,1,0:T(8,128)(2,1)}), bf16[4,336,128]{2,1,0:T(8,128)(2,1)S(1)}, u32[]{:S(2)}, u32[]{:S(2)}) async-start(bf16[4,336,128]{2,1,0:T(8,128)(2,1)} %get-tuple-element.21), calls=%async_computation.3 | async-start | bytes 688128 | tf_op jit(solution)/shard_map/all_to_all | solution.py:389
  127.2 0.7 copy-start.3
  140.7 14.6 %copy-start.5 = (bf16[32,2048]{1,0:T(8,128)(2,1)S(1)}, bf16[32,2048]{1,0:T(8,128)(2,1)}, u32[]{:S(2)}) copy-start(bf16[32,2048]{1,0:T(8,128)(2,1)} %lat_ref.1) | copy-start | bytes 393220
  143.7 11.5 %all-to-all-start.5 = ((bf16[4,32,2048]{2,1,0:T(8,128)(2,1)}), bf16[4,32,2048]{2,1,0:T(8,128)(2,1)S(1)}, u32[]{:S(2)}, u32[]{:S(2)}) async-start(bf16[4,32,2048]{2,1,0:T(8,128)(2,1)} %bitcast.10), calls=%async_computation.5 | async-start | bytes 1048576 | tf_op jit(solution)/shard_map/all_to_all | solution.py:412

commit v7 on v6

--- a/solution.py
+++ b/solution.py
@@ -21,6 +21,14 @@
 f32 = jnp.float32
 VM = pl.BlockSpec(memory_space=pltpu.VMEM)
 SM = pl.BlockSpec(memory_space=pltpu.SMEM)
+
+
+def on_chip(*arrays):
+    return tuple(pltpu.with_memory_space_constraint(a, pltpu.VMEM) for a in arrays)
+
+
+def off_chip(*arrays):
+    return tuple(pltpu.with_memory_space_constraint(a, pltpu.HBM) for a in arrays)
 
 
 def to_everyone(x, axis):
@@ -329,8 +337,9 @@
         out_shape=(sds((36, D), bf16), sds((4, 2, 96), f32)),
         in_specs=[VM] * 5,
         out_specs=(VM, VM),
+        compiler_params=pltpu.CompilerParams(vmem_limit_bytes=12 * 1024 * 1024),
         name="rows",
-    )(latents, context, sample_vector, context_vector, modulator.T)
+    )(*off_chip(latents, context, sample_vector, context_vector, modulator.T))
     mods = lax.all_to_all(mods, "tp", 0, 0, tiled=True)
     near = [rows]
     for j in range(1, 4):
@@ -340,10 +349,14 @@
         out_shape=sds((16, 16, 512), bf16),
         in_specs=[VM] * 5,
         out_specs=VM,
+        compiler_params=pltpu.CompilerParams(vmem_limit_bytes=12 * 1024 * 1024),
         name="pack",
     )(
-        mods, query_weight, key_weight, value_weight,
-        jnp.moveaxis(decay_extra, 1, 2).reshape(4, 128),
+        *on_chip(mods),
+        *off_chip(
+            query_weight, key_weight, value_weight,
+            jnp.moveaxis(decay_extra, 1, 2).reshape(4, 128),
+        ),
     )
     rows_z = lax.all_to_all(cut, ("A", "B"), 0, 0, tiled=True)
     mine = to_everyone(rows_z[:, :, 0:384], "x")
@@ -360,19 +373,20 @@
 
     near_hidden, modulation = pl.pallas_call(
         hidden_kernel,
-        out_shape=(sds((432, D), bf16), sds((2, 3 * D), f32)),
+        out_shape=(sds((432, D), bf16), pltpu.HBM((2, 3 * D), f32)),
         in_specs=[VM] * 5,
         out_specs=(VM, VM),
+        compiler_params=pltpu.CompilerParams(vmem_limit_bytes=16 * 1024 * 1024),
         name="hidden",
-    )(own, minus, plus, ride, norm_gain.reshape(1, D))
+    )(*on_chip(own, minus, plus, ride), *off_chip(norm_gain.reshape(1, D)))
     payload, q, k, v, cum = pl.pallas_call(
         project_kernel,
         out_shape=(
             sds((4, PAYLOAD, DK), bf16),
-            sds((SEG, DK), bf16),
-            sds((SEG, DK), bf16),
-            sds((SEG, DK), bf16),
-            sds((2, SEG, DK), f32),
+            pltpu.HBM((SEG, DK), bf16),
+            pltpu.HBM((SEG, DK), bf16),
+            pltpu.HBM((SEG, DK), bf16),
+            pltpu.HBM((2, SEG, DK), f32),
         ),
         in_specs=[VM] * 11,
         out_specs=(VM,) * 5,
@@ -381,10 +395,11 @@
             pltpu.VMEM((D, 384), bf16),
             pltpu.VMEM((ROWS, 512), bf16),
         ],
+        compiler_params=pltpu.CompilerParams(vmem_limit_bytes=24 * 1024 * 1024),
         name="project",
     )(
-        near_hidden, low, high, modulation, norm_gain.reshape(1, D), mine, other,
-        decay_down.T, decay_up, decay_bias, ride,
+        *on_chip(near_hidden), *on_chip(low, high), *off_chip(modulation, norm_gain.reshape(1, D)),
+        *on_chip(mine, other), *off_chip(decay_down.T, decay_up, decay_bias), *on_chip(ride),
     )
     got = lax.all_to_all(payload, "A", 0, 0, tiled=True)
     local, lift_f, lift_b = pl.pallas_call(
@@ -392,23 +407,26 @@
         out_shape=(sds((SEG, DK), f32), sds((SEG, DK), bf16), sds((SEG, DK), bf16)),
         in_specs=[VM] * 4,
         out_specs=(VM,) * 3,
+        compiler_params=pltpu.CompilerParams(vmem_limit_bytes=12 * 1024 * 1024),
         name="local",
-    )(q, k, v, cum)
+    )(*off_chip(q, k, v, cum))
     mixed = pl.pallas_call(
         combine_kernel,
         out_shape=sds((SEG, DK), bf16),
         in_specs=[VM] * 4,
         out_specs=VM,
+        compiler_params=pltpu.CompilerParams(vmem_limit_bytes=12 * 1024 * 1024),
         name="combine",
-    )(got, local, lift_f, lift_b)
+    )(*on_chip(got, local, lift_f, lift_b))
     heads = lax.all_to_all(mixed.reshape(4, 128, DK), "B", 0, 0, tiled=True)
     partial = pl.pallas_call(
         output_kernel,
         out_shape=sds((128, D), bf16),
         in_specs=[VM] * 3,
         out_specs=VM,
+        compiler_params=pltpu.CompilerParams(vmem_limit_bytes=16 * 1024 * 1024),
         name="output",
-    )(heads, head_gain.reshape(1, 256), out_weight)
+    )(*on_chip(heads), *off_chip(head_gain.reshape(1, 256)), *on_chip(out_weight))
     shares = lax.all_to_all(partial.reshape(4, 32, D), "tp", 0, 0, tiled=True)
     projected = shares.astype(f32).sum(axis=0)
     projected = lax.optimization_barrier(projected.astype(bf16)).astype(f32)

time: 157 us -> 148 us (0.943)
  Pallas kernels: 22.1 us -> 14.2 us
  waiting for transfers between devices: 36.6 us -> 39.6 us
  local copies, waits for them, and re-layouts: 4.77 us -> 1.95 us
    pallas_call x2, Pallas kernels: 10.1 us -> 6.92 us  [the longest x1 5.2 us: device_body(): pl.pallas_call(project_kernel, out_shape=(sds((4, PAYLOAD, DK), bf16), pl...]
    ppermute x1, waiting for transfers between devices: 3.53 us -> 5.8 us  [device_body(): low = lax.ppermute(minus[:64], 'tp', up_shift)]
    pallas_call x1, Pallas kernels: 2.28 us -> 0.49 us  [device_body(): pl.pallas_call(combine_kernel, out_shape=sds((SEG, DK), bf16), in_specs=[...]
  transfers between devices with their start and end apart: 11 -> 11, of which waited for: 6 -> 6; matrix products, arithmetic and copies ran while one was open for 1% -> 1% of each run, Pallas kernels for 4% -> 3%
where the time goes in v7:
time: 148 us; the launch traced here: 147 us
  blocking collectives  52 us (35%)
  waiting for transfers between devices  39.6 us (27%)
  starting transfers between devices  38.7 us (26%)
  Pallas kernels  14.2 us (10%)
  local copies, waits for them, and re-layouts  1.95 us (1%)
    all_to_all x1, blocking collectives, device_body(): rows_z = lax.all_to_all(cut, ('A', 'B'), 0, 0, tiled=True)  32.3 us
    all_to_all x1, waiting for transfers between devices, device_body(): got = lax.all_to_all(payload, 'A', 0, 0, tiled=True)  15.1 us
    ppermute x3, starting transfers between devices, device_body(): near.append(lax.ppermute(rows, 'B', [(b, b ^ j) for b in range(4)]))  10.4 us
    all_to_all x1, blocking collectives, device_body(): heads = lax.all_to_all(mixed.reshape(4, 128, DK), 'B', 0, 0, tiled=True)  10.2 us
    all_to_all x1, blocking collectives, device_body(): mods = lax.all_to_all(mods, 'tp', 0, 0, tiled=True)  9.57 us
    all_to_all x1, waiting for transfers between devices, device_body(): shares = lax.all_to_all(partial.reshape(4, 32, D), 'tp', 0, 0, tiled=True)  7.32 us
    ppermute x3, waiting for transfers between devices, device_body(): near.append(lax.ppermute(rows, 'B', [(b, b ^ j) for b in range(4)]))  6.23 us
    all_to_all x1, starting transfers between devices, device_body(): got = lax.all_to_all(payload, 'A', 0, 0, tiled=True)  6.11 us
  transfers between devices with their start and end apart: 11, of which 6 were waited for; matrix products, arithmetic and copies ran while one was open for 1% of the time, Pallas kernels for 3%

profile of v7, /device:TPU:6, one launch (start us, length us, event | category | flops | bytes accessed | tf_op | source)
XLA Modules:
  0.0 147.4 jit_solution(872379368028478761)
XLA Ops:
  0.0 1.4 rows.1
  1.4 9.6 %all_to_all.30.mods_ref = f32[4,2,96]{2,1,0:T(2,128)S(1)} all-to-all(f32[4,2,96]{2,1,0:T(2,128)S(1)} %get-tuple-element.18), channel_id=1, replica_groups=mesh['A'=4,'B'=4,'tp'=4,'x'=4,'core'=2] {'tp'}, dimensions={0} | all-to-all | bytes 6144 | tf_op jit(solution)/shard_map/all_to_all | solution.py:343
  10.9 1.1 pack.1
  12.0 32.3 %all_to_all.31 = bf16[16,16,512]{2,1,0:T(8,128)(2,1)S(1)} all-to-all(bf16[16,16,512]{2,1,0:T(8,128)(2,1)S(1)} %pack.1), channel_id=1, replica_groups=mesh['A'=4,'B'=4,'tp'=4,'x'=4,'core'=2] {'A','B'}, dimensions={0} | all-to-all | bytes 524288 | tf_op jit(solution)/shard_map/all_to_all | solution.py:361
  44.3 1.0 broadcast_in_dim.2
  45.3 4.8 %all-to-all-start.2 = ((bf16[4,16,16,384]{3,2,1,0:T(8,128)(2,1)}), bf16[4,16,16,384]{3,2,1,0:T(8,128)(2,1)S(1)}, u32[]{:S(2)}, u32[]{:S(2)}) async-start(bf16[4,16,16,384]{3,2,1,0:T(8,128)(2,1)} %broadcast_in_dim.2), calls=%async_computation.2 | async-start | bytes 1572864 | tf_op jit(solution)/shard_map/all_to_all | solution.py:36
  50.0 4.2 %collective-permute-start = (bf16[36,2048]{1,0:T(8,128)(2,1)S(1)}, bf16[36,2048]{1,0:T(8,128)(2,1)S(1)}, u32[]{:S(2)}, u32[]{:S(2)}) collective-permute-start(bf16[36,2048]{1,0:T(8,128)(2,1)S(1)} %get-tuple-element.17), channel_id=1, source_target_pairs={{0,32},{32,0},{64,96},{96,64},{1,33},{33,1},{65,97},{97,65},{2,34}... | collective-permute-start | bytes 442376 | tf_op jit(solution)/shard_map/ppermute | solution.py:346
  54.2 3.4 %collective-permute-start.1 = (bf16[36,2048]{1,0:T(8,128)(2,1)S(1)}, bf16[36,2048]{1,0:T(8,128)(2,1)S(1)}, u32[]{:S(2)}, u32[]{:S(2)}) collective-permute-start(bf16[36,2048]{1,0:T(8,128)(2,1)S(1)} %get-tuple-element.17), channel_id=1, source_target_pairs={{0,64},{32,96},{64,0},{96,32},{1,65},{33,97},{65,1},{97,33},{2,66}... | collective-permute-start | bytes 442376 | tf_op jit(solution)/shard_map/ppermute | solution.py:346
  57.7 2.8 %collective-permute-start.2 = (bf16[36,2048]{1,0:T(8,128)(2,1)S(1)}, bf16[36,2048]{1,0:T(8,128)(2,1)S(1)}, u32[]{:S(2)}, u32[]{:S(2)}) collective-permute-start(bf16[36,2048]{1,0:T(8,128)(2,1)S(1)} %get-tuple-element.17), channel_id=1, source_target_pairs={{0,96},{32,64},{64,32},{96,0},{1,97},{33,65},{65,33},{97,1},{2,98}... | collective-permute-start | bytes 442376 | tf_op jit(solution)/shard_map/ppermute | solution.py:346
  60.5 0.0 collective-permute-done
  60.5 4.3 %collective-permute-done.1 = bf16[36,2048]{1,0:T(8,128)(2,1)S(1)} collective-permute-done((bf16[36,2048]{1,0:T(8,128)(2,1)S(1)}, bf16[36,2048]{1,0:T(8,128)(2,1)S(1)}, u32[]{:S(2)}, u32[]{:S(2)}) %collective-permute-start.1) | collective-permute-done | bytes 147488 | tf_op jit(solution)/shard_map/ppermute | solution.py:346
  64.9 1.9 %collective-permute-done.2 = bf16[36,2048]{1,0:T(8,128)(2,1)S(1)} collective-permute-done((bf16[36,2048]{1,0:T(8,128)(2,1)S(1)}, bf16[36,2048]{1,0:T(8,128)(2,1)S(1)}, u32[]{:S(2)}, u32[]{:S(2)}) %collective-permute-start.2) | collective-permute-done | bytes 147488 | tf_op jit(solution)/shard_map/ppermute | solution.py:346
  66.8 0.1 concatenate.3.own_ref
  66.9 3.1 %collective-permute-start.4 = (bf16[144,2048]{1,0:T(8,128)(2,1)S(1)}, bf16[144,2048]{1,0:T(8,128)(2,1)S(1)}, u32[]{:S(2)}, u32[]{:S(2)}) collective-permute-start(bf16[144,2048]{1,0:T(8,128)(2,1)S(1)} %concatenate.3.own_ref), channel_id=1, source_target_pairs={{0,24},{8,0},{16,8},{24,16},{1,25},{9,1},{17,9},{25,17},{2,26},{10... | collective-permute-start | bytes 1769480 | tf_op jit(solution)/shard_map/ppermute | solution.py:370
  70.0 2.8 %collective-permute-start.3 = (bf16[144,2048]{1,0:T(8,128)(2,1)S(1)}, bf16[144,2048]{1,0:T(8,128)(2,1)S(1)}, u32[]{:S(2)}, u32[]{:S(2)}) collective-permute-start(bf16[144,2048]{1,0:T(8,128)(2,1)S(1)} %concatenate.3.own_ref), channel_id=1, source_target_pairs={{0,8},{8,16},{16,24},{24,0},{1,9},{9,17},{17,25},{25,1},{2,10},{10... | collective-permute-start | bytes 1769480 | tf_op jit(solution)/shard_map/ppermute | solution.py:369
  72.8 0.0 all-to-all-done.2.mine_ref
  72.8 1.9 %collective-permute-start.7 = (bf16[4,16,16,384]{3,2,1,0:T(8,128)(2,1)S(1)}, bf16[4,16,16,384]{3,2,1,0:T(8,128)(2,1)S(1)}, u32[]{:S(2)}, u32[]{:S(2)}) collective-permute-start(bf16[4,16,16,384]{3,2,1,0:T(8,128)(2,1)S(1)} %all-to-all-done.2.mine_ref), channel_id=1, source_target_pairs={{0,1},{1,0},{2,3},{3,2},{4,5},{5,4},{6,7},{7,6},{8,9},{9,8},{10,11... | collective-permute-start | bytes 2359304 | tf_op jit(solution)/shard_map/ppermute | solution.py:363
  74.7 5.1 %collective-permute-done.4.plus_ref = bf16[144,2048]{1,0:T(8,128)(2,1)S(1)} collective-permute-done((bf16[144,2048]{1,0:T(8,128)(2,1)S(1)}, bf16[144,2048]{1,0:T(8,128)(2,1)S(1)}, u32[]{:S(2)}, u32[]{:S(2)}) %collective-permute-start.4) | collective-permute-done | bytes 589856 | tf_op jit(solution)/shard_map/ppermute | solution.py:370
  79.9 4.2 %collective-permute-start.6 = (bf16[80,2048]{1,0:T(8,128)(2,1)S(1)}, bf16[80,2048]{1,0:T(8,128)(2,1)S(1)}, u32[]{:S(2)}, u32[]{:S(2)}) collective-permute-start(bf16[80,2048]{1,0:T(8,128)(2,1)S(1)} %slice.60), channel_id=1, source_target_pairs={{0,24},{8,0},{16,8},{24,16},{1,25},{9,1},{17,9},{25,17},{2,26},{10... | collective-permute-start | bytes 983048 | tf_op jit(solution)/shard_map/ppermute | solution.py:372
  84.1 0.0 collective-permute-done.3.minus_ref
  84.2 1.9 %collective-permute-start.5 = (bf16[64,2048]{1,0:T(8,128)(2,1)S(1)}, bf16[64,2048]{1,0:T(8,128)(2,1)S(1)}, u32[]{:S(2)}, u32[]{:S(2)}) collective-permute-start(bf16[64,2048]{1,0:T(8,128)(2,1)S(1)} %slice.59), channel_id=1, source_target_pairs={{0,8},{8,16},{16,24},{24,0},{1,9},{9,17},{17,25},{25,1},{2,10},{10... | collective-permute-start | bytes 786440 | tf_op jit(solution)/shard_map/ppermute | solution.py:371
  86.1 1.7 %hidden.1 = (bf16[432,2048]{1,0:T(8,128)(2,1)S(1)}, f32[2,6144]{1,0:T(2,128)}) custom-call(bf16[144,2048]{1,0:T(8,128)(2,1)S(1)} %concatenate.3.own_ref, bf16[144,2048]{1,0:T(8,128)(2,1)S(1)} %collective-permute-done.3.minus_ref, bf16[144,2048]{1,0:T(8,128)(2,1)S(1)} %collective-permute-done.4.plus_ref, bf16[16,16,128]{2,1,0:T(8,128)(2,1)S(1)} %slice.58.ride_ref, ...), custom_call_target="tpu_custom_call" | custom-call | tf_op jit(solution)/shard_map/hidden/pallas_call | solution.py:374
  87.8 5.8 %collective-permute-done.5.low_ref = bf16[64,2048]{1,0:T(8,128)(2,1)S(1)} collective-permute-done((bf16[64,2048]{1,0:T(8,128)(2,1)S(1)}, bf16[64,2048]{1,0:T(8,128)(2,1)S(1)}, u32[]{:S(2)}, u32[]{:S(2)}) %collective-permute-start.5) | collective-permute-done | bytes 262176 | tf_op jit(solution)/shard_map/ppermute | solution.py:371
  93.6 0.0 collective-permute-done.6.high_ref
  93.6 0.0 collective-permute-done.7.other_ref
  93.6 5.2 %project.1 = (bf16[4,336,128]{2,1,0:T(8,128)(2,1)}, bf16[512,128]{1,0:T(8,128)(2,1)}, bf16[512,128]{1,0:T(8,128)(2,1)}, bf16[512,128]{1,0:T(8,128)(2,1)}, f32[2,512,128]{2,1,0:T(8,128)}) custom-call(bf16[432,2048]{1,0:T(8,128)(2,1)S(1)} %get-tuple-element.20.h_ref, bf16[64,2048]{1,0:T(8,128)(2,1)S(1)} %collective-permute-done.5.low_ref, ...), custom_call_target="tpu_custom_call" | custom-call | tf_op jit(solution)/shard_map/project/pallas_call | solution.py:382
  98.8 0.0 copy-start
  98.8 6.1 %all-to-all-start.3 = ((bf16[4,336,128]{2,1,0:T(8,128)(2,1)}), bf16[4,336,128]{2,1,0:T(8,128)(2,1)S(1)}, u32[]{:S(2)}, u32[]{:S(2)}) async-start(bf16[4,336,128]{2,1,0:T(8,128)(2,1)} %get-tuple-element.21), calls=%async_computation.3 | async-start | bytes 688128 | tf_op jit(solution)/shard_map/all_to_all | solution.py:404
  105.0 2.3 %local.1 = (f32[512,128]{1,0:T(8,128)S(1)}, bf16[512,128]{1,0:T(8,128)(2,1)S(1)}, bf16[512,128]{1,0:T(8,128)(2,1)S(1)}) custom-call(bf16[512,128]{1,0:T(8,128)(2,1)} %get-tuple-element.22.q_ref, bf16[512,128]{1,0:T(8,128)(2,1)} %get-tuple-element.23.k_ref, bf16[512,128]{1,0:T(8,128)(2,1)} %get-tuple-element.24.v_ref, f32[2,512,128]{2,1,0:T(8,128)} %get-tuple-element.25.cum_ref), custom_call_target="tpu_custom_call" | custom-call | tf_op jit(solution)/shard_map/local/pallas_call | solution.py:405
  107.3 15.1 %all-to-all-done.3.in_ref = bf16[4,336,128]{2,1,0:T(8,128)(2,1)S(1)} async-done(((bf16[4,336,128]{2,1,0:T(8,128)(2,1)}), bf16[4,336,128]{2,1,0:T(8,128)(2,1)S(1)}, u32[]{:S(2)}, u32[]{:S(2)}) %all-to-all-start.3) | async-done | bytes 344096 | tf_op jit(solution)/shard_map/all_to_all | solution.py:404
  122.4 0.5 combine.1
  122.9 10.2 %all_to_all.32.mix_ref = bf16[4,128,128]{2,1,0:T(8,128)(2,1)S(1)} all-to-all(bf16[4,128,128]{2,1,0:T(8,128)(2,1)S(1)} %bitcast.10), channel_id=1, replica_groups=mesh['A'=4,'B'=4,'tp'=4,'x'=4,'core'=2] {'B'}, dimensions={0} | all-to-all | bytes 262144 | tf_op jit(solution)/shard_map/all_to_all | solution.py:421
  133.1 0.0 copy-done
  133.1 0.0 copy-start.1
  133.1 2.0 %output.1 = bf16[128,2048]{1,0:T(8,128)(2,1)} custom-call(bf16[4,128,128]{2,1,0:T(8,128)(2,1)S(1)} %all_to_all.32.mix_ref, f32[1,256]{1,0:T(1,128)} %bitcast.17, bf16[512,2048]{1,0:T(8,128)(2,1)S(1)} %copy-done), custom_call_target="tpu_custom_call" | custom-call | tf_op jit(solution)/shard_map/output/pallas_call | solution.py:422
  135.1 3.5 %all-to-all-start.5 = ((bf16[4,32,2048]{2,1,0:T(8,128)(2,1)}), bf16[4,32,2048]{2,1,0:T(8,128)(2,1)S(1)}, u32[]{:S(2)}, u32[]{:S(2)}) async-start(bf16[4,32,2048]{2,1,0:T(8,128)(2,1)} %bitcast.8), calls=%async_computation.5 | async-start | bytes 1048576 | tf_op jit(solution)/shard_map/all_to_all | solution.py:430
  138.6 0.7 slice.48
  139.3 7.3 %all-to-all-done.5 = bf16[4,32,2048]{2,1,0:T(8,128)(2,1)S(1)} async-done(((bf16[4,32,2048]{2,1,0:T(8,128)(2,1)}), bf16[4,32,2048]{2,1,0:T(8,128)(2,1)S(1)}, u32[]{:S(2)}, u32[]{:S(2)}) %all-to-all-start.5) | async-done | bytes 524320 | tf_op jit(solution)/shard_map/all_to_all | solution.py:430
  146.6 0.1 reduce_sum.12
  146.7 0.0 copy-done.1
  146.7 0.7 add_convert_fusion
  (12 shorter events, 0.2 us)
Async XLA Ops:
  45.3 27.5 %all-to-all-start.2 = ((bf16[4,16,16,384]{3,2,1,0:T(8,128)(2,1)}), bf16[4,16,16,384]{3,2,1,0:T(8,128)(2,1)S(1)}, u32[]{:S(2)}, u32[]{:S(2)}) async-start(bf16[4,16,16,384]{3,2,1,0:T(8,128)(2,1)} %broadcast_in_dim.2), calls=%async_computation.2 | async-start | bytes 1572864 | tf_op jit(solution)/shard_map/all_to_all | solution.py:36
  50.0 10.5 %collective-permute-start = (bf16[36,2048]{1,0:T(8,128)(2,1)S(1)}, bf16[36,2048]{1,0:T(8,128)(2,1)S(1)}, u32[]{:S(2)}, u32[]{:S(2)}) collective-permute-start(bf16[36,2048]{1,0:T(8,128)(2,1)S(1)} %get-tuple-element.17), channel_id=1, source_target_pairs={{0,32},{32,0},{64,96},{96,64},{1,33},{33,1},{65,97},{97,65},{2,34}... | collective-permute-start | bytes 442376 | tf_op jit(solution)/shard_map/ppermute | solution.py:346
  54.2 10.6 %collective-permute-start.1 = (bf16[36,2048]{1,0:T(8,128)(2,1)S(1)}, bf16[36,2048]{1,0:T(8,128)(2,1)S(1)}, u32[]{:S(2)}, u32[]{:S(2)}) collective-permute-start(bf16[36,2048]{1,0:T(8,128)(2,1)S(1)} %get-tuple-element.17), channel_id=1, source_target_pairs={{0,64},{32,96},{64,0},{96,32},{1,65},{33,97},{65,1},{97,33},{2,66}... | collective-permute-start | bytes 442376 | tf_op jit(solution)/shard_map/ppermute | solution.py:346
  57.7 9.1 %collective-permute-start.2 = (bf16[36,2048]{1,0:T(8,128)(2,1)S(1)}, bf16[36,2048]{1,0:T(8,128)(2,1)S(1)}, u32[]{:S(2)}, u32[]{:S(2)}) collective-permute-start(bf16[36,2048]{1,0:T(8,128)(2,1)S(1)} %get-tuple-element.17), channel_id=1, source_target_pairs={{0,96},{32,64},{64,32},{96,0},{1,97},{33,65},{65,33},{97,1},{2,98}... | collective-permute-start | bytes 442376 | tf_op jit(solution)/shard_map/ppermute | solution.py:346
  66.9 12.9 %collective-permute-start.4 = (bf16[144,2048]{1,0:T(8,128)(2,1)S(1)}, bf16[144,2048]{1,0:T(8,128)(2,1)S(1)}, u32[]{:S(2)}, u32[]{:S(2)}) collective-permute-start(bf16[144,2048]{1,0:T(8,128)(2,1)S(1)} %concatenate.3.own_ref), channel_id=1, source_target_pairs={{0,24},{8,0},{16,8},{24,16},{1,25},{9,1},{17,9},{25,17},{2,26},{10... | collective-permute-start | bytes 1769480 | tf_op jit(solution)/shard_map/ppermute | solution.py:370
  70.0 14.1 %collective-permute-start.3 = (bf16[144,2048]{1,0:T(8,128)(2,1)S(1)}, bf16[144,2048]{1,0:T(8,128)(2,1)S(1)}, u32[]{:S(2)}, u32[]{:S(2)}) collective-permute-start(bf16[144,2048]{1,0:T(8,128)(2,1)S(1)} %concatenate.3.own_ref), channel_id=1, source_target_pairs={{0,8},{8,16},{16,24},{24,0},{1,9},{9,17},{17,25},{25,1},{2,10},{10... | collective-permute-start | bytes 1769480 | tf_op jit(solution)/shard_map/ppermute | solution.py:369
  72.8 20.9 %collective-permute-start.7 = (bf16[4,16,16,384]{3,2,1,0:T(8,128)(2,1)S(1)}, bf16[4,16,16,384]{3,2,1,0:T(8,128)(2,1)S(1)}, u32[]{:S(2)}, u32[]{:S(2)}) collective-permute-start(bf16[4,16,16,384]{3,2,1,0:T(8,128)(2,1)S(1)} %all-to-all-done.2.mine_ref), channel_id=1, source_target_pairs={{0,1},{1,0},{2,3},{3,2},{4,5},{5,4},{6,7},{7,6},{8,9},{9,8},{10,11... | collective-permute-start | bytes 2359304 | tf_op jit(solution)/shard_map/ppermute | solution.py:363
  79.9 13.8 %collective-permute-start.6 = (bf16[80,2048]{1,0:T(8,128)(2,1)S(1)}, bf16[80,2048]{1,0:T(8,128)(2,1)S(1)}, u32[]{:S(2)}, u32[]{:S(2)}) collective-permute-start(bf16[80,2048]{1,0:T(8,128)(2,1)S(1)} %slice.60), channel_id=1, source_target_pairs={{0,24},{8,0},{16,8},{24,16},{1,25},{9,1},{17,9},{25,17},{2,26},{10... | collective-permute-start | bytes 983048 | tf_op jit(solution)/shard_map/ppermute | solution.py:372
  84.2 9.5 %collective-permute-start.5 = (bf16[64,2048]{1,0:T(8,128)(2,1)S(1)}, bf16[64,2048]{1,0:T(8,128)(2,1)S(1)}, u32[]{:S(2)}, u32[]{:S(2)}) collective-permute-start(bf16[64,2048]{1,0:T(8,128)(2,1)S(1)} %slice.59), channel_id=1, source_target_pairs={{0,8},{8,16},{16,24},{24,0},{1,9},{9,17},{17,25},{25,1},{2,10},{10... | collective-permute-start | bytes 786440 | tf_op jit(solution)/shard_map/ppermute | solution.py:371
  98.8 34.3 %copy-start = (bf16[512,2048]{1,0:T(8,128)(2,1)S(1)}, bf16[512,2048]{1,0:T(8,128)(2,1)}, u32[]{:S(2)}) copy-start(bf16[512,2048]{1,0:T(8,128)(2,1)} %w_ref.1) | copy-start | bytes 6291460
  98.8 23.6 %all-to-all-start.3 = ((bf16[4,336,128]{2,1,0:T(8,128)(2,1)}), bf16[4,336,128]{2,1,0:T(8,128)(2,1)S(1)}, u32[]{:S(2)}, u32[]{:S(2)}) async-start(bf16[4,336,128]{2,1,0:T(8,128)(2,1)} %get-tuple-element.21), calls=%async_computation.3 | async-start | bytes 688128 | tf_op jit(solution)/shard_map/all_to_all | solution.py:404
  133.1 13.6 %copy-start.1 = (bf16[32,2048]{1,0:T(8,128)(2,1)S(1)}, bf16[32,2048]{1,0:T(8,128)(2,1)}, u32[]{:S(2)}) copy-start(bf16[32,2048]{1,0:T(8,128)(2,1)} %lat_ref.1) | copy-start | bytes 393220
  135.1 11.5 %all-to-all-start.5 = ((bf16[4,32,2048]{2,1,0:T(8,128)(2,1)}), bf16[4,32,2048]{2,1,0:T(8,128)(2,1)S(1)}, u32[]{:S(2)}, u32[]{:S(2)}) async-start(bf16[4,32,2048]{2,1,0:T(8,128)(2,1)} %bitcast.8), calls=%async_computation.5 | async-start | bytes 1048576 | tf_op jit(solution)/shard_map/all_to_all | solution.py:430

commit v8 on v7

--- a/solution.py
+++ b/solution.py
@@ -16,7 +16,7 @@
 SEG = 512
 CTX_SEG = 64
 ROWS = SEG + CTX_SEG
-PAYLOAD = 336
+PAYLOAD = 328
 bf16 = jnp.bfloat16
 f32 = jnp.float32
 VM = pl.BlockSpec(memory_space=pltpu.VMEM)
@@ -121,14 +121,25 @@
         h_ref[at : at + 16, :] = normed_rows(ref[128:144, :], 1, mod_ref, gain_ref)
 
 
-def project_kernel(
-    h_ref, low_ref, high_ref, mod_ref, gain_ref, mine_ref, other_ref,
-    down_ref, up_ref, bias_ref, ride_ref,
-    pay_ref, q_ref, k_ref, v_ref, cum_ref, far_ref, w_ref, out_ref,
+def decays_of(low, up_ref, bias_ref):
+    second = lax.axis_index("B") >= 2
+
+    def of_head(a):
+        return jnp.where(second, a[:, 128:256].astype(f32), a[:, 0:128].astype(f32))
+
+    raw = []
+    for z in range(2):
+        up = of_head(up_ref[z]).astype(bf16)
+        part = jnp.dot(low[:, z * RANK : (z + 1) * RANK], up, preferred_element_type=f32)
+        raw.append(part + of_head(bias_ref[z : z + 1, :]))
+    raw = jnp.concatenate(raw, axis=1)
+    return (jnp.minimum(raw, 0.0) - jnp.log1p(jnp.exp(-jnp.abs(raw)))) * (1.0 / SHARP)
+
+
+def near_kernel(
+    h_ref, mine_ref, other_ref, down_ref, up_ref, bias_ref, w_ref, qkv_ref, logs_ref
 ):
-    seg, sub = lax.axis_index("A"), lax.axis_index("B")
-    y, core = lax.axis_index("tp"), lax.axis_index("core")
-    second = sub >= 2
+    core = lax.axis_index("core")
     for xi in range(4):
         for z in range(16):
             at = z * 128 + xi * 32
@@ -136,36 +147,44 @@
             there = pl.ds(pl.multiple_of(at + 16 - core * 16, 16), 16)
             w_ref[here, :] = mine_ref[xi, z]
             w_ref[there, :] = other_ref[xi, z]
+    rows = h_ref[...]
+    low = nt(rows, down_ref[...]).astype(bf16)
+    logs_ref[...] = decays_of(low, up_ref, bias_ref)
+    qkv_ref[...] = jnp.dot(rows, w_ref[...], preferred_element_type=f32).astype(bf16)
+
+
+def project_kernel(
+    low_ref, high_ref, mod_ref, gain_ref, w_ref, qkv_ref, logs_ref,
+    down_ref, up_ref, bias_ref, ride_ref,
+    pay_ref, q_ref, k_ref, v_ref, cum_ref, far_ref, out_ref, all_logs_ref,
+):
+    seg, sub = lax.axis_index("A"), lax.axis_index("B")
+    y = lax.axis_index("tp")
     for j in range(4):
         rows = (low_ref, high_ref)[j // 2][(j % 2) * 32 : (j % 2) * 32 + 32, :]
         far_ref[j * 32 : j * 32 + 32, :] = normed_rows(rows, 0, mod_ref, gain_ref)
     far_ref[128:144, :] = normed_rows(high_ref[64:80, :], 1, mod_ref, gain_ref)
     y_of = [y, (y + 3) % 4, (y + 1) % 4, (y + 2) % 4]
-    for first, rows in ((0, h_ref[...]), (3, far_ref[...])):
-        res = jnp.dot(rows, w_ref[...], preferred_element_type=f32).astype(bf16)
-        res = jnp.concatenate([res, nt(rows, down_ref[...]).astype(bf16)], axis=1)
-        for n in range(rows.shape[0] // 144):
-            for j in range(4):
-                at = pl.multiple_of((sub ^ j) * 128 + y_of[first + n] * 32, 32)
-                out_ref[pl.ds(at, 32), 0:448] = res[n * 144 + j * 32 : n * 144 + j * 32 + 32]
-            at = SEG + (first + n) * 16
-            out_ref[at : at + 16, 0:448] = res[n * 144 + 128 : n * 144 + 144]
-    out = out_ref[:, 0:448]
+    rows = far_ref[...]
+    low = nt(rows, down_ref[...]).astype(bf16)
+    far_logs = decays_of(low, up_ref, bias_ref)
+    far_qkv = jnp.dot(rows, w_ref[...], preferred_element_type=f32).astype(bf16)
+    for n in range(4):
+        for j in range(5):
+            size = 32 if j < 4 else 16
+            first = n * 144 + j * 32 if n < 3 else j * 32
+            took = slice(first, first + size)
+            if j < 4:
+                at = pl.ds(pl.multiple_of((sub ^ j) * 128 + y_of[n] * 32, 32), size)
+            else:
+                at = pl.ds(SEG + n * 16, size)
+            out_ref[at, :] = qkv_ref[took, :] if n < 3 else far_qkv[took]
+            all_logs_ref[at, :] = logs_ref[took, :] if n < 3 else far_logs[took]
+    out = out_ref[...]
+    logs = all_logs_ref[...]
     q_ref[...] = out[:SEG, 0:128]
     k_ref[...] = out[:SEG, 128:256]
     v_ref[...] = out[:SEG, 256:384]
-    low = out[:, 384:448]
-
-    def of_head(a):
-        return jnp.where(second, a[:, 128:256].astype(f32), a[:, 0:128].astype(f32))
-
-    raw = []
-    for z in range(2):
-        up = of_head(up_ref[z]).astype(bf16)
-        part = jnp.dot(low[:, z * RANK : (z + 1) * RANK], up, preferred_element_type=f32)
-        raw.append(part + of_head(bias_ref[z : z + 1, :]))
-    raw = jnp.concatenate(raw, axis=1)
-    logs = (jnp.minimum(raw, 0.0) - jnp.log1p(jnp.exp(-jnp.abs(raw)))) * (1.0 / SHARP)
     ef, eb = [], []
     for zb in range(4):
         t = jnp.transpose(ride_ref[seg * 4 + zb].astype(f32))
@@ -219,7 +238,7 @@
     ckf = (ck * jnp.exp(later)).astype(bf16)
     ckb = (ck * jnp.exp(earlier)).astype(bf16)
     cv = out[SEG:, 256:384]
-    zero = jnp.zeros((7, DK), bf16)
+    zero = jnp.zeros((2, DK), bf16)
     for peer in range(4):
         ahead = peer > seg
         pay_ref[peer, 0:128, :] = jnp.where(ahead, states[:, 0:128], states[:, 128:256])
@@ -227,9 +246,8 @@
         pay_ref[peer, 192:256, :] = ckb
         pay_ref[peer, 256:320, :] = cv
         dev = jnp.where(ahead, dev_f, dev_b)
-        pay_ref[peer, 320:336, :] = jnp.concatenate(
-            [*three_parts(dev), *three_parts(ctx_f), *three_parts(ctx_b), zero], axis=0
-        )
+        two = [p for t in (dev, ctx_f, ctx_b) for p in three_parts(t)[:2]]
+        pay_ref[peer, 320:328, :] = jnp.concatenate([*two, zero], axis=0)
 
 
 def local_kernel(q_ref, k_ref, v_ref, cum_ref, o_ref, lift_f_ref, lift_b_ref):
@@ -282,15 +300,15 @@
     seg = lax.axis_index("A")
 
     def vec(peer, at):
-        rows = in_ref[peer, 320:336, :].astype(f32)
-        return rows[at : at + 1] + rows[at + 1 : at + 2] + rows[at + 2 : at + 3]
+        rows = in_ref[peer, 320:328, :].astype(f32)
+        return rows[at : at + 1] + rows[at + 1 : at + 2]
 
     ctx_f = jnp.zeros((DK, DK), f32)
     ctx_b = jnp.zeros((DK, DK), f32)
     for q in range(4):
-        ctx_f = jnp.exp(vec(q, 3)) * ctx_f + tn(in_ref[q, 256:320, :], in_ref[q, 128:192, :])
+        ctx_f = jnp.exp(vec(q, 2)) * ctx_f + tn(in_ref[q, 256:320, :], in_ref[q, 128:192, :])
     for q in reversed(range(4)):
-        ctx_b = jnp.exp(vec(q, 6)) * ctx_b + tn(in_ref[q, 256:320, :], in_ref[q, 192:256, :])
+        ctx_b = jnp.exp(vec(q, 4)) * ctx_b + tn(in_ref[q, 256:320, :], in_ref[q, 192:256, :])
     fwd = CTX_LIFT * ctx_f
     for a in range(3):
         moved = jnp.exp(vec(a, 0)) * fwd + in_ref[a, 0:128, :].astype(f32)
@@ -379,6 +397,14 @@
         compiler_params=pltpu.CompilerParams(vmem_limit_bytes=16 * 1024 * 1024),
         name="hidden",
     )(*on_chip(own, minus, plus, ride), *off_chip(norm_gain.reshape(1, D)))
+    weights, near_qkv, near_logs = pl.pallas_call(
+        near_kernel,
+        out_shape=(sds((D, 384), bf16), sds((432, 384), bf16), sds((432, 256), f32)),
+        in_specs=[VM] * 6,
+        out_specs=(VM,) * 3,
+        compiler_params=pltpu.CompilerParams(vmem_limit_bytes=16 * 1024 * 1024),
+        name="near",
+    )(*on_chip(near_hidden, mine, other), *off_chip(decay_down.T, decay_up, decay_bias))
     payload, q, k, v, cum = pl.pallas_call(
         project_kernel,
         out_shape=(
@@ -392,14 +418,15 @@
         out_specs=(VM,) * 5,
         scratch_shapes=[
             pltpu.VMEM((144, D), bf16),
-            pltpu.VMEM((D, 384), bf16),
-            pltpu.VMEM((ROWS, 512), bf16),
+            pltpu.VMEM((ROWS, 384), bf16),
+            pltpu.VMEM((ROWS, 256), f32),
         ],
-        compiler_params=pltpu.CompilerParams(vmem_limit_bytes=24 * 1024 * 1024),
+        compiler_params=pltpu.CompilerParams(vmem_limit_bytes=20 * 1024 * 1024),
         name="project",
     )(
-        *on_chip(near_hidden), *on_chip(low, high), *off_chip(modulation, norm_gain.reshape(1, D)),
-        *on_chip(mine, other), *off_chip(decay_down.T, decay_up, decay_bias), *on_chip(ride),
+        *on_chip(low, high), *off_chip(modulation, norm_gain.reshape(1, D)),
+        *on_chip(weights, near_qkv, near_logs),
+        *off_chip(decay_down.T, decay_up, decay_bias), *on_chip(ride),
     )
     got = lax.all_to_all(payload, "A", 0, 0, tiled=True)
     local, lift_f, lift_b = pl.pallas_call(

time: 148 us -> 147 us (level)
  waiting for transfers between devices: 39.6 us -> 36.5 us
    ppermute x1, waiting for transfers between devices: 5.8 us -> 2.87 us  [device_body(): low = lax.ppermute(minus[:64], 'tp', up_shift)]
    pallas_call x0 -> x1, Pallas kernels: none -> 2.91 us  [device_body(): pl.pallas_call(near_kernel, out_shape=(sds((D, 384), bf16), sds((432, 384...]
    pallas_call x1, Pallas kernels: 5.2 us -> 3.54 us  [device_body(): pl.pallas_call(project_kernel, out_shape=(sds((4, PAYLOAD, DK), bf16), pl...]
  transfers between devices with their start and end apart: 11 -> 11, of which waited for: 6 -> 6; matrix products, arithmetic and copies ran while one was open for 1% -> 1% of each run, Pallas kernels for 3% -> 5%
where the time goes in v8:
time: 147 us; the launch traced here: 146 us
  blocking collectives  52 us (35%)
  starting transfers between devices  38.7 us (26%)
  waiting for transfers between devices  36.5 us (25%)
  Pallas kernels  15.4 us (10%)
  local copies, waits for them, and re-layouts  1.95 us (1%)
    all_to_all x1, blocking collectives, device_body(): rows_z = lax.all_to_all(cut, ('A', 'B'), 0, 0, tiled=True)  32.3 us
    all_to_all x1, waiting for transfers between devices, device_body(): got = lax.all_to_all(payload, 'A', 0, 0, tiled=True)  15 us
    ppermute x3, starting transfers between devices, device_body(): near.append(lax.ppermute(rows, 'B', [(b, b ^ j) for b in range(4)]))  10.4 us
    all_to_all x1, blocking collectives, device_body(): heads = lax.all_to_all(mixed.reshape(4, 128, DK), 'B', 0, 0, tiled=True)  10.2 us
    all_to_all x1, blocking collectives, device_body(): mods = lax.all_to_all(mods, 'tp', 0, 0, tiled=True)  9.57 us
    all_to_all x1, waiting for transfers between devices, device_body(): shares = lax.all_to_all(partial.reshape(4, 32, D), 'tp', 0, 0, tiled=True)  7.32 us
    ppermute x3, waiting for transfers between devices, device_body(): near.append(lax.ppermute(rows, 'B', [(b, b ^ j) for b in range(4)]))  6.23 us
    all_to_all x1, starting transfers between devices, device_body(): got = lax.all_to_all(payload, 'A', 0, 0, tiled=True)  6.11 us
  transfers between devices with their start and end apart: 11, of which 6 were waited for; matrix products, arithmetic and copies ran while one was open for 1% of the time, Pallas kernels for 5%

profile of v8, /device:TPU:6, one launch (start us, length us, event | category | flops | bytes accessed | tf_op | source)
XLA Modules:
  0.0 145.6 jit_solution(15661281152352817910)
XLA Ops:
  0.0 1.4 rows.1
  1.4 9.6 %all_to_all.30.mods_ref = f32[4,2,96]{2,1,0:T(2,128)S(1)} all-to-all(f32[4,2,96]{2,1,0:T(2,128)S(1)} %get-tuple-element.21), channel_id=1, replica_groups=mesh['A'=4,'B'=4,'tp'=4,'x'=4,'core'=2] {'tp'}, dimensions={0} | all-to-all | bytes 6144 | tf_op jit(solution)/shard_map/all_to_all | solution.py:361
  10.9 1.1 pack.1
  12.0 32.3 %all_to_all.31 = bf16[16,16,512]{2,1,0:T(8,128)(2,1)S(1)} all-to-all(bf16[16,16,512]{2,1,0:T(8,128)(2,1)S(1)} %pack.1), channel_id=1, replica_groups=mesh['A'=4,'B'=4,'tp'=4,'x'=4,'core'=2] {'A','B'}, dimensions={0} | all-to-all | bytes 524288 | tf_op jit(solution)/shard_map/all_to_all | solution.py:379
  44.3 1.0 broadcast_in_dim.2
  45.2 4.8 %all-to-all-start.2 = ((bf16[4,16,16,384]{3,2,1,0:T(8,128)(2,1)}), bf16[4,16,16,384]{3,2,1,0:T(8,128)(2,1)S(1)}, u32[]{:S(2)}, u32[]{:S(2)}) async-start(bf16[4,16,16,384]{3,2,1,0:T(8,128)(2,1)} %broadcast_in_dim.2), calls=%async_computation.2 | async-start | bytes 1572864 | tf_op jit(solution)/shard_map/all_to_all | solution.py:36
  50.0 4.2 %collective-permute-start = (bf16[36,2048]{1,0:T(8,128)(2,1)S(1)}, bf16[36,2048]{1,0:T(8,128)(2,1)S(1)}, u32[]{:S(2)}, u32[]{:S(2)}) collective-permute-start(bf16[36,2048]{1,0:T(8,128)(2,1)S(1)} %get-tuple-element.20), channel_id=1, source_target_pairs={{0,32},{32,0},{64,96},{96,64},{1,33},{33,1},{65,97},{97,65},{2,34}... | collective-permute-start | bytes 442376 | tf_op jit(solution)/shard_map/ppermute | solution.py:364
  54.2 3.4 %collective-permute-start.1 = (bf16[36,2048]{1,0:T(8,128)(2,1)S(1)}, bf16[36,2048]{1,0:T(8,128)(2,1)S(1)}, u32[]{:S(2)}, u32[]{:S(2)}) collective-permute-start(bf16[36,2048]{1,0:T(8,128)(2,1)S(1)} %get-tuple-element.20), channel_id=1, source_target_pairs={{0,64},{32,96},{64,0},{96,32},{1,65},{33,97},{65,1},{97,33},{2,66}... | collective-permute-start | bytes 442376 | tf_op jit(solution)/shard_map/ppermute | solution.py:364
  57.7 2.8 %collective-permute-start.2 = (bf16[36,2048]{1,0:T(8,128)(2,1)S(1)}, bf16[36,2048]{1,0:T(8,128)(2,1)S(1)}, u32[]{:S(2)}, u32[]{:S(2)}) collective-permute-start(bf16[36,2048]{1,0:T(8,128)(2,1)S(1)} %get-tuple-element.20), channel_id=1, source_target_pairs={{0,96},{32,64},{64,32},{96,0},{1,97},{33,65},{65,33},{97,1},{2,98}... | collective-permute-start | bytes 442376 | tf_op jit(solution)/shard_map/ppermute | solution.py:364
  60.5 0.0 collective-permute-done
  60.5 4.3 %collective-permute-done.1 = bf16[36,2048]{1,0:T(8,128)(2,1)S(1)} collective-permute-done((bf16[36,2048]{1,0:T(8,128)(2,1)S(1)}, bf16[36,2048]{1,0:T(8,128)(2,1)S(1)}, u32[]{:S(2)}, u32[]{:S(2)}) %collective-permute-start.1) | collective-permute-done | bytes 147488 | tf_op jit(solution)/shard_map/ppermute | solution.py:364
  64.9 1.9 %collective-permute-done.2 = bf16[36,2048]{1,0:T(8,128)(2,1)S(1)} collective-permute-done((bf16[36,2048]{1,0:T(8,128)(2,1)S(1)}, bf16[36,2048]{1,0:T(8,128)(2,1)S(1)}, u32[]{:S(2)}, u32[]{:S(2)}) %collective-permute-start.2) | collective-permute-done | bytes 147488 | tf_op jit(solution)/shard_map/ppermute | solution.py:364
  66.8 0.1 concatenate.3.own_ref
  66.9 3.1 %collective-permute-start.4 = (bf16[144,2048]{1,0:T(8,128)(2,1)S(1)}, bf16[144,2048]{1,0:T(8,128)(2,1)S(1)}, u32[]{:S(2)}, u32[]{:S(2)}) collective-permute-start(bf16[144,2048]{1,0:T(8,128)(2,1)S(1)} %concatenate.3.own_ref), channel_id=1, source_target_pairs={{0,24},{8,0},{16,8},{24,16},{1,25},{9,1},{17,9},{25,17},{2,26},{10... | collective-permute-start | bytes 1769480 | tf_op jit(solution)/shard_map/ppermute | solution.py:388
  70.0 2.8 %collective-permute-start.3 = (bf16[144,2048]{1,0:T(8,128)(2,1)S(1)}, bf16[144,2048]{1,0:T(8,128)(2,1)S(1)}, u32[]{:S(2)}, u32[]{:S(2)}) collective-permute-start(bf16[144,2048]{1,0:T(8,128)(2,1)S(1)} %concatenate.3.own_ref), channel_id=1, source_target_pairs={{0,8},{8,16},{16,24},{24,0},{1,9},{9,17},{17,25},{25,1},{2,10},{10... | collective-permute-start | bytes 1769480 | tf_op jit(solution)/shard_map/ppermute | solution.py:387
  72.8 0.0 all-to-all-done.2.mine_ref
  72.8 1.9 %collective-permute-start.7 = (bf16[4,16,16,384]{3,2,1,0:T(8,128)(2,1)S(1)}, bf16[4,16,16,384]{3,2,1,0:T(8,128)(2,1)S(1)}, u32[]{:S(2)}, u32[]{:S(2)}) collective-permute-start(bf16[4,16,16,384]{3,2,1,0:T(8,128)(2,1)S(1)} %all-to-all-done.2.mine_ref), channel_id=1, source_target_pairs={{0,1},{1,0},{2,3},{3,2},{4,5},{5,4},{6,7},{7,6},{8,9},{9,8},{10,11... | collective-permute-start | bytes 2359304 | tf_op jit(solution)/shard_map/ppermute | solution.py:381
  74.7 5.1 %collective-permute-done.4.plus_ref = bf16[144,2048]{1,0:T(8,128)(2,1)S(1)} collective-permute-done((bf16[144,2048]{1,0:T(8,128)(2,1)S(1)}, bf16[144,2048]{1,0:T(8,128)(2,1)S(1)}, u32[]{:S(2)}, u32[]{:S(2)}) %collective-permute-start.4) | collective-permute-done | bytes 589856 | tf_op jit(solution)/shard_map/ppermute | solution.py:388
  79.9 4.2 %collective-permute-start.6 = (bf16[80,2048]{1,0:T(8,128)(2,1)S(1)}, bf16[80,2048]{1,0:T(8,128)(2,1)S(1)}, u32[]{:S(2)}, u32[]{:S(2)}) collective-permute-start(bf16[80,2048]{1,0:T(8,128)(2,1)S(1)} %slice.60), channel_id=1, source_target_pairs={{0,24},{8,0},{16,8},{24,16},{1,25},{9,1},{17,9},{25,17},{2,26},{10... | collective-permute-start | bytes 983048 | tf_op jit(solution)/shard_map/ppermute | solution.py:390
  84.1 0.0 collective-permute-done.3.minus_ref
  84.2 1.9 %collective-permute-start.5 = (bf16[64,2048]{1,0:T(8,128)(2,1)S(1)}, bf16[64,2048]{1,0:T(8,128)(2,1)S(1)}, u32[]{:S(2)}, u32[]{:S(2)}) collective-permute-start(bf16[64,2048]{1,0:T(8,128)(2,1)S(1)} %slice.59), channel_id=1, source_target_pairs={{0,8},{8,16},{16,24},{24,0},{1,9},{9,17},{17,25},{25,1},{2,10},{10... | collective-permute-start | bytes 786440 | tf_op jit(solution)/shard_map/ppermute | solution.py:389
  86.1 1.7 %hidden.1 = (bf16[432,2048]{1,0:T(8,128)(2,1)S(1)}, f32[2,6144]{1,0:T(2,128)}) custom-call(bf16[144,2048]{1,0:T(8,128)(2,1)S(1)} %concatenate.3.own_ref, bf16[144,2048]{1,0:T(8,128)(2,1)S(1)} %collective-permute-done.3.minus_ref, bf16[144,2048]{1,0:T(8,128)(2,1)S(1)} %collective-permute-done.4.plus_ref, bf16[16,16,128]{2,1,0:T(8,128)(2,1)S(1)} %slice.58.ride_ref, ...), custom_call_target="tpu_custom_call" | custom-call | tf_op jit(solution)/shard_map/hidden/pallas_call | solution.py:392
  87.8 0.0 collective-permute-done.7.other_ref
  87.8 2.9 %near.1 = (bf16[2048,384]{1,0:T(8,128)(2,1)S(1)}, bf16[432,384]{1,0:T(8,128)(2,1)S(1)}, f32[432,256]{1,0:T(8,128)S(1)}) custom-call(bf16[432,2048]{1,0:T(8,128)(2,1)S(1)} %get-tuple-element.23.h_ref, bf16[4,16,16,384]{3,2,1,0:T(8,128)(2,1)S(1)} %all-to-all-done.2.mine_ref, bf16[4,16,16,384]{3,2,1,0:T(8,128)(2,1)S(1)} %collective-permute-done.7.other_ref, ...), custom_call_target="tpu_custom_call" | custom-call | tf_op jit(solution)/shard_map/near/pallas_call | solution.py:400
  90.8 2.9 %collective-permute-done.5.low_ref = bf16[64,2048]{1,0:T(8,128)(2,1)S(1)} collective-permute-done((bf16[64,2048]{1,0:T(8,128)(2,1)S(1)}, bf16[64,2048]{1,0:T(8,128)(2,1)S(1)}, u32[]{:S(2)}, u32[]{:S(2)}) %collective-permute-start.5) | collective-permute-done | bytes 262176 | tf_op jit(solution)/shard_map/ppermute | solution.py:389
  93.6 0.0 collective-permute-done.6.high_ref
  93.6 3.5 %project.1 = (bf16[4,328,128]{2,1,0:T(8,128)(2,1)}, bf16[512,128]{1,0:T(8,128)(2,1)}, bf16[512,128]{1,0:T(8,128)(2,1)}, bf16[512,128]{1,0:T(8,128)(2,1)}, f32[2,512,128]{2,1,0:T(8,128)}) custom-call(bf16[64,2048]{1,0:T(8,128)(2,1)S(1)} %collective-permute-done.5.low_ref, bf16[80,2048]{1,0:T(8,128)(2,1)S(1)} %collective-permute-done.6.high_ref, ...), custom_call_target="tpu_custom_call" | custom-call | tf_op jit(solution)/shard_map/project/pallas_call | solution.py:408
  97.2 0.0 copy-start
  97.2 6.1 %all-to-all-start.3 = ((bf16[4,328,128]{2,1,0:T(8,128)(2,1)}), bf16[4,328,128]{2,1,0:T(8,128)(2,1)S(1)}, u32[]{:S(2)}, u32[]{:S(2)}) async-start(bf16[4,328,128]{2,1,0:T(8,128)(2,1)} %get-tuple-element.27), calls=%async_computation.3 | async-start | bytes 671744 | tf_op jit(solution)/shard_map/all_to_all | solution.py:431
  103.3 2.3 %local.1 = (f32[512,128]{1,0:T(8,128)S(1)}, bf16[512,128]{1,0:T(8,128)(2,1)S(1)}, bf16[512,128]{1,0:T(8,128)(2,1)S(1)}) custom-call(bf16[512,128]{1,0:T(8,128)(2,1)} %get-tuple-element.28.q_ref, bf16[512,128]{1,0:T(8,128)(2,1)} %get-tuple-element.29.k_ref, bf16[512,128]{1,0:T(8,128)(2,1)} %get-tuple-element.30.v_ref, f32[2,512,128]{2,1,0:T(8,128)} %get-tuple-element.31.cum_ref), custom_call_target="tpu_custom_call" | custom-call | tf_op jit(solution)/shard_map/local/pallas_call | solution.py:432
  105.6 15.0 %all-to-all-done.3.in_ref = bf16[4,328,128]{2,1,0:T(8,128)(2,1)S(1)} async-done(((bf16[4,328,128]{2,1,0:T(8,128)(2,1)}), bf16[4,328,128]{2,1,0:T(8,128)(2,1)S(1)}, u32[]{:S(2)}, u32[]{:S(2)}) %all-to-all-start.3) | async-done | bytes 335904 | tf_op jit(solution)/shard_map/all_to_all | solution.py:431
  120.6 0.5 combine.1
  121.1 10.2 %all_to_all.32.mix_ref = bf16[4,128,128]{2,1,0:T(8,128)(2,1)S(1)} all-to-all(bf16[4,128,128]{2,1,0:T(8,128)(2,1)S(1)} %bitcast.10), channel_id=1, replica_groups=mesh['A'=4,'B'=4,'tp'=4,'x'=4,'core'=2] {'B'}, dimensions={0} | all-to-all | bytes 262144 | tf_op jit(solution)/shard_map/all_to_all | solution.py:448
  131.3 0.0 copy-done
  131.3 0.0 copy-start.1
  131.3 2.0 %output.1 = bf16[128,2048]{1,0:T(8,128)(2,1)} custom-call(bf16[4,128,128]{2,1,0:T(8,128)(2,1)S(1)} %all_to_all.32.mix_ref, f32[1,256]{1,0:T(1,128)} %bitcast.18, bf16[512,2048]{1,0:T(8,128)(2,1)S(1)} %copy-done), custom_call_target="tpu_custom_call" | custom-call | tf_op jit(solution)/shard_map/output/pallas_call | solution.py:449
  133.3 3.5 %all-to-all-start.5 = ((bf16[4,32,2048]{2,1,0:T(8,128)(2,1)}), bf16[4,32,2048]{2,1,0:T(8,128)(2,1)S(1)}, u32[]{:S(2)}, u32[]{:S(2)}) async-start(bf16[4,32,2048]{2,1,0:T(8,128)(2,1)} %bitcast.8), calls=%async_computation.5 | async-start | bytes 1048576 | tf_op jit(solution)/shard_map/all_to_all | solution.py:457
  136.8 0.7 slice.48
  137.5 7.3 %all-to-all-done.5 = bf16[4,32,2048]{2,1,0:T(8,128)(2,1)S(1)} async-done(((bf16[4,32,2048]{2,1,0:T(8,128)(2,1)}), bf16[4,32,2048]{2,1,0:T(8,128)(2,1)S(1)}, u32[]{:S(2)}, u32[]{:S(2)}) %all-to-all-start.5) | async-done | bytes 524320 | tf_op jit(solution)/shard_map/all_to_all | solution.py:457
  144.9 0.1 reduce_sum.12
  144.9 0.0 copy-done.1
  144.9 0.7 add_convert_fusion
  (12 shorter events, 0.2 us)
Async XLA Ops:
  45.2 27.5 %all-to-all-start.2 = ((bf16[4,16,16,384]{3,2,1,0:T(8,128)(2,1)}), bf16[4,16,16,384]{3,2,1,0:T(8,128)(2,1)S(1)}, u32[]{:S(2)}, u32[]{:S(2)}) async-start(bf16[4,16,16,384]{3,2,1,0:T(8,128)(2,1)} %broadcast_in_dim.2), calls=%async_computation.2 | async-start | bytes 1572864 | tf_op jit(solution)/shard_map/all_to_all | solution.py:36
  50.0 10.5 %collective-permute-start = (bf16[36,2048]{1,0:T(8,128)(2,1)S(1)}, bf16[36,2048]{1,0:T(8,128)(2,1)S(1)}, u32[]{:S(2)}, u32[]{:S(2)}) collective-permute-start(bf16[36,2048]{1,0:T(8,128)(2,1)S(1)} %get-tuple-element.20), channel_id=1, source_target_pairs={{0,32},{32,0},{64,96},{96,64},{1,33},{33,1},{65,97},{97,65},{2,34}... | collective-permute-start | bytes 442376 | tf_op jit(solution)/shard_map/ppermute | solution.py:364
  54.2 10.6 %collective-permute-start.1 = (bf16[36,2048]{1,0:T(8,128)(2,1)S(1)}, bf16[36,2048]{1,0:T(8,128)(2,1)S(1)}, u32[]{:S(2)}, u32[]{:S(2)}) collective-permute-start(bf16[36,2048]{1,0:T(8,128)(2,1)S(1)} %get-tuple-element.20), channel_id=1, source_target_pairs={{0,64},{32,96},{64,0},{96,32},{1,65},{33,97},{65,1},{97,33},{2,66}... | collective-permute-start | bytes 442376 | tf_op jit(solution)/shard_map/ppermute | solution.py:364
  57.7 9.1 %collective-permute-start.2 = (bf16[36,2048]{1,0:T(8,128)(2,1)S(1)}, bf16[36,2048]{1,0:T(8,128)(2,1)S(1)}, u32[]{:S(2)}, u32[]{:S(2)}) collective-permute-start(bf16[36,2048]{1,0:T(8,128)(2,1)S(1)} %get-tuple-element.20), channel_id=1, source_target_pairs={{0,96},{32,64},{64,32},{96,0},{1,97},{33,65},{65,33},{97,1},{2,98}... | collective-permute-start | bytes 442376 | tf_op jit(solution)/shard_map/ppermute | solution.py:364
  66.9 12.9 %collective-permute-start.4 = (bf16[144,2048]{1,0:T(8,128)(2,1)S(1)}, bf16[144,2048]{1,0:T(8,128)(2,1)S(1)}, u32[]{:S(2)}, u32[]{:S(2)}) collective-permute-start(bf16[144,2048]{1,0:T(8,128)(2,1)S(1)} %concatenate.3.own_ref), channel_id=1, source_target_pairs={{0,24},{8,0},{16,8},{24,16},{1,25},{9,1},{17,9},{25,17},{2,26},{10... | collective-permute-start | bytes 1769480 | tf_op jit(solution)/shard_map/ppermute | solution.py:388
  70.0 14.1 %collective-permute-start.3 = (bf16[144,2048]{1,0:T(8,128)(2,1)S(1)}, bf16[144,2048]{1,0:T(8,128)(2,1)S(1)}, u32[]{:S(2)}, u32[]{:S(2)}) collective-permute-start(bf16[144,2048]{1,0:T(8,128)(2,1)S(1)} %concatenate.3.own_ref), channel_id=1, source_target_pairs={{0,8},{8,16},{16,24},{24,0},{1,9},{9,17},{17,25},{25,1},{2,10},{10... | collective-permute-start | bytes 1769480 | tf_op jit(solution)/shard_map/ppermute | solution.py:387
  72.8 15.1 %collective-permute-start.7 = (bf16[4,16,16,384]{3,2,1,0:T(8,128)(2,1)S(1)}, bf16[4,16,16,384]{3,2,1,0:T(8,128)(2,1)S(1)}, u32[]{:S(2)}, u32[]{:S(2)}) collective-permute-start(bf16[4,16,16,384]{3,2,1,0:T(8,128)(2,1)S(1)} %all-to-all-done.2.mine_ref), channel_id=1, source_target_pairs={{0,1},{1,0},{2,3},{3,2},{4,5},{5,4},{6,7},{7,6},{8,9},{9,8},{10,11... | collective-permute-start | bytes 2359304 | tf_op jit(solution)/shard_map/ppermute | solution.py:381
  79.9 13.8 %collective-permute-start.6 = (bf16[80,2048]{1,0:T(8,128)(2,1)S(1)}, bf16[80,2048]{1,0:T(8,128)(2,1)S(1)}, u32[]{:S(2)}, u32[]{:S(2)}) collective-permute-start(bf16[80,2048]{1,0:T(8,128)(2,1)S(1)} %slice.60), channel_id=1, source_target_pairs={{0,24},{8,0},{16,8},{24,16},{1,25},{9,1},{17,9},{25,17},{2,26},{10... | collective-permute-start | bytes 983048 | tf_op jit(solution)/shard_map/ppermute | solution.py:390
  84.2 9.5 %collective-permute-start.5 = (bf16[64,2048]{1,0:T(8,128)(2,1)S(1)}, bf16[64,2048]{1,0:T(8,128)(2,1)S(1)}, u32[]{:S(2)}, u32[]{:S(2)}) collective-permute-start(bf16[64,2048]{1,0:T(8,128)(2,1)S(1)} %slice.59), channel_id=1, source_target_pairs={{0,8},{8,16},{16,24},{24,0},{1,9},{9,17},{17,25},{25,1},{2,10},{10... | collective-permute-start | bytes 786440 | tf_op jit(solution)/shard_map/ppermute | solution.py:389
  97.2 34.1 %copy-start = (bf16[512,2048]{1,0:T(8,128)(2,1)S(1)}, bf16[512,2048]{1,0:T(8,128)(2,1)}, u32[]{:S(2)}) copy-start(bf16[512,2048]{1,0:T(8,128)(2,1)} %w_ref.1) | copy-start | bytes 6291460
  97.2 23.4 %all-to-all-start.3 = ((bf16[4,328,128]{2,1,0:T(8,128)(2,1)}), bf16[4,328,128]{2,1,0:T(8,128)(2,1)S(1)}, u32[]{:S(2)}, u32[]{:S(2)}) async-start(bf16[4,328,128]{2,1,0:T(8,128)(2,1)} %get-tuple-element.27), calls=%async_computation.3 | async-start | bytes 671744 | tf_op jit(solution)/shard_map/all_to_all | solution.py:431
  131.3 13.6 %copy-start.1 = (bf16[32,2048]{1,0:T(8,128)(2,1)S(1)}, bf16[32,2048]{1,0:T(8,128)(2,1)}, u32[]{:S(2)}) copy-start(bf16[32,2048]{1,0:T(8,128)(2,1)} %lat_ref.1) | copy-start | bytes 393220
  133.3 11.5 %all-to-all-start.5 = ((bf16[4,32,2048]{2,1,0:T(8,128)(2,1)}), bf16[4,32,2048]{2,1,0:T(8,128)(2,1)S(1)}, u32[]{:S(2)}, u32[]{:S(2)}) async-start(bf16[4,32,2048]{2,1,0:T(8,128)(2,1)} %bitcast.8), calls=%async_computation.5 | async-start | bytes 1048576 | tf_op jit(solution)/shard_map/all_to_all | solution.py:457

commit v9 on v8

--- a/solution.py
+++ b/solution.py
@@ -36,6 +36,13 @@
     return lax.all_to_all(jnp.broadcast_to(x[None], (size, *x.shape)), axis, 0, 0, tiled=True)
 
 
+def role(seg, sub):
+    return sub ^ (seg // 2)
+
+
+PEERS = [[4 * a + role(a, b) for a in range(4)] for b in range(4)]
+
+
 def three_parts(x):
     hi = x.astype(bf16)
     rest = x - hi.astype(f32)
@@ -92,7 +99,7 @@
         riding.append(jnp.concatenate([*pieces, *added], axis=0).astype(bf16))
     mine = pl.ds(pl.multiple_of(dp * 16, 16), 16)
     for d in range(16):
-        b = d % 4
+        b = role(d // 4, d % 4)
         h = b // 2
         cut_ref[d, :, 0:128] = wq_ref[mine, h * 128 : (h + 1) * 128]
         cut_ref[d, :, 128:256] = wk_ref[mine, h * 128 : (h + 1) * 128]
@@ -323,8 +330,9 @@
 
 def output_kernel(mix_ref, gain_ref, w_ref, out_ref):
     total = None
+    flip = lax.axis_index("A") // 2
     for h in range(2):
-        v = jnp.concatenate([mix_ref[2 * h], mix_ref[2 * h + 1]], axis=1).astype(f32)
+        v = jnp.concatenate([mix_ref[2 * h + flip], mix_ref[2 * h + 1 - flip]], axis=1).astype(f32)
         r = lax.rsqrt(jnp.mean(v * v, axis=-1, keepdims=True) + EPS)
         n = (v * r * gain_ref[...]).astype(bf16)
         part = jnp.dot(n, w_ref[h * 256 : (h + 1) * 256, :], preferred_element_type=f32)
@@ -428,7 +436,9 @@
         *on_chip(weights, near_qkv, near_logs),
         *off_chip(decay_down.T, decay_up, decay_bias), *on_chip(ride),
     )
-    got = lax.all_to_all(payload, "A", 0, 0, tiled=True)
+    got = lax.all_to_all(
+        payload, ("A", "B"), 0, 0, tiled=True, axis_index_groups=PEERS
+    )
     local, lift_f, lift_b = pl.pallas_call(
         local_kernel,
         out_shape=(sds((SEG, DK), f32), sds((SEG, DK), bf16), sds((SEG, DK), bf16)),

time: 147 us -> 150 us (1.020)
  starting transfers between devices: 38.7 us -> 41.8 us
  waiting for transfers between devices: 36.5 us -> 39 us
  blocking collectives: 52 us -> 50.1 us
    all_to_all x1, starting transfers between devices: 6.11 us -> 9.27 us  [device_body(): lax.all_to_all(payload, ('A', 'B'), 0, 0, tiled=True, axis_index_groups=P...]
    all_to_all x1, waiting for transfers between devices: 15 us -> 17.4 us  [device_body(): lax.all_to_all(payload, ('A', 'B'), 0, 0, tiled=True, axis_index_groups=P...]
    all_to_all x1, blocking collectives: 10.2 us -> 8.31 us  [device_body(): heads = lax.all_to_all(mixed.reshape(4, 128, DK), 'B', 0, 0, tiled=True)]
where the time goes in v9:
time: 150 us; the launch traced here: 149 us
  blocking collectives  50.1 us (33%)
  starting transfers between devices  41.8 us (28%)
  waiting for transfers between devices  39 us (26%)
  Pallas kernels  15.5 us (10%)
  local copies, waits for them, and re-layouts  1.95 us (1%)
    all_to_all x1, blocking collectives, device_body(): rows_z = lax.all_to_all(cut, ('A', 'B'), 0, 0, tiled=True)  32.3 us
    all_to_all x1, waiting for transfers between devices, device_body(): lax.all_to_all(payload, ('A', 'B'), 0, 0, tiled=True, axis_index_groups=P...  17.4 us
    ppermute x3, starting transfers between devices, device_body(): near.append(lax.ppermute(rows, 'B', [(b, b ^ j) for b in range(4)]))  10.4 us
    all_to_all x1, blocking collectives, device_body(): mods = lax.all_to_all(mods, 'tp', 0, 0, tiled=True)  9.57 us
    all_to_all x1, starting transfers between devices, device_body(): lax.all_to_all(payload, ('A', 'B'), 0, 0, tiled=True, axis_index_groups=P...  9.27 us
    all_to_all x1, blocking collectives, device_body(): heads = lax.all_to_all(mixed.reshape(4, 128, DK), 'B', 0, 0, tiled=True)  8.31 us
    all_to_all x1, waiting for transfers between devices, device_body(): shares = lax.all_to_all(partial.reshape(4, 32, D), 'tp', 0, 0, tiled=True)  7.32 us
    ppermute x3, waiting for transfers between devices, device_body(): near.append(lax.ppermute(rows, 'B', [(b, b ^ j) for b in range(4)]))  6.23 us
  transfers between devices with their start and end apart: 11, of which 6 were waited for; matrix products, arithmetic and copies ran while one was open for 1% of the time, Pallas kernels for 5%

profile of v9, /device:TPU:6, one launch (start us, length us, event | category | flops | bytes accessed | tf_op | source)
XLA Modules:
  0.0 149.4 jit_solution(13629007045305873909)
XLA Ops:
  0.0 1.4 rows.1
  1.4 9.6 %all_to_all.30.mods_ref = f32[4,2,96]{2,1,0:T(2,128)S(1)} all-to-all(f32[4,2,96]{2,1,0:T(2,128)S(1)} %get-tuple-element.21), channel_id=1, replica_groups=mesh['A'=4,'B'=4,'tp'=4,'x'=4,'core'=2] {'tp'}, dimensions={0} | all-to-all | bytes 6144 | tf_op jit(solution)/shard_map/all_to_all | solution.py:369
  10.9 1.1 pack.1
  12.0 32.3 %all_to_all.31 = bf16[16,16,512]{2,1,0:T(8,128)(2,1)S(1)} all-to-all(bf16[16,16,512]{2,1,0:T(8,128)(2,1)S(1)} %pack.1), channel_id=1, replica_groups=mesh['A'=4,'B'=4,'tp'=4,'x'=4,'core'=2] {'A','B'}, dimensions={0} | all-to-all | bytes 524288 | tf_op jit(solution)/shard_map/all_to_all | solution.py:387
  44.3 1.0 broadcast_in_dim.2
  45.2 4.8 %all-to-all-start.2 = ((bf16[4,16,16,384]{3,2,1,0:T(8,128)(2,1)}), bf16[4,16,16,384]{3,2,1,0:T(8,128)(2,1)S(1)}, u32[]{:S(2)}, u32[]{:S(2)}) async-start(bf16[4,16,16,384]{3,2,1,0:T(8,128)(2,1)} %broadcast_in_dim.2), calls=%async_computation.2 | async-start | bytes 1572864 | tf_op jit(solution)/shard_map/all_to_all | solution.py:36
  50.0 4.2 %collective-permute-start = (bf16[36,2048]{1,0:T(8,128)(2,1)S(1)}, bf16[36,2048]{1,0:T(8,128)(2,1)S(1)}, u32[]{:S(2)}, u32[]{:S(2)}) collective-permute-start(bf16[36,2048]{1,0:T(8,128)(2,1)S(1)} %get-tuple-element.20), channel_id=1, source_target_pairs={{0,32},{32,0},{64,96},{96,64},{1,33},{33,1},{65,97},{97,65},{2,34}... | collective-permute-start | bytes 442376 | tf_op jit(solution)/shard_map/ppermute | solution.py:372
  54.2 3.4 %collective-permute-start.1 = (bf16[36,2048]{1,0:T(8,128)(2,1)S(1)}, bf16[36,2048]{1,0:T(8,128)(2,1)S(1)}, u32[]{:S(2)}, u32[]{:S(2)}) collective-permute-start(bf16[36,2048]{1,0:T(8,128)(2,1)S(1)} %get-tuple-element.20), channel_id=1, source_target_pairs={{0,64},{32,96},{64,0},{96,32},{1,65},{33,97},{65,1},{97,33},{2,66}... | collective-permute-start | bytes 442376 | tf_op jit(solution)/shard_map/ppermute | solution.py:372
  57.7 2.8 %collective-permute-start.2 = (bf16[36,2048]{1,0:T(8,128)(2,1)S(1)}, bf16[36,2048]{1,0:T(8,128)(2,1)S(1)}, u32[]{:S(2)}, u32[]{:S(2)}) collective-permute-start(bf16[36,2048]{1,0:T(8,128)(2,1)S(1)} %get-tuple-element.20), channel_id=1, source_target_pairs={{0,96},{32,64},{64,32},{96,0},{1,97},{33,65},{65,33},{97,1},{2,98}... | collective-permute-start | bytes 442376 | tf_op jit(solution)/shard_map/ppermute | solution.py:372
  60.5 0.0 collective-permute-done
  60.5 4.3 %collective-permute-done.1 = bf16[36,2048]{1,0:T(8,128)(2,1)S(1)} collective-permute-done((bf16[36,2048]{1,0:T(8,128)(2,1)S(1)}, bf16[36,2048]{1,0:T(8,128)(2,1)S(1)}, u32[]{:S(2)}, u32[]{:S(2)}) %collective-permute-start.1) | collective-permute-done | bytes 147488 | tf_op jit(solution)/shard_map/ppermute | solution.py:372
  64.9 1.9 %collective-permute-done.2 = bf16[36,2048]{1,0:T(8,128)(2,1)S(1)} collective-permute-done((bf16[36,2048]{1,0:T(8,128)(2,1)S(1)}, bf16[36,2048]{1,0:T(8,128)(2,1)S(1)}, u32[]{:S(2)}, u32[]{:S(2)}) %collective-permute-start.2) | collective-permute-done | bytes 147488 | tf_op jit(solution)/shard_map/ppermute | solution.py:372
  66.8 0.1 concatenate.3.own_ref
  66.9 3.1 %collective-permute-start.4 = (bf16[144,2048]{1,0:T(8,128)(2,1)S(1)}, bf16[144,2048]{1,0:T(8,128)(2,1)S(1)}, u32[]{:S(2)}, u32[]{:S(2)}) collective-permute-start(bf16[144,2048]{1,0:T(8,128)(2,1)S(1)} %concatenate.3.own_ref), channel_id=1, source_target_pairs={{0,24},{8,0},{16,8},{24,16},{1,25},{9,1},{17,9},{25,17},{2,26},{10... | collective-permute-start | bytes 1769480 | tf_op jit(solution)/shard_map/ppermute | solution.py:396
  70.0 2.8 %collective-permute-start.3 = (bf16[144,2048]{1,0:T(8,128)(2,1)S(1)}, bf16[144,2048]{1,0:T(8,128)(2,1)S(1)}, u32[]{:S(2)}, u32[]{:S(2)}) collective-permute-start(bf16[144,2048]{1,0:T(8,128)(2,1)S(1)} %concatenate.3.own_ref), channel_id=1, source_target_pairs={{0,8},{8,16},{16,24},{24,0},{1,9},{9,17},{17,25},{25,1},{2,10},{10... | collective-permute-start | bytes 1769480 | tf_op jit(solution)/shard_map/ppermute | solution.py:395
  72.8 0.0 all-to-all-done.2.mine_ref
  72.8 1.9 %collective-permute-start.7 = (bf16[4,16,16,384]{3,2,1,0:T(8,128)(2,1)S(1)}, bf16[4,16,16,384]{3,2,1,0:T(8,128)(2,1)S(1)}, u32[]{:S(2)}, u32[]{:S(2)}) collective-permute-start(bf16[4,16,16,384]{3,2,1,0:T(8,128)(2,1)S(1)} %all-to-all-done.2.mine_ref), channel_id=1, source_target_pairs={{0,1},{1,0},{2,3},{3,2},{4,5},{5,4},{6,7},{7,6},{8,9},{9,8},{10,11... | collective-permute-start | bytes 2359304 | tf_op jit(solution)/shard_map/ppermute | solution.py:389
  74.7 5.1 %collective-permute-done.4.plus_ref = bf16[144,2048]{1,0:T(8,128)(2,1)S(1)} collective-permute-done((bf16[144,2048]{1,0:T(8,128)(2,1)S(1)}, bf16[144,2048]{1,0:T(8,128)(2,1)S(1)}, u32[]{:S(2)}, u32[]{:S(2)}) %collective-permute-start.4) | collective-permute-done | bytes 589856 | tf_op jit(solution)/shard_map/ppermute | solution.py:396
  79.9 4.2 %collective-permute-start.6 = (bf16[80,2048]{1,0:T(8,128)(2,1)S(1)}, bf16[80,2048]{1,0:T(8,128)(2,1)S(1)}, u32[]{:S(2)}, u32[]{:S(2)}) collective-permute-start(bf16[80,2048]{1,0:T(8,128)(2,1)S(1)} %slice.60), channel_id=1, source_target_pairs={{0,24},{8,0},{16,8},{24,16},{1,25},{9,1},{17,9},{25,17},{2,26},{10... | collective-permute-start | bytes 983048 | tf_op jit(solution)/shard_map/ppermute | solution.py:398
  84.1 0.0 collective-permute-done.3.minus_ref
  84.2 1.9 %collective-permute-start.5 = (bf16[64,2048]{1,0:T(8,128)(2,1)S(1)}, bf16[64,2048]{1,0:T(8,128)(2,1)S(1)}, u32[]{:S(2)}, u32[]{:S(2)}) collective-permute-start(bf16[64,2048]{1,0:T(8,128)(2,1)S(1)} %slice.59), channel_id=1, source_target_pairs={{0,8},{8,16},{16,24},{24,0},{1,9},{9,17},{17,25},{25,1},{2,10},{10... | collective-permute-start | bytes 786440 | tf_op jit(solution)/shard_map/ppermute | solution.py:397
  86.1 1.7 %hidden.1 = (bf16[432,2048]{1,0:T(8,128)(2,1)S(1)}, f32[2,6144]{1,0:T(2,128)}) custom-call(bf16[144,2048]{1,0:T(8,128)(2,1)S(1)} %concatenate.3.own_ref, bf16[144,2048]{1,0:T(8,128)(2,1)S(1)} %collective-permute-done.3.minus_ref, bf16[144,2048]{1,0:T(8,128)(2,1)S(1)} %collective-permute-done.4.plus_ref, bf16[16,16,128]{2,1,0:T(8,128)(2,1)S(1)} %slice.58.ride_ref, ...), custom_call_target="tpu_custom_call" | custom-call | tf_op jit(solution)/shard_map/hidden/pallas_call | solution.py:400
  87.8 0.0 collective-permute-done.7.other_ref
  87.8 2.9 %near.1 = (bf16[2048,384]{1,0:T(8,128)(2,1)S(1)}, bf16[432,384]{1,0:T(8,128)(2,1)S(1)}, f32[432,256]{1,0:T(8,128)S(1)}) custom-call(bf16[432,2048]{1,0:T(8,128)(2,1)S(1)} %get-tuple-element.23.h_ref, bf16[4,16,16,384]{3,2,1,0:T(8,128)(2,1)S(1)} %all-to-all-done.2.mine_ref, bf16[4,16,16,384]{3,2,1,0:T(8,128)(2,1)S(1)} %collective-permute-done.7.other_ref, ...), custom_call_target="tpu_custom_call" | custom-call | tf_op jit(solution)/shard_map/near/pallas_call | solution.py:408
  90.8 2.9 %collective-permute-done.5.low_ref = bf16[64,2048]{1,0:T(8,128)(2,1)S(1)} collective-permute-done((bf16[64,2048]{1,0:T(8,128)(2,1)S(1)}, bf16[64,2048]{1,0:T(8,128)(2,1)S(1)}, u32[]{:S(2)}, u32[]{:S(2)}) %collective-permute-start.5) | collective-permute-done | bytes 262176 | tf_op jit(solution)/shard_map/ppermute | solution.py:397
  93.6 0.0 collective-permute-done.6.high_ref
  93.6 3.5 %project.1 = (bf16[4,328,128]{2,1,0:T(8,128)(2,1)}, bf16[512,128]{1,0:T(8,128)(2,1)}, bf16[512,128]{1,0:T(8,128)(2,1)}, bf16[512,128]{1,0:T(8,128)(2,1)}, f32[2,512,128]{2,1,0:T(8,128)}) custom-call(bf16[64,2048]{1,0:T(8,128)(2,1)S(1)} %collective-permute-done.5.low_ref, bf16[80,2048]{1,0:T(8,128)(2,1)S(1)} %collective-permute-done.6.high_ref, ...), custom_call_target="tpu_custom_call" | custom-call | tf_op jit(solution)/shard_map/project/pallas_call | solution.py:416
  97.2 0.0 copy-start
  97.2 9.3 %all-to-all-start.3 = ((bf16[4,328,128]{2,1,0:T(8,128)(2,1)}), bf16[4,328,128]{2,1,0:T(8,128)(2,1)S(1)}, u32[]{:S(2)}, u32[]{:S(2)}) async-start(bf16[4,328,128]{2,1,0:T(8,128)(2,1)} %get-tuple-element.27), calls=%async_computation.3 | async-start | bytes 671744 | tf_op jit(solution)/shard_map/all_to_all | solution.py:439
  106.5 2.3 %local.1 = (f32[512,128]{1,0:T(8,128)S(1)}, bf16[512,128]{1,0:T(8,128)(2,1)S(1)}, bf16[512,128]{1,0:T(8,128)(2,1)S(1)}) custom-call(bf16[512,128]{1,0:T(8,128)(2,1)} %get-tuple-element.28.q_ref, bf16[512,128]{1,0:T(8,128)(2,1)} %get-tuple-element.29.k_ref, bf16[512,128]{1,0:T(8,128)(2,1)} %get-tuple-element.30.v_ref, f32[2,512,128]{2,1,0:T(8,128)} %get-tuple-element.31.cum_ref), custom_call_target="tpu_custom_call" | custom-call | tf_op jit(solution)/shard_map/local/pallas_call | solution.py:442
  108.8 17.4 %all-to-all-done.3.in_ref = bf16[4,328,128]{2,1,0:T(8,128)(2,1)S(1)} async-done(((bf16[4,328,128]{2,1,0:T(8,128)(2,1)}), bf16[4,328,128]{2,1,0:T(8,128)(2,1)S(1)}, u32[]{:S(2)}, u32[]{:S(2)}) %all-to-all-start.3) | async-done | bytes 335904 | tf_op jit(solution)/shard_map/all_to_all | solution.py:439
  126.2 0.5 combine.1
  126.7 8.3 %all_to_all.32.mix_ref = bf16[4,128,128]{2,1,0:T(8,128)(2,1)S(1)} all-to-all(bf16[4,128,128]{2,1,0:T(8,128)(2,1)S(1)} %bitcast.10), channel_id=1, replica_groups=mesh['A'=4,'B'=4,'tp'=4,'x'=4,'core'=2] {'B'}, dimensions={0} | all-to-all | bytes 262144 | tf_op jit(solution)/shard_map/all_to_all | solution.py:458
  135.0 0.0 copy-done
  135.0 0.0 copy-start.1
  135.0 2.0 %output.1 = bf16[128,2048]{1,0:T(8,128)(2,1)} custom-call(bf16[4,128,128]{2,1,0:T(8,128)(2,1)S(1)} %all_to_all.32.mix_ref, f32[1,256]{1,0:T(1,128)} %bitcast.18, bf16[512,2048]{1,0:T(8,128)(2,1)S(1)} %copy-done), custom_call_target="tpu_custom_call" | custom-call | tf_op jit(solution)/shard_map/output/pallas_call | solution.py:459
  137.1 3.5 %all-to-all-start.5 = ((bf16[4,32,2048]{2,1,0:T(8,128)(2,1)}), bf16[4,32,2048]{2,1,0:T(8,128)(2,1)S(1)}, u32[]{:S(2)}, u32[]{:S(2)}) async-start(bf16[4,32,2048]{2,1,0:T(8,128)(2,1)} %bitcast.8), calls=%async_computation.5 | async-start | bytes 1048576 | tf_op jit(solution)/shard_map/all_to_all | solution.py:467
  140.5 0.7 slice.48
  141.3 7.3 %all-to-all-done.5 = bf16[4,32,2048]{2,1,0:T(8,128)(2,1)S(1)} async-done(((bf16[4,32,2048]{2,1,0:T(8,128)(2,1)}), bf16[4,32,2048]{2,1,0:T(8,128)(2,1)S(1)}, u32[]{:S(2)}, u32[]{:S(2)}) %all-to-all-start.5) | async-done | bytes 524320 | tf_op jit(solution)/shard_map/all_to_all | solution.py:467
  148.6 0.1 reduce_sum.12
  148.7 0.0 copy-done.1
  148.7 0.7 add_convert_fusion
  (12 shorter events, 0.2 us)
Async XLA Ops:
  45.2 27.5 %all-to-all-start.2 = ((bf16[4,16,16,384]{3,2,1,0:T(8,128)(2,1)}), bf16[4,16,16,384]{3,2,1,0:T(8,128)(2,1)S(1)}, u32[]{:S(2)}, u32[]{:S(2)}) async-start(bf16[4,16,16,384]{3,2,1,0:T(8,128)(2,1)} %broadcast_in_dim.2), calls=%async_computation.2 | async-start | bytes 1572864 | tf_op jit(solution)/shard_map/all_to_all | solution.py:36
  50.0 10.5 %collective-permute-start = (bf16[36,2048]{1,0:T(8,128)(2,1)S(1)}, bf16[36,2048]{1,0:T(8,128)(2,1)S(1)}, u32[]{:S(2)}, u32[]{:S(2)}) collective-permute-start(bf16[36,2048]{1,0:T(8,128)(2,1)S(1)} %get-tuple-element.20), channel_id=1, source_target_pairs={{0,32},{32,0},{64,96},{96,64},{1,33},{33,1},{65,97},{97,65},{2,34}... | collective-permute-start | bytes 442376 | tf_op jit(solution)/shard_map/ppermute | solution.py:372
  54.2 10.6 %collective-permute-start.1 = (bf16[36,2048]{1,0:T(8,128)(2,1)S(1)}, bf16[36,2048]{1,0:T(8,128)(2,1)S(1)}, u32[]{:S(2)}, u32[]{:S(2)}) collective-permute-start(bf16[36,2048]{1,0:T(8,128)(2,1)S(1)} %get-tuple-element.20), channel_id=1, source_target_pairs={{0,64},{32,96},{64,0},{96,32},{1,65},{33,97},{65,1},{97,33},{2,66}... | collective-permute-start | bytes 442376 | tf_op jit(solution)/shard_map/ppermute | solution.py:372
  57.7 9.1 %collective-permute-start.2 = (bf16[36,2048]{1,0:T(8,128)(2,1)S(1)}, bf16[36,2048]{1,0:T(8,128)(2,1)S(1)}, u32[]{:S(2)}, u32[]{:S(2)}) collective-permute-start(bf16[36,2048]{1,0:T(8,128)(2,1)S(1)} %get-tuple-element.20), channel_id=1, source_target_pairs={{0,96},{32,64},{64,32},{96,0},{1,97},{33,65},{65,33},{97,1},{2,98}... | collective-permute-start | bytes 442376 | tf_op jit(solution)/shard_map/ppermute | solution.py:372
  66.9 12.9 %collective-permute-start.4 = (bf16[144,2048]{1,0:T(8,128)(2,1)S(1)}, bf16[144,2048]{1,0:T(8,128)(2,1)S(1)}, u32[]{:S(2)}, u32[]{:S(2)}) collective-permute-start(bf16[144,2048]{1,0:T(8,128)(2,1)S(1)} %concatenate.3.own_ref), channel_id=1, source_target_pairs={{0,24},{8,0},{16,8},{24,16},{1,25},{9,1},{17,9},{25,17},{2,26},{10... | collective-permute-start | bytes 1769480 | tf_op jit(solution)/shard_map/ppermute | solution.py:396
  70.0 14.1 %collective-permute-start.3 = (bf16[144,2048]{1,0:T(8,128)(2,1)S(1)}, bf16[144,2048]{1,0:T(8,128)(2,1)S(1)}, u32[]{:S(2)}, u32[]{:S(2)}) collective-permute-start(bf16[144,2048]{1,0:T(8,128)(2,1)S(1)} %concatenate.3.own_ref), channel_id=1, source_target_pairs={{0,8},{8,16},{16,24},{24,0},{1,9},{9,17},{17,25},{25,1},{2,10},{10... | collective-permute-start | bytes 1769480 | tf_op jit(solution)/shard_map/ppermute | solution.py:395
  72.8 15.1 %collective-permute-start.7 = (bf16[4,16,16,384]{3,2,1,0:T(8,128)(2,1)S(1)}, bf16[4,16,16,384]{3,2,1,0:T(8,128)(2,1)S(1)}, u32[]{:S(2)}, u32[]{:S(2)}) collective-permute-start(bf16[4,16,16,384]{3,2,1,0:T(8,128)(2,1)S(1)} %all-to-all-done.2.mine_ref), channel_id=1, source_target_pairs={{0,1},{1,0},{2,3},{3,2},{4,5},{5,4},{6,7},{7,6},{8,9},{9,8},{10,11... | collective-permute-start | bytes 2359304 | tf_op jit(solution)/shard_map/ppermute | solution.py:389
  79.9 13.8 %collective-permute-start.6 = (bf16[80,2048]{1,0:T(8,128)(2,1)S(1)}, bf16[80,2048]{1,0:T(8,128)(2,1)S(1)}, u32[]{:S(2)}, u32[]{:S(2)}) collective-permute-start(bf16[80,2048]{1,0:T(8,128)(2,1)S(1)} %slice.60), channel_id=1, source_target_pairs={{0,24},{8,0},{16,8},{24,16},{1,25},{9,1},{17,9},{25,17},{2,26},{10... | collective-permute-start | bytes 983048 | tf_op jit(solution)/shard_map/ppermute | solution.py:398
  84.2 9.5 %collective-permute-start.5 = (bf16[64,2048]{1,0:T(8,128)(2,1)S(1)}, bf16[64,2048]{1,0:T(8,128)(2,1)S(1)}, u32[]{:S(2)}, u32[]{:S(2)}) collective-permute-start(bf16[64,2048]{1,0:T(8,128)(2,1)S(1)} %slice.59), channel_id=1, source_target_pairs={{0,8},{8,16},{16,24},{24,0},{1,9},{9,17},{17,25},{25,1},{2,10},{10... | collective-permute-start | bytes 786440 | tf_op jit(solution)/shard_map/ppermute | solution.py:397
  97.2 37.8 %copy-start = (bf16[512,2048]{1,0:T(8,128)(2,1)S(1)}, bf16[512,2048]{1,0:T(8,128)(2,1)}, u32[]{:S(2)}) copy-start(bf16[512,2048]{1,0:T(8,128)(2,1)} %w_ref.1) | copy-start | bytes 6291460
  97.2 29.0 %all-to-all-start.3 = ((bf16[4,328,128]{2,1,0:T(8,128)(2,1)}), bf16[4,328,128]{2,1,0:T(8,128)(2,1)S(1)}, u32[]{:S(2)}, u32[]{:S(2)}) async-start(bf16[4,328,128]{2,1,0:T(8,128)(2,1)} %get-tuple-element.27), calls=%async_computation.3 | async-start | bytes 671744 | tf_op jit(solution)/shard_map/all_to_all | solution.py:439
  135.0 13.7 %copy-start.1 = (bf16[32,2048]{1,0:T(8,128)(2,1)S(1)}, bf16[32,2048]{1,0:T(8,128)(2,1)}, u32[]{:S(2)}) copy-start(bf16[32,2048]{1,0:T(8,128)(2,1)} %lat_ref.1) | copy-start | bytes 393220
  137.1 11.5 %all-to-all-start.5 = ((bf16[4,32,2048]{2,1,0:T(8,128)(2,1)}), bf16[4,32,2048]{2,1,0:T(8,128)(2,1)S(1)}, u32[]{:S(2)}, u32[]{:S(2)}) async-start(bf16[4,32,2048]{2,1,0:T(8,128)(2,1)} %bitcast.8), calls=%async_computation.5 | async-start | bytes 1048576 | tf_op jit(solution)/shard_map/all_to_all | solution.py:467

commit v10 on v9

--- a/solution.py
+++ b/solution.py
@@ -37,7 +37,7 @@
 
 
 def role(seg, sub):
-    return sub ^ (seg // 2)
+    return sub ^ (seg // 2 * 2)
 
 
 PEERS = [[4 * a + role(a, b) for a in range(4)] for b in range(4)]
@@ -71,40 +71,37 @@
     return lax.dot_general(a, b, (((0,), (0,)), ((), ())), preferred_element_type=f32)
 
 
-def rows_kernel(lat_ref, ctx_ref, sv_ref, cv_ref, mod_ref, rows_ref, mods_ref):
+def pack_kernel(
+    lat_ref, ctx_ref, sv_ref, cv_ref, mod_ref, wq_ref, wk_ref, wv_ref, extra_ref, rows_ref, cut_ref
+):
     y = lax.axis_index("tp")
+    dp = lax.axis_index("x") * 2 + lax.axis_index("core")
     rows_ref[0:32, :] = lat_ref[...]
     ctx = ctx_ref[...].astype(f32)
     picked = ctx[12:16]
     for i in range(3):
         picked = jnp.where(y == i, ctx[4 * i : 4 * i + 4], picked)
     rows_ref[32:36, :] = picked.astype(bf16)
+
     both = jnp.concatenate([sv_ref[...], cv_ref[...]], axis=0)
     conditions = (both / (1.0 + jnp.exp(-both))).astype(bf16)
     local_mods = nt(conditions, mod_ref[...])
-    for i in range(4):
-        mods_ref[i] = local_mods
-
-
-def pack_kernel(mods_ref, wq_ref, wk_ref, wv_ref, extra_ref, cut_ref):
-    dp = lax.axis_index("x") * 2 + lax.axis_index("core")
-    mods = jnp.concatenate([mods_ref[i] for i in range(4)], axis=1)
-    hi, mid, _ = three_parts(mods)
-    pieces = [p[:, 128 * j : 128 * (j + 1)].astype(f32) for p in (hi, mid) for j in range(3)]
+    mods = jnp.concatenate([p.astype(f32) for p in three_parts(local_mods)[:2]], axis=0)
+    mods = jnp.concatenate([mods, jnp.zeros((4, 32), f32)], axis=1)
     e_hi, e_mid, _ = three_parts(extra_ref[...])
     e_hi, e_mid = e_hi.astype(f32), e_mid.astype(f32)
     riding = []
     for h in range(2):
         added = [e_hi[h : h + 1], e_mid[h : h + 1], e_hi[2 + h : 3 + h], e_mid[2 + h : 3 + h]]
-        riding.append(jnp.concatenate([*pieces, *added], axis=0).astype(bf16))
+        riding.append(jnp.concatenate([mods, *added], axis=0).astype(bf16))
     mine = pl.ds(pl.multiple_of(dp * 16, 16), 16)
     for d in range(16):
         b = role(d // 4, d % 4)
         h = b // 2
-        cut_ref[d, :, 0:128] = wq_ref[mine, h * 128 : (h + 1) * 128]
-        cut_ref[d, :, 128:256] = wk_ref[mine, h * 128 : (h + 1) * 128]
-        cut_ref[d, :, 256:384] = wv_ref[mine, b * 128 : (b + 1) * 128]
-        cut_ref[d, :, 384:512] = riding[h]
+        cut_ref[d, 0:16, :] = wq_ref[mine, h * 128 : (h + 1) * 128]
+        cut_ref[d, 16:32, :] = wk_ref[mine, h * 128 : (h + 1) * 128]
+        cut_ref[d, 32:48, :] = wv_ref[mine, b * 128 : (b + 1) * 128]
+        cut_ref[d, 48:56, :] = riding[h]
 
 
 def normed_rows(rows, which, mod_ref, gain_ref):
@@ -114,22 +111,34 @@
     return (v * r * scale + mod_ref[which : which + 1, 0:D]).astype(bf16)
 
 
-def hidden_kernel(own_ref, minus_ref, plus_ref, ride_ref, gain_ref, h_ref, mod_ref):
+def hidden_kernel(
+    own_ref, minus_ref, plus_ref, low_ref, high_ref, own_mods_ref, far_mods_ref, gain_ref,
+    h_ref, mod_ref, mods_ref,
+):
+    y = lax.axis_index("tp")
+    mods_ref[y] = own_mods_ref[...].astype(f32)
+    mods_ref[(y + 3) % 4] = low_ref[64:72, :].astype(f32)
+    mods_ref[(y + 1) % 4] = high_ref[80:88, :].astype(f32)
+    mods_ref[(y + 2) % 4] = far_mods_ref[...].astype(f32)
     for z in range(16):
-        r = ride_ref[z].astype(f32)
-        for j in range(3):
-            both = r[2 * j : 2 * j + 2] + r[6 + 2 * j : 8 + 2 * j]
-            mod_ref[:, (z * 3 + j) * 128 : (z * 3 + j + 1) * 128] = both
-    for slot, ref in enumerate((own_ref, minus_ref, plus_ref)):
-        for j in range(4):
+        at = slice(z * 128, z * 128 + 96)
+        parts = [mods_ref[i, 0:2, at] + mods_ref[i, 2:4, at] for i in range(4)]
+        mod_ref[:, z * 384 : (z + 1) * 384] = jnp.concatenate(parts, axis=1)
+    for slot in range(4):
+        for j in range(5):
+            size = 32 if j < 4 else 16
+            if slot < 3:
+                rows = (own_ref, minus_ref, plus_ref)[slot][j * 32 : j * 32 + size, :]
+            elif j < 2:
+                rows = low_ref[j * 32 : j * 32 + 32, :]
+            else:
+                rows = high_ref[j * 32 - 64 : j * 32 - 64 + size, :]
             at = slot * 144 + j * 32
-            h_ref[at : at + 32, :] = normed_rows(ref[j * 32 : j * 32 + 32, :], 0, mod_ref, gain_ref)
-        at = slot * 144 + 128
-        h_ref[at : at + 16, :] = normed_rows(ref[128:144, :], 1, mod_ref, gain_ref)
+            h_ref[at : at + size, :] = normed_rows(rows, j // 4, mod_ref, gain_ref)
 
 
 def decays_of(low, up_ref, bias_ref):
-    second = lax.axis_index("B") >= 2
+    second = role(lax.axis_index("A"), lax.axis_index("B")) >= 2
 
     def of_head(a):
         return jnp.where(second, a[:, 128:256].astype(f32), a[:, 0:128].astype(f32))
@@ -143,50 +152,36 @@
     return (jnp.minimum(raw, 0.0) - jnp.log1p(jnp.exp(-jnp.abs(raw)))) * (1.0 / SHARP)
 
 
-def near_kernel(
-    h_ref, mine_ref, other_ref, down_ref, up_ref, bias_ref, w_ref, qkv_ref, logs_ref
+def project_kernel(
+    h_ref, mine_ref, other_ref, down_ref, up_ref, bias_ref, ride_ref,
+    pay_ref, q_ref, k_ref, v_ref, cum_ref, w_ref, out_ref, all_logs_ref,
 ):
-    core = lax.axis_index("core")
+    seg, sub = lax.axis_index("A"), lax.axis_index("B")
+    y, core = lax.axis_index("tp"), lax.axis_index("core")
     for xi in range(4):
         for z in range(16):
             at = z * 128 + xi * 32
             here = pl.ds(pl.multiple_of(at + core * 16, 16), 16)
             there = pl.ds(pl.multiple_of(at + 16 - core * 16, 16), 16)
-            w_ref[here, :] = mine_ref[xi, z]
-            w_ref[there, :] = other_ref[xi, z]
+            for j in range(3):
+                cols = slice(j * 128, (j + 1) * 128)
+                w_ref[here, cols] = mine_ref[xi, z, j * 16 : (j + 1) * 16, :]
+                w_ref[there, cols] = other_ref[xi, z, j * 16 : (j + 1) * 16, :]
+    y_of = [y, (y + 3) % 4, (y + 1) % 4, (y + 2) % 4]
     rows = h_ref[...]
     low = nt(rows, down_ref[...]).astype(bf16)
-    logs_ref[...] = decays_of(low, up_ref, bias_ref)
-    qkv_ref[...] = jnp.dot(rows, w_ref[...], preferred_element_type=f32).astype(bf16)
-
-
-def project_kernel(
-    low_ref, high_ref, mod_ref, gain_ref, w_ref, qkv_ref, logs_ref,
-    down_ref, up_ref, bias_ref, ride_ref,
-    pay_ref, q_ref, k_ref, v_ref, cum_ref, far_ref, out_ref, all_logs_ref,
-):
-    seg, sub = lax.axis_index("A"), lax.axis_index("B")
-    y = lax.axis_index("tp")
-    for j in range(4):
-        rows = (low_ref, high_ref)[j // 2][(j % 2) * 32 : (j % 2) * 32 + 32, :]
-        far_ref[j * 32 : j * 32 + 32, :] = normed_rows(rows, 0, mod_ref, gain_ref)
-    far_ref[128:144, :] = normed_rows(high_ref[64:80, :], 1, mod_ref, gain_ref)
-    y_of = [y, (y + 3) % 4, (y + 1) % 4, (y + 2) % 4]
-    rows = far_ref[...]
-    low = nt(rows, down_ref[...]).astype(bf16)
-    far_logs = decays_of(low, up_ref, bias_ref)
-    far_qkv = jnp.dot(rows, w_ref[...], preferred_element_type=f32).astype(bf16)
+    slot_logs = decays_of(low, up_ref, bias_ref)
+    slot_qkv = jnp.dot(rows, w_ref[...], preferred_element_type=f32).astype(bf16)
     for n in range(4):
         for j in range(5):
             size = 32 if j < 4 else 16
-            first = n * 144 + j * 32 if n < 3 else j * 32
-            took = slice(first, first + size)
+            took = slice(n * 144 + j * 32, n * 144 + j * 32 + size)
             if j < 4:
                 at = pl.ds(pl.multiple_of((sub ^ j) * 128 + y_of[n] * 32, 32), size)
             else:
                 at = pl.ds(SEG + n * 16, size)
-            out_ref[at, :] = qkv_ref[took, :] if n < 3 else far_qkv[took]
-            all_logs_ref[at, :] = logs_ref[took, :] if n < 3 else far_logs[took]
+            out_ref[at, :] = slot_qkv[took]
+            all_logs_ref[at, :] = slot_logs[took]
     out = out_ref[...]
     logs = all_logs_ref[...]
     q_ref[...] = out[:SEG, 0:128]
@@ -195,8 +190,8 @@
     ef, eb = [], []
     for zb in range(4):
         t = jnp.transpose(ride_ref[seg * 4 + zb].astype(f32))
-        ef.append(t[:, 12:13] + t[:, 13:14])
-        eb.append(t[:, 14:15] + t[:, 15:16])
+        ef.append(t[:, 4:5] + t[:, 5:6])
+        eb.append(t[:, 6:7] + t[:, 7:8])
     ef = jnp.concatenate(ef, axis=0)
     eb = jnp.concatenate(eb, axis=0)
     af = logs[:SEG, 0:128] + ef
@@ -332,7 +327,8 @@
     total = None
     flip = lax.axis_index("A") // 2
     for h in range(2):
-        v = jnp.concatenate([mix_ref[2 * h + flip], mix_ref[2 * h + 1 - flip]], axis=1).astype(f32)
+        at = 2 * (h ^ flip)
+        v = jnp.concatenate([mix_ref[at], mix_ref[at + 1]], axis=1).astype(f32)
         r = lax.rsqrt(jnp.mean(v * v, axis=-1, keepdims=True) + EPS)
         n = (v * r * gain_ref[...]).astype(bf16)
         part = jnp.dot(n, w_ref[h * 256 : (h + 1) * 256, :], preferred_element_type=f32)
@@ -358,61 +354,47 @@
     out_weight,
 ):
     sds = jax.ShapeDtypeStruct
-    rows, mods = pl.pallas_call(
-        rows_kernel,
-        out_shape=(sds((36, D), bf16), sds((4, 2, 96), f32)),
-        in_specs=[VM] * 5,
+    rows, cut = pl.pallas_call(
+        pack_kernel,
+        out_shape=(sds((36, D), bf16), sds((16, 56, 128), bf16)),
+        in_specs=[VM] * 9,
         out_specs=(VM, VM),
         compiler_params=pltpu.CompilerParams(vmem_limit_bytes=12 * 1024 * 1024),
-        name="rows",
-    )(*off_chip(latents, context, sample_vector, context_vector, modulator.T))
-    mods = lax.all_to_all(mods, "tp", 0, 0, tiled=True)
+        name="pack",
+    )(
+        *off_chip(
+            latents, context, sample_vector, context_vector, modulator.T,
+            query_weight, key_weight, value_weight,
+            jnp.moveaxis(decay_extra, 1, 2).reshape(4, 128),
+        )
+    )
     near = [rows]
     for j in range(1, 4):
         near.append(lax.ppermute(rows, "B", [(b, b ^ j) for b in range(4)]))
-    cut = pl.pallas_call(
-        pack_kernel,
-        out_shape=sds((16, 16, 512), bf16),
-        in_specs=[VM] * 5,
-        out_specs=VM,
-        compiler_params=pltpu.CompilerParams(vmem_limit_bytes=12 * 1024 * 1024),
-        name="pack",
-    )(
-        *on_chip(mods),
-        *off_chip(
-            query_weight, key_weight, value_weight,
-            jnp.moveaxis(decay_extra, 1, 2).reshape(4, 128),
-        ),
-    )
     rows_z = lax.all_to_all(cut, ("A", "B"), 0, 0, tiled=True)
-    mine = to_everyone(rows_z[:, :, 0:384], "x")
+    mine = to_everyone(rows_z[:, 0:48], "x")
     other = lax.ppermute(mine, "core", [(0, 1), (1, 0)])
-    ride = rows_z[:, :, 384:512]
+    ride = rows_z[:, 48:56]
+    mods = jnp.transpose(ride, (1, 0, 2)).reshape(8, D)
+    far_mods = lax.ppermute(mods, "tp", [(i, i ^ 2) for i in range(4)])
 
     own = jnp.concatenate([n[:32] for n in near] + [n[32:36] for n in near], axis=0)
     up_shift = [(i, (i + 1) % 4) for i in range(4)]
     down_shift = [(i, (i + 3) % 4) for i in range(4)]
     minus = lax.ppermute(own, "tp", up_shift)
     plus = lax.ppermute(own, "tp", down_shift)
-    low = lax.ppermute(minus[:64], "tp", up_shift)
-    high = lax.ppermute(plus[64:], "tp", down_shift)
-
-    near_hidden, modulation = pl.pallas_call(
+    low = lax.ppermute(jnp.concatenate([minus[:64], mods]), "tp", up_shift)
+    high = lax.ppermute(jnp.concatenate([plus[64:], mods]), "tp", down_shift)
+
+    hidden, modulation = pl.pallas_call(
         hidden_kernel,
-        out_shape=(sds((432, D), bf16), pltpu.HBM((2, 3 * D), f32)),
-        in_specs=[VM] * 5,
+        out_shape=(sds((ROWS, D), bf16), pltpu.HBM((2, 3 * D), f32)),
+        in_specs=[VM] * 8,
         out_specs=(VM, VM),
+        scratch_shapes=[pltpu.VMEM((4, 8, D), f32)],
         compiler_params=pltpu.CompilerParams(vmem_limit_bytes=16 * 1024 * 1024),
         name="hidden",
-    )(*on_chip(own, minus, plus, ride), *off_chip(norm_gain.reshape(1, D)))
-    weights, near_qkv, near_logs = pl.pallas_call(
-        near_kernel,
-        out_shape=(sds((D, 384), bf16), sds((432, 384), bf16), sds((432, 256), f32)),
-        in_specs=[VM] * 6,
-        out_specs=(VM,) * 3,
-        compiler_params=pltpu.CompilerParams(vmem_limit_bytes=16 * 1024 * 1024),
-        name="near",
-    )(*on_chip(near_hidden, mine, other), *off_chip(decay_down.T, decay_up, decay_bias))
+    )(*on_chip(own, minus, plus, low, high, mods, far_mods), *off_chip(norm_gain.reshape(1, D)))
     payload, q, k, v, cum = pl.pallas_call(
         project_kernel,
         out_shape=(
@@ -422,19 +404,17 @@
             pltpu.HBM((SEG, DK), bf16),
             pltpu.HBM((2, SEG, DK), f32),
         ),
-        in_specs=[VM] * 11,
+        in_specs=[VM] * 7,
         out_specs=(VM,) * 5,
         scratch_shapes=[
-            pltpu.VMEM((144, D), bf16),
+            pltpu.VMEM((D, 384), bf16),
             pltpu.VMEM((ROWS, 384), bf16),
             pltpu.VMEM((ROWS, 256), f32),
         ],
-        compiler_params=pltpu.CompilerParams(vmem_limit_bytes=20 * 1024 * 1024),
+        compiler_params=pltpu.CompilerParams(vmem_limit_bytes=24 * 1024 * 1024),
         name="project",
     )(
-        *on_chip(low, high), *off_chip(modulation, norm_gain.reshape(1, D)),
-        *on_chip(weights, near_qkv, near_logs),
-        *off_chip(decay_down.T, decay_up, decay_bias), *on_chip(ride),
+        *on_chip(hidden, mine, other), *off_chip(decay_down.T, decay_up, decay_bias), *on_chip(ride),
     )
     got = lax.all_to_all(
         payload, ("A", "B"), 0, 0, tiled=True, axis_index_groups=PEERS

time: 150 us -> 147 us (0.980)
  blocking collectives: 50.1 us -> 10.1 us
  starting transfers between devices: 41.8 us -> 63.6 us
  waiting for transfers between devices: 39 us -> 54 us
    all_to_all x2 -> x0, blocking collectives: 41.8 us -> none  [the longest x1 32.3 us: device_body(): rows_z = lax.all_to_all(cut, ('A', 'B'), 0, 0, tiled=True)]
    all_to_all x0 -> x1, starting transfers between devices: none -> 15.2 us  [device_body(): rows_z = lax.all_to_all(cut, ('A', 'B'), 0, 0, tiled=True)]
    ppermute x3, waiting for transfers between devices: 6.23 us -> 14.4 us  [device_body(): near.append(lax.ppermute(rows, 'B', [(b, b ^ j) for b in range(4)]))]
    ppermute x1, waiting for transfers between devices: 0.01 us -> 5.3 us  [device_body(): minus = lax.ppermute(own, 'tp', up_shift)]
    ppermute x2 -> x3, waiting for transfers between devices: 2.87 us -> 7.63 us  [the longest x1 6.25 us: device_body(): far_mods = lax.ppermute(mods, 'tp', [(i, i ^ 2) for i in range(4)])]
    ppermute x2 -> x3, starting transfers between devices: 6.15 us -> 9.86 us  [the longest x1 4.57 us: device_body(): high = lax.ppermute(jnp.concatenate([plus[64:], mods]), 'tp', down_shift)]
    pallas_call x4 -> x2, Pallas kernels: 7.05 us -> 3.98 us  [the longest x1 2.15 us: device_body(): pl.pallas_call(pack_kernel, out_shape=(sds((36, D), bf16), sds((16, 56, 1...]
    all_to_all x1, waiting for transfers between devices: 17.4 us -> 14.9 us  [device_body(): lax.all_to_all(payload, ('A', 'B'), 0, 0, tiled=True, axis_index_groups=P...]
  transfers between devices with their start and end apart: 11 -> 13, of which waited for: 6 -> 8; matrix products, arithmetic and copies ran while one was open for 1% -> 1% of each run, Pallas kernels for 5% -> 3%
where the time goes in v10:
time: 147 us; the launch traced here: 145 us
  starting transfers between devices  63.6 us (43%)
  waiting for transfers between devices  54 us (37%)
  Pallas kernels  14.2 us (10%)
  blocking collectives  10.1 us (7%)
  local copies, waits for them, and re-layouts  1.95 us (1%)
    all_to_all x1, starting transfers between devices, device_body(): rows_z = lax.all_to_all(cut, ('A', 'B'), 0, 0, tiled=True)  15.2 us
    all_to_all x1, waiting for transfers between devices, device_body(): lax.all_to_all(payload, ('A', 'B'), 0, 0, tiled=True, axis_index_groups=P...  14.9 us
    ppermute x3, waiting for transfers between devices, device_body(): near.append(lax.ppermute(rows, 'B', [(b, b ^ j) for b in range(4)]))  14.4 us
    all_to_all x1, starting transfers between devices, device_body(): lax.all_to_all(payload, ('A', 'B'), 0, 0, tiled=True, axis_index_groups=P...  11.5 us
    ppermute x3, starting transfers between devices, device_body(): near.append(lax.ppermute(rows, 'B', [(b, b ^ j) for b in range(4)]))  10.1 us
    all_to_all x1, blocking collectives, device_body(): heads = lax.all_to_all(mixed.reshape(4, 128, DK), 'B', 0, 0, tiled=True)  10.1 us
    all_to_all x1, waiting for transfers between devices, device_body(): shares = lax.all_to_all(partial.reshape(4, 32, D), 'tp', 0, 0, tiled=True)  7.32 us
    ppermute x1, waiting for transfers between devices, device_body(): far_mods = lax.ppermute(mods, 'tp', [(i, i ^ 2) for i in range(4)])  6.25 us
  transfers between devices with their start and end apart: 13, of which 8 were waited for; matrix products, arithmetic and copies ran while one was open for 1% of the time, Pallas kernels for 3%

profile of v10, /device:TPU:6, one launch (start us, length us, event | category | flops | bytes accessed | tf_op | source)
XLA Modules:
  0.0 144.9 jit_solution(7396760740592119393)
XLA Ops:
  0.0 2.2 %pack.1 = (bf16[36,2048]{1,0:T(8,128)(2,1)S(1)}, bf16[16,56,128]{2,1,0:T(8,128)(2,1)}) custom-call(bf16[32,2048]{1,0:T(8,128)(2,1)} %lat_ref.1, bf16[16,2048]{1,0:T(8,128)(2,1)} %ctx_ref.1, f32[1,2048]{1,0:T(1,128)} %sv_ref.1, f32[1,2048]{1,0:T(1,128)} %cv_ref.1, bf16[96,2048]{1,0:T(8,128)(2,1)} %bitcast.15, bf16[128,256]{1,0:T(8,128)(2,1)} %wq_ref.1, ...), custom_call_target="tpu_custom_call" | custom-call | tf_op jit(solution)/shard_map/pack/pallas_call | solution.py:357
  2.2 15.2 %all-to-all-start = ((bf16[16,56,128]{2,1,0:T(8,128)(2,1)}), bf16[16,56,128]{2,1,0:T(8,128)(2,1)S(1)}, u32[]{:S(2)}, u32[]{:S(2)}) async-start(bf16[16,56,128]{2,1,0:T(8,128)(2,1)} %get-tuple-element.18), calls=%async_computation | async-start | bytes 458752 | tf_op jit(solution)/shard_map/all_to_all | solution.py:374
  17.4 3.8 %collective-permute-start = (bf16[36,2048]{1,0:T(8,128)(2,1)S(1)}, bf16[36,2048]{1,0:T(8,128)(2,1)S(1)}, u32[]{:S(2)}, u32[]{:S(2)}) collective-permute-start(bf16[36,2048]{1,0:T(8,128)(2,1)S(1)} %get-tuple-element.17), channel_id=1, source_target_pairs={{0,32},{32,0},{64,96},{96,64},{1,33},{33,1},{65,97},{97,65},{2,34}... | collective-permute-start | bytes 442376 | tf_op jit(solution)/shard_map/ppermute | solution.py:373
  21.2 4.3 %collective-permute-start.1 = (bf16[36,2048]{1,0:T(8,128)(2,1)S(1)}, bf16[36,2048]{1,0:T(8,128)(2,1)S(1)}, u32[]{:S(2)}, u32[]{:S(2)}) collective-permute-start(bf16[36,2048]{1,0:T(8,128)(2,1)S(1)} %get-tuple-element.17), channel_id=1, source_target_pairs={{0,64},{32,96},{64,0},{96,32},{1,65},{33,97},{65,1},{97,33},{2,66}... | collective-permute-start | bytes 442376 | tf_op jit(solution)/shard_map/ppermute | solution.py:373
  25.5 2.0 %collective-permute-start.2 = (bf16[36,2048]{1,0:T(8,128)(2,1)S(1)}, bf16[36,2048]{1,0:T(8,128)(2,1)S(1)}, u32[]{:S(2)}, u32[]{:S(2)}) collective-permute-start(bf16[36,2048]{1,0:T(8,128)(2,1)S(1)} %get-tuple-element.17), channel_id=1, source_target_pairs={{0,96},{32,64},{64,32},{96,0},{1,97},{33,65},{65,33},{97,1},{2,98}... | collective-permute-start | bytes 442376 | tf_op jit(solution)/shard_map/ppermute | solution.py:373
  27.5 9.0 %collective-permute-done = bf16[36,2048]{1,0:T(8,128)(2,1)S(1)} collective-permute-done((bf16[36,2048]{1,0:T(8,128)(2,1)S(1)}, bf16[36,2048]{1,0:T(8,128)(2,1)S(1)}, u32[]{:S(2)}, u32[]{:S(2)}) %collective-permute-start) | collective-permute-done | bytes 147488 | tf_op jit(solution)/shard_map/ppermute | solution.py:373
  36.5 0.0 collective-permute-done.1
  36.6 5.4 %collective-permute-done.2 = bf16[36,2048]{1,0:T(8,128)(2,1)S(1)} collective-permute-done((bf16[36,2048]{1,0:T(8,128)(2,1)S(1)}, bf16[36,2048]{1,0:T(8,128)(2,1)S(1)}, u32[]{:S(2)}, u32[]{:S(2)}) %collective-permute-start.2) | collective-permute-done | bytes 147488 | tf_op jit(solution)/shard_map/ppermute | solution.py:373
  42.0 0.1 concatenate.9.own_ref
  42.1 4.9 %collective-permute-start.4 = (bf16[144,2048]{1,0:T(8,128)(2,1)S(1)}, bf16[144,2048]{1,0:T(8,128)(2,1)S(1)}, u32[]{:S(2)}, u32[]{:S(2)}) collective-permute-start(bf16[144,2048]{1,0:T(8,128)(2,1)S(1)} %concatenate.9.own_ref), channel_id=1, source_target_pairs={{0,24},{8,0},{16,8},{24,16},{1,25},{9,1},{17,9},{25,17},{2,26},{10... | collective-permute-start | bytes 1769480 | tf_op jit(solution)/shard_map/ppermute | solution.py:385
  47.0 1.9 %collective-permute-start.3 = (bf16[144,2048]{1,0:T(8,128)(2,1)S(1)}, bf16[144,2048]{1,0:T(8,128)(2,1)S(1)}, u32[]{:S(2)}, u32[]{:S(2)}) collective-permute-start(bf16[144,2048]{1,0:T(8,128)(2,1)S(1)} %concatenate.9.own_ref), channel_id=1, source_target_pairs={{0,8},{8,16},{16,24},{24,0},{1,9},{9,17},{17,25},{25,1},{2,10},{10... | collective-permute-start | bytes 1769480 | tf_op jit(solution)/shard_map/ppermute | solution.py:384
  49.0 0.0 all-to-all-done
  49.0 1.0 broadcast_in_dim.2
  50.0 4.8 %all-to-all-start.1 = ((bf16[4,16,48,128]{3,2,1,0:T(8,128)(2,1)}), bf16[4,16,48,128]{3,2,1,0:T(8,128)(2,1)S(1)}, u32[]{:S(2)}, u32[]{:S(2)}) async-start(bf16[4,16,48,128]{3,2,1,0:T(8,128)(2,1)} %broadcast_in_dim.2), calls=%async_computation.1 | async-start | bytes 1572864 | tf_op jit(solution)/shard_map/all_to_all | solution.py:36
  54.7 4.4 %collective-permute-done.4.plus_ref = bf16[144,2048]{1,0:T(8,128)(2,1)S(1)} collective-permute-done((bf16[144,2048]{1,0:T(8,128)(2,1)S(1)}, bf16[144,2048]{1,0:T(8,128)(2,1)S(1)}, u32[]{:S(2)}, u32[]{:S(2)}) %collective-permute-start.4) | collective-permute-done | bytes 589856 | tf_op jit(solution)/shard_map/ppermute | solution.py:385
  59.2 5.3 %collective-permute-done.3.minus_ref = bf16[144,2048]{1,0:T(8,128)(2,1)S(1)} collective-permute-done((bf16[144,2048]{1,0:T(8,128)(2,1)S(1)}, bf16[144,2048]{1,0:T(8,128)(2,1)S(1)}, u32[]{:S(2)}, u32[]{:S(2)}) %collective-permute-start.3) | collective-permute-done | bytes 589856 | tf_op jit(solution)/shard_map/ppermute | solution.py:384
  64.5 0.0 all-to-all-done.1.mine_ref
  64.5 1.9 %collective-permute-start.8 = (bf16[4,16,48,128]{3,2,1,0:T(8,128)(2,1)S(1)}, bf16[4,16,48,128]{3,2,1,0:T(8,128)(2,1)S(1)}, u32[]{:S(2)}, u32[]{:S(2)}) collective-permute-start(bf16[4,16,48,128]{3,2,1,0:T(8,128)(2,1)S(1)} %all-to-all-done.1.mine_ref), channel_id=1, source_target_pairs={{0,1},{1,0},{2,3},{3,2},{4,5},{5,4},{6,7},{7,6},{8,9},{9,8},{10,11... | collective-permute-start | bytes 2359304 | tf_op jit(solution)/shard_map/ppermute | solution.py:376
  66.5 4.6 %collective-permute-start.6 = (bf16[88,2048]{1,0:T(8,128)(2,1)S(1)}, bf16[88,2048]{1,0:T(8,128)(2,1)S(1)}, u32[]{:S(2)}, u32[]{:S(2)}) collective-permute-start(bf16[88,2048]{1,0:T(8,128)(2,1)S(1)} %pad_maximum_fusion), channel_id=1, source_target_pairs={{0,24},{8,0},{16,8},{24,16},{1,25},{9,1},{17,9},{25,17},{2,26},{10... | collective-permute-start | bytes 1081352 | tf_op jit(solution)/shard_map/ppermute | solution.py:387
  71.1 1.9 %collective-permute-start.5 = (bf16[72,2048]{1,0:T(8,128)(2,1)S(1)}, bf16[72,2048]{1,0:T(8,128)(2,1)S(1)}, u32[]{:S(2)}, u32[]{:S(2)}) collective-permute-start(bf16[72,2048]{1,0:T(8,128)(2,1)S(1)} %pad_maximum_fusion.1), channel_id=1, source_target_pairs={{0,8},{8,16},{16,24},{24,0},{1,9},{9,17},{17,25},{25,1},{2,10},{10... | collective-permute-start | bytes 884744 | tf_op jit(solution)/shard_map/ppermute | solution.py:386
  73.1 3.4 %collective-permute-start.7 = (bf16[8,2048]{1,0:T(8,128)(2,1)S(1)}, bf16[8,2048]{1,0:T(8,128)(2,1)S(1)}, u32[]{:S(2)}, u32[]{:S(2)}) collective-permute-start(bf16[8,2048]{1,0:T(8,128)(2,1)S(1)} %get-tuple-element.30.own_mods_ref), channel_id=1, source_target_pairs={{0,16},{8,24},{16,0},{24,8},{1,17},{9,25},{17,1},{25,9},{2,18},{10... | collective-permute-start | bytes 98312 | tf_op jit(solution)/shard_map/ppermute | solution.py:379
  76.4 6.2 %collective-permute-done.7.far_mods_ref = bf16[8,2048]{1,0:T(8,128)(2,1)S(1)} collective-permute-done((bf16[8,2048]{1,0:T(8,128)(2,1)S(1)}, bf16[8,2048]{1,0:T(8,128)(2,1)S(1)}, u32[]{:S(2)}, u32[]{:S(2)}) %collective-permute-start.7) | collective-permute-done | bytes 32800 | tf_op jit(solution)/shard_map/ppermute | solution.py:379
  82.7 1.4 collective-permute-done.5.low_ref
  84.1 0.0 collective-permute-done.6.high_ref
  84.1 1.8 %hidden.1 = (bf16[576,2048]{1,0:T(8,128)(2,1)S(1)}, f32[2,6144]{1,0:T(2,128)}) custom-call(bf16[144,2048]{1,0:T(8,128)(2,1)S(1)} %concatenate.9.own_ref, bf16[144,2048]{1,0:T(8,128)(2,1)S(1)} %collective-permute-done.3.minus_ref, bf16[144,2048]{1,0:T(8,128)(2,1)S(1)} %collective-permute-done.4.plus_ref, bf16[72,2048]{1,0:T(8,128)(2,1)S(1)} %collective-permute-done.5.low_ref, ...), custom_call_target="tpu_custom_call" | custom-call | tf_op jit(solution)/shard_map/hidden/pallas_call | solution.py:389
  85.9 0.0 collective-permute-done.8.other_ref
  85.9 5.4 %project.1 = (bf16[4,328,128]{2,1,0:T(8,128)(2,1)}, bf16[512,128]{1,0:T(8,128)(2,1)}, bf16[512,128]{1,0:T(8,128)(2,1)}, bf16[512,128]{1,0:T(8,128)(2,1)}, f32[2,512,128]{2,1,0:T(8,128)}) custom-call(bf16[576,2048]{1,0:T(8,128)(2,1)S(1)} %get-tuple-element.20.h_ref, bf16[4,16,48,128]{3,2,1,0:T(8,128)(2,1)S(1)} %all-to-all-done.1.mine_ref, ...), custom_call_target="tpu_custom_call" | custom-call | tf_op jit(solution)/shard_map/project/pallas_call | solution.py:398
  91.3 0.0 copy-start
  91.3 11.5 %all-to-all-start.2 = ((bf16[4,328,128]{2,1,0:T(8,128)(2,1)}), bf16[4,328,128]{2,1,0:T(8,128)(2,1)S(1)}, u32[]{:S(2)}, u32[]{:S(2)}) async-start(bf16[4,328,128]{2,1,0:T(8,128)(2,1)} %get-tuple-element.21), calls=%async_computation.2 | async-start | bytes 671744 | tf_op jit(solution)/shard_map/all_to_all | solution.py:419
  102.7 2.3 %local.1 = (f32[512,128]{1,0:T(8,128)S(1)}, bf16[512,128]{1,0:T(8,128)(2,1)S(1)}, bf16[512,128]{1,0:T(8,128)(2,1)S(1)}) custom-call(bf16[512,128]{1,0:T(8,128)(2,1)} %get-tuple-element.22.q_ref, bf16[512,128]{1,0:T(8,128)(2,1)} %get-tuple-element.23.k_ref, bf16[512,128]{1,0:T(8,128)(2,1)} %get-tuple-element.24.v_ref, f32[2,512,128]{2,1,0:T(8,128)} %get-tuple-element.25.cum_ref), custom_call_target="tpu_custom_call" | custom-call | tf_op jit(solution)/shard_map/local/pallas_call | solution.py:422
  105.1 14.9 %all-to-all-done.2.in_ref = bf16[4,328,128]{2,1,0:T(8,128)(2,1)S(1)} async-done(((bf16[4,328,128]{2,1,0:T(8,128)(2,1)}), bf16[4,328,128]{2,1,0:T(8,128)(2,1)S(1)}, u32[]{:S(2)}, u32[]{:S(2)}) %all-to-all-start.2) | async-done | bytes 335904 | tf_op jit(solution)/shard_map/all_to_all | solution.py:419
  120.0 0.5 combine.1
  120.5 0.0 copy-start.1
  120.5 10.1 %all_to_all.25.mix_ref = bf16[4,128,128]{2,1,0:T(8,128)(2,1)S(1)} all-to-all(bf16[4,128,128]{2,1,0:T(8,128)(2,1)S(1)} %bitcast.14), channel_id=1, replica_groups=mesh['A'=4,'B'=4,'tp'=4,'x'=4,'core'=2] {'B'}, dimensions={0} | all-to-all | bytes 262144 | tf_op jit(solution)/shard_map/all_to_all | solution.py:438
  130.6 0.0 copy-done
  130.6 2.0 %output.1 = bf16[128,2048]{1,0:T(8,128)(2,1)} custom-call(bf16[4,128,128]{2,1,0:T(8,128)(2,1)S(1)} %all_to_all.25.mix_ref, f32[1,256]{1,0:T(1,128)} %bitcast.20, bf16[512,2048]{1,0:T(8,128)(2,1)S(1)} %copy-done), custom_call_target="tpu_custom_call" | custom-call | tf_op jit(solution)/shard_map/output/pallas_call | solution.py:439
  132.6 3.5 %all-to-all-start.4 = ((bf16[4,32,2048]{2,1,0:T(8,128)(2,1)}), bf16[4,32,2048]{2,1,0:T(8,128)(2,1)S(1)}, u32[]{:S(2)}, u32[]{:S(2)}) async-start(bf16[4,32,2048]{2,1,0:T(8,128)(2,1)} %bitcast.11), calls=%async_computation.4 | async-start | bytes 1048576 | tf_op jit(solution)/shard_map/all_to_all | solution.py:447
  136.1 0.7 slice.50
  136.8 7.3 %all-to-all-done.4 = bf16[4,32,2048]{2,1,0:T(8,128)(2,1)S(1)} async-done(((bf16[4,32,2048]{2,1,0:T(8,128)(2,1)}), bf16[4,32,2048]{2,1,0:T(8,128)(2,1)S(1)}, u32[]{:S(2)}, u32[]{:S(2)}) %all-to-all-start.4) | async-done | bytes 524320 | tf_op jit(solution)/shard_map/all_to_all | solution.py:447
  144.1 0.1 reduce_sum.12
  144.2 0.0 copy-done.1
  144.2 0.7 add_convert_fusion
  (14 shorter events, 0.2 us)
Async XLA Ops:
  2.2 46.8 %all-to-all-start = ((bf16[16,56,128]{2,1,0:T(8,128)(2,1)}), bf16[16,56,128]{2,1,0:T(8,128)(2,1)S(1)}, u32[]{:S(2)}, u32[]{:S(2)}) async-start(bf16[16,56,128]{2,1,0:T(8,128)(2,1)} %get-tuple-element.18), calls=%async_computation | async-start | bytes 458752 | tf_op jit(solution)/shard_map/all_to_all | solution.py:374
  17.4 19.2 %collective-permute-start = (bf16[36,2048]{1,0:T(8,128)(2,1)S(1)}, bf16[36,2048]{1,0:T(8,128)(2,1)S(1)}, u32[]{:S(2)}, u32[]{:S(2)}) collective-permute-start(bf16[36,2048]{1,0:T(8,128)(2,1)S(1)} %get-tuple-element.17), channel_id=1, source_target_pairs={{0,32},{32,0},{64,96},{96,64},{1,33},{33,1},{65,97},{97,65},{2,34}... | collective-permute-start | bytes 442376 | tf_op jit(solution)/shard_map/ppermute | solution.py:373
  21.2 15.4 %collective-permute-start.1 = (bf16[36,2048]{1,0:T(8,128)(2,1)S(1)}, bf16[36,2048]{1,0:T(8,128)(2,1)S(1)}, u32[]{:S(2)}, u32[]{:S(2)}) collective-permute-start(bf16[36,2048]{1,0:T(8,128)(2,1)S(1)} %get-tuple-element.17), channel_id=1, source_target_pairs={{0,64},{32,96},{64,0},{96,32},{1,65},{33,97},{65,1},{97,33},{2,66}... | collective-permute-start | bytes 442376 | tf_op jit(solution)/shard_map/ppermute | solution.py:373
  25.5 16.5 %collective-permute-start.2 = (bf16[36,2048]{1,0:T(8,128)(2,1)S(1)}, bf16[36,2048]{1,0:T(8,128)(2,1)S(1)}, u32[]{:S(2)}, u32[]{:S(2)}) collective-permute-start(bf16[36,2048]{1,0:T(8,128)(2,1)S(1)} %get-tuple-element.17), channel_id=1, source_target_pairs={{0,96},{32,64},{64,32},{96,0},{1,97},{33,65},{65,33},{97,1},{2,98}... | collective-permute-start | bytes 442376 | tf_op jit(solution)/shard_map/ppermute | solution.py:373
  42.1 17.1 %collective-permute-start.4 = (bf16[144,2048]{1,0:T(8,128)(2,1)S(1)}, bf16[144,2048]{1,0:T(8,128)(2,1)S(1)}, u32[]{:S(2)}, u32[]{:S(2)}) collective-permute-start(bf16[144,2048]{1,0:T(8,128)(2,1)S(1)} %concatenate.9.own_ref), channel_id=1, source_target_pairs={{0,24},{8,0},{16,8},{24,16},{1,25},{9,1},{17,9},{25,17},{2,26},{10... | collective-permute-start | bytes 1769480 | tf_op jit(solution)/shard_map/ppermute | solution.py:385
  47.0 17.5 %collective-permute-start.3 = (bf16[144,2048]{1,0:T(8,128)(2,1)S(1)}, bf16[144,2048]{1,0:T(8,128)(2,1)S(1)}, u32[]{:S(2)}, u32[]{:S(2)}) collective-permute-start(bf16[144,2048]{1,0:T(8,128)(2,1)S(1)} %concatenate.9.own_ref), channel_id=1, source_target_pairs={{0,8},{8,16},{16,24},{24,0},{1,9},{9,17},{17,25},{25,1},{2,10},{10... | collective-permute-start | bytes 1769480 | tf_op jit(solution)/shard_map/ppermute | solution.py:384
  50.0 14.6 %all-to-all-start.1 = ((bf16[4,16,48,128]{3,2,1,0:T(8,128)(2,1)}), bf16[4,16,48,128]{3,2,1,0:T(8,128)(2,1)S(1)}, u32[]{:S(2)}, u32[]{:S(2)}) async-start(bf16[4,16,48,128]{3,2,1,0:T(8,128)(2,1)} %broadcast_in_dim.2), calls=%async_computation.1 | async-start | bytes 1572864 | tf_op jit(solution)/shard_map/all_to_all | solution.py:36
  64.5 21.4 %collective-permute-start.8 = (bf16[4,16,48,128]{3,2,1,0:T(8,128)(2,1)S(1)}, bf16[4,16,48,128]{3,2,1,0:T(8,128)(2,1)S(1)}, u32[]{:S(2)}, u32[]{:S(2)}) collective-permute-start(bf16[4,16,48,128]{3,2,1,0:T(8,128)(2,1)S(1)} %all-to-all-done.1.mine_ref), channel_id=1, source_target_pairs={{0,1},{1,0},{2,3},{3,2},{4,5},{5,4},{6,7},{7,6},{8,9},{9,8},{10,11... | collective-permute-start | bytes 2359304 | tf_op jit(solution)/shard_map/ppermute | solution.py:376
  66.5 17.5 %collective-permute-start.6 = (bf16[88,2048]{1,0:T(8,128)(2,1)S(1)}, bf16[88,2048]{1,0:T(8,128)(2,1)S(1)}, u32[]{:S(2)}, u32[]{:S(2)}) collective-permute-start(bf16[88,2048]{1,0:T(8,128)(2,1)S(1)} %pad_maximum_fusion), channel_id=1, source_target_pairs={{0,24},{8,0},{16,8},{24,16},{1,25},{9,1},{17,9},{25,17},{2,26},{10... | collective-permute-start | bytes 1081352 | tf_op jit(solution)/shard_map/ppermute | solution.py:387
  71.1 12.9 %collective-permute-start.5 = (bf16[72,2048]{1,0:T(8,128)(2,1)S(1)}, bf16[72,2048]{1,0:T(8,128)(2,1)S(1)}, u32[]{:S(2)}, u32[]{:S(2)}) collective-permute-start(bf16[72,2048]{1,0:T(8,128)(2,1)S(1)} %pad_maximum_fusion.1), channel_id=1, source_target_pairs={{0,8},{8,16},{16,24},{24,0},{1,9},{9,17},{17,25},{25,1},{2,10},{10... | collective-permute-start | bytes 884744 | tf_op jit(solution)/shard_map/ppermute | solution.py:386
  73.1 9.6 %collective-permute-start.7 = (bf16[8,2048]{1,0:T(8,128)(2,1)S(1)}, bf16[8,2048]{1,0:T(8,128)(2,1)S(1)}, u32[]{:S(2)}, u32[]{:S(2)}) collective-permute-start(bf16[8,2048]{1,0:T(8,128)(2,1)S(1)} %get-tuple-element.30.own_mods_ref), channel_id=1, source_target_pairs={{0,16},{8,24},{16,0},{24,8},{1,17},{9,25},{17,1},{25,9},{2,18},{10... | collective-permute-start | bytes 98312 | tf_op jit(solution)/shard_map/ppermute | solution.py:379
  91.3 39.3 %copy-start = (bf16[512,2048]{1,0:T(8,128)(2,1)S(1)}, bf16[512,2048]{1,0:T(8,128)(2,1)}, u32[]{:S(2)}) copy-start(bf16[512,2048]{1,0:T(8,128)(2,1)} %w_ref.1) | copy-start | bytes 6291460
  91.3 28.7 %all-to-all-start.2 = ((bf16[4,328,128]{2,1,0:T(8,128)(2,1)}), bf16[4,328,128]{2,1,0:T(8,128)(2,1)S(1)}, u32[]{:S(2)}, u32[]{:S(2)}) async-start(bf16[4,328,128]{2,1,0:T(8,128)(2,1)} %get-tuple-element.21), calls=%async_computation.2 | async-start | bytes 671744 | tf_op jit(solution)/shard_map/all_to_all | solution.py:419
  120.5 23.7 %copy-start.1 = (bf16[32,2048]{1,0:T(8,128)(2,1)S(1)}, bf16[32,2048]{1,0:T(8,128)(2,1)}, u32[]{:S(2)}) copy-start(bf16[32,2048]{1,0:T(8,128)(2,1)} %lat_ref.1) | copy-start | bytes 393220
  132.6 11.5 %all-to-all-start.4 = ((bf16[4,32,2048]{2,1,0:T(8,128)(2,1)}), bf16[4,32,2048]{2,1,0:T(8,128)(2,1)S(1)}, u32[]{:S(2)}, u32[]{:S(2)}) async-start(bf16[4,32,2048]{2,1,0:T(8,128)(2,1)} %bitcast.11), calls=%async_computation.4 | async-start | bytes 1048576 | tf_op jit(solution)/shard_map/all_to_all | solution.py:447

commit v11 on v10

--- a/solution.py
+++ b/solution.py
@@ -356,7 +356,7 @@
     sds = jax.ShapeDtypeStruct
     rows, cut = pl.pallas_call(
         pack_kernel,
-        out_shape=(sds((36, D), bf16), sds((16, 56, 128), bf16)),
+        out_shape=(sds((36, D), bf16), pltpu.VMEM((16, 56, 128), bf16)),
         in_specs=[VM] * 9,
         out_specs=(VM, VM),
         compiler_params=pltpu.CompilerParams(vmem_limit_bytes=12 * 1024 * 1024),
@@ -398,7 +398,7 @@
     payload, q, k, v, cum = pl.pallas_call(
         project_kernel,
         out_shape=(
-            sds((4, PAYLOAD, DK), bf16),
+            pltpu.VMEM((4, PAYLOAD, DK), bf16),
             pltpu.HBM((SEG, DK), bf16),
             pltpu.HBM((SEG, DK), bf16),
             pltpu.HBM((SEG, DK), bf16),
@@ -438,7 +438,7 @@
     heads = lax.all_to_all(mixed.reshape(4, 128, DK), "B", 0, 0, tiled=True)
     partial = pl.pallas_call(
         output_kernel,
-        out_shape=sds((128, D), bf16),
+        out_shape=pltpu.VMEM((128, D), bf16),
         in_specs=[VM] * 3,
         out_specs=VM,
         compiler_params=pltpu.CompilerParams(vmem_limit_bytes=16 * 1024 * 1024),

time: 147 us -> 147 us (level)
  no operation moved by 1% of the time
where the time goes in v11:
time: 147 us; the launch traced here: 145 us
  starting transfers between devices  63.6 us (43%)
  waiting for transfers between devices  54 us (37%)
  Pallas kernels  14.2 us (10%)
  blocking collectives  10.1 us (7%)
  local copies, waits for them, and re-layouts  1.95 us (1%)
    all_to_all x1, starting transfers between devices, device_body(): rows_z = lax.all_to_all(cut, ('A', 'B'), 0, 0, tiled=True)  15.2 us
    all_to_all x1, waiting for transfers between devices, device_body(): lax.all_to_all(payload, ('A', 'B'), 0, 0, tiled=True, axis_index_groups=P...  14.9 us
    ppermute x3, waiting for transfers between devices, device_body(): near.append(lax.ppermute(rows, 'B', [(b, b ^ j) for b in range(4)]))  14.4 us
    all_to_all x1, starting transfers between devices, device_body(): lax.all_to_all(payload, ('A', 'B'), 0, 0, tiled=True, axis_index_groups=P...  11.5 us
    ppermute x3, starting transfers between devices, device_body(): near.append(lax.ppermute(rows, 'B', [(b, b ^ j) for b in range(4)]))  10.1 us
    all_to_all x1, blocking collectives, device_body(): heads = lax.all_to_all(mixed.reshape(4, 128, DK), 'B', 0, 0, tiled=True)  10.1 us
    all_to_all x1, waiting for transfers between devices, device_body(): shares = lax.all_to_all(partial.reshape(4, 32, D), 'tp', 0, 0, tiled=True)  7.32 us
    ppermute x1, waiting for transfers between devices, device_body(): far_mods = lax.ppermute(mods, 'tp', [(i, i ^ 2) for i in range(4)])  6.25 us
  transfers between devices with their start and end apart: 13, of which 8 were waited for; matrix products, arithmetic and copies ran while one was open for 1% of the time, Pallas kernels for 3%

profile of v11, /device:TPU:6, one launch (start us, length us, event | category | flops | bytes accessed | tf_op | source)
XLA Modules:
  0.0 144.9 jit_solution(7396760740592119393)
XLA Ops:
  0.0 2.2 %pack.1 = (bf16[36,2048]{1,0:T(8,128)(2,1)S(1)}, bf16[16,56,128]{2,1,0:T(8,128)(2,1)}) custom-call(bf16[32,2048]{1,0:T(8,128)(2,1)} %lat_ref.1, bf16[16,2048]{1,0:T(8,128)(2,1)} %ctx_ref.1, f32[1,2048]{1,0:T(1,128)} %sv_ref.1, f32[1,2048]{1,0:T(1,128)} %cv_ref.1, bf16[96,2048]{1,0:T(8,128)(2,1)} %bitcast.15, bf16[128,256]{1,0:T(8,128)(2,1)} %wq_ref.1, ...), custom_call_target="tpu_custom_call" | custom-call | tf_op jit(solution)/shard_map/pack/pallas_call | solution.py:357
  2.2 15.2 %all-to-all-start = ((bf16[16,56,128]{2,1,0:T(8,128)(2,1)}), bf16[16,56,128]{2,1,0:T(8,128)(2,1)S(1)}, u32[]{:S(2)}, u32[]{:S(2)}) async-start(bf16[16,56,128]{2,1,0:T(8,128)(2,1)} %get-tuple-element.18), calls=%async_computation | async-start | bytes 458752 | tf_op jit(solution)/shard_map/all_to_all | solution.py:374
  17.4 3.8 %collective-permute-start = (bf16[36,2048]{1,0:T(8,128)(2,1)S(1)}, bf16[36,2048]{1,0:T(8,128)(2,1)S(1)}, u32[]{:S(2)}, u32[]{:S(2)}) collective-permute-start(bf16[36,2048]{1,0:T(8,128)(2,1)S(1)} %get-tuple-element.17), channel_id=1, source_target_pairs={{0,32},{32,0},{64,96},{96,64},{1,33},{33,1},{65,97},{97,65},{2,34}... | collective-permute-start | bytes 442376 | tf_op jit(solution)/shard_map/ppermute | solution.py:373
  21.2 4.3 %collective-permute-start.1 = (bf16[36,2048]{1,0:T(8,128)(2,1)S(1)}, bf16[36,2048]{1,0:T(8,128)(2,1)S(1)}, u32[]{:S(2)}, u32[]{:S(2)}) collective-permute-start(bf16[36,2048]{1,0:T(8,128)(2,1)S(1)} %get-tuple-element.17), channel_id=1, source_target_pairs={{0,64},{32,96},{64,0},{96,32},{1,65},{33,97},{65,1},{97,33},{2,66}... | collective-permute-start | bytes 442376 | tf_op jit(solution)/shard_map/ppermute | solution.py:373
  25.5 2.0 %collective-permute-start.2 = (bf16[36,2048]{1,0:T(8,128)(2,1)S(1)}, bf16[36,2048]{1,0:T(8,128)(2,1)S(1)}, u32[]{:S(2)}, u32[]{:S(2)}) collective-permute-start(bf16[36,2048]{1,0:T(8,128)(2,1)S(1)} %get-tuple-element.17), channel_id=1, source_target_pairs={{0,96},{32,64},{64,32},{96,0},{1,97},{33,65},{65,33},{97,1},{2,98}... | collective-permute-start | bytes 442376 | tf_op jit(solution)/shard_map/ppermute | solution.py:373
  27.5 9.0 %collective-permute-done = bf16[36,2048]{1,0:T(8,128)(2,1)S(1)} collective-permute-done((bf16[36,2048]{1,0:T(8,128)(2,1)S(1)}, bf16[36,2048]{1,0:T(8,128)(2,1)S(1)}, u32[]{:S(2)}, u32[]{:S(2)}) %collective-permute-start) | collective-permute-done | bytes 147488 | tf_op jit(solution)/shard_map/ppermute | solution.py:373
  36.5 0.0 collective-permute-done.1
  36.6 5.4 %collective-permute-done.2 = bf16[36,2048]{1,0:T(8,128)(2,1)S(1)} collective-permute-done((bf16[36,2048]{1,0:T(8,128)(2,1)S(1)}, bf16[36,2048]{1,0:T(8,128)(2,1)S(1)}, u32[]{:S(2)}, u32[]{:S(2)}) %collective-permute-start.2) | collective-permute-done | bytes 147488 | tf_op jit(solution)/shard_map/ppermute | solution.py:373
  42.0 0.1 concatenate.9.own_ref
  42.1 4.9 %collective-permute-start.4 = (bf16[144,2048]{1,0:T(8,128)(2,1)S(1)}, bf16[144,2048]{1,0:T(8,128)(2,1)S(1)}, u32[]{:S(2)}, u32[]{:S(2)}) collective-permute-start(bf16[144,2048]{1,0:T(8,128)(2,1)S(1)} %concatenate.9.own_ref), channel_id=1, source_target_pairs={{0,24},{8,0},{16,8},{24,16},{1,25},{9,1},{17,9},{25,17},{2,26},{10... | collective-permute-start | bytes 1769480 | tf_op jit(solution)/shard_map/ppermute | solution.py:385
  47.0 1.9 %collective-permute-start.3 = (bf16[144,2048]{1,0:T(8,128)(2,1)S(1)}, bf16[144,2048]{1,0:T(8,128)(2,1)S(1)}, u32[]{:S(2)}, u32[]{:S(2)}) collective-permute-start(bf16[144,2048]{1,0:T(8,128)(2,1)S(1)} %concatenate.9.own_ref), channel_id=1, source_target_pairs={{0,8},{8,16},{16,24},{24,0},{1,9},{9,17},{17,25},{25,1},{2,10},{10... | collective-permute-start | bytes 1769480 | tf_op jit(solution)/shard_map/ppermute | solution.py:384
  49.0 0.0 all-to-all-done
  49.0 1.0 broadcast_in_dim.2
  50.0 4.8 %all-to-all-start.1 = ((bf16[4,16,48,128]{3,2,1,0:T(8,128)(2,1)}), bf16[4,16,48,128]{3,2,1,0:T(8,128)(2,1)S(1)}, u32[]{:S(2)}, u32[]{:S(2)}) async-start(bf16[4,16,48,128]{3,2,1,0:T(8,128)(2,1)} %broadcast_in_dim.2), calls=%async_computation.1 | async-start | bytes 1572864 | tf_op jit(solution)/shard_map/all_to_all | solution.py:36
  54.7 4.4 %collective-permute-done.4.plus_ref = bf16[144,2048]{1,0:T(8,128)(2,1)S(1)} collective-permute-done((bf16[144,2048]{1,0:T(8,128)(2,1)S(1)}, bf16[144,2048]{1,0:T(8,128)(2,1)S(1)}, u32[]{:S(2)}, u32[]{:S(2)}) %collective-permute-start.4) | collective-permute-done | bytes 589856 | tf_op jit(solution)/shard_map/ppermute | solution.py:385
  59.2 5.3 %collective-permute-done.3.minus_ref = bf16[144,2048]{1,0:T(8,128)(2,1)S(1)} collective-permute-done((bf16[144,2048]{1,0:T(8,128)(2,1)S(1)}, bf16[144,2048]{1,0:T(8,128)(2,1)S(1)}, u32[]{:S(2)}, u32[]{:S(2)}) %collective-permute-start.3) | collective-permute-done | bytes 589856 | tf_op jit(solution)/shard_map/ppermute | solution.py:384
  64.5 0.0 all-to-all-done.1.mine_ref
  64.5 1.9 %collective-permute-start.8 = (bf16[4,16,48,128]{3,2,1,0:T(8,128)(2,1)S(1)}, bf16[4,16,48,128]{3,2,1,0:T(8,128)(2,1)S(1)}, u32[]{:S(2)}, u32[]{:S(2)}) collective-permute-start(bf16[4,16,48,128]{3,2,1,0:T(8,128)(2,1)S(1)} %all-to-all-done.1.mine_ref), channel_id=1, source_target_pairs={{0,1},{1,0},{2,3},{3,2},{4,5},{5,4},{6,7},{7,6},{8,9},{9,8},{10,11... | collective-permute-start | bytes 2359304 | tf_op jit(solution)/shard_map/ppermute | solution.py:376
  66.5 4.6 %collective-permute-start.6 = (bf16[88,2048]{1,0:T(8,128)(2,1)S(1)}, bf16[88,2048]{1,0:T(8,128)(2,1)S(1)}, u32[]{:S(2)}, u32[]{:S(2)}) collective-permute-start(bf16[88,2048]{1,0:T(8,128)(2,1)S(1)} %pad_maximum_fusion), channel_id=1, source_target_pairs={{0,24},{8,0},{16,8},{24,16},{1,25},{9,1},{17,9},{25,17},{2,26},{10... | collective-permute-start | bytes 1081352 | tf_op jit(solution)/shard_map/ppermute | solution.py:387
  71.1 1.9 %collective-permute-start.5 = (bf16[72,2048]{1,0:T(8,128)(2,1)S(1)}, bf16[72,2048]{1,0:T(8,128)(2,1)S(1)}, u32[]{:S(2)}, u32[]{:S(2)}) collective-permute-start(bf16[72,2048]{1,0:T(8,128)(2,1)S(1)} %pad_maximum_fusion.1), channel_id=1, source_target_pairs={{0,8},{8,16},{16,24},{24,0},{1,9},{9,17},{17,25},{25,1},{2,10},{10... | collective-permute-start | bytes 884744 | tf_op jit(solution)/shard_map/ppermute | solution.py:386
  73.1 3.4 %collective-permute-start.7 = (bf16[8,2048]{1,0:T(8,128)(2,1)S(1)}, bf16[8,2048]{1,0:T(8,128)(2,1)S(1)}, u32[]{:S(2)}, u32[]{:S(2)}) collective-permute-start(bf16[8,2048]{1,0:T(8,128)(2,1)S(1)} %get-tuple-element.30.own_mods_ref), channel_id=1, source_target_pairs={{0,16},{8,24},{16,0},{24,8},{1,17},{9,25},{17,1},{25,9},{2,18},{10... | collective-permute-start | bytes 98312 | tf_op jit(solution)/shard_map/ppermute | solution.py:379
  76.4 6.2 %collective-permute-done.7.far_mods_ref = bf16[8,2048]{1,0:T(8,128)(2,1)S(1)} collective-permute-done((bf16[8,2048]{1,0:T(8,128)(2,1)S(1)}, bf16[8,2048]{1,0:T(8,128)(2,1)S(1)}, u32[]{:S(2)}, u32[]{:S(2)}) %collective-permute-start.7) | collective-permute-done | bytes 32800 | tf_op jit(solution)/shard_map/ppermute | solution.py:379
  82.7 1.4 collective-permute-done.5.low_ref
  84.1 0.0 collective-permute-done.6.high_ref
  84.1 1.8 %hidden.1 = (bf16[576,2048]{1,0:T(8,128)(2,1)S(1)}, f32[2,6144]{1,0:T(2,128)}) custom-call(bf16[144,2048]{1,0:T(8,128)(2,1)S(1)} %concatenate.9.own_ref, bf16[144,2048]{1,0:T(8,128)(2,1)S(1)} %collective-permute-done.3.minus_ref, bf16[144,2048]{1,0:T(8,128)(2,1)S(1)} %collective-permute-done.4.plus_ref, bf16[72,2048]{1,0:T(8,128)(2,1)S(1)} %collective-permute-done.5.low_ref, ...), custom_call_target="tpu_custom_call" | custom-call | tf_op jit(solution)/shard_map/hidden/pallas_call | solution.py:389
  85.9 0.0 collective-permute-done.8.other_ref
  85.9 5.4 %project.1 = (bf16[4,328,128]{2,1,0:T(8,128)(2,1)}, bf16[512,128]{1,0:T(8,128)(2,1)}, bf16[512,128]{1,0:T(8,128)(2,1)}, bf16[512,128]{1,0:T(8,128)(2,1)}, f32[2,512,128]{2,1,0:T(8,128)}) custom-call(bf16[576,2048]{1,0:T(8,128)(2,1)S(1)} %get-tuple-element.20.h_ref, bf16[4,16,48,128]{3,2,1,0:T(8,128)(2,1)S(1)} %all-to-all-done.1.mine_ref, ...), custom_call_target="tpu_custom_call" | custom-call | tf_op jit(solution)/shard_map/project/pallas_call | solution.py:398
  91.3 0.0 copy-start
  91.3 11.5 %all-to-all-start.2 = ((bf16[4,328,128]{2,1,0:T(8,128)(2,1)}), bf16[4,328,128]{2,1,0:T(8,128)(2,1)S(1)}, u32[]{:S(2)}, u32[]{:S(2)}) async-start(bf16[4,328,128]{2,1,0:T(8,128)(2,1)} %get-tuple-element.21), calls=%async_computation.2 | async-start | bytes 671744 | tf_op jit(solution)/shard_map/all_to_all | solution.py:419
  102.7 2.3 %local.1 = (f32[512,128]{1,0:T(8,128)S(1)}, bf16[512,128]{1,0:T(8,128)(2,1)S(1)}, bf16[512,128]{1,0:T(8,128)(2,1)S(1)}) custom-call(bf16[512,128]{1,0:T(8,128)(2,1)} %get-tuple-element.22.q_ref, bf16[512,128]{1,0:T(8,128)(2,1)} %get-tuple-element.23.k_ref, bf16[512,128]{1,0:T(8,128)(2,1)} %get-tuple-element.24.v_ref, f32[2,512,128]{2,1,0:T(8,128)} %get-tuple-element.25.cum_ref), custom_call_target="tpu_custom_call" | custom-call | tf_op jit(solution)/shard_map/local/pallas_call | solution.py:422
  105.1 14.9 %all-to-all-done.2.in_ref = bf16[4,328,128]{2,1,0:T(8,128)(2,1)S(1)} async-done(((bf16[4,328,128]{2,1,0:T(8,128)(2,1)}), bf16[4,328,128]{2,1,0:T(8,128)(2,1)S(1)}, u32[]{:S(2)}, u32[]{:S(2)}) %all-to-all-start.2) | async-done | bytes 335904 | tf_op jit(solution)/shard_map/all_to_all | solution.py:419
  120.0 0.5 combine.1
  120.5 0.0 copy-start.1
  120.5 10.1 %all_to_all.25.mix_ref = bf16[4,128,128]{2,1,0:T(8,128)(2,1)S(1)} all-to-all(bf16[4,128,128]{2,1,0:T(8,128)(2,1)S(1)} %bitcast.14), channel_id=1, replica_groups=mesh['A'=4,'B'=4,'tp'=4,'x'=4,'core'=2] {'B'}, dimensions={0} | all-to-all | bytes 262144 | tf_op jit(solution)/shard_map/all_to_all | solution.py:438
  130.6 0.0 copy-done
  130.6 2.0 %output.1 = bf16[128,2048]{1,0:T(8,128)(2,1)} custom-call(bf16[4,128,128]{2,1,0:T(8,128)(2,1)S(1)} %all_to_all.25.mix_ref, f32[1,256]{1,0:T(1,128)} %bitcast.20, bf16[512,2048]{1,0:T(8,128)(2,1)S(1)} %copy-done), custom_call_target="tpu_custom_call" | custom-call | tf_op jit(solution)/shard_map/output/pallas_call | solution.py:439
  132.6 3.5 %all-to-all-start.4 = ((bf16[4,32,2048]{2,1,0:T(8,128)(2,1)}), bf16[4,32,2048]{2,1,0:T(8,128)(2,1)S(1)}, u32[]{:S(2)}, u32[]{:S(2)}) async-start(bf16[4,32,2048]{2,1,0:T(8,128)(2,1)} %bitcast.11), calls=%async_computation.4 | async-start | bytes 1048576 | tf_op jit(solution)/shard_map/all_to_all | solution.py:447
  136.1 0.7 slice.50
  136.8 7.3 %all-to-all-done.4 = bf16[4,32,2048]{2,1,0:T(8,128)(2,1)S(1)} async-done(((bf16[4,32,2048]{2,1,0:T(8,128)(2,1)}), bf16[4,32,2048]{2,1,0:T(8,128)(2,1)S(1)}, u32[]{:S(2)}, u32[]{:S(2)}) %all-to-all-start.4) | async-done | bytes 524320 | tf_op jit(solution)/shard_map/all_to_all | solution.py:447
  144.1 0.1 reduce_sum.12
  144.2 0.0 copy-done.1
  144.2 0.7 add_convert_fusion
  (14 shorter events, 0.2 us)
Async XLA Ops:
  2.2 46.8 %all-to-all-start = ((bf16[16,56,128]{2,1,0:T(8,128)(2,1)}), bf16[16,56,128]{2,1,0:T(8,128)(2,1)S(1)}, u32[]{:S(2)}, u32[]{:S(2)}) async-start(bf16[16,56,128]{2,1,0:T(8,128)(2,1)} %get-tuple-element.18), calls=%async_computation | async-start | bytes 458752 | tf_op jit(solution)/shard_map/all_to_all | solution.py:374
  17.4 19.2 %collective-permute-start = (bf16[36,2048]{1,0:T(8,128)(2,1)S(1)}, bf16[36,2048]{1,0:T(8,128)(2,1)S(1)}, u32[]{:S(2)}, u32[]{:S(2)}) collective-permute-start(bf16[36,2048]{1,0:T(8,128)(2,1)S(1)} %get-tuple-element.17), channel_id=1, source_target_pairs={{0,32},{32,0},{64,96},{96,64},{1,33},{33,1},{65,97},{97,65},{2,34}... | collective-permute-start | bytes 442376 | tf_op jit(solution)/shard_map/ppermute | solution.py:373
  21.2 15.4 %collective-permute-start.1 = (bf16[36,2048]{1,0:T(8,128)(2,1)S(1)}, bf16[36,2048]{1,0:T(8,128)(2,1)S(1)}, u32[]{:S(2)}, u32[]{:S(2)}) collective-permute-start(bf16[36,2048]{1,0:T(8,128)(2,1)S(1)} %get-tuple-element.17), channel_id=1, source_target_pairs={{0,64},{32,96},{64,0},{96,32},{1,65},{33,97},{65,1},{97,33},{2,66}... | collective-permute-start | bytes 442376 | tf_op jit(solution)/shard_map/ppermute | solution.py:373
  25.5 16.5 %collective-permute-start.2 = (bf16[36,2048]{1,0:T(8,128)(2,1)S(1)}, bf16[36,2048]{1,0:T(8,128)(2,1)S(1)}, u32[]{:S(2)}, u32[]{:S(2)}) collective-permute-start(bf16[36,2048]{1,0:T(8,128)(2,1)S(1)} %get-tuple-element.17), channel_id=1, source_target_pairs={{0,96},{32,64},{64,32},{96,0},{1,97},{33,65},{65,33},{97,1},{2,98}... | collective-permute-start | bytes 442376 | tf_op jit(solution)/shard_map/ppermute | solution.py:373
  42.1 17.1 %collective-permute-start.4 = (bf16[144,2048]{1,0:T(8,128)(2,1)S(1)}, bf16[144,2048]{1,0:T(8,128)(2,1)S(1)}, u32[]{:S(2)}, u32[]{:S(2)}) collective-permute-start(bf16[144,2048]{1,0:T(8,128)(2,1)S(1)} %concatenate.9.own_ref), channel_id=1, source_target_pairs={{0,24},{8,0},{16,8},{24,16},{1,25},{9,1},{17,9},{25,17},{2,26},{10... | collective-permute-start | bytes 1769480 | tf_op jit(solution)/shard_map/ppermute | solution.py:385
  47.0 17.5 %collective-permute-start.3 = (bf16[144,2048]{1,0:T(8,128)(2,1)S(1)}, bf16[144,2048]{1,0:T(8,128)(2,1)S(1)}, u32[]{:S(2)}, u32[]{:S(2)}) collective-permute-start(bf16[144,2048]{1,0:T(8,128)(2,1)S(1)} %concatenate.9.own_ref), channel_id=1, source_target_pairs={{0,8},{8,16},{16,24},{24,0},{1,9},{9,17},{17,25},{25,1},{2,10},{10... | collective-permute-start | bytes 1769480 | tf_op jit(solution)/shard_map/ppermute | solution.py:384
  50.0 14.6 %all-to-all-start.1 = ((bf16[4,16,48,128]{3,2,1,0:T(8,128)(2,1)}), bf16[4,16,48,128]{3,2,1,0:T(8,128)(2,1)S(1)}, u32[]{:S(2)}, u32[]{:S(2)}) async-start(bf16[4,16,48,128]{3,2,1,0:T(8,128)(2,1)} %broadcast_in_dim.2), calls=%async_computation.1 | async-start | bytes 1572864 | tf_op jit(solution)/shard_map/all_to_all | solution.py:36
  64.5 21.4 %collective-permute-start.8 = (bf16[4,16,48,128]{3,2,1,0:T(8,128)(2,1)S(1)}, bf16[4,16,48,128]{3,2,1,0:T(8,128)(2,1)S(1)}, u32[]{:S(2)}, u32[]{:S(2)}) collective-permute-start(bf16[4,16,48,128]{3,2,1,0:T(8,128)(2,1)S(1)} %all-to-all-done.1.mine_ref), channel_id=1, source_target_pairs={{0,1},{1,0},{2,3},{3,2},{4,5},{5,4},{6,7},{7,6},{8,9},{9,8},{10,11... | collective-permute-start | bytes 2359304 | tf_op jit(solution)/shard_map/ppermute | solution.py:376
  66.5 17.5 %collective-permute-start.6 = (bf16[88,2048]{1,0:T(8,128)(2,1)S(1)}, bf16[88,2048]{1,0:T(8,128)(2,1)S(1)}, u32[]{:S(2)}, u32[]{:S(2)}) collective-permute-start(bf16[88,2048]{1,0:T(8,128)(2,1)S(1)} %pad_maximum_fusion), channel_id=1, source_target_pairs={{0,24},{8,0},{16,8},{24,16},{1,25},{9,1},{17,9},{25,17},{2,26},{10... | collective-permute-start | bytes 1081352 | tf_op jit(solution)/shard_map/ppermute | solution.py:387
  71.1 12.9 %collective-permute-start.5 = (bf16[72,2048]{1,0:T(8,128)(2,1)S(1)}, bf16[72,2048]{1,0:T(8,128)(2,1)S(1)}, u32[]{:S(2)}, u32[]{:S(2)}) collective-permute-start(bf16[72,2048]{1,0:T(8,128)(2,1)S(1)} %pad_maximum_fusion.1), channel_id=1, source_target_pairs={{0,8},{8,16},{16,24},{24,0},{1,9},{9,17},{17,25},{25,1},{2,10},{10... | collective-permute-start | bytes 884744 | tf_op jit(solution)/shard_map/ppermute | solution.py:386
  73.1 9.6 %collective-permute-start.7 = (bf16[8,2048]{1,0:T(8,128)(2,1)S(1)}, bf16[8,2048]{1,0:T(8,128)(2,1)S(1)}, u32[]{:S(2)}, u32[]{:S(2)}) collective-permute-start(bf16[8,2048]{1,0:T(8,128)(2,1)S(1)} %get-tuple-element.30.own_mods_ref), channel_id=1, source_target_pairs={{0,16},{8,24},{16,0},{24,8},{1,17},{9,25},{17,1},{25,9},{2,18},{10... | collective-permute-start | bytes 98312 | tf_op jit(solution)/shard_map/ppermute | solution.py:379
  91.3 39.3 %copy-start = (bf16[512,2048]{1,0:T(8,128)(2,1)S(1)}, bf16[512,2048]{1,0:T(8,128)(2,1)}, u32[]{:S(2)}) copy-start(bf16[512,2048]{1,0:T(8,128)(2,1)} %w_ref.1) | copy-start | bytes 6291460
  91.3 28.7 %all-to-all-start.2 = ((bf16[4,328,128]{2,1,0:T(8,128)(2,1)}), bf16[4,328,128]{2,1,0:T(8,128)(2,1)S(1)}, u32[]{:S(2)}, u32[]{:S(2)}) async-start(bf16[4,328,128]{2,1,0:T(8,128)(2,1)} %get-tuple-element.21), calls=%async_computation.2 | async-start | bytes 671744 | tf_op jit(solution)/shard_map/all_to_all | solution.py:419
  120.5 23.7 %copy-start.1 = (bf16[32,2048]{1,0:T(8,128)(2,1)S(1)}, bf16[32,2048]{1,0:T(8,128)(2,1)}, u32[]{:S(2)}) copy-start(bf16[32,2048]{1,0:T(8,128)(2,1)} %lat_ref.1) | copy-start | bytes 393220
  132.6 11.5 %all-to-all-start.4 = ((bf16[4,32,2048]{2,1,0:T(8,128)(2,1)}), bf16[4,32,2048]{2,1,0:T(8,128)(2,1)S(1)}, u32[]{:S(2)}, u32[]{:S(2)}) async-start(bf16[4,32,2048]{2,1,0:T(8,128)(2,1)} %bitcast.11), calls=%async_computation.4 | async-start | bytes 1048576 | tf_op jit(solution)/shard_map/all_to_all | solution.py:447

commit v12 on v10

--- a/solution.py
+++ b/solution.py
@@ -167,11 +167,11 @@
                 cols = slice(j * 128, (j + 1) * 128)
                 w_ref[here, cols] = mine_ref[xi, z, j * 16 : (j + 1) * 16, :]
                 w_ref[there, cols] = other_ref[xi, z, j * 16 : (j + 1) * 16, :]
+    w_ref[:, 384:448] = down_ref[...]
     y_of = [y, (y + 3) % 4, (y + 1) % 4, (y + 2) % 4]
-    rows = h_ref[...]
-    low = nt(rows, down_ref[...]).astype(bf16)
-    slot_logs = decays_of(low, up_ref, bias_ref)
-    slot_qkv = jnp.dot(rows, w_ref[...], preferred_element_type=f32).astype(bf16)
+    res = jnp.dot(h_ref[...], w_ref[...], preferred_element_type=f32).astype(bf16)
+    slot_logs = decays_of(res[:, 384:448], up_ref, bias_ref)
+    slot_qkv = res[:, 0:384]
     for n in range(4):
         for j in range(5):
             size = 32 if j < 4 else 16
@@ -368,6 +368,7 @@
             jnp.moveaxis(decay_extra, 1, 2).reshape(4, 128),
         )
     )
+    down = lax.optimization_barrier(decay_down.T.reshape(64, D)).T
     near = [rows]
     for j in range(1, 4):
         near.append(lax.ppermute(rows, "B", [(b, b ^ j) for b in range(4)]))
@@ -407,14 +408,14 @@
         in_specs=[VM] * 7,
         out_specs=(VM,) * 5,
         scratch_shapes=[
-            pltpu.VMEM((D, 384), bf16),
+            pltpu.VMEM((D, 448), bf16),
             pltpu.VMEM((ROWS, 384), bf16),
             pltpu.VMEM((ROWS, 256), f32),
         ],
         compiler_params=pltpu.CompilerParams(vmem_limit_bytes=24 * 1024 * 1024),
         name="project",
     )(
-        *on_chip(hidden, mine, other), *off_chip(decay_down.T, decay_up, decay_bias), *on_chip(ride),
+        *on_chip(hidden, mine, other), *off_chip(down, decay_up, decay_bias), *on_chip(ride),
     )
     got = lax.all_to_all(
         payload, ("A", "B"), 0, 0, tiled=True, axis_index_groups=PEERS

time: 147 us -> 152 us (1.034)
  local copies, waits for them, and re-layouts: 1.95 us -> 6.85 us
  other arithmetic: 0.83 us -> 4.19 us
  waiting for transfers between devices: 54 us -> 51.6 us
    unnamed x4 -> x9, local copies, waits for them, and re-layouts: 0.01 us -> 2.69 us
    ppermute x1, waiting for transfers between devices: 6.25 us -> 4.49 us  [device_body(): far_mods = lax.ppermute(mods, 'tp', [(i, i ^ 2) for i in range(4)])]
    concatenate x1, other arithmetic: 0.03 us -> 1.74 us  [device_body(): high = lax.ppermute(jnp.concatenate([plus[64:], mods]), 'tp', down_shift)]
    concatenate x1, other arithmetic: 0.02 us -> 1.68 us  [device_body(): low = lax.ppermute(jnp.concatenate([minus[:64], mods]), 'tp', up_shift)]
  transfers between devices with their start and end apart: 13 -> 13, of which waited for: 8 -> 8; matrix products, arithmetic and copies ran while one was open for 1% -> 6% of each run, Pallas kernels for 3% -> 3%
where the time goes in v12:
time: 152 us; the launch traced here: 150 us
  starting transfers between devices  62.9 us (41%)
  waiting for transfers between devices  51.6 us (34%)
  Pallas kernels  13.9 us (9%)
  blocking collectives  10.1 us (7%)
  local copies, waits for them, and re-layouts  6.85 us (5%)
  other arithmetic  4.19 us (3%)
    all_to_all x1, starting transfers between devices, device_body(): rows_z = lax.all_to_all(cut, ('A', 'B'), 0, 0, tiled=True)  15.2 us
    all_to_all x1, waiting for transfers between devices, device_body(): lax.all_to_all(payload, ('A', 'B'), 0, 0, tiled=True, axis_index_groups=P...  14.9 us
    ppermute x3, waiting for transfers between devices, device_body(): near.append(lax.ppermute(rows, 'B', [(b, b ^ j) for b in range(4)]))  14.4 us
    all_to_all x1, starting transfers between devices, device_body(): lax.all_to_all(payload, ('A', 'B'), 0, 0, tiled=True, axis_index_groups=P...  11.5 us
    ppermute x3, starting transfers between devices, device_body(): near.append(lax.ppermute(rows, 'B', [(b, b ^ j) for b in range(4)]))  10.1 us
    all_to_all x1, blocking collectives, device_body(): heads = lax.all_to_all(mixed.reshape(4, 128, DK), 'B', 0, 0, tiled=True)  10.1 us
    all_to_all x1, waiting for transfers between devices, device_body(): shares = lax.all_to_all(partial.reshape(4, 32, D), 'tp', 0, 0, tiled=True)  7.32 us
    ppermute x1, starting transfers between devices, device_body(): plus = lax.ppermute(own, 'tp', down_shift)  4.92 us
  transfers between devices with their start and end apart: 13, of which 8 were waited for; matrix products, arithmetic and copies ran while one was open for 6% of the time, Pallas kernels for 3%

profile of v12, /device:TPU:6, one launch (start us, length us, event | category | flops | bytes accessed | tf_op | source)
XLA Modules:
  0.0 149.8 jit_solution(18275888156225951328)
XLA Ops:
  0.0 2.2 %pack.1 = (bf16[36,2048]{1,0:T(8,128)(2,1)S(1)}, bf16[16,56,128]{2,1,0:T(8,128)(2,1)}) custom-call(bf16[32,2048]{1,0:T(8,128)(2,1)} %lat_ref.1, bf16[16,2048]{1,0:T(8,128)(2,1)} %ctx_ref.1, f32[1,2048]{1,0:T(1,128)} %sv_ref.1, f32[1,2048]{1,0:T(1,128)} %cv_ref.1, bf16[96,2048]{1,0:T(8,128)(2,1)} %bitcast.16, bf16[128,256]{1,0:T(8,128)(2,1)} %wq_ref.1, ...), custom_call_target="tpu_custom_call" | custom-call | tf_op jit(solution)/shard_map/pack/pallas_call | solution.py:357
  2.2 15.2 %all-to-all-start = ((bf16[16,56,128]{2,1,0:T(8,128)(2,1)}), bf16[16,56,128]{2,1,0:T(8,128)(2,1)S(1)}, u32[]{:S(2)}, u32[]{:S(2)}) async-start(bf16[16,56,128]{2,1,0:T(8,128)(2,1)} %get-tuple-element.18), calls=%async_computation | async-start | bytes 458752 | tf_op jit(solution)/shard_map/all_to_all | solution.py:375
  17.4 3.8 %collective-permute-start = (bf16[36,2048]{1,0:T(8,128)(2,1)S(1)}, bf16[36,2048]{1,0:T(8,128)(2,1)S(1)}, u32[]{:S(2)}, u32[]{:S(2)}) collective-permute-start(bf16[36,2048]{1,0:T(8,128)(2,1)S(1)} %get-tuple-element.17), channel_id=1, source_target_pairs={{0,32},{32,0},{64,96},{96,64},{1,33},{33,1},{65,97},{97,65},{2,34}... | collective-permute-start | bytes 442376 | tf_op jit(solution)/shard_map/ppermute | solution.py:374
  21.2 4.3 %collective-permute-start.1 = (bf16[36,2048]{1,0:T(8,128)(2,1)S(1)}, bf16[36,2048]{1,0:T(8,128)(2,1)S(1)}, u32[]{:S(2)}, u32[]{:S(2)}) collective-permute-start(bf16[36,2048]{1,0:T(8,128)(2,1)S(1)} %get-tuple-element.17), channel_id=1, source_target_pairs={{0,64},{32,96},{64,0},{96,32},{1,65},{33,97},{65,1},{97,33},{2,66}... | collective-permute-start | bytes 442376 | tf_op jit(solution)/shard_map/ppermute | solution.py:374
  25.5 2.0 %collective-permute-start.2 = (bf16[36,2048]{1,0:T(8,128)(2,1)S(1)}, bf16[36,2048]{1,0:T(8,128)(2,1)S(1)}, u32[]{:S(2)}, u32[]{:S(2)}) collective-permute-start(bf16[36,2048]{1,0:T(8,128)(2,1)S(1)} %get-tuple-element.17), channel_id=1, source_target_pairs={{0,96},{32,64},{64,32},{96,0},{1,97},{33,65},{65,33},{97,1},{2,98}... | collective-permute-start | bytes 442376 | tf_op jit(solution)/shard_map/ppermute | solution.py:374
  27.5 9.0 %collective-permute-done = bf16[36,2048]{1,0:T(8,128)(2,1)S(1)} collective-permute-done((bf16[36,2048]{1,0:T(8,128)(2,1)S(1)}, bf16[36,2048]{1,0:T(8,128)(2,1)S(1)}, u32[]{:S(2)}, u32[]{:S(2)}) %collective-permute-start) | collective-permute-done | bytes 147488 | tf_op jit(solution)/shard_map/ppermute | solution.py:374
  36.5 0.0 collective-permute-done.1
  36.6 5.4 %collective-permute-done.2 = bf16[36,2048]{1,0:T(8,128)(2,1)S(1)} collective-permute-done((bf16[36,2048]{1,0:T(8,128)(2,1)S(1)}, bf16[36,2048]{1,0:T(8,128)(2,1)S(1)}, u32[]{:S(2)}, u32[]{:S(2)}) %collective-permute-start.2) | collective-permute-done | bytes 147488 | tf_op jit(solution)/shard_map/ppermute | solution.py:374
  42.0 0.1 concatenate.9.own_ref
  42.1 4.9 %collective-permute-start.4 = (bf16[144,2048]{1,0:T(8,128)(2,1)S(1)}, bf16[144,2048]{1,0:T(8,128)(2,1)S(1)}, u32[]{:S(2)}, u32[]{:S(2)}) collective-permute-start(bf16[144,2048]{1,0:T(8,128)(2,1)S(1)} %concatenate.9.own_ref), channel_id=1, source_target_pairs={{0,24},{8,0},{16,8},{24,16},{1,25},{9,1},{17,9},{25,17},{2,26},{10... | collective-permute-start | bytes 1769480 | tf_op jit(solution)/shard_map/ppermute | solution.py:386
  47.0 1.9 %collective-permute-start.3 = (bf16[144,2048]{1,0:T(8,128)(2,1)S(1)}, bf16[144,2048]{1,0:T(8,128)(2,1)S(1)}, u32[]{:S(2)}, u32[]{:S(2)}) collective-permute-start(bf16[144,2048]{1,0:T(8,128)(2,1)S(1)} %concatenate.9.own_ref), channel_id=1, source_target_pairs={{0,8},{8,16},{16,24},{24,0},{1,9},{9,17},{17,25},{25,1},{2,10},{10... | collective-permute-start | bytes 1769480 | tf_op jit(solution)/shard_map/ppermute | solution.py:385
  49.0 0.0 all-to-all-done
  49.0 0.0 copy-start.2
  49.0 1.0 broadcast_in_dim.2
  50.0 4.8 %all-to-all-start.1 = ((bf16[4,16,48,128]{3,2,1,0:T(8,128)(2,1)}), bf16[4,16,48,128]{3,2,1,0:T(8,128)(2,1)S(1)}, u32[]{:S(2)}, u32[]{:S(2)}) async-start(bf16[4,16,48,128]{3,2,1,0:T(8,128)(2,1)} %broadcast_in_dim.2), calls=%async_computation.1 | async-start | bytes 1572864 | tf_op jit(solution)/shard_map/all_to_all | solution.py:36
  54.8 4.4 %collective-permute-done.4.plus_ref = bf16[144,2048]{1,0:T(8,128)(2,1)S(1)} collective-permute-done((bf16[144,2048]{1,0:T(8,128)(2,1)S(1)}, bf16[144,2048]{1,0:T(8,128)(2,1)S(1)}, u32[]{:S(2)}, u32[]{:S(2)}) %collective-permute-start.4) | collective-permute-done | bytes 589856 | tf_op jit(solution)/shard_map/ppermute | solution.py:386
  59.2 0.8 slice.60
  60.0 4.6 %collective-permute-done.3.minus_ref = bf16[144,2048]{1,0:T(8,128)(2,1)S(1)} collective-permute-done((bf16[144,2048]{1,0:T(8,128)(2,1)S(1)}, bf16[144,2048]{1,0:T(8,128)(2,1)S(1)}, u32[]{:S(2)}, u32[]{:S(2)}) %collective-permute-start.3) | collective-permute-done | bytes 589856 | tf_op jit(solution)/shard_map/ppermute | solution.py:385
  64.5 0.7 slice.58
  65.2 0.0 all-to-all-done.1.mine_ref
  65.2 1.9 %collective-permute-start.8 = (bf16[4,16,48,128]{3,2,1,0:T(8,128)(2,1)S(1)}, bf16[4,16,48,128]{3,2,1,0:T(8,128)(2,1)S(1)}, u32[]{:S(2)}, u32[]{:S(2)}) collective-permute-start(bf16[4,16,48,128]{3,2,1,0:T(8,128)(2,1)S(1)} %all-to-all-done.1.mine_ref), channel_id=1, source_target_pairs={{0,1},{1,0},{2,3},{3,2},{4,5},{5,4},{6,7},{7,6},{8,9},{9,8},{10,11... | collective-permute-start | bytes 2359304 | tf_op jit(solution)/shard_map/ppermute | solution.py:377
  67.2 0.8 fusion
  67.9 1.7 %pad_maximum_fusion = bf16[88,2048]{1,0:T(8,128)(2,1)} fusion(bf16[8,2048]{1,0:T(8,128)(2,1)S(1)} %get-tuple-element.30.own_mods_ref, bf16[80,2048]{1,0:T(8,128)(2,1)} %slice.60), kind=kLoop, calls=%fused_computation | loop fusion | flops 720896 | bytes 720896 | tf_op jit(solution)/shard_map/concatenate | solution.py:388
  69.7 3.9 %collective-permute-start.6 = (bf16[88,2048]{1,0:T(8,128)(2,1)}, bf16[88,2048]{1,0:T(8,128)(2,1)}, u32[]{:S(2)}, u32[]{:S(2)}) collective-permute-start(bf16[88,2048]{1,0:T(8,128)(2,1)} %pad_maximum_fusion), channel_id=1, source_target_pairs={{0,24},{8,0},{16,8},{24,16},{1,25},{9,1},{17,9},{25,17},{2,26},{10... | collective-permute-start | bytes 1081352 | tf_op jit(solution)/shard_map/ppermute | solution.py:388
  73.6 1.7 %pad_maximum_fusion.1 = bf16[72,2048]{1,0:T(8,128)(2,1)} fusion(bf16[8,2048]{1,0:T(8,128)(2,1)S(1)} %get-tuple-element.30.own_mods_ref, bf16[64,2048]{1,0:T(8,128)(2,1)} %slice.58), kind=kLoop, calls=%fused_computation.1 | loop fusion | flops 589824 | bytes 589824 | tf_op jit(solution)/shard_map/concatenate | solution.py:387
  75.3 1.9 %collective-permute-start.5 = (bf16[72,2048]{1,0:T(8,128)(2,1)}, bf16[72,2048]{1,0:T(8,128)(2,1)}, u32[]{:S(2)}, u32[]{:S(2)}) collective-permute-start(bf16[72,2048]{1,0:T(8,128)(2,1)} %pad_maximum_fusion.1), channel_id=1, source_target_pairs={{0,8},{8,16},{16,24},{24,0},{1,9},{9,17},{17,25},{25,1},{2,10},{10... | collective-permute-start | bytes 884744 | tf_op jit(solution)/shard_map/ppermute | solution.py:387
  77.2 3.4 %collective-permute-start.7 = (bf16[8,2048]{1,0:T(8,128)(2,1)S(1)}, bf16[8,2048]{1,0:T(8,128)(2,1)S(1)}, u32[]{:S(2)}, u32[]{:S(2)}) collective-permute-start(bf16[8,2048]{1,0:T(8,128)(2,1)S(1)} %get-tuple-element.30.own_mods_ref), channel_id=1, source_target_pairs={{0,16},{8,24},{16,0},{24,8},{1,17},{9,25},{17,1},{25,9},{2,18},{10... | collective-permute-start | bytes 98312 | tf_op jit(solution)/shard_map/ppermute | solution.py:380
  80.5 2.0 %copy.16 = bf16[2048,64]{1,0:T(8,128)(2,1)} copy(bf16[2048,64]{0,1:T(8,128)(2,1)} %param.24) | data formatting | bytes 524288 | tf_op args[9]
  82.5 4.5 %collective-permute-done.7.far_mods_ref = bf16[8,2048]{1,0:T(8,128)(2,1)S(1)} collective-permute-done((bf16[8,2048]{1,0:T(8,128)(2,1)S(1)}, bf16[8,2048]{1,0:T(8,128)(2,1)S(1)}, u32[]{:S(2)}, u32[]{:S(2)}) %collective-permute-start.7) | collective-permute-done | bytes 32800 | tf_op jit(solution)/shard_map/ppermute | solution.py:380
  87.0 1.5 collective-permute-done.5.low_ref
  88.5 0.0 collective-permute-done.6.high_ref
  88.5 2.2 %hidden.1 = (bf16[576,2048]{1,0:T(8,128)(2,1)S(1)}, f32[2,6144]{1,0:T(2,128)}) custom-call(bf16[144,2048]{1,0:T(8,128)(2,1)S(1)} %concatenate.9.own_ref, bf16[144,2048]{1,0:T(8,128)(2,1)S(1)} %collective-permute-done.3.minus_ref, bf16[144,2048]{1,0:T(8,128)(2,1)S(1)} %collective-permute-done.4.plus_ref, bf16[72,2048]{1,0:T(8,128)(2,1)} %collective-permute-done.5.low_ref, ...), custom_call_target="tpu_custom_call" | custom-call | tf_op jit(solution)/shard_map/hidden/pallas_call | solution.py:390
  90.7 0.0 collective-permute-done.8.other_ref
  90.7 4.7 %project.1 = (bf16[4,328,128]{2,1,0:T(8,128)(2,1)S(1)}, bf16[512,128]{1,0:T(8,128)(2,1)}, bf16[512,128]{1,0:T(8,128)(2,1)}, bf16[512,128]{1,0:T(8,128)(2,1)}, f32[2,512,128]{2,1,0:T(8,128)}) custom-call(bf16[576,2048]{1,0:T(8,128)(2,1)S(1)} %get-tuple-element.20.h_ref, bf16[4,16,48,128]{3,2,1,0:T(8,128)(2,1)S(1)} %all-to-all-done.1.mine_ref, ...), custom_call_target="tpu_custom_call" | custom-call | tf_op jit(solution)/shard_map/project/pallas_call | solution.py:399
  95.4 0.7 copy-done.1
  96.1 11.5 %all-to-all-start.2 = ((bf16[4,328,128]{2,1,0:T(8,128)(2,1)}), bf16[4,328,128]{2,1,0:T(8,128)(2,1)S(1)}, u32[]{:S(2)}, u32[]{:S(2)}) async-start(bf16[4,328,128]{2,1,0:T(8,128)(2,1)} %copy-done.1), calls=%async_computation.2 | async-start | bytes 671744 | tf_op jit(solution)/shard_map/all_to_all | solution.py:420
  107.6 2.3 %local.1 = (f32[512,128]{1,0:T(8,128)S(1)}, bf16[512,128]{1,0:T(8,128)(2,1)S(1)}, bf16[512,128]{1,0:T(8,128)(2,1)S(1)}) custom-call(bf16[512,128]{1,0:T(8,128)(2,1)} %get-tuple-element.22.q_ref, bf16[512,128]{1,0:T(8,128)(2,1)} %get-tuple-element.23.k_ref, bf16[512,128]{1,0:T(8,128)(2,1)} %get-tuple-element.24.v_ref, f32[2,512,128]{2,1,0:T(8,128)} %get-tuple-element.25.cum_ref), custom_call_target="tpu_custom_call" | custom-call | tf_op jit(solution)/shard_map/local/pallas_call | solution.py:423
  109.9 14.9 %all-to-all-done.2.in_ref = bf16[4,328,128]{2,1,0:T(8,128)(2,1)S(1)} async-done(((bf16[4,328,128]{2,1,0:T(8,128)(2,1)}), bf16[4,328,128]{2,1,0:T(8,128)(2,1)S(1)}, u32[]{:S(2)}, u32[]{:S(2)}) %all-to-all-start.2) | async-done | bytes 335904 | tf_op jit(solution)/shard_map/all_to_all | solution.py:420
  124.9 0.5 combine.1
  125.4 0.0 copy-start.3
  125.4 10.1 %all_to_all.25.mix_ref = bf16[4,128,128]{2,1,0:T(8,128)(2,1)S(1)} all-to-all(bf16[4,128,128]{2,1,0:T(8,128)(2,1)S(1)} %bitcast.15), channel_id=1, replica_groups=mesh['A'=4,'B'=4,'tp'=4,'x'=4,'core'=2] {'B'}, dimensions={0} | all-to-all | bytes 262144 | tf_op jit(solution)/shard_map/all_to_all | solution.py:439
  135.5 0.0 copy-done
  135.5 2.0 %output.1 = bf16[128,2048]{1,0:T(8,128)(2,1)} custom-call(bf16[4,128,128]{2,1,0:T(8,128)(2,1)S(1)} %all_to_all.25.mix_ref, f32[1,256]{1,0:T(1,128)} %bitcast.20, bf16[512,2048]{1,0:T(8,128)(2,1)S(1)} %copy-done), custom_call_target="tpu_custom_call" | custom-call | tf_op jit(solution)/shard_map/output/pallas_call | solution.py:440
  137.5 3.5 %all-to-all-start.4 = ((bf16[4,32,2048]{2,1,0:T(8,128)(2,1)}), bf16[4,32,2048]{2,1,0:T(8,128)(2,1)S(1)}, u32[]{:S(2)}, u32[]{:S(2)}) async-start(bf16[4,32,2048]{2,1,0:T(8,128)(2,1)} %bitcast.12), calls=%async_computation.4 | async-start | bytes 1048576 | tf_op jit(solution)/shard_map/all_to_all | solution.py:448
  141.0 0.7 slice.50
  141.7 7.3 %all-to-all-done.4 = bf16[4,32,2048]{2,1,0:T(8,128)(2,1)S(1)} async-done(((bf16[4,32,2048]{2,1,0:T(8,128)(2,1)}), bf16[4,32,2048]{2,1,0:T(8,128)(2,1)S(1)}, u32[]{:S(2)}, u32[]{:S(2)}) %all-to-all-start.4) | async-done | bytes 524320 | tf_op jit(solution)/shard_map/all_to_all | solution.py:448
  149.0 0.1 reduce_sum.12
  149.1 0.7 add_convert_fusion
  (13 shorter events, 0.1 us)
Async XLA Ops:
  2.2 46.8 %all-to-all-start = ((bf16[16,56,128]{2,1,0:T(8,128)(2,1)}), bf16[16,56,128]{2,1,0:T(8,128)(2,1)S(1)}, u32[]{:S(2)}, u32[]{:S(2)}) async-start(bf16[16,56,128]{2,1,0:T(8,128)(2,1)} %get-tuple-element.18), calls=%async_computation | async-start | bytes 458752 | tf_op jit(solution)/shard_map/all_to_all | solution.py:375
  17.4 19.2 %collective-permute-start = (bf16[36,2048]{1,0:T(8,128)(2,1)S(1)}, bf16[36,2048]{1,0:T(8,128)(2,1)S(1)}, u32[]{:S(2)}, u32[]{:S(2)}) collective-permute-start(bf16[36,2048]{1,0:T(8,128)(2,1)S(1)} %get-tuple-element.17), channel_id=1, source_target_pairs={{0,32},{32,0},{64,96},{96,64},{1,33},{33,1},{65,97},{97,65},{2,34}... | collective-permute-start | bytes 442376 | tf_op jit(solution)/shard_map/ppermute | solution.py:374
  21.2 15.4 %collective-permute-start.1 = (bf16[36,2048]{1,0:T(8,128)(2,1)S(1)}, bf16[36,2048]{1,0:T(8,128)(2,1)S(1)}, u32[]{:S(2)}, u32[]{:S(2)}) collective-permute-start(bf16[36,2048]{1,0:T(8,128)(2,1)S(1)} %get-tuple-element.17), channel_id=1, source_target_pairs={{0,64},{32,96},{64,0},{96,32},{1,65},{33,97},{65,1},{97,33},{2,66}... | collective-permute-start | bytes 442376 | tf_op jit(solution)/shard_map/ppermute | solution.py:374
  25.5 16.5 %collective-permute-start.2 = (bf16[36,2048]{1,0:T(8,128)(2,1)S(1)}, bf16[36,2048]{1,0:T(8,128)(2,1)S(1)}, u32[]{:S(2)}, u32[]{:S(2)}) collective-permute-start(bf16[36,2048]{1,0:T(8,128)(2,1)S(1)} %get-tuple-element.17), channel_id=1, source_target_pairs={{0,96},{32,64},{64,32},{96,0},{1,97},{33,65},{65,33},{97,1},{2,98}... | collective-permute-start | bytes 442376 | tf_op jit(solution)/shard_map/ppermute | solution.py:374
  42.1 17.1 %collective-permute-start.4 = (bf16[144,2048]{1,0:T(8,128)(2,1)S(1)}, bf16[144,2048]{1,0:T(8,128)(2,1)S(1)}, u32[]{:S(2)}, u32[]{:S(2)}) collective-permute-start(bf16[144,2048]{1,0:T(8,128)(2,1)S(1)} %concatenate.9.own_ref), channel_id=1, source_target_pairs={{0,24},{8,0},{16,8},{24,16},{1,25},{9,1},{17,9},{25,17},{2,26},{10... | collective-permute-start | bytes 1769480 | tf_op jit(solution)/shard_map/ppermute | solution.py:386
  47.0 17.5 %collective-permute-start.3 = (bf16[144,2048]{1,0:T(8,128)(2,1)S(1)}, bf16[144,2048]{1,0:T(8,128)(2,1)S(1)}, u32[]{:S(2)}, u32[]{:S(2)}) collective-permute-start(bf16[144,2048]{1,0:T(8,128)(2,1)S(1)} %concatenate.9.own_ref), channel_id=1, source_target_pairs={{0,8},{8,16},{16,24},{24,0},{1,9},{9,17},{17,25},{25,1},{2,10},{10... | collective-permute-start | bytes 1769480 | tf_op jit(solution)/shard_map/ppermute | solution.py:385
  49.0 1.0 copy-start.2
  50.0 15.3 %all-to-all-start.1 = ((bf16[4,16,48,128]{3,2,1,0:T(8,128)(2,1)}), bf16[4,16,48,128]{3,2,1,0:T(8,128)(2,1)S(1)}, u32[]{:S(2)}, u32[]{:S(2)}) async-start(bf16[4,16,48,128]{3,2,1,0:T(8,128)(2,1)} %broadcast_in_dim.2), calls=%async_computation.1 | async-start | bytes 1572864 | tf_op jit(solution)/shard_map/all_to_all | solution.py:36
  65.2 25.5 %collective-permute-start.8 = (bf16[4,16,48,128]{3,2,1,0:T(8,128)(2,1)S(1)}, bf16[4,16,48,128]{3,2,1,0:T(8,128)(2,1)S(1)}, u32[]{:S(2)}, u32[]{:S(2)}) collective-permute-start(bf16[4,16,48,128]{3,2,1,0:T(8,128)(2,1)S(1)} %all-to-all-done.1.mine_ref), channel_id=1, source_target_pairs={{0,1},{1,0},{2,3},{3,2},{4,5},{5,4},{6,7},{7,6},{8,9},{9,8},{10,11... | collective-permute-start | bytes 2359304 | tf_op jit(solution)/shard_map/ppermute | solution.py:377
  69.7 18.8 %collective-permute-start.6 = (bf16[88,2048]{1,0:T(8,128)(2,1)}, bf16[88,2048]{1,0:T(8,128)(2,1)}, u32[]{:S(2)}, u32[]{:S(2)}) collective-permute-start(bf16[88,2048]{1,0:T(8,128)(2,1)} %pad_maximum_fusion), channel_id=1, source_target_pairs={{0,24},{8,0},{16,8},{24,16},{1,25},{9,1},{17,9},{25,17},{2,26},{10... | collective-permute-start | bytes 1081352 | tf_op jit(solution)/shard_map/ppermute | solution.py:388
  75.3 13.2 %collective-permute-start.5 = (bf16[72,2048]{1,0:T(8,128)(2,1)}, bf16[72,2048]{1,0:T(8,128)(2,1)}, u32[]{:S(2)}, u32[]{:S(2)}) collective-permute-start(bf16[72,2048]{1,0:T(8,128)(2,1)} %pad_maximum_fusion.1), channel_id=1, source_target_pairs={{0,8},{8,16},{16,24},{24,0},{1,9},{9,17},{17,25},{25,1},{2,10},{10... | collective-permute-start | bytes 884744 | tf_op jit(solution)/shard_map/ppermute | solution.py:387
  77.2 9.8 %collective-permute-start.7 = (bf16[8,2048]{1,0:T(8,128)(2,1)S(1)}, bf16[8,2048]{1,0:T(8,128)(2,1)S(1)}, u32[]{:S(2)}, u32[]{:S(2)}) collective-permute-start(bf16[8,2048]{1,0:T(8,128)(2,1)S(1)} %get-tuple-element.30.own_mods_ref), channel_id=1, source_target_pairs={{0,16},{8,24},{16,0},{24,8},{1,17},{9,25},{17,1},{25,9},{2,18},{10... | collective-permute-start | bytes 98312 | tf_op jit(solution)/shard_map/ppermute | solution.py:380
  95.4 0.7 copy-start.1
  96.1 39.3 %copy-start = (bf16[512,2048]{1,0:T(8,128)(2,1)S(1)}, bf16[512,2048]{1,0:T(8,128)(2,1)}, u32[]{:S(2)}) copy-start(bf16[512,2048]{1,0:T(8,128)(2,1)} %w_ref.1) | copy-start | bytes 6291460
  96.1 28.7 %all-to-all-start.2 = ((bf16[4,328,128]{2,1,0:T(8,128)(2,1)}), bf16[4,328,128]{2,1,0:T(8,128)(2,1)S(1)}, u32[]{:S(2)}, u32[]{:S(2)}) async-start(bf16[4,328,128]{2,1,0:T(8,128)(2,1)} %copy-done.1), calls=%async_computation.2 | async-start | bytes 671744 | tf_op jit(solution)/shard_map/all_to_all | solution.py:420
  125.4 23.7 %copy-start.3 = (bf16[32,2048]{1,0:T(8,128)(2,1)S(1)}, bf16[32,2048]{1,0:T(8,128)(2,1)}, u32[]{:S(2)}) copy-start(bf16[32,2048]{1,0:T(8,128)(2,1)} %lat_ref.1) | copy-start | bytes 393220
  137.5 11.5 %all-to-all-start.4 = ((bf16[4,32,2048]{2,1,0:T(8,128)(2,1)}), bf16[4,32,2048]{2,1,0:T(8,128)(2,1)S(1)}, u32[]{:S(2)}, u32[]{:S(2)}) async-start(bf16[4,32,2048]{2,1,0:T(8,128)(2,1)} %bitcast.12), calls=%async_computation.4 | async-start | bytes 1048576 | tf_op jit(solution)/shard_map/all_to_all | solution.py:448

commit v13 on v12

--- a/solution.py
+++ b/solution.py
@@ -113,7 +113,7 @@
 
 def hidden_kernel(
     own_ref, minus_ref, plus_ref, low_ref, high_ref, own_mods_ref, far_mods_ref, gain_ref,
-    h_ref, mod_ref, mods_ref,
+    h_ref, gate_ref, mod_ref, mods_ref,
 ):
     y = lax.axis_index("tp")
     mods_ref[y] = own_mods_ref[...].astype(f32)
@@ -124,6 +124,7 @@
         at = slice(z * 128, z * 128 + 96)
         parts = [mods_ref[i, 0:2, at] + mods_ref[i, 2:4, at] for i in range(4)]
         mod_ref[:, z * 384 : (z + 1) * 384] = jnp.concatenate(parts, axis=1)
+    gate_ref[...] = mod_ref[0:1, 2 * D : 3 * D]
     for slot in range(4):
         for j in range(5):
             size = 32 if j < 4 else 16
@@ -387,12 +388,12 @@
     low = lax.ppermute(jnp.concatenate([minus[:64], mods]), "tp", up_shift)
     high = lax.ppermute(jnp.concatenate([plus[64:], mods]), "tp", down_shift)
 
-    hidden, modulation = pl.pallas_call(
+    hidden, gate = pl.pallas_call(
         hidden_kernel,
-        out_shape=(sds((ROWS, D), bf16), pltpu.HBM((2, 3 * D), f32)),
+        out_shape=(sds((ROWS, D), bf16), pltpu.HBM((1, D), f32)),
         in_specs=[VM] * 8,
         out_specs=(VM, VM),
-        scratch_shapes=[pltpu.VMEM((4, 8, D), f32)],
+        scratch_shapes=[pltpu.VMEM((2, 3 * D), f32), pltpu.VMEM((4, 8, D), f32)],
         compiler_params=pltpu.CompilerParams(vmem_limit_bytes=16 * 1024 * 1024),
         name="hidden",
     )(*on_chip(own, minus, plus, low, high, mods, far_mods), *off_chip(norm_gain.reshape(1, D)))
@@ -447,8 +448,8 @@
     )(*on_chip(heads), *off_chip(head_gain.reshape(1, 256)), *on_chip(out_weight))
     shares = lax.all_to_all(partial.reshape(4, 32, D), "tp", 0, 0, tiled=True)
     projected = shares.astype(f32).sum(axis=0)
-    projected = lax.optimization_barrier(projected.astype(bf16)).astype(f32)
-    return (latents.astype(f32) + modulation[0:1, 2 * D :] * projected).astype(bf16)
+    projected = lax.reduce_precision(projected, 8, 7)
+    return (latents.astype(f32) + gate * projected).astype(bf16)
 
 
 def solution(mesh):

time: 152 us -> 150 us (0.987)
  blocking collectives: 10.1 us -> 20.5 us
  waiting for transfers between devices: 51.6 us -> 44.2 us
  starting transfers between devices: 62.9 us -> 59.5 us
    all_to_all x0 -> x1, blocking collectives: none -> 10.5 us  [device_body(): shares = lax.all_to_all(partial.reshape(4, 32, D), 'tp', 0, 0, tiled=True)]
    all_to_all x1 -> x0, waiting for transfers between devices: 7.32 us -> none  [device_body(): shares = lax.all_to_all(partial.reshape(4, 32, D), 'tp', 0, 0, tiled=True)]
    all_to_all x1 -> x0, starting transfers between devices: 3.47 us -> none  [device_body(): shares = lax.all_to_all(partial.reshape(4, 32, D), 'tp', 0, 0, tiled=True)]
  transfers between devices with their start and end apart: 13 -> 12, of which waited for: 8 -> 7; matrix products, arithmetic and copies ran while one was open for 6% -> 6% of each run, Pallas kernels for 3% -> 3%
where the time goes in v13:
time: 150 us; the launch traced here: 148 us
  starting transfers between devices  59.5 us (40%)
  waiting for transfers between devices  44.2 us (29%)
  blocking collectives  20.5 us (14%)
  Pallas kernels  13.5 us (9%)
  local copies, waits for them, and re-layouts  6.14 us (4%)
  other arithmetic  4.22 us (3%)
    all_to_all x1, starting transfers between devices, device_body(): rows_z = lax.all_to_all(cut, ('A', 'B'), 0, 0, tiled=True)  15.2 us
    all_to_all x1, waiting for transfers between devices, device_body(): lax.all_to_all(payload, ('A', 'B'), 0, 0, tiled=True, axis_index_groups=P...  14.9 us
    ppermute x3, waiting for transfers between devices, device_body(): near.append(lax.ppermute(rows, 'B', [(b, b ^ j) for b in range(4)]))  14.4 us
    all_to_all x1, starting transfers between devices, device_body(): lax.all_to_all(payload, ('A', 'B'), 0, 0, tiled=True, axis_index_groups=P...  11.5 us
    all_to_all x1, blocking collectives, device_body(): shares = lax.all_to_all(partial.reshape(4, 32, D), 'tp', 0, 0, tiled=True)  10.5 us
    ppermute x3, starting transfers between devices, device_body(): near.append(lax.ppermute(rows, 'B', [(b, b ^ j) for b in range(4)]))  10.1 us
    all_to_all x1, blocking collectives, device_body(): heads = lax.all_to_all(mixed.reshape(4, 128, DK), 'B', 0, 0, tiled=True)  9.98 us
    ppermute x1, starting transfers between devices, device_body(): plus = lax.ppermute(own, 'tp', down_shift)  4.92 us
  transfers between devices with their start and end apart: 12, of which 7 were waited for; matrix products, arithmetic and copies ran while one was open for 6% of the time, Pallas kernels for 3%

profile of v13, /device:TPU:6, one launch (start us, length us, event | category | flops | bytes accessed | tf_op | source)
XLA Modules:
  0.0 148.3 jit_solution(16169731912842075396)
XLA Ops:
  0.0 2.2 %pack.1 = (bf16[36,2048]{1,0:T(8,128)(2,1)S(1)}, bf16[16,56,128]{2,1,0:T(8,128)(2,1)}) custom-call(bf16[32,2048]{1,0:T(8,128)(2,1)} %lat_ref.1, bf16[16,2048]{1,0:T(8,128)(2,1)} %ctx_ref.1, f32[1,2048]{1,0:T(1,128)} %sv_ref.1, f32[1,2048]{1,0:T(1,128)} %cv_ref.1, bf16[96,2048]{1,0:T(8,128)(2,1)} %bitcast.17, bf16[128,256]{1,0:T(8,128)(2,1)} %wq_ref.1, ...), custom_call_target="tpu_custom_call" | custom-call | tf_op jit(solution)/shard_map/pack/pallas_call | solution.py:358
  2.2 15.2 %all-to-all-start = ((bf16[16,56,128]{2,1,0:T(8,128)(2,1)}), bf16[16,56,128]{2,1,0:T(8,128)(2,1)S(1)}, u32[]{:S(2)}, u32[]{:S(2)}) async-start(bf16[16,56,128]{2,1,0:T(8,128)(2,1)} %get-tuple-element.18), calls=%async_computation | async-start | bytes 458752 | tf_op jit(solution)/shard_map/all_to_all | solution.py:376
  17.4 3.8 %collective-permute-start = (bf16[36,2048]{1,0:T(8,128)(2,1)S(1)}, bf16[36,2048]{1,0:T(8,128)(2,1)S(1)}, u32[]{:S(2)}, u32[]{:S(2)}) collective-permute-start(bf16[36,2048]{1,0:T(8,128)(2,1)S(1)} %get-tuple-element.17), channel_id=1, source_target_pairs={{0,32},{32,0},{64,96},{96,64},{1,33},{33,1},{65,97},{97,65},{2,34}... | collective-permute-start | bytes 442376 | tf_op jit(solution)/shard_map/ppermute | solution.py:375
  21.2 4.3 %collective-permute-start.1 = (bf16[36,2048]{1,0:T(8,128)(2,1)S(1)}, bf16[36,2048]{1,0:T(8,128)(2,1)S(1)}, u32[]{:S(2)}, u32[]{:S(2)}) collective-permute-start(bf16[36,2048]{1,0:T(8,128)(2,1)S(1)} %get-tuple-element.17), channel_id=1, source_target_pairs={{0,64},{32,96},{64,0},{96,32},{1,65},{33,97},{65,1},{97,33},{2,66}... | collective-permute-start | bytes 442376 | tf_op jit(solution)/shard_map/ppermute | solution.py:375
  25.5 2.0 %collective-permute-start.2 = (bf16[36,2048]{1,0:T(8,128)(2,1)S(1)}, bf16[36,2048]{1,0:T(8,128)(2,1)S(1)}, u32[]{:S(2)}, u32[]{:S(2)}) collective-permute-start(bf16[36,2048]{1,0:T(8,128)(2,1)S(1)} %get-tuple-element.17), channel_id=1, source_target_pairs={{0,96},{32,64},{64,32},{96,0},{1,97},{33,65},{65,33},{97,1},{2,98}... | collective-permute-start | bytes 442376 | tf_op jit(solution)/shard_map/ppermute | solution.py:375
  27.5 9.0 %collective-permute-done = bf16[36,2048]{1,0:T(8,128)(2,1)S(1)} collective-permute-done((bf16[36,2048]{1,0:T(8,128)(2,1)S(1)}, bf16[36,2048]{1,0:T(8,128)(2,1)S(1)}, u32[]{:S(2)}, u32[]{:S(2)}) %collective-permute-start) | collective-permute-done | bytes 147488 | tf_op jit(solution)/shard_map/ppermute | solution.py:375
  36.6 0.0 collective-permute-done.1
  36.6 5.4 %collective-permute-done.2 = bf16[36,2048]{1,0:T(8,128)(2,1)S(1)} collective-permute-done((bf16[36,2048]{1,0:T(8,128)(2,1)S(1)}, bf16[36,2048]{1,0:T(8,128)(2,1)S(1)}, u32[]{:S(2)}, u32[]{:S(2)}) %collective-permute-start.2) | collective-permute-done | bytes 147488 | tf_op jit(solution)/shard_map/ppermute | solution.py:375
  42.0 0.1 concatenate.9.own_ref
  42.1 4.9 %collective-permute-start.4 = (bf16[144,2048]{1,0:T(8,128)(2,1)S(1)}, bf16[144,2048]{1,0:T(8,128)(2,1)S(1)}, u32[]{:S(2)}, u32[]{:S(2)}) collective-permute-start(bf16[144,2048]{1,0:T(8,128)(2,1)S(1)} %concatenate.9.own_ref), channel_id=1, source_target_pairs={{0,24},{8,0},{16,8},{24,16},{1,25},{9,1},{17,9},{25,17},{2,26},{10... | collective-permute-start | bytes 1769480 | tf_op jit(solution)/shard_map/ppermute | solution.py:387
  47.0 1.9 %collective-permute-start.3 = (bf16[144,2048]{1,0:T(8,128)(2,1)S(1)}, bf16[144,2048]{1,0:T(8,128)(2,1)S(1)}, u32[]{:S(2)}, u32[]{:S(2)}) collective-permute-start(bf16[144,2048]{1,0:T(8,128)(2,1)S(1)} %concatenate.9.own_ref), channel_id=1, source_target_pairs={{0,8},{8,16},{16,24},{24,0},{1,9},{9,17},{17,25},{25,1},{2,10},{10... | collective-permute-start | bytes 1769480 | tf_op jit(solution)/shard_map/ppermute | solution.py:386
  49.0 0.0 all-to-all-done
  49.0 0.0 copy-start.2
  49.0 1.0 broadcast_in_dim.2
  50.0 0.0 copy-done.2
  50.0 4.8 %all-to-all-start.1 = ((bf16[4,16,48,128]{3,2,1,0:T(8,128)(2,1)}), bf16[4,16,48,128]{3,2,1,0:T(8,128)(2,1)S(1)}, u32[]{:S(2)}, u32[]{:S(2)}) async-start(bf16[4,16,48,128]{3,2,1,0:T(8,128)(2,1)} %broadcast_in_dim.2), calls=%async_computation.1 | async-start | bytes 1572864 | tf_op jit(solution)/shard_map/all_to_all | solution.py:36
  54.8 4.4 %collective-permute-done.4.plus_ref = bf16[144,2048]{1,0:T(8,128)(2,1)S(1)} collective-permute-done((bf16[144,2048]{1,0:T(8,128)(2,1)S(1)}, bf16[144,2048]{1,0:T(8,128)(2,1)S(1)}, u32[]{:S(2)}, u32[]{:S(2)}) %collective-permute-start.4) | collective-permute-done | bytes 589856 | tf_op jit(solution)/shard_map/ppermute | solution.py:387
  59.2 0.8 slice.56
  60.0 4.6 %collective-permute-done.3.minus_ref = bf16[144,2048]{1,0:T(8,128)(2,1)S(1)} collective-permute-done((bf16[144,2048]{1,0:T(8,128)(2,1)S(1)}, bf16[144,2048]{1,0:T(8,128)(2,1)S(1)}, u32[]{:S(2)}, u32[]{:S(2)}) %collective-permute-start.3) | collective-permute-done | bytes 589856 | tf_op jit(solution)/shard_map/ppermute | solution.py:386
  64.5 0.7 slice.54
  65.2 0.0 all-to-all-done.1.mine_ref
  65.2 1.9 %collective-permute-start.8 = (bf16[4,16,48,128]{3,2,1,0:T(8,128)(2,1)S(1)}, bf16[4,16,48,128]{3,2,1,0:T(8,128)(2,1)S(1)}, u32[]{:S(2)}, u32[]{:S(2)}) collective-permute-start(bf16[4,16,48,128]{3,2,1,0:T(8,128)(2,1)S(1)} %all-to-all-done.1.mine_ref), channel_id=1, source_target_pairs={{0,1},{1,0},{2,3},{3,2},{4,5},{5,4},{6,7},{7,6},{8,9},{9,8},{10,11... | collective-permute-start | bytes 2359304 | tf_op jit(solution)/shard_map/ppermute | solution.py:378
  67.2 0.8 fusion
  67.9 1.7 %pad_maximum_fusion = bf16[88,2048]{1,0:T(8,128)(2,1)} fusion(bf16[8,2048]{1,0:T(8,128)(2,1)S(1)} %get-tuple-element.30.own_mods_ref, bf16[80,2048]{1,0:T(8,128)(2,1)} %slice.56), kind=kLoop, calls=%fused_computation.1 | loop fusion | flops 720896 | bytes 720896 | tf_op jit(solution)/shard_map/concatenate | solution.py:389
  69.7 3.9 %collective-permute-start.6 = (bf16[88,2048]{1,0:T(8,128)(2,1)}, bf16[88,2048]{1,0:T(8,128)(2,1)}, u32[]{:S(2)}, u32[]{:S(2)}) collective-permute-start(bf16[88,2048]{1,0:T(8,128)(2,1)} %pad_maximum_fusion), channel_id=1, source_target_pairs={{0,24},{8,0},{16,8},{24,16},{1,25},{9,1},{17,9},{25,17},{2,26},{10... | collective-permute-start | bytes 1081352 | tf_op jit(solution)/shard_map/ppermute | solution.py:389
  73.6 1.7 %pad_maximum_fusion.1 = bf16[72,2048]{1,0:T(8,128)(2,1)} fusion(bf16[8,2048]{1,0:T(8,128)(2,1)S(1)} %get-tuple-element.30.own_mods_ref, bf16[64,2048]{1,0:T(8,128)(2,1)} %slice.54), kind=kLoop, calls=%fused_computation.2 | loop fusion | flops 589824 | bytes 589824 | tf_op jit(solution)/shard_map/concatenate | solution.py:388
  75.3 1.9 %collective-permute-start.5 = (bf16[72,2048]{1,0:T(8,128)(2,1)}, bf16[72,2048]{1,0:T(8,128)(2,1)}, u32[]{:S(2)}, u32[]{:S(2)}) collective-permute-start(bf16[72,2048]{1,0:T(8,128)(2,1)} %pad_maximum_fusion.1), channel_id=1, source_target_pairs={{0,8},{8,16},{16,24},{24,0},{1,9},{9,17},{17,25},{25,1},{2,10},{10... | collective-permute-start | bytes 884744 | tf_op jit(solution)/shard_map/ppermute | solution.py:388
  77.2 3.4 %collective-permute-start.7 = (bf16[8,2048]{1,0:T(8,128)(2,1)S(1)}, bf16[8,2048]{1,0:T(8,128)(2,1)S(1)}, u32[]{:S(2)}, u32[]{:S(2)}) collective-permute-start(bf16[8,2048]{1,0:T(8,128)(2,1)S(1)} %get-tuple-element.30.own_mods_ref), channel_id=1, source_target_pairs={{0,16},{8,24},{16,0},{24,8},{1,17},{9,25},{17,1},{25,9},{2,18},{10... | collective-permute-start | bytes 98312 | tf_op jit(solution)/shard_map/ppermute | solution.py:381
  80.6 2.0 %copy.16 = bf16[2048,64]{1,0:T(8,128)(2,1)} copy(bf16[2048,64]{0,1:T(8,128)(2,1)} %param.24) | data formatting | bytes 524288 | tf_op args[9]
  82.5 4.5 %collective-permute-done.7.far_mods_ref = bf16[8,2048]{1,0:T(8,128)(2,1)S(1)} collective-permute-done((bf16[8,2048]{1,0:T(8,128)(2,1)S(1)}, bf16[8,2048]{1,0:T(8,128)(2,1)S(1)}, u32[]{:S(2)}, u32[]{:S(2)}) %collective-permute-start.7) | collective-permute-done | bytes 32800 | tf_op jit(solution)/shard_map/ppermute | solution.py:381
  87.0 1.5 %collective-permute-done.5.low_ref = bf16[72,2048]{1,0:T(8,128)(2,1)} collective-permute-done((bf16[72,2048]{1,0:T(8,128)(2,1)}, bf16[72,2048]{1,0:T(8,128)(2,1)}, u32[]{:S(2)}, u32[]{:S(2)}) %collective-permute-start.5) | collective-permute-done | bytes 294944 | tf_op jit(solution)/shard_map/ppermute | solution.py:388
  88.5 0.0 collective-permute-done.6.high_ref
  88.5 2.6 %hidden.1 = (bf16[576,2048]{1,0:T(8,128)(2,1)S(1)}, f32[1,2048]{1,0:T(1,128)}) custom-call(bf16[144,2048]{1,0:T(8,128)(2,1)S(1)} %concatenate.9.own_ref, bf16[144,2048]{1,0:T(8,128)(2,1)S(1)} %collective-permute-done.3.minus_ref, bf16[144,2048]{1,0:T(8,128)(2,1)S(1)} %collective-permute-done.4.plus_ref, bf16[72,2048]{1,0:T(8,128)(2,1)} %collective-permute-done.5.low_ref, ...), custom_call_target="tpu_custom_call" | custom-call | tf_op jit(solution)/shard_map/hidden/pallas_call | solution.py:391
  91.1 0.0 collective-permute-done.8.other_ref
  91.1 4.7 %project.1 = (bf16[4,328,128]{2,1,0:T(8,128)(2,1)S(1)}, bf16[512,128]{1,0:T(8,128)(2,1)}, bf16[512,128]{1,0:T(8,128)(2,1)}, bf16[512,128]{1,0:T(8,128)(2,1)}, f32[2,512,128]{2,1,0:T(8,128)}) custom-call(bf16[576,2048]{1,0:T(8,128)(2,1)S(1)} %get-tuple-element.20.h_ref, bf16[4,16,48,128]{3,2,1,0:T(8,128)(2,1)S(1)} %all-to-all-done.1.mine_ref, ...), custom_call_target="tpu_custom_call" | custom-call | tf_op jit(solution)/shard_map/project/pallas_call | solution.py:400
  95.8 0.7 copy-done.1
  96.6 11.5 %all-to-all-start.2 = ((bf16[4,328,128]{2,1,0:T(8,128)(2,1)}), bf16[4,328,128]{2,1,0:T(8,128)(2,1)S(1)}, u32[]{:S(2)}, u32[]{:S(2)}) async-start(bf16[4,328,128]{2,1,0:T(8,128)(2,1)} %copy-done.1), calls=%async_computation.2 | async-start | bytes 671744 | tf_op jit(solution)/shard_map/all_to_all | solution.py:421
  108.0 2.3 %local.1 = (f32[512,128]{1,0:T(8,128)S(1)}, bf16[512,128]{1,0:T(8,128)(2,1)S(1)}, bf16[512,128]{1,0:T(8,128)(2,1)S(1)}) custom-call(bf16[512,128]{1,0:T(8,128)(2,1)} %get-tuple-element.22.q_ref, bf16[512,128]{1,0:T(8,128)(2,1)} %get-tuple-element.23.k_ref, bf16[512,128]{1,0:T(8,128)(2,1)} %get-tuple-element.24.v_ref, f32[2,512,128]{2,1,0:T(8,128)} %get-tuple-element.25.cum_ref), custom_call_target="tpu_custom_call" | custom-call | tf_op jit(solution)/shard_map/local/pallas_call | solution.py:424
  110.4 14.9 %all-to-all-done.2.in_ref = bf16[4,328,128]{2,1,0:T(8,128)(2,1)S(1)} async-done(((bf16[4,328,128]{2,1,0:T(8,128)(2,1)}), bf16[4,328,128]{2,1,0:T(8,128)(2,1)S(1)}, u32[]{:S(2)}, u32[]{:S(2)}) %all-to-all-start.2) | async-done | bytes 335904 | tf_op jit(solution)/shard_map/all_to_all | solution.py:421
  125.3 0.5 combine.1
  125.8 10.0 %all_to_all.25.mix_ref = bf16[4,128,128]{2,1,0:T(8,128)(2,1)S(1)} all-to-all(bf16[4,128,128]{2,1,0:T(8,128)(2,1)S(1)} %bitcast.16), channel_id=1, replica_groups=mesh['A'=4,'B'=4,'tp'=4,'x'=4,'core'=2] {'B'}, dimensions={0} | all-to-all | bytes 262144 | tf_op jit(solution)/shard_map/all_to_all | solution.py:440
  135.8 0.0 copy-done
  135.8 1.2 output.1
  137.0 10.5 %all_to_all.26 = bf16[4,32,2048]{2,1,0:T(8,128)(2,1)S(1)} all-to-all(bf16[4,32,2048]{2,1,0:T(8,128)(2,1)S(1)} %bitcast.15), channel_id=1, replica_groups=mesh['A'=4,'B'=4,'tp'=4,'x'=4,'core'=2] {'tp'}, dimensions={0} | all-to-all | bytes 1048576 | tf_op jit(solution)/shard_map/all_to_all | solution.py:449
  147.5 0.1 convert_reduce_fusion
  147.6 0.0 copy-done.3
  147.6 0.0 copy-done.4
  147.6 0.7 add_convert_fusion
  (13 shorter events, 0.1 us)
Async XLA Ops:
  2.2 46.8 %all-to-all-start = ((bf16[16,56,128]{2,1,0:T(8,128)(2,1)}), bf16[16,56,128]{2,1,0:T(8,128)(2,1)S(1)}, u32[]{:S(2)}, u32[]{:S(2)}) async-start(bf16[16,56,128]{2,1,0:T(8,128)(2,1)} %get-tuple-element.18), calls=%async_computation | async-start | bytes 458752 | tf_op jit(solution)/shard_map/all_to_all | solution.py:376
  17.4 19.2 %collective-permute-start = (bf16[36,2048]{1,0:T(8,128)(2,1)S(1)}, bf16[36,2048]{1,0:T(8,128)(2,1)S(1)}, u32[]{:S(2)}, u32[]{:S(2)}) collective-permute-start(bf16[36,2048]{1,0:T(8,128)(2,1)S(1)} %get-tuple-element.17), channel_id=1, source_target_pairs={{0,32},{32,0},{64,96},{96,64},{1,33},{33,1},{65,97},{97,65},{2,34}... | collective-permute-start | bytes 442376 | tf_op jit(solution)/shard_map/ppermute | solution.py:375
  21.2 15.4 %collective-permute-start.1 = (bf16[36,2048]{1,0:T(8,128)(2,1)S(1)}, bf16[36,2048]{1,0:T(8,128)(2,1)S(1)}, u32[]{:S(2)}, u32[]{:S(2)}) collective-permute-start(bf16[36,2048]{1,0:T(8,128)(2,1)S(1)} %get-tuple-element.17), channel_id=1, source_target_pairs={{0,64},{32,96},{64,0},{96,32},{1,65},{33,97},{65,1},{97,33},{2,66}... | collective-permute-start | bytes 442376 | tf_op jit(solution)/shard_map/ppermute | solution.py:375
  25.5 16.5 %collective-permute-start.2 = (bf16[36,2048]{1,0:T(8,128)(2,1)S(1)}, bf16[36,2048]{1,0:T(8,128)(2,1)S(1)}, u32[]{:S(2)}, u32[]{:S(2)}) collective-permute-start(bf16[36,2048]{1,0:T(8,128)(2,1)S(1)} %get-tuple-element.17), channel_id=1, source_target_pairs={{0,96},{32,64},{64,32},{96,0},{1,97},{33,65},{65,33},{97,1},{2,98}... | collective-permute-start | bytes 442376 | tf_op jit(solution)/shard_map/ppermute | solution.py:375
  42.1 17.1 %collective-permute-start.4 = (bf16[144,2048]{1,0:T(8,128)(2,1)S(1)}, bf16[144,2048]{1,0:T(8,128)(2,1)S(1)}, u32[]{:S(2)}, u32[]{:S(2)}) collective-permute-start(bf16[144,2048]{1,0:T(8,128)(2,1)S(1)} %concatenate.9.own_ref), channel_id=1, source_target_pairs={{0,24},{8,0},{16,8},{24,16},{1,25},{9,1},{17,9},{25,17},{2,26},{10... | collective-permute-start | bytes 1769480 | tf_op jit(solution)/shard_map/ppermute | solution.py:387
  47.0 17.5 %collective-permute-start.3 = (bf16[144,2048]{1,0:T(8,128)(2,1)S(1)}, bf16[144,2048]{1,0:T(8,128)(2,1)S(1)}, u32[]{:S(2)}, u32[]{:S(2)}) collective-permute-start(bf16[144,2048]{1,0:T(8,128)(2,1)S(1)} %concatenate.9.own_ref), channel_id=1, source_target_pairs={{0,8},{8,16},{16,24},{24,0},{1,9},{9,17},{17,25},{25,1},{2,10},{10... | collective-permute-start | bytes 1769480 | tf_op jit(solution)/shard_map/ppermute | solution.py:386
  49.0 1.0 copy-start.2
  50.0 15.2 %all-to-all-start.1 = ((bf16[4,16,48,128]{3,2,1,0:T(8,128)(2,1)}), bf16[4,16,48,128]{3,2,1,0:T(8,128)(2,1)S(1)}, u32[]{:S(2)}, u32[]{:S(2)}) async-start(bf16[4,16,48,128]{3,2,1,0:T(8,128)(2,1)} %broadcast_in_dim.2), calls=%async_computation.1 | async-start | bytes 1572864 | tf_op jit(solution)/shard_map/all_to_all | solution.py:36
  65.2 25.9 %collective-permute-start.8 = (bf16[4,16,48,128]{3,2,1,0:T(8,128)(2,1)S(1)}, bf16[4,16,48,128]{3,2,1,0:T(8,128)(2,1)S(1)}, u32[]{:S(2)}, u32[]{:S(2)}) collective-permute-start(bf16[4,16,48,128]{3,2,1,0:T(8,128)(2,1)S(1)} %all-to-all-done.1.mine_ref), channel_id=1, source_target_pairs={{0,1},{1,0},{2,3},{3,2},{4,5},{5,4},{6,7},{7,6},{8,9},{9,8},{10,11... | collective-permute-start | bytes 2359304 | tf_op jit(solution)/shard_map/ppermute | solution.py:378
  69.7 18.9 %collective-permute-start.6 = (bf16[88,2048]{1,0:T(8,128)(2,1)}, bf16[88,2048]{1,0:T(8,128)(2,1)}, u32[]{:S(2)}, u32[]{:S(2)}) collective-permute-start(bf16[88,2048]{1,0:T(8,128)(2,1)} %pad_maximum_fusion), channel_id=1, source_target_pairs={{0,24},{8,0},{16,8},{24,16},{1,25},{9,1},{17,9},{25,17},{2,26},{10... | collective-permute-start | bytes 1081352 | tf_op jit(solution)/shard_map/ppermute | solution.py:389
  75.3 13.2 %collective-permute-start.5 = (bf16[72,2048]{1,0:T(8,128)(2,1)}, bf16[72,2048]{1,0:T(8,128)(2,1)}, u32[]{:S(2)}, u32[]{:S(2)}) collective-permute-start(bf16[72,2048]{1,0:T(8,128)(2,1)} %pad_maximum_fusion.1), channel_id=1, source_target_pairs={{0,8},{8,16},{16,24},{24,0},{1,9},{9,17},{17,25},{25,1},{2,10},{10... | collective-permute-start | bytes 884744 | tf_op jit(solution)/shard_map/ppermute | solution.py:388
  77.2 9.8 %collective-permute-start.7 = (bf16[8,2048]{1,0:T(8,128)(2,1)S(1)}, bf16[8,2048]{1,0:T(8,128)(2,1)S(1)}, u32[]{:S(2)}, u32[]{:S(2)}) collective-permute-start(bf16[8,2048]{1,0:T(8,128)(2,1)S(1)} %get-tuple-element.30.own_mods_ref), channel_id=1, source_target_pairs={{0,16},{8,24},{16,0},{24,8},{1,17},{9,25},{17,1},{25,9},{2,18},{10... | collective-permute-start | bytes 98312 | tf_op jit(solution)/shard_map/ppermute | solution.py:381
  95.8 0.7 copy-start.1
  96.6 39.2 %copy-start = (bf16[512,2048]{1,0:T(8,128)(2,1)S(1)}, bf16[512,2048]{1,0:T(8,128)(2,1)}, u32[]{:S(2)}) copy-start(bf16[512,2048]{1,0:T(8,128)(2,1)} %w_ref.1) | copy-start | bytes 6291460
  96.6 28.7 %all-to-all-start.2 = ((bf16[4,328,128]{2,1,0:T(8,128)(2,1)}), bf16[4,328,128]{2,1,0:T(8,128)(2,1)S(1)}, u32[]{:S(2)}, u32[]{:S(2)}) async-start(bf16[4,328,128]{2,1,0:T(8,128)(2,1)} %copy-done.1), calls=%async_computation.2 | async-start | bytes 671744 | tf_op jit(solution)/shard_map/all_to_all | solution.py:421
  135.8 11.8 %copy-start.3 = (bf16[32,2048]{1,0:T(8,128)(2,1)S(1)}, bf16[32,2048]{1,0:T(8,128)(2,1)}, u32[]{:S(2)}) copy-start(bf16[32,2048]{1,0:T(8,128)(2,1)} %lat_ref.1) | copy-start | bytes 393220
  135.8 11.8 %copy-start.4 = (f32[1,2048]{1,0:T(1,128)S(1)}, f32[1,2048]{1,0:T(1,128)}, u32[]{:S(2)}) copy-start(f32[1,2048]{1,0:T(1,128)} %get-tuple-element.19) | copy-start | bytes 24580

commit v14 on v13

--- a/solution.py
+++ b/solution.py
@@ -124,7 +124,7 @@
         at = slice(z * 128, z * 128 + 96)
         parts = [mods_ref[i, 0:2, at] + mods_ref[i, 2:4, at] for i in range(4)]
         mod_ref[:, z * 384 : (z + 1) * 384] = jnp.concatenate(parts, axis=1)
-    gate_ref[...] = mod_ref[0:1, 2 * D : 3 * D]
+    gate_ref[...] = jnp.broadcast_to(mod_ref[0:1, 2 * D : 3 * D], (8, D))
     for slot in range(4):
         for j in range(5):
             size = 32 if j < 4 else 16
@@ -390,13 +390,13 @@
 
     hidden, gate = pl.pallas_call(
         hidden_kernel,
-        out_shape=(sds((ROWS, D), bf16), pltpu.HBM((1, D), f32)),
+        out_shape=(sds((ROWS, D), bf16), pltpu.HBM((8, D), f32)),
         in_specs=[VM] * 8,
         out_specs=(VM, VM),
         scratch_shapes=[pltpu.VMEM((2, 3 * D), f32), pltpu.VMEM((4, 8, D), f32)],
         compiler_params=pltpu.CompilerParams(vmem_limit_bytes=16 * 1024 * 1024),
         name="hidden",
-    )(*on_chip(own, minus, plus, low, high, mods, far_mods), *off_chip(norm_gain.reshape(1, D)))
+    )(*off_chip(own), *on_chip(minus, plus, low, high, mods, far_mods), *off_chip(norm_gain.reshape(1, D)))
     payload, q, k, v, cum = pl.pallas_call(
         project_kernel,
         out_shape=(
@@ -449,7 +449,9 @@
     shares = lax.all_to_all(partial.reshape(4, 32, D), "tp", 0, 0, tiled=True)
     projected = shares.astype(f32).sum(axis=0)
     projected = lax.reduce_precision(projected, 8, 7)
-    return (latents.astype(f32) + gate * projected).astype(bf16)
+    eight = (4, 8, D)
+    updated = latents.astype(f32).reshape(eight) + gate[None] * projected.reshape(eight)
+    return updated.astype(bf16).reshape(32, D)
 
 
 def solution(mesh):

time: 150 us -> 147 us (0.980)
  local copies, waits for them, and re-layouts: 6.14 us -> 4 us
  other arithmetic: 4.22 us -> 2.28 us
  transfers between devices with their start and end apart: 12 -> 12, of which waited for: 7 -> 7; matrix products, arithmetic and copies ran while one was open for 6% -> 4% of each run, Pallas kernels for 3% -> 3%
where the time goes in v14:
time: 147 us; the launch traced here: 145 us
  starting transfers between devices  60.2 us (41%)
  waiting for transfers between devices  44.9 us (31%)
  blocking collectives  20.4 us (14%)
  Pallas kernels  13.2 us (9%)
  local copies, waits for them, and re-layouts  4 us (3%)
  other arithmetic  2.28 us (2%)
    all_to_all x1, starting transfers between devices, device_body(): rows_z = lax.all_to_all(cut, ('A', 'B'), 0, 0, tiled=True)  15.2 us
    all_to_all x1, waiting for transfers between devices, device_body(): lax.all_to_all(payload, ('A', 'B'), 0, 0, tiled=True, axis_index_groups=P...  14.9 us
    ppermute x3, waiting for transfers between devices, device_body(): near.append(lax.ppermute(rows, 'B', [(b, b ^ j) for b in range(4)]))  14.4 us
    all_to_all x1, starting transfers between devices, device_body(): lax.all_to_all(payload, ('A', 'B'), 0, 0, tiled=True, axis_index_groups=P...  11.5 us
    all_to_all x1, blocking collectives, device_body(): shares = lax.all_to_all(partial.reshape(4, 32, D), 'tp', 0, 0, tiled=True)  10.5 us
    ppermute x3, starting transfers between devices, device_body(): near.append(lax.ppermute(rows, 'B', [(b, b ^ j) for b in range(4)]))  10.1 us
    all_to_all x1, blocking collectives, device_body(): heads = lax.all_to_all(mixed.reshape(4, 128, DK), 'B', 0, 0, tiled=True)  9.97 us
    ppermute x1, waiting for transfers between devices, device_body(): minus = lax.ppermute(own, 'tp', up_shift)  5.3 us
  transfers between devices with their start and end apart: 12, of which 7 were waited for; matrix products, arithmetic and copies ran while one was open for 4% of the time, Pallas kernels for 3%

profile of v14, /device:TPU:6, one launch (start us, length us, event | category | flops | bytes accessed | tf_op | source)
XLA Modules:
  0.0 145.2 jit_solution(5339198072916712639)
XLA Ops:
  0.0 2.2 %pack.1 = (bf16[36,2048]{1,0:T(8,128)(2,1)S(1)}, bf16[16,56,128]{2,1,0:T(8,128)(2,1)}) custom-call(bf16[32,2048]{1,0:T(8,128)(2,1)} %lat_ref.1, bf16[16,2048]{1,0:T(8,128)(2,1)} %ctx_ref.1, f32[1,2048]{1,0:T(1,128)} %sv_ref.1, f32[1,2048]{1,0:T(1,128)} %cv_ref.1, bf16[96,2048]{1,0:T(8,128)(2,1)} %bitcast.22, bf16[128,256]{1,0:T(8,128)(2,1)} %wq_ref.1, ...), custom_call_target="tpu_custom_call" | custom-call | tf_op jit(solution)/shard_map/pack/pallas_call | solution.py:358
  2.2 15.2 %all-to-all-start = ((bf16[16,56,128]{2,1,0:T(8,128)(2,1)}), bf16[16,56,128]{2,1,0:T(8,128)(2,1)S(1)}, u32[]{:S(2)}, u32[]{:S(2)}) async-start(bf16[16,56,128]{2,1,0:T(8,128)(2,1)} %get-tuple-element.18), calls=%async_computation | async-start | bytes 458752 | tf_op jit(solution)/shard_map/all_to_all | solution.py:376
  17.4 3.8 %collective-permute-start = (bf16[36,2048]{1,0:T(8,128)(2,1)S(1)}, bf16[36,2048]{1,0:T(8,128)(2,1)S(1)}, u32[]{:S(2)}, u32[]{:S(2)}) collective-permute-start(bf16[36,2048]{1,0:T(8,128)(2,1)S(1)} %get-tuple-element.17), channel_id=1, source_target_pairs={{0,32},{32,0},{64,96},{96,64},{1,33},{33,1},{65,97},{97,65},{2,34}... | collective-permute-start | bytes 442376 | tf_op jit(solution)/shard_map/ppermute | solution.py:375
  21.2 4.3 %collective-permute-start.1 = (bf16[36,2048]{1,0:T(8,128)(2,1)S(1)}, bf16[36,2048]{1,0:T(8,128)(2,1)S(1)}, u32[]{:S(2)}, u32[]{:S(2)}) collective-permute-start(bf16[36,2048]{1,0:T(8,128)(2,1)S(1)} %get-tuple-element.17), channel_id=1, source_target_pairs={{0,64},{32,96},{64,0},{96,32},{1,65},{33,97},{65,1},{97,33},{2,66}... | collective-permute-start | bytes 442376 | tf_op jit(solution)/shard_map/ppermute | solution.py:375
  25.5 2.0 %collective-permute-start.2 = (bf16[36,2048]{1,0:T(8,128)(2,1)S(1)}, bf16[36,2048]{1,0:T(8,128)(2,1)S(1)}, u32[]{:S(2)}, u32[]{:S(2)}) collective-permute-start(bf16[36,2048]{1,0:T(8,128)(2,1)S(1)} %get-tuple-element.17), channel_id=1, source_target_pairs={{0,96},{32,64},{64,32},{96,0},{1,97},{33,65},{65,33},{97,1},{2,98}... | collective-permute-start | bytes 442376 | tf_op jit(solution)/shard_map/ppermute | solution.py:375
  27.5 9.0 %collective-permute-done = bf16[36,2048]{1,0:T(8,128)(2,1)S(1)} collective-permute-done((bf16[36,2048]{1,0:T(8,128)(2,1)S(1)}, bf16[36,2048]{1,0:T(8,128)(2,1)S(1)}, u32[]{:S(2)}, u32[]{:S(2)}) %collective-permute-start) | collective-permute-done | bytes 147488 | tf_op jit(solution)/shard_map/ppermute | solution.py:375
  36.6 0.0 collective-permute-done.1
  36.6 5.4 %collective-permute-done.2 = bf16[36,2048]{1,0:T(8,128)(2,1)S(1)} collective-permute-done((bf16[36,2048]{1,0:T(8,128)(2,1)S(1)}, bf16[36,2048]{1,0:T(8,128)(2,1)S(1)}, u32[]{:S(2)}, u32[]{:S(2)}) %collective-permute-start.2) | collective-permute-done | bytes 147488 | tf_op jit(solution)/shard_map/ppermute | solution.py:375
  42.0 0.1 concatenate.9.own_ref
  42.1 0.0 copy-start.1
  42.1 4.9 %collective-permute-start.4 = (bf16[144,2048]{1,0:T(8,128)(2,1)S(1)}, bf16[144,2048]{1,0:T(8,128)(2,1)S(1)}, u32[]{:S(2)}, u32[]{:S(2)}) collective-permute-start(bf16[144,2048]{1,0:T(8,128)(2,1)S(1)} %concatenate.9.own_ref), channel_id=1, source_target_pairs={{0,24},{8,0},{16,8},{24,16},{1,25},{9,1},{17,9},{25,17},{2,26},{10... | collective-permute-start | bytes 1769480 | tf_op jit(solution)/shard_map/ppermute | solution.py:387
  47.0 1.9 %collective-permute-start.3 = (bf16[144,2048]{1,0:T(8,128)(2,1)S(1)}, bf16[144,2048]{1,0:T(8,128)(2,1)S(1)}, u32[]{:S(2)}, u32[]{:S(2)}) collective-permute-start(bf16[144,2048]{1,0:T(8,128)(2,1)S(1)} %concatenate.9.own_ref), channel_id=1, source_target_pairs={{0,8},{8,16},{16,24},{24,0},{1,9},{9,17},{17,25},{25,1},{2,10},{10... | collective-permute-start | bytes 1769480 | tf_op jit(solution)/shard_map/ppermute | solution.py:386
  49.0 0.0 all-to-all-done
  49.0 0.0 copy-start.2
  49.0 1.0 broadcast_in_dim.2
  50.0 0.0 copy-done.2
  50.0 4.8 %all-to-all-start.1 = ((bf16[4,16,48,128]{3,2,1,0:T(8,128)(2,1)}), bf16[4,16,48,128]{3,2,1,0:T(8,128)(2,1)S(1)}, u32[]{:S(2)}, u32[]{:S(2)}) async-start(bf16[4,16,48,128]{3,2,1,0:T(8,128)(2,1)} %broadcast_in_dim.2), calls=%async_computation.1 | async-start | bytes 1572864 | tf_op jit(solution)/shard_map/all_to_all | solution.py:36
  54.8 4.4 %collective-permute-done.4.plus_ref = bf16[144,2048]{1,0:T(8,128)(2,1)S(1)} collective-permute-done((bf16[144,2048]{1,0:T(8,128)(2,1)S(1)}, bf16[144,2048]{1,0:T(8,128)(2,1)S(1)}, u32[]{:S(2)}, u32[]{:S(2)}) %collective-permute-start.4) | collective-permute-done | bytes 589856 | tf_op jit(solution)/shard_map/ppermute | solution.py:387
  59.2 5.3 %collective-permute-done.3.minus_ref = bf16[144,2048]{1,0:T(8,128)(2,1)S(1)} collective-permute-done((bf16[144,2048]{1,0:T(8,128)(2,1)S(1)}, bf16[144,2048]{1,0:T(8,128)(2,1)S(1)}, u32[]{:S(2)}, u32[]{:S(2)}) %collective-permute-start.3) | collective-permute-done | bytes 589856 | tf_op jit(solution)/shard_map/ppermute | solution.py:386
  64.6 0.0 copy-done.1
  64.6 0.0 all-to-all-done.1.mine_ref
  64.6 1.9 %collective-permute-start.8 = (bf16[4,16,48,128]{3,2,1,0:T(8,128)(2,1)S(1)}, bf16[4,16,48,128]{3,2,1,0:T(8,128)(2,1)S(1)}, u32[]{:S(2)}, u32[]{:S(2)}) collective-permute-start(bf16[4,16,48,128]{3,2,1,0:T(8,128)(2,1)S(1)} %all-to-all-done.1.mine_ref), channel_id=1, source_target_pairs={{0,1},{1,0},{2,3},{3,2},{4,5},{5,4},{6,7},{7,6},{8,9},{9,8},{10,11... | collective-permute-start | bytes 2359304 | tf_op jit(solution)/shard_map/ppermute | solution.py:378
  66.5 0.8 fusion.2
  67.3 0.8 pad_maximum_fusion
  68.0 4.6 %collective-permute-start.6 = (bf16[88,2048]{1,0:T(8,128)(2,1)}, bf16[88,2048]{1,0:T(8,128)(2,1)S(1)}, u32[]{:S(2)}, u32[]{:S(2)}) collective-permute-start(bf16[88,2048]{1,0:T(8,128)(2,1)} %pad_maximum_fusion), channel_id=1, source_target_pairs={{0,24},{8,0},{16,8},{24,16},{1,25},{9,1},{17,9},{25,17},{2,26},{10... | collective-permute-start | bytes 1081352 | tf_op jit(solution)/shard_map/ppermute | solution.py:389
  72.6 0.7 pad_maximum_fusion.1
  73.4 1.9 %collective-permute-start.5 = (bf16[72,2048]{1,0:T(8,128)(2,1)}, bf16[72,2048]{1,0:T(8,128)(2,1)S(1)}, u32[]{:S(2)}, u32[]{:S(2)}) collective-permute-start(bf16[72,2048]{1,0:T(8,128)(2,1)} %pad_maximum_fusion.1), channel_id=1, source_target_pairs={{0,8},{8,16},{16,24},{24,0},{1,9},{9,17},{17,25},{25,1},{2,10},{10... | collective-permute-start | bytes 884744 | tf_op jit(solution)/shard_map/ppermute | solution.py:388
  75.3 3.4 %collective-permute-start.7 = (bf16[8,2048]{1,0:T(8,128)(2,1)S(1)}, bf16[8,2048]{1,0:T(8,128)(2,1)S(1)}, u32[]{:S(2)}, u32[]{:S(2)}) collective-permute-start(bf16[8,2048]{1,0:T(8,128)(2,1)S(1)} %get-tuple-element.30.own_mods_ref), channel_id=1, source_target_pairs={{0,16},{8,24},{16,0},{24,8},{1,17},{9,25},{17,1},{25,9},{2,18},{10... | collective-permute-start | bytes 98312 | tf_op jit(solution)/shard_map/ppermute | solution.py:381
  78.7 2.0 %copy.16 = bf16[2048,64]{1,0:T(8,128)(2,1)} copy(bf16[2048,64]{0,1:T(8,128)(2,1)} %param.24) | data formatting | bytes 524288 | tf_op args[9]
  80.6 4.5 %collective-permute-done.7.far_mods_ref = bf16[8,2048]{1,0:T(8,128)(2,1)S(1)} collective-permute-done((bf16[8,2048]{1,0:T(8,128)(2,1)S(1)}, bf16[8,2048]{1,0:T(8,128)(2,1)S(1)}, u32[]{:S(2)}, u32[]{:S(2)}) %collective-permute-start.7) | collective-permute-done | bytes 32800 | tf_op jit(solution)/shard_map/ppermute | solution.py:381
  85.1 1.4 collective-permute-done.5.low_ref
  86.5 0.0 collective-permute-done.6.high_ref
  86.5 2.2 %hidden.1 = (bf16[576,2048]{1,0:T(8,128)(2,1)S(1)}, f32[8,2048]{1,0:T(8,128)}) custom-call(bf16[144,2048]{1,0:T(8,128)(2,1)} %copy-done.1, bf16[144,2048]{1,0:T(8,128)(2,1)S(1)} %collective-permute-done.3.minus_ref, bf16[144,2048]{1,0:T(8,128)(2,1)S(1)} %collective-permute-done.4.plus_ref, bf16[72,2048]{1,0:T(8,128)(2,1)S(1)} %collective-permute-done.5.low_ref, ...), custom_call_target="tpu_custom_call" | custom-call | tf_op jit(solution)/shard_map/hidden/pallas_call | solution.py:391
  88.7 0.0 collective-permute-done.8.other_ref
  88.7 4.8 %project.1 = (bf16[4,328,128]{2,1,0:T(8,128)(2,1)}, bf16[512,128]{1,0:T(8,128)(2,1)}, bf16[512,128]{1,0:T(8,128)(2,1)}, bf16[512,128]{1,0:T(8,128)(2,1)}, f32[2,512,128]{2,1,0:T(8,128)}) custom-call(bf16[576,2048]{1,0:T(8,128)(2,1)S(1)} %get-tuple-element.20.h_ref, bf16[4,16,48,128]{3,2,1,0:T(8,128)(2,1)S(1)} %all-to-all-done.1.mine_ref, ...), custom_call_target="tpu_custom_call" | custom-call | tf_op jit(solution)/shard_map/project/pallas_call | solution.py:400
  93.5 0.0 copy-start
  93.5 11.5 %all-to-all-start.2 = ((bf16[4,328,128]{2,1,0:T(8,128)(2,1)}), bf16[4,328,128]{2,1,0:T(8,128)(2,1)S(1)}, u32[]{:S(2)}, u32[]{:S(2)}) async-start(bf16[4,328,128]{2,1,0:T(8,128)(2,1)} %get-tuple-element.21), calls=%async_computation.2 | async-start | bytes 671744 | tf_op jit(solution)/shard_map/all_to_all | solution.py:421
  105.0 2.3 %local.1 = (f32[512,128]{1,0:T(8,128)S(1)}, bf16[512,128]{1,0:T(8,128)(2,1)S(1)}, bf16[512,128]{1,0:T(8,128)(2,1)S(1)}) custom-call(bf16[512,128]{1,0:T(8,128)(2,1)} %get-tuple-element.22.q_ref, bf16[512,128]{1,0:T(8,128)(2,1)} %get-tuple-element.23.k_ref, bf16[512,128]{1,0:T(8,128)(2,1)} %get-tuple-element.24.v_ref, f32[2,512,128]{2,1,0:T(8,128)} %get-tuple-element.25.cum_ref), custom_call_target="tpu_custom_call" | custom-call | tf_op jit(solution)/shard_map/local/pallas_call | solution.py:424
  107.3 14.9 %all-to-all-done.2.in_ref = bf16[4,328,128]{2,1,0:T(8,128)(2,1)S(1)} async-done(((bf16[4,328,128]{2,1,0:T(8,128)(2,1)}), bf16[4,328,128]{2,1,0:T(8,128)(2,1)S(1)}, u32[]{:S(2)}, u32[]{:S(2)}) %all-to-all-start.2) | async-done | bytes 335904 | tf_op jit(solution)/shard_map/all_to_all | solution.py:421
  122.2 0.5 combine.1
  122.7 10.0 %all_to_all.25.mix_ref = bf16[4,128,128]{2,1,0:T(8,128)(2,1)S(1)} all-to-all(bf16[4,128,128]{2,1,0:T(8,128)(2,1)S(1)} %bitcast.21), channel_id=1, replica_groups=mesh['A'=4,'B'=4,'tp'=4,'x'=4,'core'=2] {'B'}, dimensions={0} | all-to-all | bytes 262144 | tf_op jit(solution)/shard_map/all_to_all | solution.py:440
  132.7 0.0 copy-done
  132.7 1.2 output.1
  134.0 10.5 %all_to_all.26 = bf16[4,32,2048]{2,1,0:T(8,128)(2,1)S(1)} all-to-all(bf16[4,32,2048]{2,1,0:T(8,128)(2,1)S(1)} %bitcast.20), channel_id=1, replica_groups=mesh['A'=4,'B'=4,'tp'=4,'x'=4,'core'=2] {'tp'}, dimensions={0} | all-to-all | bytes 1048576 | tf_op jit(solution)/shard_map/all_to_all | solution.py:449
  144.4 0.1 convert_reduce_fusion
  144.5 0.0 copy-done.3
  144.5 0.0 copy-done.4
  144.5 0.7 fusion.1
  (13 shorter events, 0.1 us)
Async XLA Ops:
  2.2 46.8 %all-to-all-start = ((bf16[16,56,128]{2,1,0:T(8,128)(2,1)}), bf16[16,56,128]{2,1,0:T(8,128)(2,1)S(1)}, u32[]{:S(2)}, u32[]{:S(2)}) async-start(bf16[16,56,128]{2,1,0:T(8,128)(2,1)} %get-tuple-element.18), calls=%async_computation | async-start | bytes 458752 | tf_op jit(solution)/shard_map/all_to_all | solution.py:376
  17.4 19.2 %collective-permute-start = (bf16[36,2048]{1,0:T(8,128)(2,1)S(1)}, bf16[36,2048]{1,0:T(8,128)(2,1)S(1)}, u32[]{:S(2)}, u32[]{:S(2)}) collective-permute-start(bf16[36,2048]{1,0:T(8,128)(2,1)S(1)} %get-tuple-element.17), channel_id=1, source_target_pairs={{0,32},{32,0},{64,96},{96,64},{1,33},{33,1},{65,97},{97,65},{2,34}... | collective-permute-start | bytes 442376 | tf_op jit(solution)/shard_map/ppermute | solution.py:375
  21.2 15.4 %collective-permute-start.1 = (bf16[36,2048]{1,0:T(8,128)(2,1)S(1)}, bf16[36,2048]{1,0:T(8,128)(2,1)S(1)}, u32[]{:S(2)}, u32[]{:S(2)}) collective-permute-start(bf16[36,2048]{1,0:T(8,128)(2,1)S(1)} %get-tuple-element.17), channel_id=1, source_target_pairs={{0,64},{32,96},{64,0},{96,32},{1,65},{33,97},{65,1},{97,33},{2,66}... | collective-permute-start | bytes 442376 | tf_op jit(solution)/shard_map/ppermute | solution.py:375
  25.5 16.5 %collective-permute-start.2 = (bf16[36,2048]{1,0:T(8,128)(2,1)S(1)}, bf16[36,2048]{1,0:T(8,128)(2,1)S(1)}, u32[]{:S(2)}, u32[]{:S(2)}) collective-permute-start(bf16[36,2048]{1,0:T(8,128)(2,1)S(1)} %get-tuple-element.17), channel_id=1, source_target_pairs={{0,96},{32,64},{64,32},{96,0},{1,97},{33,65},{65,33},{97,1},{2,98}... | collective-permute-start | bytes 442376 | tf_op jit(solution)/shard_map/ppermute | solution.py:375
  42.1 22.5 %copy-start.1 = (bf16[144,2048]{1,0:T(8,128)(2,1)}, bf16[144,2048]{1,0:T(8,128)(2,1)S(1)}, u32[]{:S(2)}) copy-start(bf16[144,2048]{1,0:T(8,128)(2,1)S(1)} %concatenate.9.own_ref) | copy-start | bytes 1769476
  42.1 17.1 %collective-permute-start.4 = (bf16[144,2048]{1,0:T(8,128)(2,1)S(1)}, bf16[144,2048]{1,0:T(8,128)(2,1)S(1)}, u32[]{:S(2)}, u32[]{:S(2)}) collective-permute-start(bf16[144,2048]{1,0:T(8,128)(2,1)S(1)} %concatenate.9.own_ref), channel_id=1, source_target_pairs={{0,24},{8,0},{16,8},{24,16},{1,25},{9,1},{17,9},{25,17},{2,26},{10... | collective-permute-start | bytes 1769480 | tf_op jit(solution)/shard_map/ppermute | solution.py:387
  47.0 17.5 %collective-permute-start.3 = (bf16[144,2048]{1,0:T(8,128)(2,1)S(1)}, bf16[144,2048]{1,0:T(8,128)(2,1)S(1)}, u32[]{:S(2)}, u32[]{:S(2)}) collective-permute-start(bf16[144,2048]{1,0:T(8,128)(2,1)S(1)} %concatenate.9.own_ref), channel_id=1, source_target_pairs={{0,8},{8,16},{16,24},{24,0},{1,9},{9,17},{17,25},{25,1},{2,10},{10... | collective-permute-start | bytes 1769480 | tf_op jit(solution)/shard_map/ppermute | solution.py:386
  49.0 1.1 copy-start.2
  50.0 14.5 %all-to-all-start.1 = ((bf16[4,16,48,128]{3,2,1,0:T(8,128)(2,1)}), bf16[4,16,48,128]{3,2,1,0:T(8,128)(2,1)S(1)}, u32[]{:S(2)}, u32[]{:S(2)}) async-start(bf16[4,16,48,128]{3,2,1,0:T(8,128)(2,1)} %broadcast_in_dim.2), calls=%async_computation.1 | async-start | bytes 1572864 | tf_op jit(solution)/shard_map/all_to_all | solution.py:36
  64.6 24.2 %collective-permute-start.8 = (bf16[4,16,48,128]{3,2,1,0:T(8,128)(2,1)S(1)}, bf16[4,16,48,128]{3,2,1,0:T(8,128)(2,1)S(1)}, u32[]{:S(2)}, u32[]{:S(2)}) collective-permute-start(bf16[4,16,48,128]{3,2,1,0:T(8,128)(2,1)S(1)} %all-to-all-done.1.mine_ref), channel_id=1, source_target_pairs={{0,1},{1,0},{2,3},{3,2},{4,5},{5,4},{6,7},{7,6},{8,9},{9,8},{10,11... | collective-permute-start | bytes 2359304 | tf_op jit(solution)/shard_map/ppermute | solution.py:378
  68.0 18.5 %collective-permute-start.6 = (bf16[88,2048]{1,0:T(8,128)(2,1)}, bf16[88,2048]{1,0:T(8,128)(2,1)S(1)}, u32[]{:S(2)}, u32[]{:S(2)}) collective-permute-start(bf16[88,2048]{1,0:T(8,128)(2,1)} %pad_maximum_fusion), channel_id=1, source_target_pairs={{0,24},{8,0},{16,8},{24,16},{1,25},{9,1},{17,9},{25,17},{2,26},{10... | collective-permute-start | bytes 1081352 | tf_op jit(solution)/shard_map/ppermute | solution.py:389
  73.4 13.1 %collective-permute-start.5 = (bf16[72,2048]{1,0:T(8,128)(2,1)}, bf16[72,2048]{1,0:T(8,128)(2,1)S(1)}, u32[]{:S(2)}, u32[]{:S(2)}) collective-permute-start(bf16[72,2048]{1,0:T(8,128)(2,1)} %pad_maximum_fusion.1), channel_id=1, source_target_pairs={{0,8},{8,16},{16,24},{24,0},{1,9},{9,17},{17,25},{25,1},{2,10},{10... | collective-permute-start | bytes 884744 | tf_op jit(solution)/shard_map/ppermute | solution.py:388
  75.3 9.8 %collective-permute-start.7 = (bf16[8,2048]{1,0:T(8,128)(2,1)S(1)}, bf16[8,2048]{1,0:T(8,128)(2,1)S(1)}, u32[]{:S(2)}, u32[]{:S(2)}) collective-permute-start(bf16[8,2048]{1,0:T(8,128)(2,1)S(1)} %get-tuple-element.30.own_mods_ref), channel_id=1, source_target_pairs={{0,16},{8,24},{16,0},{24,8},{1,17},{9,25},{17,1},{25,9},{2,18},{10... | collective-permute-start | bytes 98312 | tf_op jit(solution)/shard_map/ppermute | solution.py:381
  93.5 39.2 %copy-start = (bf16[512,2048]{1,0:T(8,128)(2,1)S(1)}, bf16[512,2048]{1,0:T(8,128)(2,1)}, u32[]{:S(2)}) copy-start(bf16[512,2048]{1,0:T(8,128)(2,1)} %w_ref.1) | copy-start | bytes 6291460
  93.5 28.7 %all-to-all-start.2 = ((bf16[4,328,128]{2,1,0:T(8,128)(2,1)}), bf16[4,328,128]{2,1,0:T(8,128)(2,1)S(1)}, u32[]{:S(2)}, u32[]{:S(2)}) async-start(bf16[4,328,128]{2,1,0:T(8,128)(2,1)} %get-tuple-element.21), calls=%async_computation.2 | async-start | bytes 671744 | tf_op jit(solution)/shard_map/all_to_all | solution.py:421
  132.7 11.8 %copy-start.3 = (bf16[32,2048]{1,0:T(8,128)(2,1)S(1)}, bf16[32,2048]{1,0:T(8,128)(2,1)}, u32[]{:S(2)}) copy-start(bf16[32,2048]{1,0:T(8,128)(2,1)} %lat_ref.1) | copy-start | bytes 393220
  132.7 11.8 %copy-start.4 = (f32[8,2048]{1,0:T(8,128)S(1)}, f32[8,2048]{1,0:T(8,128)}, u32[]{:S(2)}) copy-start(f32[8,2048]{1,0:T(8,128)} %get-tuple-element.19) | copy-start | bytes 196612
